TPU v7x, 512 devices: a whole 4x8x8 slice. The times are simulated.
512 devices in a mesh: sp: 32 (over z, x), tp: 16 (over y, core).
Axes of the slice: x: 4, y: 8, z: 8, core: 2. Of those that a mesh axis runs over, the one named last changes fastest.
Arguments:
- mixed: bfloat16 [4096, 2048], P('sp'), may hold values from -6 to 6
- cotangent: bfloat16 [4096, 2048], P('sp'), may hold values from -6 to 6
- routes: int32 [4096, 2], P('sp'), may hold values from 0 to 31, all different within a row; in each aligned block of 128 rows (0 to 127, 128 to 255, ...) at most 16 rows name the same one
- gates: float32 [4096, 2], P('sp'), may hold values from 0.1 to 1
- w_gate: bfloat16 [32, 2048, 1024], P('sp', None, 'tp'), may hold values from -0.125 to 0.125
- w_up: bfloat16 [32, 2048, 1024], P('sp', None, 'tp'), may hold values from -0.125 to 0.125
- w_down: bfloat16 [32, 1024, 2048], P('sp', 'tp'), may hold values from -0.1875 to 0.1875
- out_weight: bfloat16 [4096, 2048], P('tp'), may hold values from -0.09375 to 0.09375
- gate_pre: bfloat16 [4096, 4096], P('sp', 'tp'), may hold values from -8 to 8
- mixer_out: bfloat16 [4096, 4096], P('sp', 'tp'), may hold values from -6 to 6
- values: bfloat16 [4096, 4096], P('sp', 'tp'), may hold values from -6 to 6
- write_keys: bfloat16 [4096, 2048], P('sp', 'tp'), may hold values from -1.25 to 1.25
- read_keys: bfloat16 [4096, 2048], P('sp', 'tp'), may hold values from -1.25 to 1.25
- log_decay: float32 [64, 4096], P('tp', 'sp'), may hold values from -0.08 to 0
- entry_states: float32 [32, 64, 64, 128], P('sp', 'tp'), may hold values from -6 to 6
Outputs:
- d_w_gate: bfloat16 [32, 2048, 1024], P('sp', None, 'tp')
- d_w_up: bfloat16 [32, 2048, 1024], P('sp', None, 'tp')
- d_w_down: bfloat16 [32, 1024, 2048], P('sp', 'tp')
- d_out_weight: float32 [2048, 4096], P('sp', 'tp')
- d_input: bfloat16 [4096, 2048], P('sp', 'tp')
- d_values: bfloat16 [4096, 4096], P('sp', 'tp')
- d_write: float32 [4096, 2048], P('sp', 'tp')
- d_read: float32 [4096, 2048], P('sp', 'tp')
- d_gate: bfloat16 [4096, 4096], P('sp', 'tp')
Inputs may be any that keep to these rules, and one draw needn't show every extreme that they name: `routes`: each row names 2 different experts; in the 128 rows of one device no expert is named more than 16 times, and in some blocks one is named exactly 16 times.
All inputs are finite; a program needn't handle non-finite values.
Results may differ from a plain program's by a relative error of at most 0.0062.
Values may be sent and summed in bfloat16 or wider, within the bound.
No kernel may reach another device: no remote copies, remote signals or barrier semaphores. Data moves between devices by JAX's collectives and lax.ppermute only.
A program may use at most 64 MiB of HBM per device.

v0:
```python
import jax
import jax.numpy as jnp
from jax import lax
from jax.sharding import Mesh
from jax.sharding import PartitionSpec as P

D = 2048
HEAD_DIM = 64
BLOCK = 128
TOPK = 2
TOK_DEV = 128
SP = ("sp_0", "sp_1")


precise = lax.Precision.HIGHEST


def sent_together(arrays, axis, split_dim, concat_dim, along):
    widths = [a.shape[along] for a in arrays]
    both = jnp.concatenate(arrays, axis=along)
    out = lax.all_to_all(both, axis, split_axis=split_dim, concat_axis=concat_dim, tiled=True)
    return tuple(jnp.split(out, [sum(widths[:k]) for k in range(1, len(widths))], axis=along))


def in_one_piece(arrays, axis, dim, along):
    widths = [a.shape[along] for a in arrays]
    both = jnp.concatenate(arrays, axis=along)
    out = lax.all_gather(both, axis, axis=dim, tiled=True)
    return tuple(jnp.split(out, [sum(widths[:k]) for k in range(1, len(widths))], axis=along))


def split_up(value, dim, count):
    before, after = (value.shape[:dim], value.shape[dim + 1 :])
    return jnp.moveaxis(value.reshape(*before, count, -1, *after), dim, 0)


def sent_and_summed(value, axis, dim):
    count = lax.axis_size(axis)
    parts = lax.all_to_all(split_up(value, dim, count), axis, 0, 0, tiled=True)
    return jnp.sum(parts, axis=0)


def filled_with(value, identity):
    return jax.tree.map(
        lambda a, e: jnp.broadcast_to(jnp.asarray(e, a.dtype), a.shape), value, identity
    )


def prefix_by_axis(value, axes, combine, identity):
    before = start = filled_with(value, identity)
    running = value
    for axis in reversed(axes):
        count, mine = (lax.axis_size(axis), lax.axis_index(axis))
        pieces = jax.tree.map(lambda part: lax.all_gather(part, axis), running)
        inside, running = (start, start)
        for k in reversed(range(count)):
            passed = k > mine
            running = combine(running, jax.tree.map(lambda part: part[k], pieces))
            inside = jax.tree.map(lambda new, old: jnp.where(passed, new, old), running, inside)
        before = combine(inside, before)
    return before


def silu_grad(pre_act):
    logistic = jax.nn.sigmoid(pre_act)
    return logistic * (1.0 + pre_act * (1.0 - logistic))


def contract_rows(first_op, second_op):
    return lax.dot_general(
        first_op, second_op, (((0,), (0,)), ((), ())), preferred_element_type=jnp.float32
    )


def contract_cols(first_op, second_op):
    return lax.dot_general(
        first_op, second_op, (((1,), (1,)), ((), ())), preferred_element_type=jnp.float32
    )


def combine_state(earlier, later):
    return (later[0] * earlier[0], later[1] + later[0][:, None, None] * earlier[1])


def block_back(grad_state, inputs_x, grad_y, log_rate, write_rows, read_rows, start_state):
    block_len = log_rate.shape[0]
    running = jnp.cumsum(log_rate, axis=0)
    causal_mask = (jnp.arange(block_len)[:, None] >= jnp.arange(block_len)[None, :])[:, :, None]
    spread = running[:, None, :] - running[None, :, :]
    decay_mat = jnp.where(causal_mask, jnp.exp(jnp.where(causal_mask, spread, 0.0)), 0.0)
    intersection = jnp.dot(read_rows, write_rows.T, precision=precise)
    mixing = intersection[:, :, None] * decay_mat
    to_end = jnp.exp(running[-1][None, :] - running)
    from_start = jnp.exp(running)
    grad_x = jnp.einsum("lsj,ljp->sjp", mixing, grad_y, precision=precise) + to_end[
        :, :, None
    ] * jnp.einsum("sn,jpn->sjp", write_rows, grad_state, precision=precise)
    weighted = jnp.einsum("ljp,sjp->lsj", grad_y, inputs_x, precision=precise) * decay_mat
    grad_w = jnp.einsum("lsj,ln->sn", weighted, read_rows, precision=precise) + jnp.einsum(
        "sj,sjp,jpn->sn", to_end, inputs_x, grad_state, precision=precise
    )
    grad_r = jnp.einsum("lsj,sn->ln", weighted, write_rows, precision=precise) + jnp.einsum(
        "lj,ljp,jpn->ln", from_start, grad_y, start_state, precision=precise
    )
    earlier = jnp.exp(running[-1])[:, None, None] * grad_state + jnp.einsum(
        "lj,ljp,ln->jpn", from_start, grad_y, read_rows, precision=precise
    )
    return (earlier, grad_x, grad_w, grad_r)


def body(
    mixed,
    cotangent,
    routes,
    gates,
    w_gate,
    w_up,
    w_down,
    out_weight,
    gate_pre,
    mixer_out,
    values,
    write_keys,
    read_keys,
    log_decay,
    entry_states,
):
    sp_count = lax.axis_size(SP)
    tp_count = lax.axis_size("tp")
    capacity = 4 * TOK_DEV // sp_count
    assigned = TOK_DEV * TOPK
    picks = routes.reshape(assigned)
    onehot = (picks[:, None] == jnp.arange(sp_count, dtype=jnp.int32)[None, :]).astype(jnp.int32)
    earlier_same = jnp.cumsum(onehot, axis=0) - onehot
    slot_of = jnp.sum(earlier_same * onehot, axis=1)
    target = picks * capacity + slot_of
    anchor = (
        jnp.full((sp_count * capacity,), assigned, jnp.int32)
        .at[target]
        .set(jnp.arange(assigned, dtype=jnp.int32))
    )
    weight_g = w_gate[0]
    weight_u = w_up[0]
    weight_d = w_down[0]
    column_count = D // tp_count
    offset = lax.axis_index("tp") * column_count
    tok_slice = lax.dynamic_slice_in_dim(mixed, offset, column_count, 1)
    cot_slice = lax.dynamic_slice_in_dim(cotangent, offset, column_count, 1)
    columns = tok_slice.shape[1]
    scaled = (
        (gates[:, :, None] * cot_slice[:, None, :].astype(jnp.float32))
        .astype(jnp.bfloat16)
        .reshape(assigned, columns)
    )
    empty_row = jnp.zeros((1, columns), jnp.bfloat16)
    cot_buffer = jnp.concatenate([scaled, empty_row])[anchor].reshape(sp_count, capacity, columns)
    tok_buffer = jnp.concatenate([tok_slice, empty_row])[anchor // TOPK].reshape(
        sp_count, capacity, columns
    )
    tok_buffer, cot_buffer = (tok_buffer, cot_buffer)
    tok_part, cot_part = sent_together((tok_buffer, cot_buffer), SP, 0, 0, 1)
    tok_rows, cot_rows = in_one_piece((tok_part, cot_part), "tp", 2, 0)
    expert_tok_rows = tok_rows
    expert_cot_rows = cot_rows
    expert_tok_rows = expert_tok_rows.reshape(-1, D)
    expert_cot_rows = expert_cot_rows.reshape(-1, D)
    pre_gate = jnp.dot(expert_tok_rows, weight_g, preferred_element_type=jnp.float32)
    pre_up = jnp.dot(expert_tok_rows, weight_u, preferred_element_type=jnp.float32)
    active = jax.nn.silu(pre_gate)
    hidden = (active * pre_up).astype(jnp.bfloat16)
    grad_down = contract_rows(hidden, expert_cot_rows)
    grad_hidden = contract_cols(expert_cot_rows, weight_d)
    grad_gate = (grad_hidden * pre_up * silu_grad(pre_gate)).astype(jnp.bfloat16)
    grad_upval = (grad_hidden * active).astype(jnp.bfloat16)
    grad_wg = contract_rows(expert_tok_rows, grad_gate)
    grad_wu = contract_rows(expert_tok_rows, grad_upval)
    partial_value = contract_cols(grad_gate, weight_g) + contract_cols(grad_upval, weight_u)
    grad_wg, grad_wu, grad_down, partial_value = (grad_wg, grad_wu, grad_down, partial_value)
    row_total = partial_value.shape[0]
    pieces = partial_value.astype(jnp.bfloat16).reshape(row_total, tp_count, column_count)
    received = lax.all_to_all(pieces, "tp", split_axis=1, concat_axis=1, tiled=True)
    summed = (
        jnp.sum(received.astype(jnp.float32), axis=1)
        .astype(jnp.bfloat16)
        .reshape(sp_count, capacity, column_count)
    )
    returned = lax.all_to_all(summed, SP, split_axis=0, concat_axis=0, tiled=True)
    columns = returned.shape[-1]
    picked = returned.reshape(sp_count * capacity, columns)[target].reshape(TOK_DEV, TOPK, columns)
    d_input = (cot_slice.astype(jnp.float32) + jnp.sum(picked.astype(jnp.float32), axis=1)).astype(
        jnp.bfloat16
    )
    whole = lax.all_gather(d_input, "tp", axis=1, tiled=True)
    back_proj = contract_cols(whole, out_weight)
    pre_act = gate_pre.astype(jnp.float32)
    gate_act = jax.nn.silu(pre_act)
    saved_out = mixer_out.astype(jnp.float32)
    d_gate = (back_proj * saved_out * silu_grad(pre_act)).astype(jnp.bfloat16)
    gated = (saved_out * gate_act).astype(jnp.bfloat16)
    d_out_weight = sent_and_summed(contract_rows(whole, gated), SP, 0)
    head_count = out_weight.shape[0] // HEAD_DIM
    grad_y = (back_proj * gate_act).reshape(TOK_DEV, head_count, HEAD_DIM)
    inputs_x = values.astype(jnp.float32).reshape(TOK_DEV, head_count, HEAD_DIM)
    write_rows = write_keys.astype(jnp.float32)
    read_rows = read_keys.astype(jnp.float32)
    log_rate = log_decay.T
    total_run = jnp.cumsum(log_rate, axis=0)
    shard_decay = jnp.exp(total_run[-1])
    shard_grad = jnp.einsum(
        "lj,ljp,ln->jpn", jnp.exp(total_run), grad_y, read_rows, precision=precise
    )
    identity = (jnp.ones_like(shard_decay), jnp.zeros_like(shard_grad))
    incoming = prefix_by_axis((shard_decay, shard_grad), SP, combine_state, identity)
    grad_state = incoming[1]
    pieces_x = []
    pieces_w = []
    pieces_r = []
    for block_id in reversed(range(TOK_DEV // BLOCK)):
        grad_state, grad_x, grad_w, grad_r = block_back(
            grad_state, inputs_x, grad_y, log_rate, write_rows, read_rows, entry_states[block_id]
        )
        pieces_x.insert(0, grad_x)
        pieces_w.insert(0, grad_w)
        pieces_r.insert(0, grad_r)
    d_values = pieces_x[0].reshape(TOK_DEV, head_count * HEAD_DIM).astype(jnp.bfloat16)
    d_write = pieces_w[0]
    d_read = pieces_r[0]
    return (
        grad_wg.astype(jnp.bfloat16)[None],
        grad_wu.astype(jnp.bfloat16)[None],
        grad_down.astype(jnp.bfloat16)[None],
        d_out_weight,
        d_input,
        d_values,
        d_write,
        d_read,
        d_gate,
    )


def solution(mesh):
    finer = Mesh(mesh.devices.reshape(8, 4, mesh.shape["tp"]), ("sp_0", "sp_1", "tp"))
    return jax.shard_map(
        body,
        mesh=finer,
        in_specs=(
            P(SP, None),
            P(SP, None),
            P(SP, None),
            P(SP, None),
            P(SP, None, "tp"),
            P(SP, None, "tp"),
            P(SP, "tp", None),
            P("tp", None),
            P(SP, "tp"),
            P(SP, "tp"),
            P(SP, "tp"),
            P(SP, "tp"),
            P(SP, "tp"),
            P("tp", SP),
            P(SP, "tp", None, None),
        ),
        out_specs=(
            P(SP, None, "tp"),
            P(SP, None, "tp"),
            P(SP, "tp", None),
            P(SP, "tp"),
            P(SP, "tp"),
            P(SP, "tp"),
            P(SP, "tp"),
            P(SP, "tp"),
            P(SP, "tp"),
        ),
        check_vma=False,
    )
```

profile of v0, /device:TPU:2, one launch (start us, length us, event | category | flops | bytes accessed | tf_op | source)
XLA Modules:
  0.0 289.5 jit_solution(18188501029784762102)
XLA Ops:
  11.2 1.4 scatter_custom_fusion
  13.6 1.3 gather_fusion.1
  15.0 1.3 gather_fusion
  16.4 24.5 %all_to_all.20 = bf16[32,32,128]{2,1,0:T(8,128)(2,1)S(1)} all-to-all(bf16[32,32,128]{2,1,0:T(8,128)(2,1)S(1)} %pad_maximum_fusion), channel_id=1, replica_groups=mesh['sp_0'=8,'sp_1'=4,'tp'=16] {'sp_0','sp_1'}, dimensions={0} | all-to-all | bytes 524288 | tf_op jit(solution)/shard_map/all_to_all | solution.py:21
  41.6 48.4 %all-gather.6.cloned.1.call-done = bf16[64,16,2048]{2,1,0:T(8,128)(2,1)} async-done(((bf16[64,16,128]{2,1,0:T(8,128)(2,1)}), bf16[64,16,2048]{2,1,0:T(8,128)(2,1)}) %all-gather.6.cloned.1.call-update) | async-done | bytes 4194320 | tf_op jit(solution)/shard_map/all_gather | solution.py:28
  90.1 2.6 fusion.77
  96.9 1.9 copy.65
  98.8 4.6 %all-to-all-start.1 = ((bf16[512,16,128]{2,0,1:T(8,128)(2,1)}), bf16[512,16,128]{2,0,1:T(8,128)(2,1)}, u32[]{:S(2)}, u32[]{:S(2)}) async-start(bf16[512,16,128]{2,0,1:T(8,128)(2,1)} %bitcast.231), calls=%async_computation.1 | async-start | bytes 4194304 | tf_op jit(solution)/shard_map/all_to_all | solution.py:181
  103.7 49.0 %all-to-all-done.1 = bf16[512,16,128]{2,0,1:T(8,128)(2,1)} async-done(((bf16[512,16,128]{2,0,1:T(8,128)(2,1)}), bf16[512,16,128]{2,0,1:T(8,128)(2,1)}, u32[]{:S(2)}, u32[]{:S(2)}) %all-to-all-start.1) | async-done | bytes 2097184 | tf_op jit(solution)/shard_map/all_to_all | solution.py:181
  152.6 2.6 reduce_sum.56
  155.2 10.5 %all-to-all-start.2 = ((bf16[32,16,128]{2,1,0:T(8,128)(2,1)}), bf16[32,16,128]{2,1,0:T(8,128)(2,1)S(1)}, u32[]{:S(2)}, u32[]{:S(2)}) async-start(bf16[32,16,128]{2,1,0:T(8,128)(2,1)} %bitcast.237), calls=%async_computation.2 | async-start | bytes 262144 | tf_op jit(solution)/shard_map/all_to_all | solution.py:187
  165.7 7.8 %all-gather.1 = f32[4,1,4]{2,1,0:T(1,128)S(1)} all-gather(f32[1,1,4]{2,1,0:T(1,128)S(1)} %get-tuple-element.47), channel_id=1, replica_groups=mesh['sp_0'=8,'sp_1'=4,'tp'=16] {'sp_1'}, dimensions={0}, use_global_device_ids=true | all-gather | bytes 80 | tf_op jit(solution)/shard_map/all_gather | solution.py:54
  174.8 0.9 gather_fusion.2
  176.6 16.8 %all_gather.25 = bf16[128,2048]{1,0:T(8,128)(2,1)S(1)} all-gather(bf16[128,128]{1,0:T(8,128)(2,1)S(1)} %add_convert_fusion.1), channel_id=1, replica_groups=mesh['sp_0'=8,'sp_1'=4,'tp'=16] {'tp'}, dimensions={1}, use_global_device_ids=true | all-gather | bytes 557056 | tf_op jit(solution)/shard_map/all_gather | solution.py:193
  194.3 2.7 fusion.56
  196.9 9.3 %all-to-all-start.3 = ((f32[32,64,256]{2,1,0:T(8,128)}), f32[32,64,256]{2,1,0:T(8,128)}, u32[]{:S(2)}, u32[]{:S(2)}) async-start(f32[32,64,256]{2,1,0:T(8,128)} %bitcast.230), calls=%async_computation.3 | async-start | bytes 4194304 | tf_op jit(solution)/shard_map/all_to_all | solution.py:39
  207.5 2.3 fusion.21
  209.7 1.0 copy.53
  210.9 18.1 %all-gather = f32[16,64,128]{2,1,0:T(8,128)S(1)} all-gather(f32[4,64,128]{2,1,0:T(8,128)S(1)} %fusion.54), channel_id=2, replica_groups=mesh['sp_0'=8,'sp_1'=4,'tp'=16] {'sp_1'}, dimensions={0}, use_global_device_ids=true | all-gather | bytes 655360 | tf_op jit(solution)/shard_map/all_gather | solution.py:54
  229.0 0.8 copy-done.3
  229.8 1.3 fusion.44
  231.9 0.9 copy.57
  232.8 1.6 copy.59
  234.4 31.4 %all-gather.2 = f32[8,1,4]{2,1,0:T(1,128)S(1)} all-gather(f32[1,1,4]{2,1,0:T(1,128)} %get-tuple-element.58), channel_id=1, replica_groups=mesh['sp_0'=8,'sp_1'=4,'tp'=16] {'sp_0'}, dimensions={0}, use_global_device_ids=true | all-gather | bytes 144 | tf_op jit(solution)/shard_map/all_gather | solution.py:54
  267.2 2.2 fusion.1
  269.4 1.2 fusion.2
  270.7 1.2 fusion
  272.7 0.8 convolution_add_fusion
  273.6 2.3 all-gather.8.cloned.1.call-done
  276.0 1.6 fusion.37
  279.4 0.9 convolution_add_fusion.1
  280.3 2.3 reduce_sum.58
  (139 shorter events, 19.4 us)
Async XLA Ops:
  7.2 200.3 %copy-start = (bf16[256,2048]{1,0:T(8,128)(2,1)S(1)}, bf16[256,2048]{1,0:T(8,128)(2,1)}, u32[]{:S(2)}) copy-start(bf16[256,2048]{1,0:T(8,128)(2,1)} %param.22) | copy-start | bytes 3145732
  7.2 82.9 %all-gather.6.cloned.1.call-start = ((), (), s32[]{:S(2)}) async-start(), calls=%async_computation.4 | async-start | bytes 4456448 | tf_op jit(solution)/shard_map/all_gather | solution.py:28
  41.6 51.1 %copy-start.6 = (bf16[1,2048,64]{1,2,0:T(8,128)(2,1)S(1)}, bf16[1,2048,64]{1,2,0:T(8,128)(2,1)}, u32[]{:S(2)}) copy-start(bf16[1,2048,64]{1,2,0:T(8,128)(2,1)} %param.19) | copy-start | bytes 786436
  98.8 4.6 %copy-start.37 = (f32[4,128]{1,0:T(4,128)S(1)}, f32[4,128]{1,0:T(4,128)}, u32[]{:S(2)}) copy-start(f32[4,128]{1,0:T(4,128)} %param.28) | copy-start | bytes 6148
  98.8 53.9 %all-to-all-start.1 = ((bf16[512,16,128]{2,0,1:T(8,128)(2,1)}), bf16[512,16,128]{2,0,1:T(8,128)(2,1)}, u32[]{:S(2)}, u32[]{:S(2)}) async-start(bf16[512,16,128]{2,0,1:T(8,128)(2,1)} %bitcast.231), calls=%async_computation.1 | async-start | bytes 4194304 | tf_op jit(solution)/shard_map/all_to_all | solution.py:181
  155.2 19.6 %all-to-all-start.2 = ((bf16[32,16,128]{2,1,0:T(8,128)(2,1)}), bf16[32,16,128]{2,1,0:T(8,128)(2,1)S(1)}, u32[]{:S(2)}, u32[]{:S(2)}) async-start(bf16[32,16,128]{2,1,0:T(8,128)(2,1)} %bitcast.237), calls=%async_computation.2 | async-start | bytes 262144 | tf_op jit(solution)/shard_map/all_to_all | solution.py:187
  176.6 20.3 %copy-start.21 = (bf16[128,128]{1,0:T(8,128)(2,1)}, bf16[128,128]{1,0:T(8,128)(2,1)S(1)}, u32[]{:S(2)}) copy-start(bf16[128,128]{1,0:T(8,128)(2,1)S(1)} %add_convert_fusion.1) | copy-start | bytes 98308
  196.9 9.9 %copy-start.17 = (f32[128,4]{1,0:T(8,128)S(1)}, f32[128,4]{1,0:T(8,128)}, u32[]{:S(2)}) copy-start(f32[128,4]{1,0:T(8,128)} %get-tuple-element.45) | copy-start | bytes 6148
  196.9 83.4 %all-to-all-start.3 = ((f32[32,64,256]{2,1,0:T(8,128)}), f32[32,64,256]{2,1,0:T(8,128)}, u32[]{:S(2)}, u32[]{:S(2)}) async-start(f32[32,64,256]{2,1,0:T(8,128)} %bitcast.230), calls=%async_computation.3 | async-start | bytes 4194304 | tf_op jit(solution)/shard_map/all_to_all | solution.py:39
  206.3 4.5 %copy-start.12 = (bf16[128,128]{1,0:T(8,128)(2,1)S(1)}, bf16[128,128]{1,0:T(8,128)(2,1)}, u32[]{:S(2)}) copy-start(bf16[128,128]{1,0:T(8,128)(2,1)} %param.27) | copy-start | bytes 98308
  206.3 69.6 %all-gather.8.cloned.1.call-start = ((), (), s32[]{:S(2)}) async-start(), calls=%async_computation.5 | async-start | bytes 1179648 | tf_op jit(solution)/shard_map/all_gather | solution.py:54
  207.5 22.4 %copy-start.25 = (f32[4]{0:T(128)S(1)}, f32[4]{0:T(128)}, u32[]{:S(2)}) copy-start(f32[4]{0:T(128)} %get-tuple-element.60) | copy-start | bytes 52
  207.5 58.9 %copy-start.10 = (bf16[128,128]{1,0:T(8,128)(2,1)S(1)}, bf16[128,128]{1,0:T(8,128)(2,1)}, u32[]{:S(2)}) copy-start(bf16[128,128]{1,0:T(8,128)(2,1)} %param.26) | copy-start | bytes 98308
  234.4 35.0 %copy-start.15 = (bf16[512,64]{0,1:T(8,128)(2,1)S(1)}, bf16[512,64]{0,1:T(8,128)(2,1)}, u32[]{:S(2)}) copy-start(bf16[512,64]{0,1:T(8,128)(2,1)} %copy-done.14) | copy-start | bytes 196612
  265.8 6.5 %copy-start.23 = (pred[128,128]{1,0:T(8,128)(4,1)}, pred[128,128]{1,0:T(8,128)(4,1)S(1)}, u32[]{:S(2)}) copy-start(pred[128,128]{1,0:T(8,128)(4,1)S(1)} %iota_compare_fusion) | copy-start | bytes 49156
  270.6 5.3 %copy-start.4 = (f32[16,64,128]{2,1,0:T(8,128)S(1)}, f32[16,64,128]{2,1,0:T(8,128)}, u32[]{:S(2)}) copy-start(f32[16,64,128]{2,1,0:T(8,128)} %copy-done.3) | copy-start | bytes 1572868
  270.6 5.3 %copy-start.26 = (f32[4]{0:T(128)S(1)}, f32[4]{0:T(128)}, u32[]{:S(2)}) copy-start(f32[4]{0:T(128)} %get-tuple-element.60) | copy-start | bytes 52
  270.6 5.3 %copy-start.27 = (f32[4]{0:T(128)S(1)}, f32[4]{0:T(128)}, u32[]{:S(2)}) copy-start(f32[4]{0:T(128)} %get-tuple-element.61) | copy-start | bytes 52
  270.6 5.3 %copy-start.28 = (f32[4]{0:T(128)S(1)}, f32[4]{0:T(128)}, u32[]{:S(2)}) copy-start(f32[4]{0:T(128)} %get-tuple-element.56) | copy-start | bytes 52
  270.6 5.3 %copy-start.29 = (f32[4]{0:T(128)S(1)}, f32[4]{0:T(128)}, u32[]{:S(2)}) copy-start(f32[4]{0:T(128)} %get-tuple-element.48) | copy-start | bytes 52
  270.6 5.3 %copy-start.30 = (f32[4]{0:T(128)S(1)}, f32[4]{0:T(128)}, u32[]{:S(2)}) copy-start(f32[4]{0:T(128)} %get-tuple-element.49) | copy-start | bytes 52
  270.6 5.3 %copy-start.31 = (f32[4]{0:T(128)S(1)}, f32[4]{0:T(128)}, u32[]{:S(2)}) copy-start(f32[4]{0:T(128)} %get-tuple-element.50) | copy-start | bytes 52
  270.6 5.3 %copy-start.32 = (f32[4]{0:T(128)S(1)}, f32[4]{0:T(128)}, u32[]{:S(2)}) copy-start(f32[4]{0:T(128)} %get-tuple-element.51) | copy-start | bytes 52
  270.6 5.3 %copy-start.33 = (f32[4]{0:T(128)S(1)}, f32[4]{0:T(128)}, u32[]{:S(2)}) copy-start(f32[4]{0:T(128)} %get-tuple-element.52) | copy-start | bytes 52
  270.6 5.3 %copy-start.34 = (f32[4]{0:T(128)S(1)}, f32[4]{0:T(128)}, u32[]{:S(2)}) copy-start(f32[4]{0:T(128)} %get-tuple-element.53) | copy-start | bytes 52
  270.6 5.3 %copy-start.35 = (f32[4]{0:T(128)S(1)}, f32[4]{0:T(128)}, u32[]{:S(2)}) copy-start(f32[4]{0:T(128)} %get-tuple-element.54) | copy-start | bytes 52
  270.7 5.3 %copy-start.36 = (f32[4]{0:T(128)S(1)}, f32[4]{0:T(128)}, u32[]{:S(2)}) copy-start(f32[4]{0:T(128)} %get-tuple-element.55) | copy-start | bytes 52
  271.9 5.9 %copy-start.22 = (f32[128,128]{1,0:T(8,128)S(1)}, f32[128,128]{1,0:T(8,128)}, u32[]{:S(2)}) copy-start(f32[128,128]{1,0:T(8,128)} %fusion.79) | copy-start | bytes 196612
  271.9 5.9 %copy-start.39 = (f32[128,4]{0,1:T(4,128)S(1)}, f32[128,4]{0,1:T(4,128)}, u32[]{:S(2)}) copy-start(f32[128,4]{0,1:T(4,128)} %copy.55) | copy-start | bytes 6148
  271.9 7.2 %copy-start.19 = (bf16[128,256]{0,1:T(8,128)(2,1)S(1)}, bf16[128,256]{0,1:T(8,128)(2,1)}, u32[]{:S(2)}) copy-start(bf16[128,256]{0,1:T(8,128)(2,1)} %copy.59) | copy-start | bytes 196612
  271.9 7.6 %copy-start.13 = (bf16[128,128]{1,0:T(8,128)(2,1)S(1)}, bf16[128,128]{1,0:T(8,128)(2,1)}, u32[]{:S(2)}) copy-start(bf16[128,128]{1,0:T(8,128)(2,1)} %param.27) | copy-start | bytes 98308
  272.7 5.1 %copy-start.24 = (pred[128,128]{1,0:T(8,128)(4,1)S(1)}, pred[128,128]{1,0:T(8,128)(4,1)}, u32[]{:S(2)}) copy-start(pred[128,128]{1,0:T(8,128)(4,1)} %copy-done.23) | copy-start | bytes 49156
  (14 other events, 27.0 us)
Sparse Core Ops, SparseCore 0:
  41.7 48.2 all-gather.5
  231.3 44.5 all-gather.7
where the time goes:
time: 290 us
  waiting for transfers between devices  100 us (34%)
  blocking collectives  98.5 us (34%)
  starting transfers between devices  24.5 us (8%)
  local copies, waits for them, and re-layouts  19.1 us (7%)
  matrix products  17.8 us (6%)
  between operations  14.7 us (5%)
  other arithmetic  14.5 us (5%)
    all_gather x3, blocking collectives, prefix_by_axis(): pieces = jax.tree.map(lambda part: lax.all_gather(part, axis), running)  57.3 us
    all_to_all x1, waiting for transfers between devices, body(): lax.all_to_all(pieces, 'tp', split_axis=1, concat_axis=1, tiled=True)  49 us
    all_gather x1, waiting for transfers between devices, in_one_piece(): out = lax.all_gather(both, axis, axis=dim, tiled=True)  48.4 us
    all_to_all x1, blocking collectives, sent_together(): lax.all_to_all(both, axis, split_axis=split_dim, concat_axis=concat_dim,...  24.5 us
    all_gather x1, blocking collectives, body(): whole = lax.all_gather(d_input, 'tp', axis=1, tiled=True)  16.8 us
    all_to_all x1, starting transfers between devices, body(): lax.all_to_all(summed, SP, split_axis=0, concat_axis=0, tiled=True)  10.5 us
    all_to_all x1, starting transfers between devices, sent_and_summed(): parts = lax.all_to_all(split_up(value, dim, count), axis, 0, 0, tiled=True)  9.32 us
    dot_general x4, matrix products, contract_rows(): lax.dot_general(first_op, second_op, (((0,), (0,)), ((), ())), preferred_...  7.22 us
  transfers between devices with their start and end apart: 5, of which 4 were waited for; matrix products, arithmetic and copies ran while one was open for 8% of the time, Pallas kernels for 0%

commit v1 on v0

--- a/solution.py
+++ b/solution.py
@@ -37,28 +37,33 @@
 def sent_and_summed(value, axis, dim):
     count = lax.axis_size(axis)
     parts = lax.all_to_all(split_up(value, dim, count), axis, 0, 0, tiled=True)
-    return jnp.sum(parts, axis=0)
-
-
-def filled_with(value, identity):
-    return jax.tree.map(
-        lambda a, e: jnp.broadcast_to(jnp.asarray(e, a.dtype), a.shape), value, identity
-    )
-
-
-def prefix_by_axis(value, axes, combine, identity):
-    before = start = filled_with(value, identity)
-    running = value
-    for axis in reversed(axes):
-        count, mine = (lax.axis_size(axis), lax.axis_index(axis))
-        pieces = jax.tree.map(lambda part: lax.all_gather(part, axis), running)
-        inside, running = (start, start)
-        for k in reversed(range(count)):
-            passed = k > mine
-            running = combine(running, jax.tree.map(lambda part: part[k], pieces))
-            inside = jax.tree.map(lambda new, old: jnp.where(passed, new, old), running, inside)
-        before = combine(inside, before)
-    return before
+    return jnp.sum(parts.astype(jnp.float32), axis=0)
+
+
+def three_parts(value):
+    first = lax.reduce_precision(value, 8, 7)
+    second = lax.reduce_precision(value - first, 8, 7)
+    third = value - first - second
+    return jnp.stack([first, second, third]).astype(jnp.bfloat16)
+
+
+def later_states(shard_grad, logs):
+    sp_count = lax.axis_size(SP)
+    mine = lax.axis_index(SP)
+    heads = shard_grad.shape[0]
+    pieces = shard_grad.reshape(sp_count, -1, shard_grad.shape[-1])
+    received = lax.all_to_all(pieces, SP, 0, 0, tiled=True)
+    head = mine * heads // sp_count
+    own = lax.dynamic_index_in_dim(logs, head, 1, keepdims=False)
+    through = jnp.cumsum(own)
+    before = through - own
+    span = before[None, :] - through[:, None]
+    later = jnp.arange(sp_count)[None, :] > jnp.arange(sp_count)[:, None]
+    weights = jnp.where(later, jnp.exp(jnp.where(later, span, 0.0)), 0.0)
+    flat = received.reshape(sp_count, -1)
+    summed = jnp.dot(weights, flat, precision=precise).reshape(received.shape)
+    back = lax.all_to_all(summed, SP, 0, 0, tiled=True)
+    return back.reshape(shard_grad.shape)
 
 
 def silu_grad(pre_act):
@@ -76,10 +81,6 @@
     return lax.dot_general(
         first_op, second_op, (((1,), (1,)), ((), ())), preferred_element_type=jnp.float32
     )
-
-
-def combine_state(earlier, later):
-    return (later[0] * earlier[0], later[1] + later[0][:, None, None] * earlier[1])
 
 
 def block_back(grad_state, inputs_x, grad_y, log_rate, write_rows, read_rows, start_state):
@@ -184,7 +185,13 @@
         .astype(jnp.bfloat16)
         .reshape(sp_count, capacity, column_count)
     )
-    returned = lax.all_to_all(summed, SP, split_axis=0, concat_axis=0, tiled=True)
+    head_count = out_weight.shape[0] // HEAD_DIM
+    parts = three_parts(jnp.sum(log_decay, axis=1))
+    extra = jnp.pad(parts, ((0, 5), (0, column_count - head_count)))
+    extra = jnp.broadcast_to(extra[None], (sp_count, *extra.shape))
+    both = lax.all_to_all(jnp.concatenate([summed, extra], axis=1), SP, 0, 0, tiled=True)
+    returned = both[:, :capacity]
+    logs = jnp.sum(both[:, capacity : capacity + 3, :head_count].astype(jnp.float32), axis=1)
     columns = returned.shape[-1]
     picked = returned.reshape(sp_count * capacity, columns)[target].reshape(TOK_DEV, TOPK, columns)
     d_input = (cot_slice.astype(jnp.float32) + jnp.sum(picked.astype(jnp.float32), axis=1)).astype(
@@ -197,21 +204,18 @@
     saved_out = mixer_out.astype(jnp.float32)
     d_gate = (back_proj * saved_out * silu_grad(pre_act)).astype(jnp.bfloat16)
     gated = (saved_out * gate_act).astype(jnp.bfloat16)
-    d_out_weight = sent_and_summed(contract_rows(whole, gated), SP, 0)
-    head_count = out_weight.shape[0] // HEAD_DIM
+    weight_part = contract_rows(whole, gated).astype(jnp.bfloat16)
+    d_out_weight = sent_and_summed(weight_part, SP, 0)
     grad_y = (back_proj * gate_act).reshape(TOK_DEV, head_count, HEAD_DIM)
     inputs_x = values.astype(jnp.float32).reshape(TOK_DEV, head_count, HEAD_DIM)
     write_rows = write_keys.astype(jnp.float32)
     read_rows = read_keys.astype(jnp.float32)
     log_rate = log_decay.T
     total_run = jnp.cumsum(log_rate, axis=0)
-    shard_decay = jnp.exp(total_run[-1])
     shard_grad = jnp.einsum(
         "lj,ljp,ln->jpn", jnp.exp(total_run), grad_y, read_rows, precision=precise
     )
-    identity = (jnp.ones_like(shard_decay), jnp.zeros_like(shard_grad))
-    incoming = prefix_by_axis((shard_decay, shard_grad), SP, combine_state, identity)
-    grad_state = incoming[1]
+    grad_state = later_states(shard_grad, logs)
     pieces_x = []
     pieces_w = []
     pieces_r = []

time: 290 us -> 277 us (0.955)
  blocking collectives: 98.5 us -> 41 us
  waiting for transfers between devices: 100 us -> 136 us
  starting transfers between devices: 24.5 us -> 33.5 us
  other arithmetic: 14.5 us -> 10.7 us
    all_gather x3 -> x0, blocking collectives: 57.3 us -> none  [prefix_by_axis(): pieces = jax.tree.map(lambda part: lax.all_gather(part, axis), running)]
    all_to_all x1 -> x3, waiting for transfers between devices: 0.57 us -> 20.9 us  [the longest x1 9.47 us: body(): lax.all_to_all(jnp.concatenate([summed, extra], axis=1), SP, 0, 0, tiled=...]
    all_to_all x1, waiting for transfers between devices: 0.01 us -> 18.2 us  [sent_and_summed(): parts = lax.all_to_all(split_up(value, dim, count), axis, 0, 0, tiled=True)]
    all_to_all x1 -> x3, starting transfers between devices: 10.5 us -> 22.5 us  [the longest x1 10.5 us: body(): lax.all_to_all(jnp.concatenate([summed, extra], axis=1), SP, 0, 0, tiled=...]
    add x2 -> x0, other arithmetic: 2.9 us -> none  [combine_state(): later[1] + later[0][:, None, None] * earlier[1]]
    unnamed x86 -> x48, local copies, waits for them, and re-layouts: 6.07 us -> 5.75 us
  transfers between devices with their start and end apart: 5 -> 6, of which waited for: 4 -> 6; matrix products, arithmetic and copies ran while one was open for 8% -> 6% of each run, Pallas kernels for 0% -> 0%
where the time goes in v1:
time: 277 us; the launch traced here: 276 us
  waiting for transfers between devices  136 us (49%)
  blocking collectives  41 us (15%)
  starting transfers between devices  33.5 us (12%)
  local copies, waits for them, and re-layouts  19.9 us (7%)
  matrix products  19.9 us (7%)
  between operations  14.6 us (5%)
  other arithmetic  10.7 us (4%)
    all_to_all x1, waiting for transfers between devices, body(): lax.all_to_all(pieces, 'tp', split_axis=1, concat_axis=1, tiled=True)  48.8 us
    all_gather x1, waiting for transfers between devices, in_one_piece(): out = lax.all_gather(both, axis, axis=dim, tiled=True)  48.4 us
    all_to_all x1, blocking collectives, sent_together(): lax.all_to_all(both, axis, split_axis=split_dim, concat_axis=concat_dim,...  24.5 us
    all_to_all x1, waiting for transfers between devices, sent_and_summed(): parts = lax.all_to_all(split_up(value, dim, count), axis, 0, 0, tiled=True)  18.2 us
    all_gather x1, blocking collectives, body(): whole = lax.all_gather(d_input, 'tp', axis=1, tiled=True)  16.5 us
    all_to_all x1, starting transfers between devices, body(): lax.all_to_all(jnp.concatenate([summed, extra], axis=1), SP, 0, 0, tiled=...  10.5 us
    all_to_all x1, waiting for transfers between devices, body(): lax.all_to_all(jnp.concatenate([summed, extra], axis=1), SP, 0, 0, tiled=...  9.47 us
    all_to_all x1, waiting for transfers between devices, later_states(): back = lax.all_to_all(summed, SP, 0, 0, tiled=True)  6.48 us
  transfers between devices with their start and end apart: 6, of which 6 were waited for; matrix products, arithmetic and copies ran while one was open for 6% of the time, Pallas kernels for 0%

profile of v1, /device:TPU:2, one launch (start us, length us, event | category | flops | bytes accessed | tf_op | source)
XLA Modules:
  0.0 276.1 jit_solution(3933162403917365709)
XLA Ops:
  11.2 1.4 scatter_custom_fusion
  13.6 1.3 gather_fusion.1
  15.0 1.3 gather_fusion
  16.4 24.5 %all_to_all.30 = bf16[32,32,128]{2,1,0:T(8,128)(2,1)S(1)} all-to-all(bf16[32,32,128]{2,1,0:T(8,128)(2,1)S(1)} %pad_maximum_fusion), channel_id=1, replica_groups=mesh['sp_0'=8,'sp_1'=4,'tp'=16] {'sp_0','sp_1'}, dimensions={0} | all-to-all | bytes 524288 | tf_op jit(solution)/shard_map/all_to_all | solution.py:21
  41.6 48.4 %all-gather.2.cloned.1.call-done = bf16[64,16,2048]{2,1,0:T(8,128)(2,1)} async-done(((bf16[64,16,128]{2,1,0:T(8,128)(2,1)}), bf16[64,16,2048]{2,1,0:T(8,128)(2,1)}) %all-gather.2.cloned.1.call-update) | async-done | bytes 4194320 | tf_op jit(solution)/shard_map/all_gather | solution.py:28
  90.1 2.8 fusion.81
  97.1 1.9 copy.96
  98.9 4.6 %all-to-all-start.1 = ((bf16[512,16,128]{2,0,1:T(8,128)(2,1)}), bf16[512,16,128]{2,0,1:T(8,128)(2,1)}, u32[]{:S(2)}, u32[]{:S(2)}) async-start(bf16[512,16,128]{2,0,1:T(8,128)(2,1)} %bitcast.147), calls=%async_computation.1 | async-start | bytes 4194304 | tf_op jit(solution)/shard_map/all_to_all | solution.py:182
  104.0 48.8 %all-to-all-done.1 = bf16[512,16,128]{2,0,1:T(8,128)(2,1)} async-done(((bf16[512,16,128]{2,0,1:T(8,128)(2,1)}), bf16[512,16,128]{2,0,1:T(8,128)(2,1)}, u32[]{:S(2)}, u32[]{:S(2)}) %all-to-all-start.1) | async-done | bytes 2097184 | tf_op jit(solution)/shard_map/all_to_all | solution.py:182
  152.8 1.9 reduce_sum.76
  155.4 10.5 %all-to-all-start.2 = ((bf16[32,24,128]{2,1,0:T(8,128)(2,1)}), bf16[32,24,128]{2,1,0:T(8,128)(2,1)S(1)}, u32[]{:S(2)}, u32[]{:S(2)}) async-start(bf16[32,24,128]{2,1,0:T(8,128)(2,1)} %pad_maximum_fusion.2), calls=%async_computation.2 | async-start | bytes 393216 | tf_op jit(solution)/shard_map/all_to_all | solution.py:192
  166.6 9.5 %all-to-all-done.2 = bf16[32,24,128]{2,1,0:T(8,128)(2,1)S(1)} async-done(((bf16[32,24,128]{2,1,0:T(8,128)(2,1)}), bf16[32,24,128]{2,1,0:T(8,128)(2,1)S(1)}, u32[]{:S(2)}, u32[]{:S(2)}) %all-to-all-start.2) | async-done | bytes 196640 | tf_op jit(solution)/shard_map/all_to_all | solution.py:192
  176.1 1.5 gather_fusion.2
  177.6 1.0 convert_reduce_fusion.1
  180.0 16.5 %all_gather.7 = bf16[128,2048]{1,0:T(8,128)(2,1)S(1)} all-gather(bf16[128,128]{1,0:T(8,128)(2,1)S(1)} %add_convert_fusion.1), channel_id=1, replica_groups=mesh['sp_0'=8,'sp_1'=4,'tp'=16] {'tp'}, dimensions={1}, use_global_device_ids=true | all-gather | bytes 557056 | tf_op jit(solution)/shard_map/all_gather | solution.py:200
  197.3 2.0 fusion.21
  199.3 1.0 copy.73
  200.3 1.6 fusion.40
  201.9 6.2 %all-to-all-start.4 = ((f32[32,8,128]{2,1,0:T(8,128)}), f32[32,8,128]{2,1,0:T(8,128)}, u32[]{:S(2)}, u32[]{:S(2)}) async-start(f32[32,8,128]{2,1,0:T(8,128)} %bitcast.157), calls=%async_computation.4 | async-start | bytes 262144 | tf_op jit(solution)/shard_map/all_to_all | solution.py:55
  208.1 1.6 fusion.83
  210.7 1.6 copy.81
  212.7 5.0 %all-to-all-done.4 = f32[32,8,128]{2,1,0:T(8,128)} async-done(((f32[32,8,128]{2,1,0:T(8,128)}), f32[32,8,128]{2,1,0:T(8,128)}, u32[]{:S(2)}, u32[]{:S(2)}) %all-to-all-start.4) | async-done | bytes 131104 | tf_op jit(solution)/shard_map/all_to_all | solution.py:55
  217.7 1.2 fusion.27
  219.6 5.8 %all-to-all-start.5 = ((f32[32,8,128]{2,1,0:T(8,128)}), f32[32,8,128]{2,1,0:T(8,128)S(1)}, u32[]{:S(2)}, u32[]{:S(2)}) async-start(f32[32,8,128]{2,1,0:T(8,128)} %copy.80), calls=%async_computation.5 | async-start | bytes 262144 | tf_op jit(solution)/shard_map/all_to_all | solution.py:65
  225.5 2.5 convolution_convert_fusion
  228.0 6.5 %all-to-all-done.5 = f32[32,8,128]{2,1,0:T(8,128)S(1)} async-done(((f32[32,8,128]{2,1,0:T(8,128)}), f32[32,8,128]{2,1,0:T(8,128)S(1)}, u32[]{:S(2)}, u32[]{:S(2)}) %all-to-all-start.5) | async-done | bytes 131104 | tf_op jit(solution)/shard_map/all_to_all | solution.py:65
  234.5 6.4 %all-to-all-start.3 = ((bf16[32,64,256]{2,1,0:T(8,128)(2,1)}), bf16[32,64,256]{2,1,0:T(8,128)(2,1)}, u32[]{:S(2)}, u32[]{:S(2)}) async-start(bf16[32,64,256]{2,1,0:T(8,128)(2,1)} %bitcast.148), calls=%async_computation.3 | async-start | bytes 2097152 | tf_op jit(solution)/shard_map/all_to_all | solution.py:39
  241.0 1.2 fusion.1
  242.2 1.2 fusion.2
  243.4 1.2 fusion
  249.0 18.2 %all-to-all-done.3 = bf16[32,64,256]{2,1,0:T(8,128)(2,1)} async-done(((bf16[32,64,256]{2,1,0:T(8,128)(2,1)}), bf16[32,64,256]{2,1,0:T(8,128)(2,1)}, u32[]{:S(2)}, u32[]{:S(2)}) %all-to-all-start.3) | async-done | bytes 1048608 | tf_op jit(solution)/shard_map/all_to_all | solution.py:39
  267.2 2.0 convert_reduce_fusion
  (107 shorter events, 20.4 us)
Async XLA Ops:
  7.2 190.1 %copy-start = (bf16[256,2048]{1,0:T(8,128)(2,1)S(1)}, bf16[256,2048]{1,0:T(8,128)(2,1)}, u32[]{:S(2)}) copy-start(bf16[256,2048]{1,0:T(8,128)(2,1)} %param.22) | copy-start | bytes 3145732
  7.2 82.9 %all-gather.2.cloned.1.call-start = ((), (), s32[]{:S(2)}) async-start(), calls=%async_computation.6 | async-start | bytes 4456448 | tf_op jit(solution)/shard_map/all_gather | solution.py:28
  41.6 51.2 %copy-start.4 = (bf16[1,2048,64]{1,2,0:T(8,128)(2,1)S(1)}, bf16[1,2048,64]{1,2,0:T(8,128)(2,1)}, u32[]{:S(2)}) copy-start(bf16[1,2048,64]{1,2,0:T(8,128)(2,1)} %param.19) | copy-start | bytes 786436
  92.8 1.9 copy-start.1
  92.8 1.1 copy-start.5
  92.9 1.9 copy-start.21
  94.0 1.6 copy-start.6
  94.7 1.6 copy-start.8
  95.5 0.8 copy-start.14
  95.6 0.8 copy-start.12
  98.9 4.6 %copy-start.20 = (f32[4,128]{1,0:T(4,128)S(1)}, f32[4,128]{1,0:T(4,128)}, u32[]{:S(2)}) copy-start(f32[4,128]{1,0:T(4,128)} %param.28) | copy-start | bytes 6148
  98.9 53.9 %all-to-all-start.1 = ((bf16[512,16,128]{2,0,1:T(8,128)(2,1)}), bf16[512,16,128]{2,0,1:T(8,128)(2,1)}, u32[]{:S(2)}, u32[]{:S(2)}) async-start(bf16[512,16,128]{2,0,1:T(8,128)(2,1)} %bitcast.147), calls=%async_computation.1 | async-start | bytes 4194304 | tf_op jit(solution)/shard_map/all_to_all | solution.py:182
  155.4 20.7 %all-to-all-start.2 = ((bf16[32,24,128]{2,1,0:T(8,128)(2,1)}), bf16[32,24,128]{2,1,0:T(8,128)(2,1)S(1)}, u32[]{:S(2)}, u32[]{:S(2)}) async-start(bf16[32,24,128]{2,1,0:T(8,128)(2,1)} %pad_maximum_fusion.2), calls=%async_computation.2 | async-start | bytes 393216 | tf_op jit(solution)/shard_map/all_to_all | solution.py:192
  179.4 0.6 copy-start.18
  196.5 0.8 copy-start.3
  201.9 15.7 %all-to-all-start.4 = ((f32[32,8,128]{2,1,0:T(8,128)}), f32[32,8,128]{2,1,0:T(8,128)}, u32[]{:S(2)}, u32[]{:S(2)}) async-start(f32[32,8,128]{2,1,0:T(8,128)} %bitcast.157), calls=%async_computation.4 | async-start | bytes 262144 | tf_op jit(solution)/shard_map/all_to_all | solution.py:55
  219.6 21.3 %copy-start.15 = (bf16[512,64]{0,1:T(8,128)(2,1)S(1)}, bf16[512,64]{0,1:T(8,128)(2,1)}, u32[]{:S(2)}) copy-start(bf16[512,64]{0,1:T(8,128)(2,1)} %copy-done.14) | copy-start | bytes 196612
  219.6 14.9 %all-to-all-start.5 = ((f32[32,8,128]{2,1,0:T(8,128)}), f32[32,8,128]{2,1,0:T(8,128)S(1)}, u32[]{:S(2)}, u32[]{:S(2)}) async-start(f32[32,8,128]{2,1,0:T(8,128)} %copy.80), calls=%async_computation.5 | async-start | bytes 262144 | tf_op jit(solution)/shard_map/all_to_all | solution.py:65
  234.5 7.7 %copy-start.13 = (bf16[512,64]{0,1:T(8,128)(2,1)S(1)}, bf16[512,64]{0,1:T(8,128)(2,1)}, u32[]{:S(2)}) copy-start(bf16[512,64]{0,1:T(8,128)(2,1)} %copy-done.12) | copy-start | bytes 196612
  234.5 32.7 %all-to-all-start.3 = ((bf16[32,64,256]{2,1,0:T(8,128)(2,1)}), bf16[32,64,256]{2,1,0:T(8,128)(2,1)}, u32[]{:S(2)}, u32[]{:S(2)}) async-start(bf16[32,64,256]{2,1,0:T(8,128)(2,1)} %bitcast.148), calls=%async_computation.3 | async-start | bytes 2097152 | tf_op jit(solution)/shard_map/all_to_all | solution.py:39
  241.0 2.4 copy-start.2
  241.0 2.4 copy-start.7
  241.0 2.4 copy-start.9
  242.2 2.4 copy-start.17
  242.2 2.8 %copy-start.16 = (bf16[128,256]{0,1:T(8,128)(2,1)S(1)}, bf16[128,256]{0,1:T(8,128)(2,1)}, u32[]{:S(2)}) copy-start(bf16[128,256]{0,1:T(8,128)(2,1)} %copy.81) | copy-start | bytes 196612
  243.4 2.0 copy-start.10
  243.4 3.1 %copy-start.19 = (f32[128,128]{1,0:T(8,128)S(1)}, f32[128,128]{1,0:T(8,128)}, u32[]{:S(2)}) copy-start(f32[128,128]{1,0:T(8,128)} %fusion.83) | copy-start | bytes 196612
  243.4 4.7 %copy-start.11 = (bf16[128,128]{1,0:T(8,128)(2,1)S(1)}, bf16[128,128]{1,0:T(8,128)(2,1)}, u32[]{:S(2)}) copy-start(bf16[128,128]{1,0:T(8,128)(2,1)} %param.27) | copy-start | bytes 98308
Sparse Core Ops, SparseCore 0:
  41.7 48.2 all-gather.1

commit v2 on v0

v2 whole, which is shorter than its diff:
```python
import jax
import jax.numpy as jnp
from jax import lax
from jax.experimental import pallas as pl
from jax.experimental.pallas import tpu as pltpu
from jax.sharding import Mesh
from jax.sharding import PartitionSpec as P

D = 2048
TOK = 128
EXP = 32
CAP = 16
ROWS = EXP * CAP
QUART = 512
HALF = 1024
FF = 64
HEADS = 4
HD = 64
STATE = 128
SP = ("z", "x")
TP = ("y", "core")
BF = jnp.bfloat16
F32 = jnp.float32


def iota(shape, dim):
    return lax.broadcasted_iota(jnp.int32, shape, dim)


def mm(a, b, precision=None):
    return lax.dot_general(a, b, (((1,), (0,)), ((), ())), precision=precision, preferred_element_type=F32)


def mm_nt(a, b):
    return lax.dot_general(a, b, (((1,), (1,)), ((), ())), preferred_element_type=F32)


def columns(row):
    return jnp.broadcast_to(row, (8, row.shape[1])).T[:, 0:1]


def vmem():
    return pl.BlockSpec(memory_space=pltpu.VMEM)


def smem():
    return pl.BlockSpec(memory_space=pltpu.SMEM)


def call(kernel, name, outs, specs, args, flops=0):
    return pl.pallas_call(
        kernel,
        out_shape=outs,
        in_specs=specs,
        out_specs=jax.tree.map(lambda _: vmem(), outs),
        compiler_params=pltpu.CompilerParams(vmem_limit_bytes=48 * 1024 * 1024),
        cost_estimate=pl.CostEstimate(flops=flops, bytes_accessed=0, transcendentals=0),
        name=name,
    )(*args)


def prepare_kernel(where, routes, gates, mix, cot, buf, target):
    picks = routes[...]
    expert = iota((EXP, TOK), 0)
    hits = [expert == picks[k : k + 1] for k in range(2)]
    both = jnp.where(hits[0] | hits[1], 1.0, 0.0).astype(BF)
    before = jnp.where(iota((TOK, TOK), 0) < iota((TOK, TOK), 1), 1.0, 0.0).astype(BF)
    count = mm(both, before)
    row = iota((ROWS, TOK), 0)
    cots = cot[...].astype(F32)
    places, scaled, rows = [], [], []
    for k in range(2):
        slot = jnp.sum(jnp.where(hits[k], count, 0.0), axis=0, keepdims=True)
        place = picks[k : k + 1] * CAP + slot.astype(jnp.int32)
        rows.append(place)
        places.append(jnp.where(row == place, 1.0, 0.0).astype(BF))
        scaled.append((columns(gates[k : k + 1, :]) * cots).astype(BF))
    target[...] = jnp.concatenate(rows + [jnp.zeros((6, TOK), jnp.int32)], axis=0)
    toks = mm(places[0] + places[1], mix[...]).astype(BF)
    buf[:, 0:CAP, :] = toks.reshape(EXP, CAP, QUART)
    spread = mm(jnp.concatenate(places, axis=1), jnp.concatenate(scaled, axis=0)).astype(BF)
    buf[:, CAP : 2 * CAP, :] = spread.reshape(EXP, CAP, QUART)


def prepare(quarter, routes, gates, mixed, cotangent):
    whole = lambda i, q: (0, 0)
    part = lambda i, q: (0, q[0])
    return pl.pallas_call(
        prepare_kernel,
        out_shape=(
            jax.ShapeDtypeStruct((EXP, 2 * CAP, QUART), BF),
            jax.ShapeDtypeStruct((8, TOK), jnp.int32),
        ),
        grid_spec=pltpu.PrefetchScalarGridSpec(
            num_scalar_prefetch=1,
            grid=(1,),
            in_specs=[
                pl.BlockSpec((2, TOK), whole),
                pl.BlockSpec((2, TOK), whole),
                pl.BlockSpec((TOK, QUART), part),
                pl.BlockSpec((TOK, QUART), part),
            ],
            out_specs=(
                pl.BlockSpec((EXP, 2 * CAP, QUART), lambda i, q: (0, 0, 0)),
                pl.BlockSpec((8, TOK), whole),
            ),
        ),
        name="prepare",
    )(quarter, routes, gates, mixed, cotangent)


def row_blocks(chunk):
    toks = chunk[:, 0:CAP, :].reshape(ROWS, QUART)
    cots = chunk[:, CAP : 2 * CAP, :].reshape(ROWS, QUART)
    return toks, cots


def expert_kernel(where, c0, c1, c2, c3, own, other, out, g_gate, g_up, g_hid):
    quarter = where[0]
    core = where[1]
    pre = jnp.zeros((ROWS, 4 * FF), F32)
    grad_hidden = jnp.zeros((ROWS, 2 * FF), F32)
    for k, chunk in enumerate((c0, c1, c2, c3)):
        at = pl.ds(pl.multiple_of((quarter ^ k) * QUART, QUART), QUART)
        toks, cots = row_blocks(chunk)
        up_gate = jnp.concatenate([own[0, :, at], other[0, :, at], own[1, :, at], other[1, :, at]], axis=0)
        pre = pre + mm_nt(toks, up_gate)
        grad_hidden = grad_hidden + mm_nt(cots, jnp.concatenate([own[2, :, at], other[2, :, at]], axis=0))
    pre_gate = pre[:, : 2 * FF]
    pre_up = pre[:, 2 * FF :]
    logistic = 1.0 / (1.0 + jnp.exp(-pre_gate))
    active = pre_gate * logistic
    slope = logistic * (1.0 + pre_gate * (1.0 - logistic))
    gate = (grad_hidden * pre_up * slope).astype(BF)
    up = (grad_hidden * active).astype(BF)
    g_gate[...] = gate
    g_up[...] = up
    g_hid[...] = (active * pre_up).astype(BF)
    grads = jnp.concatenate([gate, up], axis=1)
    for k in range(8):
        at = pl.ds(pl.multiple_of((2 * k + core) * TOK, TOK), TOK)
        block = jnp.concatenate([own[0, :, at], other[0, :, at], own[1, :, at], other[1, :, at]], axis=0)
        part = mm(grads, block).astype(BF)
        out[:, :, k * TOK : (k + 1) * TOK] = part.reshape(EXP, CAP, TOK)


def weights_kernel(where, c0, c1, c2, c3, g_gate, g_up, g_hid, d_gate, d_up, d_down):
    quarter = where[0]
    gates = jnp.concatenate([g_gate[...].T[:FF], g_up[...].T[:FF]], axis=0)
    hidden = g_hid[...].T[:FF]
    for k, chunk in enumerate((c0, c1, c2, c3)):
        at = pl.ds(pl.multiple_of((quarter ^ k) * QUART, QUART), QUART)
        toks, cots = row_blocks(chunk)
        both = mm(gates, toks).astype(BF)
        d_gate[:, at] = both[:FF]
        d_up[:, at] = both[FF:]
        d_down[:, at] = mm(hidden, cots).astype(BF)


def combine_kernel(target, rows, out):
    lane = iota((TOK, ROWS), 1)
    places = target[...].T
    pick = jnp.where((lane == places[:, 0:1]) | (lane == places[:, 1:2]), 1.0, 0.0).astype(BF)
    total = mm(pick, rows[...].reshape(ROWS, HALF)).astype(BF)
    for k in range(8):
        out[k] = total[:, k * TOK : (k + 1) * TOK]


def project_kernel(whole, weight, gate_pre, mixer, logs, read, d_gate, gated, grad_y, run, buf):
    back = mm_nt(whole[...], weight[...])
    pre = gate_pre[...].astype(F32)
    saved = mixer[...].astype(F32)
    logistic = 1.0 / (1.0 + jnp.exp(-pre))
    active = pre * logistic
    d_gate[...] = (back * saved * (logistic * (1.0 + pre * (1.0 - logistic)))).astype(BF)
    gated[...] = (saved * active).astype(BF)
    grad = back * active
    grad_y[...] = grad.astype(BF)
    upto = jnp.where(iota((TOK, TOK), 0) <= iota((TOK, TOK), 1), 1.0, 0.0)
    rates = jnp.concatenate([logs[...], jnp.zeros((4, TOK), F32)], axis=0)
    running = mm(rates, upto, lax.Precision.HIGHEST)
    run[...] = running
    start = jnp.exp(running)
    turned = grad.T
    scale = jnp.concatenate([jnp.broadcast_to(start[j : j + 1], (HD, TOK)) for j in range(HEADS)], axis=0)
    state = mm((turned * scale).astype(BF), read[...])
    total = running[0:HEADS, TOK - 1 : TOK]
    first = total.astype(BF).astype(F32)
    second = (total - first).astype(BF).astype(F32)
    third = total - first - second
    line = iota((8, STATE), 0)
    notes = []
    for j in range(HEADS):
        note = jnp.where(line == 0, first[j : j + 1], jnp.where(line == 1, second[j : j + 1], third[j : j + 1]))
        note = jnp.where(line < 3, note, 0.0)
        notes.append(jnp.broadcast_to(note[None], (EXP // HEADS, 8, STATE)))
    sent = jnp.concatenate([state.reshape(EXP, 8, STATE), jnp.concatenate(notes, axis=0)], axis=1)
    buf[...] = sent.astype(BF)


def scan_kernel(received, out):
    state = jnp.zeros((8, STATE), F32)
    for k in reversed(range(EXP)):
        out[k] = state.astype(BF)
        if k > 0:
            piece = received[k].astype(F32)
            log = piece[8:9] + piece[9:10] + piece[10:11]
            state = jnp.exp(log) * state + piece[0:8]


def inner_kernel(grad_y, values, write, read, run, entry, dx, dw, dr):
    running = run[...]
    cols = running.T
    grads = grad_y[...]
    vals = values[...]
    cross = mm_nt(write[...], read[...])
    later = iota((TOK, TOK), 1) >= iota((TOK, TOK), 0)
    total = jnp.zeros((TOK, TOK), F32)
    parts = []
    starts = []
    for j in range(HEADS):
        spread = running[j : j + 1] - cols[:, j : j + 1]
        decay = jnp.where(later, jnp.exp(jnp.where(later, spread, 0.0)), 0.0)
        grad = grads[:, j * HD : (j + 1) * HD]
        parts.append(mm((cross * decay).astype(BF), grad))
        total = total + mm_nt(vals[:, j * HD : (j + 1) * HD], grad) * decay
        starts.append((grad.astype(F32) * jnp.exp(cols[:, j : j + 1])).astype(BF))
    dx[...] = jnp.concatenate(parts, axis=1)
    dw[...] = mm(total.astype(BF), read[...])
    entry_rows = entry[...].reshape(HEADS * HD, STATE).astype(BF)
    dr[...] = mm(total.T.astype(BF), write[...]) + mm(jnp.concatenate(starts, axis=1), entry_rows)


def outer_kernel(dx, dw, values, write, run, state, d_values, d_write):
    running = run[...]
    ends = jnp.exp(running[:, TOK - 1 : TOK] - running).T
    scale = jnp.concatenate([jnp.broadcast_to(ends[:, j : j + 1], (TOK, HD)) for j in range(HEADS)], axis=1)
    later = state[...].reshape(HEADS * HD, STATE)
    d_values[...] = (dx[...] + scale * mm_nt(write[...], later)).astype(BF)
    d_write[...] = dw[...] + mm((values[...].astype(F32) * scale).astype(BF), later)


def body(mixed, cotangent, routes, gates, w_gate, w_up, w_down, out_weight, gate_pre, mixer_out, values,
         write_keys, read_keys, log_decay, entry_states):
    shape = jax.ShapeDtypeStruct
    y = lax.axis_index("y")
    core = lax.axis_index("core")
    swap = [(0, 1), (1, 0)]
    ring = []
    for k in range(8):
        ring.append((2 * k, 2 * ((k + 1) % 8)))
        ring.append((2 * k + 1, 2 * ((k - 1) % 8) + 1))
    quarter = 2 * (y % 2) + core
    where = jnp.stack([quarter, core]).astype(jnp.int32)
    own = jnp.stack([w_gate[0].T, w_up[0].T, w_down[0]])
    other = lax.ppermute(own, "core", swap)
    buf, target = prepare(where, routes.T, gates.T, mixed, cotangent)
    c0 = lax.all_to_all(buf, SP, 0, 0, tiled=True)
    c2 = lax.ppermute(c0, TP, ring)
    c1 = lax.ppermute(c0, "core", swap)
    c3 = lax.ppermute(c2, "core", swap)
    chunks = (c0, c1, c2, c3)
    grad = shape((ROWS, 2 * FF), BF)
    parts, g_gate, g_up, g_hid = call(
        expert_kernel, "expert", (shape((EXP, CAP, HALF), BF), grad, grad, grad),
        [smem()] + [vmem()] * 6, (where, *chunks, own, other))
    back = lax.all_to_all(parts, SP, 0, 0, tiled=True)
    wide = shape((FF, D), BF)
    d_wg, d_wu, d_wd = call(
        weights_kernel, "weights", (wide, wide, wide),
        [smem()] + [vmem()] * 7, (where, *chunks, g_gate, g_up, g_hid), flops=10**9)
    summed = call(combine_kernel, "combine", shape((8, TOK, TOK), BF), [vmem()] * 2, (target, back))
    pieces = lax.all_to_all(summed, "y", 0, 0, tiled=True)
    offset = (2 * y + core) * TOK
    cot_slice = lax.dynamic_slice_in_dim(cotangent, offset, TOK, 1).astype(F32)
    d_input = (cot_slice + jnp.sum(pieces.astype(F32), axis=0)).astype(BF)
    whole = lax.all_gather(d_input, TP, axis=1, tiled=True)
    flat = shape((TOK, HEADS * HD), BF)
    d_gate, gated, grad_y, run, sent = call(
        project_kernel, "project",
        (flat, flat, flat, shape((8, TOK), F32), shape((EXP, 16, STATE), BF)),
        [vmem()] * 6, (whole, out_weight, gate_pre, mixer_out, log_decay, read_keys))
    received = lax.all_to_all(sent, SP, 0, 0, tiled=True)
    part = lax.dot_general(whole, gated, (((0,), (0,)), ((), ())), preferred_element_type=F32).astype(BF)
    shares = lax.all_to_all(part.reshape(EXP, D // EXP, HEADS * HD), SP, 0, 0, tiled=True)
    states = call(scan_kernel, "scan", shape((EXP, 8, STATE), BF), [vmem()], (received,))
    later = lax.all_to_all(states, SP, 0, 0, tiled=True)
    square = shape((TOK, STATE), F32)
    dx, dw, d_read = call(
        inner_kernel, "inner", (shape((TOK, HEADS * HD), F32), square, square),
        [vmem()] * 6, (grad_y, values, write_keys, read_keys, run, entry_states[0]), flops=10**9)
    d_values, d_write = call(
        outer_kernel, "outer", (flat, square), [vmem()] * 6,
        (dx, dw, values, write_keys, run, later))
    d_out_weight = jnp.sum(shares.astype(F32), axis=0)
    return (d_wg.T[None], d_wu.T[None], d_wd[None], d_out_weight, d_input, d_values, d_write, d_read, d_gate)


def solution(mesh):
    finer = Mesh(mesh.devices.reshape(8, 4, 8, 2), ("z", "x", "y", "core"))
    return jax.shard_map(
        body,
        mesh=finer,
        in_specs=(
            P(SP, None),
            P(SP, None),
            P(SP, None),
            P(SP, None),
            P(SP, None, TP),
            P(SP, None, TP),
            P(SP, TP, None),
            P(TP, None),
            P(SP, TP),
            P(SP, TP),
            P(SP, TP),
            P(SP, TP),
            P(SP, TP),
            P(TP, SP),
            P(SP, TP, None, None),
        ),
        out_specs=(
            P(SP, None, TP),
            P(SP, None, TP),
            P(SP, TP, None),
            P(SP, TP),
            P(SP, TP),
            P(SP, TP),
            P(SP, TP),
            P(SP, TP),
            P(SP, TP),
        ),
        check_vma=False,
    )
```

time: 290 us -> 212 us (0.73)
  the two profiles are of different devices: /device:TPU:2 before, /device:TPU:8 now
where the time goes in v2:
time: 212 us; the launch traced here: 211 us
  blocking collectives  109 us (51%)
  waiting for transfers between devices  50.6 us (24%)
  starting transfers between devices  27.3 us (13%)
  Pallas kernels  14 us (7%)
  local copies, waits for them, and re-layouts  4.73 us (2%)
  other arithmetic  3.5 us (2%)
    all_to_all x1, blocking collectives, body(): c0 = lax.all_to_all(buf, SP, 0, 0, tiled=True)  41.4 us
    all_to_all x1, blocking collectives, body(): back = lax.all_to_all(parts, SP, 0, 0, tiled=True)  34 us
    all_to_all x1, waiting for transfers between devices, body(): lax.all_to_all(part.reshape(EXP, D // EXP, HEADS * HD), SP, 0, 0, tiled=T...  19.6 us
    all_gather x1, blocking collectives, body(): whole = lax.all_gather(d_input, TP, axis=1, tiled=True)  17 us
    all_to_all x1, blocking collectives, body(): received = lax.all_to_all(sent, SP, 0, 0, tiled=True)  16.5 us
    ppermute x1, waiting for transfers between devices, body(): c2 = lax.ppermute(c0, TP, ring)  11.3 us
    pallas_call x7, Pallas kernels, call(): pl.pallas_call(kernel, out_shape=outs, in_specs=specs, out_specs=jax.tree...  10.7 us
    all_to_all x1, waiting for transfers between devices, body(): pieces = lax.all_to_all(summed, 'y', 0, 0, tiled=True)  9.22 us
  transfers between devices with their start and end apart: 7, of which 5 were waited for; matrix products, arithmetic and copies ran while one was open for 1% of the time, Pallas kernels for 2%

profile of v2, /device:TPU:8, one launch (start us, length us, event | category | flops | bytes accessed | tf_op | source)
XLA Modules:
  0.0 211.2 jit_solution(11343056397172323298)
XLA Ops:
  0.7 0.6 pad_add_fusion.where
  1.2 3.3 %prepare.1 = (bf16[32,32,512]{2,1,0:T(8,128)(2,1)}, s32[8,128]{1,0:T(8,128)}) custom-call(s32[2]{0:T(128)} %pad_add_fusion.where, s32[2,128]{1,0:T(2,128)} %bitcast.29, f32[2,128]{1,0:T(2,128)} %bitcast.30, bf16[128,2048]{1,0:T(8,128)(2,1)} %mix.1, bf16[128,2048]{1,0:T(8,128)(2,1)} %cot.1), custom_call_target="tpu_custom_call" | custom-call | tf_op jit(solution)/shard_map/prepare/pallas_call | solution.py:88
  4.6 41.4 %all_to_all.30.c0 = bf16[32,32,512]{2,1,0:T(8,128)(2,1)S(1)} all-to-all(bf16[32,32,512]{2,1,0:T(8,128)(2,1)} %get-tuple-element.28), channel_id=1, replica_groups=mesh['z'=8,'x'=4,'y'=8,'core'=2] {'z','x'}, dimensions={0} | all-to-all | bytes 2097152 | tf_op jit(solution)/shard_map/all_to_all | solution.py:258
  45.9 3.6 %collective-permute-start.1 = (bf16[32,32,512]{2,1,0:T(8,128)(2,1)S(1)}, bf16[32,32,512]{2,1,0:T(8,128)(2,1)S(1)}, u32[]{:S(2)}, u32[]{:S(2)}) collective-permute-start(bf16[32,32,512]{2,1,0:T(8,128)(2,1)S(1)} %all_to_all.30.c0), channel_id=1, source_target_pairs={{0,2},{1,15},{2,4},{3,1},{4,6},{5,3},{6,8},{7,5},{8,10},{9,7},{10,... | collective-permute-start | bytes 3145736 | tf_op jit(solution)/shard_map/ppermute | solution.py:259
  49.5 1.9 collective-permute-start
  51.5 11.3 %collective-permute-done.1.c2 = bf16[32,32,512]{2,1,0:T(8,128)(2,1)S(1)} collective-permute-done((bf16[32,32,512]{2,1,0:T(8,128)(2,1)S(1)}, bf16[32,32,512]{2,1,0:T(8,128)(2,1)S(1)}, u32[]{:S(2)}, u32[]{:S(2)}) %collective-permute-start.1) | collective-permute-done | bytes 1048608 | tf_op jit(solution)/shard_map/ppermute | solution.py:259
  62.7 1.9 collective-permute-start.2
  64.8 2.4 %collective-permute-start.3 = (bf16[3,64,2048]{2,1,0:T(8,128)(2,1)S(1)}, bf16[3,64,2048]{2,1,0:T(8,128)(2,1)S(1)}, u32[]{:S(2)}, u32[]{:S(2)}) collective-permute-start(bf16[3,64,2048]{2,1,0:T(8,128)(2,1)S(1)} %pad_maximum_fusion.own), channel_id=1, source_target_pairs={{0,1},{1,0},{2,3},{3,2},{4,5},{5,4},{6,7},{7,6},{8,9},{9,8},{10,11... | collective-permute-start | bytes 2359304 | tf_op jit(solution)/shard_map/ppermute | solution.py:256
  67.2 1.9 collective-permute-done.3.other
  69.1 1.0 copy-done.2
  70.1 3.1 %expert.1 = (bf16[32,16,1024]{2,1,0:T(8,128)(2,1)S(1)}, bf16[512,128]{1,0:T(8,128)(2,1)S(1)}, bf16[512,128]{1,0:T(8,128)(2,1)S(1)}, bf16[512,128]{1,0:T(8,128)(2,1)S(1)}) custom-call(s32[2]{0:T(128)S(1)} %copy-done.10, bf16[32,32,512]{2,1,0:T(8,128)(2,1)S(1)} %all_to_all.30.c0, bf16[32,32,512]{2,1,0:T(8,128)(2,1)S(1)} %collective-permute-done.c1, ...), custom_call_target="tpu_custom_call" | custom-call | tf_op jit(solution)/shard_map/expert/pallas_call | solution.py:51
  73.2 34.0 %all_to_all.31.rows = bf16[32,16,1024]{2,1,0:T(8,128)(2,1)S(1)} all-to-all(bf16[32,16,1024]{2,1,0:T(8,128)(2,1)S(1)} %get-tuple-element.36), channel_id=1, replica_groups=mesh['z'=8,'x'=4,'y'=8,'core'=2] {'z','x'}, dimensions={0} | all-to-all | bytes 2097152 | tf_op jit(solution)/shard_map/all_to_all | solution.py:267
  107.2 1.2 combine.1
  108.3 8.9 %all-to-all-start.2 = ((bf16[8,128,128]{2,1,0:T(8,128)(2,1)}), bf16[8,128,128]{2,1,0:T(8,128)(2,1)S(1)}, u32[]{:S(2)}, u32[]{:S(2)}) async-start(bf16[8,128,128]{2,1,0:T(8,128)(2,1)} %combine.1), calls=%async_computation.2 | async-start | bytes 524288 | tf_op jit(solution)/shard_map/all_to_all | solution.py:273
  117.2 9.2 %all-to-all-done.2 = bf16[8,128,128]{2,1,0:T(8,128)(2,1)S(1)} async-done(((bf16[8,128,128]{2,1,0:T(8,128)(2,1)}), bf16[8,128,128]{2,1,0:T(8,128)(2,1)S(1)}, u32[]{:S(2)}, u32[]{:S(2)}) %all-to-all-start.2) | async-done | bytes 262176 | tf_op jit(solution)/shard_map/all_to_all | solution.py:273
  126.5 0.8 add_convert_fusion
  127.3 17.0 %all_gather.3.whole = bf16[128,2048]{1,0:T(8,128)(2,1)S(1)} all-gather(bf16[128,128]{1,0:T(8,128)(2,1)S(1)} %add_convert_fusion), channel_id=1, replica_groups=mesh['z'=8,'x'=4,'y'=8,'core'=2] {'y','core'}, dimensions={1}, use_global_device_ids=true | all-gather | bytes 557056 | tf_op jit(solution)/shard_map/all_gather | solution.py:277
  144.3 1.2 copy-done.4
  145.6 1.2 project.1
  146.7 16.5 %all_to_all.32.received = bf16[32,16,128]{2,1,0:T(8,128)(2,1)S(1)} all-to-all(bf16[32,16,128]{2,1,0:T(8,128)(2,1)S(1)} %get-tuple-element.42), channel_id=1, replica_groups=mesh['z'=8,'x'=4,'y'=8,'core'=2] {'z','x'}, dimensions={0} | all-to-all | bytes 262144 | tf_op jit(solution)/shard_map/all_to_all | solution.py:283
  163.3 0.7 scan.1
  164.0 3.9 %all-to-all-start.5 = ((bf16[32,8,128]{2,1,0:T(8,128)(2,1)}), bf16[32,8,128]{2,1,0:T(8,128)(2,1)S(1)}, u32[]{:S(2)}, u32[]{:S(2)}) async-start(bf16[32,8,128]{2,1,0:T(8,128)(2,1)} %scan.1), calls=%async_computation.5 | async-start | bytes 131072 | tf_op jit(solution)/shard_map/all_to_all | solution.py:287
  167.9 1.4 convolution_convert_fusion
  169.3 8.6 %all-to-all-done.5.state = bf16[32,8,128]{2,1,0:T(8,128)(2,1)S(1)} async-done(((bf16[32,8,128]{2,1,0:T(8,128)(2,1)}), bf16[32,8,128]{2,1,0:T(8,128)(2,1)S(1)}, u32[]{:S(2)}, u32[]{:S(2)}) %all-to-all-start.5) | async-done | bytes 65568 | tf_op jit(solution)/shard_map/all_to_all | solution.py:287
  177.9 4.7 %all-to-all-start.3 = ((bf16[32,64,256]{2,1,0:T(8,128)(2,1)}), bf16[32,64,256]{2,1,0:T(8,128)(2,1)}, u32[]{:S(2)}, u32[]{:S(2)}) async-start(bf16[32,64,256]{2,1,0:T(8,128)(2,1)} %bitcast.26), calls=%async_computation.3 | async-start | bytes 2097152 | tf_op jit(solution)/shard_map/all_to_all | solution.py:285
  182.6 1.2 copy-done.1
  183.8 1.2 copy-done.3
  185.0 2.2 %weights.1 = (bf16[64,2048]{1,0:T(8,128)(2,1)}, bf16[64,2048]{1,0:T(8,128)(2,1)}, bf16[64,2048]{1,0:T(8,128)(2,1)}) custom-call(s32[2]{0:T(128)S(1)} %copy-done.10, bf16[32,32,512]{2,1,0:T(8,128)(2,1)S(1)} %all_to_all.30.c0, bf16[32,32,512]{2,1,0:T(8,128)(2,1)S(1)} %copy-done.1, bf16[32,32,512]{2,1,0:T(8,128)(2,1)S(1)} %collective-permute-done.1.c2, ...), custom_call_target="tpu_custom_call" | custom-call | flops 1000000000 | tf_op jit(solution)/shard_map/weights/pallas_call | solution.py:51
  187.2 1.3 inner.1
  188.5 1.1 outer.1
  189.6 19.6 %all-to-all-done.3 = bf16[32,64,256]{2,1,0:T(8,128)(2,1)} async-done(((bf16[32,64,256]{2,1,0:T(8,128)(2,1)}), bf16[32,64,256]{2,1,0:T(8,128)(2,1)}, u32[]{:S(2)}, u32[]{:S(2)}) %all-to-all-start.3) | async-done | bytes 1048608 | tf_op jit(solution)/shard_map/all_to_all | solution.py:285
  209.2 2.0 convert_reduce_fusion
  (36 shorter events, 0.2 us)
Async XLA Ops:
  4.5 60.1 %copy-start.14 = (bf16[1,64,2048]{2,1,0:T(8,128)(2,1)S(1)}, bf16[1,64,2048]{2,1,0:T(8,128)(2,1)}, u32[]{:S(2)}) copy-start(bf16[1,64,2048]{2,1,0:T(8,128)(2,1)} %param.21) | copy-start | bytes 786436
  4.5 60.1 %copy-start.15 = (bf16[1,2048,64]{1,2,0:T(8,128)(2,1)S(1)}, bf16[1,2048,64]{1,2,0:T(8,128)(2,1)}, u32[]{:S(2)}) copy-start(bf16[1,2048,64]{1,2,0:T(8,128)(2,1)} %param.20) | copy-start | bytes 786436
  4.5 60.1 %copy-start.16 = (bf16[1,2048,64]{1,2,0:T(8,128)(2,1)S(1)}, bf16[1,2048,64]{1,2,0:T(8,128)(2,1)}, u32[]{:S(2)}) copy-start(bf16[1,2048,64]{1,2,0:T(8,128)(2,1)} %param.19) | copy-start | bytes 786436
  45.9 24.2 %copy-start.10 = (s32[2]{0:T(128)S(1)}, s32[2]{0:T(128)}, u32[]{:S(2)}) copy-start(s32[2]{0:T(128)} %pad_add_fusion.where) | copy-start | bytes 28
  45.9 16.8 %collective-permute-start.1 = (bf16[32,32,512]{2,1,0:T(8,128)(2,1)S(1)}, bf16[32,32,512]{2,1,0:T(8,128)(2,1)S(1)}, u32[]{:S(2)}, u32[]{:S(2)}) collective-permute-start(bf16[32,32,512]{2,1,0:T(8,128)(2,1)S(1)} %all_to_all.30.c0), channel_id=1, source_target_pairs={{0,2},{1,15},{2,4},{3,1},{4,6},{5,3},{6,8},{7,5},{8,10},{9,7},{10,... | collective-permute-start | bytes 3145736 | tf_op jit(solution)/shard_map/ppermute | solution.py:259
  49.5 19.6 %collective-permute-start = (bf16[32,32,512]{2,1,0:T(8,128)(2,1)S(1)}, bf16[32,32,512]{2,1,0:T(8,128)(2,1)S(1)}, u32[]{:S(2)}, u32[]{:S(2)}) collective-permute-start(bf16[32,32,512]{2,1,0:T(8,128)(2,1)S(1)} %all_to_all.30.c0), channel_id=1, source_target_pairs={{0,1},{1,0},{2,3},{3,2},{4,5},{5,4},{6,7},{7,6},{8,9},{9,8},{10,11... | collective-permute-start | bytes 3145736 | tf_op jit(solution)/shard_map/ppermute | solution.py:260
  62.7 6.4 %collective-permute-start.2 = (bf16[32,32,512]{2,1,0:T(8,128)(2,1)S(1)}, bf16[32,32,512]{2,1,0:T(8,128)(2,1)S(1)}, u32[]{:S(2)}, u32[]{:S(2)}) collective-permute-start(bf16[32,32,512]{2,1,0:T(8,128)(2,1)S(1)} %collective-permute-done.1.c2), channel_id=1, source_target_pairs={{0,1},{1,0},{2,3},{3,2},{4,5},{5,4},{6,7},{7,6},{8,9},{9,8},{10,11... | collective-permute-start | bytes 3145736 | tf_op jit(solution)/shard_map/ppermute | solution.py:261
  64.8 4.3 %collective-permute-start.3 = (bf16[3,64,2048]{2,1,0:T(8,128)(2,1)S(1)}, bf16[3,64,2048]{2,1,0:T(8,128)(2,1)S(1)}, u32[]{:S(2)}, u32[]{:S(2)}) collective-permute-start(bf16[3,64,2048]{2,1,0:T(8,128)(2,1)S(1)} %pad_maximum_fusion.own), channel_id=1, source_target_pairs={{0,1},{1,0},{2,3},{3,2},{4,5},{5,4},{6,7},{7,6},{8,9},{9,8},{10,11... | collective-permute-start | bytes 2359304 | tf_op jit(solution)/shard_map/ppermute | solution.py:256
  69.1 4.1 %copy-start = (bf16[32,32,512]{2,1,0:T(8,128)(2,1)}, bf16[32,32,512]{2,1,0:T(8,128)(2,1)S(1)}, u32[]{:S(2)}) copy-start(bf16[32,32,512]{2,1,0:T(8,128)(2,1)S(1)} %collective-permute-done.c1) | copy-start | bytes 3145732
  69.1 1.0 copy-start.2
  73.2 34.0 %copy-start.11 = (s32[8,128]{1,0:T(8,128)S(1)}, s32[8,128]{1,0:T(8,128)}, u32[]{:S(2)}) copy-start(s32[8,128]{1,0:T(8,128)} %get-tuple-element.35.target) | copy-start | bytes 12292
  108.3 36.0 %copy-start.6 = (bf16[128,256]{1,0:T(8,128)(2,1)S(1)}, bf16[128,256]{1,0:T(8,128)(2,1)}, u32[]{:S(2)}) copy-start(bf16[128,256]{1,0:T(8,128)(2,1)} %gate_pre.1) | copy-start | bytes 196612
  108.3 36.0 %copy-start.7 = (bf16[128,256]{1,0:T(8,128)(2,1)S(1)}, bf16[128,256]{1,0:T(8,128)(2,1)}, u32[]{:S(2)}) copy-start(bf16[128,256]{1,0:T(8,128)(2,1)} %mixer.1) | copy-start | bytes 196612
  108.3 36.0 %copy-start.8 = (bf16[128,128]{1,0:T(8,128)(2,1)S(1)}, bf16[128,128]{1,0:T(8,128)(2,1)}, u32[]{:S(2)}) copy-start(bf16[128,128]{1,0:T(8,128)(2,1)} %read.3) | copy-start | bytes 98308
  108.3 36.0 %copy-start.12 = (f32[4,128]{1,0:T(4,128)S(1)}, f32[4,128]{1,0:T(4,128)}, u32[]{:S(2)}) copy-start(f32[4,128]{1,0:T(4,128)} %logs.1) | copy-start | bytes 6148
  108.3 18.1 %all-to-all-start.2 = ((bf16[8,128,128]{2,1,0:T(8,128)(2,1)}), bf16[8,128,128]{2,1,0:T(8,128)(2,1)S(1)}, u32[]{:S(2)}, u32[]{:S(2)}) async-start(bf16[8,128,128]{2,1,0:T(8,128)(2,1)} %combine.1), calls=%async_computation.2 | async-start | bytes 524288 | tf_op jit(solution)/shard_map/all_to_all | solution.py:273
  127.3 19.4 %copy-start.17 = (bf16[128,128]{1,0:T(8,128)(2,1)}, bf16[128,128]{1,0:T(8,128)(2,1)S(1)}, u32[]{:S(2)}) copy-start(bf16[128,128]{1,0:T(8,128)(2,1)S(1)} %add_convert_fusion) | copy-start | bytes 98308
  144.3 1.2 copy-start.4
  164.0 13.9 %all-to-all-start.5 = ((bf16[32,8,128]{2,1,0:T(8,128)(2,1)}), bf16[32,8,128]{2,1,0:T(8,128)(2,1)S(1)}, u32[]{:S(2)}, u32[]{:S(2)}) async-start(bf16[32,8,128]{2,1,0:T(8,128)(2,1)} %scan.1), calls=%async_computation.5 | async-start | bytes 131072 | tf_op jit(solution)/shard_map/all_to_all | solution.py:287
  177.9 31.4 %all-to-all-start.3 = ((bf16[32,64,256]{2,1,0:T(8,128)(2,1)}), bf16[32,64,256]{2,1,0:T(8,128)(2,1)}, u32[]{:S(2)}, u32[]{:S(2)}) async-start(bf16[32,64,256]{2,1,0:T(8,128)(2,1)} %bitcast.26), calls=%async_computation.3 | async-start | bytes 2097152 | tf_op jit(solution)/shard_map/all_to_all | solution.py:285
  182.5 1.2 copy-start.1
  183.8 1.2 copy-start.3
  185.0 2.2 %copy-start.5 = (bf16[128,256]{1,0:T(8,128)(2,1)S(1)}, bf16[128,256]{1,0:T(8,128)(2,1)}, u32[]{:S(2)}) copy-start(bf16[128,256]{1,0:T(8,128)(2,1)} %values.3) | copy-start | bytes 196612
  185.0 2.2 %copy-start.9 = (bf16[128,128]{1,0:T(8,128)(2,1)S(1)}, bf16[128,128]{1,0:T(8,128)(2,1)}, u32[]{:S(2)}) copy-start(bf16[128,128]{1,0:T(8,128)(2,1)} %write.3) | copy-start | bytes 98308
  185.0 2.2 %copy-start.13 = (f32[1,4,64,128]{3,2,1,0:T(8,128)S(1)}, f32[1,4,64,128]{3,2,1,0:T(8,128)}, u32[]{:S(2)}) copy-start(f32[1,4,64,128]{3,2,1,0:T(8,128)} %param.29) | copy-start | bytes 393220

commit v3 on v2

--- a/solution.py
+++ b/solution.py
@@ -11,8 +11,7 @@
 EXP = 32
 CAP = 16
 ROWS = EXP * CAP
-QUART = 512
-HALF = 1024
+WIDE = 256
 FF = 64
 HEADS = 4
 HD = 64
@@ -47,15 +46,14 @@
     return pl.BlockSpec(memory_space=pltpu.SMEM)
 
 
-def call(kernel, name, outs, specs, args, flops=0):
+def call(kernel, outs, specs, args, flops=0):
     return pl.pallas_call(
         kernel,
         out_shape=outs,
         in_specs=specs,
         out_specs=jax.tree.map(lambda _: vmem(), outs),
-        compiler_params=pltpu.CompilerParams(vmem_limit_bytes=48 * 1024 * 1024),
+        compiler_params=pltpu.CompilerParams(vmem_limit_bytes=20 * 1024 * 1024),
         cost_estimate=pl.CostEstimate(flops=flops, bytes_accessed=0, transcendentals=0),
-        name=name,
     )(*args)
 
 
@@ -77,9 +75,9 @@
         scaled.append((columns(gates[k : k + 1, :]) * cots).astype(BF))
     target[...] = jnp.concatenate(rows + [jnp.zeros((6, TOK), jnp.int32)], axis=0)
     toks = mm(places[0] + places[1], mix[...]).astype(BF)
-    buf[:, 0:CAP, :] = toks.reshape(EXP, CAP, QUART)
+    buf[:, 0:CAP, :] = toks.reshape(EXP, CAP, WIDE)
     spread = mm(jnp.concatenate(places, axis=1), jnp.concatenate(scaled, axis=0)).astype(BF)
-    buf[:, CAP : 2 * CAP, :] = spread.reshape(EXP, CAP, QUART)
+    buf[:, CAP : 2 * CAP, :] = spread.reshape(EXP, CAP, WIDE)
 
 
 def prepare(quarter, routes, gates, mixed, cotangent):
@@ -88,7 +86,7 @@
     return pl.pallas_call(
         prepare_kernel,
         out_shape=(
-            jax.ShapeDtypeStruct((EXP, 2 * CAP, QUART), BF),
+            jax.ShapeDtypeStruct((EXP, 2 * CAP, WIDE), BF),
             jax.ShapeDtypeStruct((8, TOK), jnp.int32),
         ),
         grid_spec=pltpu.PrefetchScalarGridSpec(
@@ -97,11 +95,11 @@
             in_specs=[
                 pl.BlockSpec((2, TOK), whole),
                 pl.BlockSpec((2, TOK), whole),
-                pl.BlockSpec((TOK, QUART), part),
-                pl.BlockSpec((TOK, QUART), part),
+                pl.BlockSpec((TOK, WIDE), part),
+                pl.BlockSpec((TOK, WIDE), part),
             ],
             out_specs=(
-                pl.BlockSpec((EXP, 2 * CAP, QUART), lambda i, q: (0, 0, 0)),
+                pl.BlockSpec((EXP, 2 * CAP, WIDE), lambda i, q: (0, 0, 0)),
                 pl.BlockSpec((8, TOK), whole),
             ),
         ),
@@ -110,21 +108,25 @@
 
 
 def row_blocks(chunk):
-    toks = chunk[:, 0:CAP, :].reshape(ROWS, QUART)
-    cots = chunk[:, CAP : 2 * CAP, :].reshape(ROWS, QUART)
+    toks = chunk[:, 0:CAP, :].reshape(ROWS, WIDE)
+    cots = chunk[:, CAP : 2 * CAP, :].reshape(ROWS, WIDE)
     return toks, cots
 
 
-def expert_kernel(where, c0, c1, c2, c3, own, other, out, g_gate, g_up, g_hid):
-    quarter = where[0]
-    core = where[1]
+def gate_rows(own, other, at):
+    return jnp.concatenate([own[0, :, at], other[0, :, at], own[1, :, at], other[1, :, at]], axis=0)
+
+
+def expert_kernel(where, *refs):
+    chunks = refs[:8]
+    own, other, out, g_gate, g_up, g_hid = refs[8:]
+    core = where[8]
     pre = jnp.zeros((ROWS, 4 * FF), F32)
     grad_hidden = jnp.zeros((ROWS, 2 * FF), F32)
-    for k, chunk in enumerate((c0, c1, c2, c3)):
-        at = pl.ds(pl.multiple_of((quarter ^ k) * QUART, QUART), QUART)
-        toks, cots = row_blocks(chunk)
-        up_gate = jnp.concatenate([own[0, :, at], other[0, :, at], own[1, :, at], other[1, :, at]], axis=0)
-        pre = pre + mm_nt(toks, up_gate)
+    for k in range(8):
+        at = pl.ds(pl.multiple_of(where[k] * WIDE, WIDE), WIDE)
+        toks, cots = row_blocks(chunks[k])
+        pre = pre + mm_nt(toks, gate_rows(own, other, at))
         grad_hidden = grad_hidden + mm_nt(cots, jnp.concatenate([own[2, :, at], other[2, :, at]], axis=0))
     pre_gate = pre[:, : 2 * FF]
     pre_up = pre[:, 2 * FF :]
@@ -139,41 +141,59 @@
     grads = jnp.concatenate([gate, up], axis=1)
     for k in range(8):
         at = pl.ds(pl.multiple_of((2 * k + core) * TOK, TOK), TOK)
-        block = jnp.concatenate([own[0, :, at], other[0, :, at], own[1, :, at], other[1, :, at]], axis=0)
-        part = mm(grads, block).astype(BF)
-        out[:, :, k * TOK : (k + 1) * TOK] = part.reshape(EXP, CAP, TOK)
-
-
-def weights_kernel(where, c0, c1, c2, c3, g_gate, g_up, g_hid, d_gate, d_up, d_down):
-    quarter = where[0]
+        out[k] = mm(grads, gate_rows(own, other, at)).astype(BF)
+
+
+def weights_kernel(where, *refs):
+    chunks = refs[:8]
+    g_gate, g_up, g_hid, d_gate, d_up, d_down = refs[8:]
     gates = jnp.concatenate([g_gate[...].T[:FF], g_up[...].T[:FF]], axis=0)
     hidden = g_hid[...].T[:FF]
-    for k, chunk in enumerate((c0, c1, c2, c3)):
-        at = pl.ds(pl.multiple_of((quarter ^ k) * QUART, QUART), QUART)
-        toks, cots = row_blocks(chunk)
+    for k in range(8):
+        at = pl.ds(pl.multiple_of(where[k] * WIDE, WIDE), WIDE)
+        toks, cots = row_blocks(chunks[k])
         both = mm(gates, toks).astype(BF)
         d_gate[:, at] = both[:FF]
         d_up[:, at] = both[FF:]
         d_down[:, at] = mm(hidden, cots).astype(BF)
 
 
-def combine_kernel(target, rows, out):
+def combine_kernel(where, target, rows, cot, out):
     lane = iota((TOK, ROWS), 1)
     places = target[...].T
     pick = jnp.where((lane == places[:, 0:1]) | (lane == places[:, 1:2]), 1.0, 0.0).astype(BF)
-    total = mm(pick, rows[...].reshape(ROWS, HALF)).astype(BF)
-    for k in range(8):
-        out[k] = total[:, k * TOK : (k + 1) * TOK]
-
-
-def project_kernel(whole, weight, gate_pre, mixer, logs, read, d_gate, gated, grad_y, run, buf):
+    out[...] = (cot[...].astype(F32) + mm(pick, rows[...].reshape(ROWS, TOK))).astype(BF)
+
+
+def combine(slot, target, rows, cotangent):
+    return pl.pallas_call(
+        combine_kernel,
+        out_shape=jax.ShapeDtypeStruct((TOK, TOK), BF),
+        grid_spec=pltpu.PrefetchScalarGridSpec(
+            num_scalar_prefetch=1,
+            grid=(1,),
+            in_specs=[
+                pl.BlockSpec((8, TOK), lambda i, q: (0, 0)),
+                pl.BlockSpec((EXP, CAP, TOK), lambda i, q: (0, 0, 0)),
+                pl.BlockSpec((TOK, TOK), lambda i, q: (0, q[0])),
+            ],
+            out_specs=pl.BlockSpec((TOK, TOK), lambda i, q: (0, 0)),
+        ),
+        name="combine",
+    )(slot, target, rows, cotangent)
+
+
+def project_kernel(whole, weight, gate_pre, mixer, logs, read, d_gate, grad_y, run, buf):
     back = mm_nt(whole[...], weight[...])
     pre = gate_pre[...].astype(F32)
     saved = mixer[...].astype(F32)
     logistic = 1.0 / (1.0 + jnp.exp(-pre))
     active = pre * logistic
     d_gate[...] = (back * saved * (logistic * (1.0 + pre * (1.0 - logistic)))).astype(BF)
-    gated[...] = (saved * active).astype(BF)
+    gated = (saved * active).astype(BF)
+    for k in range(8):
+        turned = whole[:, k * WIDE : (k + 1) * WIDE].T
+        buf[4 * k : 4 * k + 4, 0:FF, :] = mm(turned, gated).astype(BF).reshape(4, FF, WIDE)
     grad = back * active
     grad_y[...] = grad.astype(BF)
     upto = jnp.where(iota((TOK, TOK), 0) <= iota((TOK, TOK), 1), 1.0, 0.0)
@@ -194,8 +214,8 @@
         note = jnp.where(line == 0, first[j : j + 1], jnp.where(line == 1, second[j : j + 1], third[j : j + 1]))
         note = jnp.where(line < 3, note, 0.0)
         notes.append(jnp.broadcast_to(note[None], (EXP // HEADS, 8, STATE)))
-    sent = jnp.concatenate([state.reshape(EXP, 8, STATE), jnp.concatenate(notes, axis=0)], axis=1)
-    buf[...] = sent.astype(BF)
+    buf[:, FF:, 0:STATE] = state.reshape(EXP, 8, STATE).astype(BF)
+    buf[:, FF:, STATE:] = jnp.concatenate(notes, axis=0).astype(BF)
 
 
 def scan_kernel(received, out):
@@ -203,9 +223,10 @@
     for k in reversed(range(EXP)):
         out[k] = state.astype(BF)
         if k > 0:
-            piece = received[k].astype(F32)
-            log = piece[8:9] + piece[9:10] + piece[10:11]
-            state = jnp.exp(log) * state + piece[0:8]
+            piece = received[k, FF:, :].astype(F32)
+            note = piece[:, STATE:]
+            log = note[0:1] + note[1:2] + note[2:3]
+            state = jnp.exp(log) * state + piece[:, :STATE]
 
 
 def inner_kernel(grad_y, values, write, read, run, entry, dx, dw, dr):
@@ -240,7 +261,7 @@
     d_write[...] = dw[...] + mm((values[...].astype(F32) * scale).astype(BF), later)
 
 
-def body(mixed, cotangent, routes, gates, w_gate, w_up, w_down, out_weight, gate_pre, mixer_out, values,
+def step(mixed, cotangent, routes, gates, w_gate, w_up, w_down, out_weight, gate_pre, mixer_out, values,
          write_keys, read_keys, log_decay, entry_states):
     shape = jax.ShapeDtypeStruct
     y = lax.axis_index("y")
@@ -250,56 +271,66 @@
     for k in range(8):
         ring.append((2 * k, 2 * ((k + 1) % 8)))
         ring.append((2 * k + 1, 2 * ((k - 1) % 8) + 1))
-    quarter = 2 * (y % 2) + core
-    where = jnp.stack([quarter, core]).astype(jnp.int32)
+    turn = 2 * core - 1
+    near, far, beyond = (y + turn) % 4, (y - turn) % 4, (y + 2) % 4
+    mine, theirs = core, 1 - core
+    home = 2 * (y % 4)
+    ids = [home + mine, home + theirs, 2 * near + mine, 2 * near + theirs, 2 * beyond + mine,
+           2 * far + theirs, 2 * far + mine, 2 * beyond + theirs, core]
+    where = jnp.stack(ids).astype(jnp.int32)
+    slot = (2 * y + core).astype(jnp.int32).reshape(1)
     own = jnp.stack([w_gate[0].T, w_up[0].T, w_down[0]])
     other = lax.ppermute(own, "core", swap)
     buf, target = prepare(where, routes.T, gates.T, mixed, cotangent)
     c0 = lax.all_to_all(buf, SP, 0, 0, tiled=True)
     c2 = lax.ppermute(c0, TP, ring)
     c1 = lax.ppermute(c0, "core", swap)
-    c3 = lax.ppermute(c2, "core", swap)
-    chunks = (c0, c1, c2, c3)
+    c3 = lax.ppermute(c1, TP, ring)
+    c4 = lax.ppermute(c2, TP, ring)
+    moved, other = lax.optimization_barrier((c2, other))
+    c5 = lax.ppermute(moved, "core", swap)
+    c6 = lax.ppermute(c3, "core", swap)
+    c7 = lax.ppermute(c4, "core", swap)
+    chunks = (c0, c1, c2, c3, c4, c5, c6, c7)
     grad = shape((ROWS, 2 * FF), BF)
     parts, g_gate, g_up, g_hid = call(
-        expert_kernel, "expert", (shape((EXP, CAP, HALF), BF), grad, grad, grad),
-        [smem()] + [vmem()] * 6, (where, *chunks, own, other))
-    back = lax.all_to_all(parts, SP, 0, 0, tiled=True)
+        expert_kernel, (shape((8, ROWS, TOK), BF), grad, grad, grad),
+        [smem()] + [vmem()] * 10, (where, *chunks, own, other))
+    pieces = lax.all_to_all(parts, "y", 0, 0, tiled=True)
     wide = shape((FF, D), BF)
     d_wg, d_wu, d_wd = call(
-        weights_kernel, "weights", (wide, wide, wide),
-        [smem()] + [vmem()] * 7, (where, *chunks, g_gate, g_up, g_hid), flops=10**9)
-    summed = call(combine_kernel, "combine", shape((8, TOK, TOK), BF), [vmem()] * 2, (target, back))
-    pieces = lax.all_to_all(summed, "y", 0, 0, tiled=True)
-    offset = (2 * y + core) * TOK
-    cot_slice = lax.dynamic_slice_in_dim(cotangent, offset, TOK, 1).astype(F32)
-    d_input = (cot_slice + jnp.sum(pieces.astype(F32), axis=0)).astype(BF)
+        weights_kernel, (wide, wide, wide),
+        [smem()] + [vmem()] * 11, (where, *chunks, g_gate, g_up, g_hid), flops=10**9)
+    pieces, d_wg, d_wu, d_wd = lax.optimization_barrier((pieces, d_wg, d_wu, d_wd))
+    summed = jnp.sum(pieces.astype(F32), axis=0).astype(BF).reshape(EXP, CAP, TOK)
+    back = lax.all_to_all(summed, SP, 0, 0, tiled=True)
+    d_input = combine(slot, target, back, cotangent)
     whole = lax.all_gather(d_input, TP, axis=1, tiled=True)
     flat = shape((TOK, HEADS * HD), BF)
-    d_gate, gated, grad_y, run, sent = call(
-        project_kernel, "project",
-        (flat, flat, flat, shape((8, TOK), F32), shape((EXP, 16, STATE), BF)),
+    d_gate, grad_y, run, sent = call(
+        project_kernel,
+        (flat, flat, shape((8, TOK), F32), shape((EXP, FF + 8, WIDE), BF)),
         [vmem()] * 6, (whole, out_weight, gate_pre, mixer_out, log_decay, read_keys))
     received = lax.all_to_all(sent, SP, 0, 0, tiled=True)
-    part = lax.dot_general(whole, gated, (((0,), (0,)), ((), ())), preferred_element_type=F32).astype(BF)
-    shares = lax.all_to_all(part.reshape(EXP, D // EXP, HEADS * HD), SP, 0, 0, tiled=True)
-    states = call(scan_kernel, "scan", shape((EXP, 8, STATE), BF), [vmem()], (received,))
-    later = lax.all_to_all(states, SP, 0, 0, tiled=True)
     square = shape((TOK, STATE), F32)
     dx, dw, d_read = call(
-        inner_kernel, "inner", (shape((TOK, HEADS * HD), F32), square, square),
+        inner_kernel, (shape((TOK, HEADS * HD), F32), square, square),
         [vmem()] * 6, (grad_y, values, write_keys, read_keys, run, entry_states[0]), flops=10**9)
+    received, dx, dw, d_read = lax.optimization_barrier((received, dx, dw, d_read))
+    states = call(scan_kernel, shape((EXP, 8, STATE), BF), [vmem()], (received,))
+    later = lax.all_to_all(states, SP, 0, 0, tiled=True)
+    d_out_weight = jnp.sum(received[:, :FF].astype(F32), axis=0)
+    later, d_out_weight = lax.optimization_barrier((later, d_out_weight))
     d_values, d_write = call(
-        outer_kernel, "outer", (flat, square), [vmem()] * 6,
+        outer_kernel, (flat, square), [vmem()] * 6,
         (dx, dw, values, write_keys, run, later))
-    d_out_weight = jnp.sum(shares.astype(F32), axis=0)
     return (d_wg.T[None], d_wu.T[None], d_wd[None], d_out_weight, d_input, d_values, d_write, d_read, d_gate)
 
 
 def solution(mesh):
     finer = Mesh(mesh.devices.reshape(8, 4, 8, 2), ("z", "x", "y", "core"))
     return jax.shard_map(
-        body,
+        step,
         mesh=finer,
         in_specs=(
             P(SP, None),

time: 212 us -> 201 us (0.948)
  blocking collectives: 109 us -> 48.3 us
  waiting for transfers between devices: 50.6 us -> 84.3 us
  starting transfers between devices: 27.3 us -> 44.7 us
    all_to_all x3 -> x1, blocking collectives: 91.9 us -> 31.1 us  [step(): c0 = lax.all_to_all(buf, SP, 0, 0, tiled=True)]
    all_to_all x3 -> x4, waiting for transfers between devices: 37.4 us -> 73.8 us  [the longest x1 30.6 us: step(): received = lax.all_to_all(sent, SP, 0, 0, tiled=True)]
    ppermute x4 -> x8, starting transfers between devices: 9.84 us -> 20.8 us  [the longest x1 3.79 us: step(): c3 = lax.ppermute(c1, TP, ring)]
    all_to_all x3 -> x4, starting transfers between devices: 17.4 us -> 23.9 us  [the longest x1 9.96 us: step(): pieces = lax.all_to_all(parts, 'y', 0, 0, tiled=True)]
    ppermute x4 -> x8, waiting for transfers between devices: 13.2 us -> 10.5 us  [the longest x1 3.7 us: step(): c3 = lax.ppermute(c1, TP, ring)]
    pallas_call x7 -> x6, Pallas kernels: 10.7 us -> 9.77 us  [call(): pl.pallas_call(kernel, out_shape=outs, in_specs=specs, out_specs=jax.tree...]
  transfers between devices with their start and end apart: 7 -> 12, of which waited for: 5 -> 8; matrix products, arithmetic and copies ran while one was open for 1% -> 0% of each run, Pallas kernels for 2% -> 2%
where the time goes in v3:
time: 201 us; the launch traced here: 200 us
  waiting for transfers between devices  84.3 us (42%)
  blocking collectives  48.3 us (24%)
  starting transfers between devices  44.7 us (22%)
  Pallas kernels  14.5 us (7%)
  local copies, waits for them, and re-layouts  4.41 us (2%)
  other arithmetic  3.01 us (1%)
    all_to_all x1, blocking collectives, step(): c0 = lax.all_to_all(buf, SP, 0, 0, tiled=True)  31.1 us
    all_to_all x1, waiting for transfers between devices, step(): received = lax.all_to_all(sent, SP, 0, 0, tiled=True)  30.6 us
    all_to_all x1, waiting for transfers between devices, step(): pieces = lax.all_to_all(parts, 'y', 0, 0, tiled=True)  23.4 us
    all_gather x1, blocking collectives, step(): whole = lax.all_gather(d_input, TP, axis=1, tiled=True)  17.3 us
    all_to_all x1, waiting for transfers between devices, step(): back = lax.all_to_all(summed, SP, 0, 0, tiled=True)  10.6 us
    all_to_all x1, starting transfers between devices, step(): pieces = lax.all_to_all(parts, 'y', 0, 0, tiled=True)  9.96 us
    pallas_call x6, Pallas kernels, call(): pl.pallas_call(kernel, out_shape=outs, in_specs=specs, out_specs=jax.tree...  9.77 us
    all_to_all x1, waiting for transfers between devices, step(): later = lax.all_to_all(states, SP, 0, 0, tiled=True)  9.17 us
  transfers between devices with their start and end apart: 12, of which 8 were waited for; matrix products, arithmetic and copies ran while one was open for 0% of the time, Pallas kernels for 2%

profile of v3, /device:TPU:8, one launch (start us, length us, event | category | flops | bytes accessed | tf_op | source)
XLA Modules:
  0.0 200.3 jit_solution(8297979155181320566)
XLA Ops:
  1.4 2.9 %prepare.1 = (bf16[32,32,256]{2,1,0:T(8,128)(2,1)}, s32[8,128]{1,0:T(8,128)}) custom-call(s32[9]{0:T(128)} %stack.48.where, s32[2,128]{1,0:T(2,128)} %bitcast.34, f32[2,128]{1,0:T(2,128)} %bitcast.35, bf16[128,2048]{1,0:T(8,128)(2,1)} %mix.1, bf16[128,2048]{1,0:T(8,128)(2,1)} %cot.3), custom_call_target="tpu_custom_call" | custom-call | tf_op jit(solution)/shard_map/prepare/pallas_call | solution.py:86
  4.3 31.1 %all_to_all.25.refs_0_ = bf16[32,32,256]{2,1,0:T(8,128)(2,1)S(1)} all-to-all(bf16[32,32,256]{2,1,0:T(8,128)(2,1)} %get-tuple-element.39), channel_id=1, replica_groups=mesh['z'=8,'x'=4,'y'=8,'core'=2] {'z','x'}, dimensions={0} | all-to-all | bytes 1048576 | tf_op jit(solution)/shard_map/all_to_all | solution.py:285
  35.4 3.5 %collective-permute-start.1 = (bf16[32,32,256]{2,1,0:T(8,128)(2,1)S(1)}, bf16[32,32,256]{2,1,0:T(8,128)(2,1)S(1)}, u32[]{:S(2)}, u32[]{:S(2)}) collective-permute-start(bf16[32,32,256]{2,1,0:T(8,128)(2,1)S(1)} %all_to_all.25.refs_0_), channel_id=1, source_target_pairs={{0,2},{1,15},{2,4},{3,1},{4,6},{5,3},{6,8},{7,5},{8,10},{9,7},{10,... | collective-permute-start | bytes 1572872 | tf_op jit(solution)/shard_map/ppermute | solution.py:286
  38.8 1.9 collective-permute-start
  40.9 2.4 %collective-permute-start.4 = (bf16[3,64,2048]{2,1,0:T(8,128)(2,1)S(1)}, bf16[3,64,2048]{2,1,0:T(8,128)(2,1)S(1)}, u32[]{:S(2)}, u32[]{:S(2)}) collective-permute-start(bf16[3,64,2048]{2,1,0:T(8,128)(2,1)S(1)} %pad_maximum_fusion.refs_8_), channel_id=1, source_target_pairs={{0,1},{1,0},{2,3},{3,2},{4,5},{5,4},{6,7},{7,6},{8,9},{9,8},{10,11... | collective-permute-start | bytes 2359304 | tf_op jit(solution)/shard_map/ppermute | solution.py:283
  43.3 3.1 %collective-permute-done.1.refs_2_ = bf16[32,32,256]{2,1,0:T(8,128)(2,1)S(1)} collective-permute-done((bf16[32,32,256]{2,1,0:T(8,128)(2,1)S(1)}, bf16[32,32,256]{2,1,0:T(8,128)(2,1)S(1)}, u32[]{:S(2)}, u32[]{:S(2)}) %collective-permute-start.1) | collective-permute-done | bytes 524320 | tf_op jit(solution)/shard_map/ppermute | solution.py:286
  46.4 3.5 %collective-permute-start.3 = (bf16[32,32,256]{2,1,0:T(8,128)(2,1)S(1)}, bf16[32,32,256]{2,1,0:T(8,128)(2,1)S(1)}, u32[]{:S(2)}, u32[]{:S(2)}) collective-permute-start(bf16[32,32,256]{2,1,0:T(8,128)(2,1)S(1)} %collective-permute-done.1.refs_2_), channel_id=1, source_target_pairs={{0,2},{1,15},{2,4},{3,1},{4,6},{5,3},{6,8},{7,5},{8,10},{9,7},{10,... | collective-permute-start | bytes 1572872 | tf_op jit(solution)/shard_map/ppermute | solution.py:289
  49.9 3.8 %collective-permute-start.2 = (bf16[32,32,256]{2,1,0:T(8,128)(2,1)S(1)}, bf16[32,32,256]{2,1,0:T(8,128)(2,1)S(1)}, u32[]{:S(2)}, u32[]{:S(2)}) collective-permute-start(bf16[32,32,256]{2,1,0:T(8,128)(2,1)S(1)} %collective-permute-done.refs_1_), channel_id=1, source_target_pairs={{0,2},{1,15},{2,4},{3,1},{4,6},{5,3},{6,8},{7,5},{8,10},{9,7},{10,... | collective-permute-start | bytes 1572872 | tf_op jit(solution)/shard_map/ppermute | solution.py:288
  53.7 1.9 collective-permute-start.5
  55.6 1.8 collective-permute-done.3.refs_4_
  57.5 1.9 collective-permute-start.7
  59.4 3.7 %collective-permute-done.2.refs_3_ = bf16[32,32,256]{2,1,0:T(8,128)(2,1)S(1)} collective-permute-done((bf16[32,32,256]{2,1,0:T(8,128)(2,1)S(1)}, bf16[32,32,256]{2,1,0:T(8,128)(2,1)S(1)}, u32[]{:S(2)}, u32[]{:S(2)}) %collective-permute-start.2) | collective-permute-done | bytes 524320 | tf_op jit(solution)/shard_map/ppermute | solution.py:288
  63.1 1.9 collective-permute-start.6
  65.1 1.8 collective-permute-done.6.refs_6_
  66.9 2.4 %shard_map.214 = (bf16[8,512,128]{2,1,0:T(8,128)(2,1)S(1)}, bf16[512,128]{1,0:T(8,128)(2,1)S(1)}, bf16[512,128]{1,0:T(8,128)(2,1)S(1)}, bf16[512,128]{1,0:T(8,128)(2,1)S(1)}) custom-call(s32[9]{0:T(128)S(1)} %copy-done.11, bf16[32,32,256]{2,1,0:T(8,128)(2,1)S(1)} %all_to_all.25.refs_0_, bf16[32,32,256]{2,1,0:T(8,128)(2,1)S(1)} %collective-permute-done.refs_1_, ...), custom_call_target="tpu_custom_call" | custom-call | tf_op jit(solution)/shard_map/pallas_call | solution.py:50
  70.3 10.0 %all-to-all-start.1 = ((bf16[8,512,128]{2,1,0:T(8,128)(2,1)}), bf16[8,512,128]{2,1,0:T(8,128)(2,1)}, u32[]{:S(2)}, u32[]{:S(2)}) async-start(bf16[8,512,128]{2,1,0:T(8,128)(2,1)} %copy-done.5), calls=%async_computation.1 | async-start | bytes 2097152 | tf_op jit(solution)/shard_map/all_to_all | solution.py:299
  80.3 1.0 copy-done.1
  81.3 1.0 copy-done.3
  82.3 2.2 %shard_map.215 = (bf16[64,2048]{1,0:T(8,128)(2,1)}, bf16[64,2048]{1,0:T(8,128)(2,1)}, bf16[64,2048]{1,0:T(8,128)(2,1)}) custom-call(s32[9]{0:T(128)S(1)} %copy-done.11, bf16[32,32,256]{2,1,0:T(8,128)(2,1)S(1)} %all_to_all.25.refs_0_, bf16[32,32,256]{2,1,0:T(8,128)(2,1)S(1)} %collective-permute-done.refs_1_, ...), custom_call_target="tpu_custom_call" | custom-call | flops 1000000000 | tf_op jit(solution)/shard_map/pallas_call | solution.py:50
  84.6 23.4 %all-to-all-done.1 = bf16[8,512,128]{2,1,0:T(8,128)(2,1)} async-done(((bf16[8,512,128]{2,1,0:T(8,128)(2,1)}), bf16[8,512,128]{2,1,0:T(8,128)(2,1)}, u32[]{:S(2)}, u32[]{:S(2)}) %all-to-all-start.1) | async-done | bytes 1048608 | tf_op jit(solution)/shard_map/all_to_all | solution.py:299
  108.0 2.1 %reduce_sum.21 = bf16[512,128]{1,0:T(8,128)(2,1)} reduce(bf16[8,512,128]{2,1,0:T(8,128)(2,1)} %all-to-all-done.1, bf16[]{:T(256)} %constant.41.clone.1), dimensions={0}, to_apply=%region_0.1 | reduce | flops 458752 | bytes 1179650 | tf_op jit(solution)/shard_map/reduce_sum | solution.py:305
  110.1 4.6 %all-to-all-start.2 = ((bf16[32,16,128]{2,1,0:T(8,128)(2,1)}), bf16[32,16,128]{2,1,0:T(8,128)(2,1)S(1)}, u32[]{:S(2)}, u32[]{:S(2)}) async-start(bf16[32,16,128]{2,1,0:T(8,128)(2,1)} %bitcast.23), calls=%async_computation.2 | async-start | bytes 262144 | tf_op jit(solution)/shard_map/all_to_all | solution.py:306
  114.8 10.6 %all-to-all-done.2.rows = bf16[32,16,128]{2,1,0:T(8,128)(2,1)S(1)} async-done(((bf16[32,16,128]{2,1,0:T(8,128)(2,1)}), bf16[32,16,128]{2,1,0:T(8,128)(2,1)S(1)}, u32[]{:S(2)}, u32[]{:S(2)}) %all-to-all-start.2) | async-done | bytes 131104 | tf_op jit(solution)/shard_map/all_to_all | solution.py:306
  126.0 1.9 combine.1
  127.9 17.3 %all_gather.3.whole = bf16[128,2048]{1,0:T(8,128)(2,1)S(1)} all-gather(bf16[128,128]{1,0:T(8,128)(2,1)} %combine.1), channel_id=1, replica_groups=mesh['z'=8,'x'=4,'y'=8,'core'=2] {'y','core'}, dimensions={1}, use_global_device_ids=true | all-gather | bytes 557056 | tf_op jit(solution)/shard_map/all_gather | solution.py:308
  145.2 2.0 %shard_map.216 = (bf16[128,256]{1,0:T(8,128)(2,1)}, bf16[128,256]{1,0:T(8,128)(2,1)S(1)}, f32[8,128]{1,0:T(8,128)S(1)}, bf16[32,72,256]{2,1,0:T(8,128)(2,1)}) custom-call(bf16[128,2048]{1,0:T(8,128)(2,1)S(1)} %all_gather.3.whole, bf16[256,2048]{1,0:T(8,128)(2,1)S(1)} %copy-done.4, bf16[128,256]{1,0:T(8,128)(2,1)S(1)} %copy-done.7, ...), custom_call_target="tpu_custom_call" | custom-call | tf_op jit(solution)/shard_map/pallas_call | solution.py:50
  147.2 4.1 %all-to-all-start.3 = ((bf16[32,72,256]{2,1,0:T(8,128)(2,1)}), bf16[32,72,256]{2,1,0:T(8,128)(2,1)S(1)}, u32[]{:S(2)}, u32[]{:S(2)}) async-start(bf16[32,72,256]{2,1,0:T(8,128)(2,1)} %get-tuple-element.54), calls=%async_computation.3 | async-start | bytes 2359296 | tf_op jit(solution)/shard_map/all_to_all | solution.py:314
  151.4 1.3 shard_map.217
  152.7 30.6 %all-to-all-done.3.received = bf16[32,72,256]{2,1,0:T(8,128)(2,1)S(1)} async-done(((bf16[32,72,256]{2,1,0:T(8,128)(2,1)}), bf16[32,72,256]{2,1,0:T(8,128)(2,1)S(1)}, u32[]{:S(2)}, u32[]{:S(2)}) %all-to-all-start.3) | async-done | bytes 1179680 | tf_op jit(solution)/shard_map/all_to_all | solution.py:314
  184.0 5.2 %all-to-all-start.4 = ((bf16[32,8,128]{2,1,0:T(8,128)(2,1)}), bf16[32,8,128]{2,1,0:T(8,128)(2,1)S(1)}, u32[]{:S(2)}, u32[]{:S(2)}) async-start(bf16[32,8,128]{2,1,0:T(8,128)(2,1)} %shard_map.218), calls=%async_computation.4 | async-start | bytes 131072 | tf_op jit(solution)/shard_map/all_to_all | solution.py:321
  190.0 9.2 %all-to-all-done.4.state = bf16[32,8,128]{2,1,0:T(8,128)(2,1)S(1)} async-done(((bf16[32,8,128]{2,1,0:T(8,128)(2,1)}), bf16[32,8,128]{2,1,0:T(8,128)(2,1)S(1)}, u32[]{:S(2)}, u32[]{:S(2)}) %all-to-all-start.4) | async-done | bytes 65568 | tf_op jit(solution)/shard_map/all_to_all | solution.py:321
  199.2 1.1 shard_map.219
  (42 shorter events, 3.9 us)
Async XLA Ops:
  0.6 40.1 %copy-start.15 = (bf16[1,64,2048]{2,1,0:T(8,128)(2,1)S(1)}, bf16[1,64,2048]{2,1,0:T(8,128)(2,1)}, u32[]{:S(2)}) copy-start(bf16[1,64,2048]{2,1,0:T(8,128)(2,1)} %param.21) | copy-start | bytes 786436
  0.7 40.1 %copy-start.16 = (bf16[1,2048,64]{1,2,0:T(8,128)(2,1)S(1)}, bf16[1,2048,64]{1,2,0:T(8,128)(2,1)}, u32[]{:S(2)}) copy-start(bf16[1,2048,64]{1,2,0:T(8,128)(2,1)} %param.20) | copy-start | bytes 786436
  0.7 40.1 %copy-start.17 = (bf16[1,2048,64]{1,2,0:T(8,128)(2,1)S(1)}, bf16[1,2048,64]{1,2,0:T(8,128)(2,1)}, u32[]{:S(2)}) copy-start(bf16[1,2048,64]{1,2,0:T(8,128)(2,1)} %param.19) | copy-start | bytes 786436
  4.3 62.6 %copy-start.11 = (s32[9]{0:T(128)S(1)}, s32[9]{0:T(128)}, u32[]{:S(2)}) copy-start(s32[9]{0:T(128)} %stack.48.where) | copy-start | bytes 112
  35.4 11.1 %collective-permute-start.1 = (bf16[32,32,256]{2,1,0:T(8,128)(2,1)S(1)}, bf16[32,32,256]{2,1,0:T(8,128)(2,1)S(1)}, u32[]{:S(2)}, u32[]{:S(2)}) collective-permute-start(bf16[32,32,256]{2,1,0:T(8,128)(2,1)S(1)} %all_to_all.25.refs_0_), channel_id=1, source_target_pairs={{0,2},{1,15},{2,4},{3,1},{4,6},{5,3},{6,8},{7,5},{8,10},{9,7},{10,... | collective-permute-start | bytes 1572872 | tf_op jit(solution)/shard_map/ppermute | solution.py:286
  38.8 11.1 %collective-permute-start = (bf16[32,32,256]{2,1,0:T(8,128)(2,1)S(1)}, bf16[32,32,256]{2,1,0:T(8,128)(2,1)S(1)}, u32[]{:S(2)}, u32[]{:S(2)}) collective-permute-start(bf16[32,32,256]{2,1,0:T(8,128)(2,1)S(1)} %all_to_all.25.refs_0_), channel_id=1, source_target_pairs={{0,1},{1,0},{2,3},{3,2},{4,5},{5,4},{6,7},{7,6},{8,9},{9,8},{10,11... | collective-permute-start | bytes 1572872 | tf_op jit(solution)/shard_map/ppermute | solution.py:287
  40.9 12.8 %collective-permute-start.4 = (bf16[3,64,2048]{2,1,0:T(8,128)(2,1)S(1)}, bf16[3,64,2048]{2,1,0:T(8,128)(2,1)S(1)}, u32[]{:S(2)}, u32[]{:S(2)}) collective-permute-start(bf16[3,64,2048]{2,1,0:T(8,128)(2,1)S(1)} %pad_maximum_fusion.refs_8_), channel_id=1, source_target_pairs={{0,1},{1,0},{2,3},{3,2},{4,5},{5,4},{6,7},{7,6},{8,9},{9,8},{10,11... | collective-permute-start | bytes 2359304 | tf_op jit(solution)/shard_map/ppermute | solution.py:283
  46.4 11.1 %collective-permute-start.3 = (bf16[32,32,256]{2,1,0:T(8,128)(2,1)S(1)}, bf16[32,32,256]{2,1,0:T(8,128)(2,1)S(1)}, u32[]{:S(2)}, u32[]{:S(2)}) collective-permute-start(bf16[32,32,256]{2,1,0:T(8,128)(2,1)S(1)} %collective-permute-done.1.refs_2_), channel_id=1, source_target_pairs={{0,2},{1,15},{2,4},{3,1},{4,6},{5,3},{6,8},{7,5},{8,10},{9,7},{10,... | collective-permute-start | bytes 1572872 | tf_op jit(solution)/shard_map/ppermute | solution.py:289
  49.9 13.2 %collective-permute-start.2 = (bf16[32,32,256]{2,1,0:T(8,128)(2,1)S(1)}, bf16[32,32,256]{2,1,0:T(8,128)(2,1)S(1)}, u32[]{:S(2)}, u32[]{:S(2)}) collective-permute-start(bf16[32,32,256]{2,1,0:T(8,128)(2,1)S(1)} %collective-permute-done.refs_1_), channel_id=1, source_target_pairs={{0,2},{1,15},{2,4},{3,1},{4,6},{5,3},{6,8},{7,5},{8,10},{9,7},{10,... | collective-permute-start | bytes 1572872 | tf_op jit(solution)/shard_map/ppermute | solution.py:288
  53.7 11.3 %collective-permute-start.5 = (bf16[32,32,256]{2,1,0:T(8,128)(2,1)S(1)}, bf16[32,32,256]{2,1,0:T(8,128)(2,1)S(1)}, u32[]{:S(2)}, u32[]{:S(2)}) collective-permute-start(bf16[32,32,256]{2,1,0:T(8,128)(2,1)S(1)} %collective-permute-done.1.refs_2_), channel_id=1, source_target_pairs={{0,1},{1,0},{2,3},{3,2},{4,5},{5,4},{6,7},{7,6},{8,9},{9,8},{10,11... | collective-permute-start | bytes 1572872 | tf_op jit(solution)/shard_map/ppermute | solution.py:291
  57.5 7.5 %collective-permute-start.7 = (bf16[32,32,256]{2,1,0:T(8,128)(2,1)S(1)}, bf16[32,32,256]{2,1,0:T(8,128)(2,1)S(1)}, u32[]{:S(2)}, u32[]{:S(2)}) collective-permute-start(bf16[32,32,256]{2,1,0:T(8,128)(2,1)S(1)} %collective-permute-done.3.refs_4_), channel_id=1, source_target_pairs={{0,1},{1,0},{2,3},{3,2},{4,5},{5,4},{6,7},{7,6},{8,9},{9,8},{10,11... | collective-permute-start | bytes 1572872 | tf_op jit(solution)/shard_map/ppermute | solution.py:293
  63.1 3.8 %collective-permute-start.6 = (bf16[32,32,256]{2,1,0:T(8,128)(2,1)S(1)}, bf16[32,32,256]{2,1,0:T(8,128)(2,1)S(1)}, u32[]{:S(2)}, u32[]{:S(2)}) collective-permute-start(bf16[32,32,256]{2,1,0:T(8,128)(2,1)S(1)} %collective-permute-done.2.refs_3_), channel_id=1, source_target_pairs={{0,1},{1,0},{2,3},{3,2},{4,5},{5,4},{6,7},{7,6},{8,9},{9,8},{10,11... | collective-permute-start | bytes 1572872 | tf_op jit(solution)/shard_map/ppermute | solution.py:292
  65.0 4.3 %copy-start = (bf16[32,32,256]{2,1,0:T(8,128)(2,1)}, bf16[32,32,256]{2,1,0:T(8,128)(2,1)S(1)}, u32[]{:S(2)}) copy-start(bf16[32,32,256]{2,1,0:T(8,128)(2,1)S(1)} %collective-permute-done.7.refs_7_) | copy-start | bytes 1572868
  66.9 2.4 %copy-start.2 = (bf16[32,32,256]{2,1,0:T(8,128)(2,1)}, bf16[32,32,256]{2,1,0:T(8,128)(2,1)S(1)}, u32[]{:S(2)}) copy-start(bf16[32,32,256]{2,1,0:T(8,128)(2,1)S(1)} %collective-permute-done.6.refs_6_) | copy-start | bytes 1572868
  69.3 1.0 copy-start.5
  70.3 37.7 %all-to-all-start.1 = ((bf16[8,512,128]{2,1,0:T(8,128)(2,1)}), bf16[8,512,128]{2,1,0:T(8,128)(2,1)}, u32[]{:S(2)}, u32[]{:S(2)}) async-start(bf16[8,512,128]{2,1,0:T(8,128)(2,1)} %copy-done.5), calls=%async_computation.1 | async-start | bytes 2097152 | tf_op jit(solution)/shard_map/all_to_all | solution.py:299
  80.3 1.0 copy-start.1
  81.3 1.0 copy-start.3
  107.9 37.2 %copy-start.4 = (bf16[256,2048]{1,0:T(8,128)(2,1)S(1)}, bf16[256,2048]{1,0:T(8,128)(2,1)}, u32[]{:S(2)}) copy-start(bf16[256,2048]{1,0:T(8,128)(2,1)} %weight.1) | copy-start | bytes 3145732
  107.9 37.2 %copy-start.7 = (bf16[128,256]{1,0:T(8,128)(2,1)S(1)}, bf16[128,256]{1,0:T(8,128)(2,1)}, u32[]{:S(2)}) copy-start(bf16[128,256]{1,0:T(8,128)(2,1)} %gate_pre.1) | copy-start | bytes 196612
  107.9 37.2 %copy-start.8 = (bf16[128,256]{1,0:T(8,128)(2,1)S(1)}, bf16[128,256]{1,0:T(8,128)(2,1)}, u32[]{:S(2)}) copy-start(bf16[128,256]{1,0:T(8,128)(2,1)} %mixer.1) | copy-start | bytes 196612
  107.9 37.2 %copy-start.9 = (bf16[128,128]{1,0:T(8,128)(2,1)S(1)}, bf16[128,128]{1,0:T(8,128)(2,1)}, u32[]{:S(2)}) copy-start(bf16[128,128]{1,0:T(8,128)(2,1)} %read.3) | copy-start | bytes 98308
  108.0 37.2 %copy-start.12 = (f32[4,128]{1,0:T(4,128)S(1)}, f32[4,128]{1,0:T(4,128)}, u32[]{:S(2)}) copy-start(f32[4,128]{1,0:T(4,128)} %logs.1) | copy-start | bytes 6148
  110.1 15.3 %all-to-all-start.2 = ((bf16[32,16,128]{2,1,0:T(8,128)(2,1)}), bf16[32,16,128]{2,1,0:T(8,128)(2,1)S(1)}, u32[]{:S(2)}, u32[]{:S(2)}) async-start(bf16[32,16,128]{2,1,0:T(8,128)(2,1)} %bitcast.23), calls=%async_computation.2 | async-start | bytes 262144 | tf_op jit(solution)/shard_map/all_to_all | solution.py:306
  125.4 0.6 copy-start.14
  147.2 4.1 %copy-start.6 = (bf16[128,256]{1,0:T(8,128)(2,1)S(1)}, bf16[128,256]{1,0:T(8,128)(2,1)}, u32[]{:S(2)}) copy-start(bf16[128,256]{1,0:T(8,128)(2,1)} %values.3) | copy-start | bytes 196612
  147.2 4.1 %copy-start.10 = (bf16[128,128]{1,0:T(8,128)(2,1)S(1)}, bf16[128,128]{1,0:T(8,128)(2,1)}, u32[]{:S(2)}) copy-start(bf16[128,128]{1,0:T(8,128)(2,1)} %write.3) | copy-start | bytes 98308
  147.2 4.1 %copy-start.13 = (f32[1,4,64,128]{3,2,1,0:T(8,128)S(1)}, f32[1,4,64,128]{3,2,1,0:T(8,128)}, u32[]{:S(2)}) copy-start(f32[1,4,64,128]{3,2,1,0:T(8,128)} %param.29) | copy-start | bytes 393220
  147.2 36.1 %all-to-all-start.3 = ((bf16[32,72,256]{2,1,0:T(8,128)(2,1)}), bf16[32,72,256]{2,1,0:T(8,128)(2,1)S(1)}, u32[]{:S(2)}, u32[]{:S(2)}) async-start(bf16[32,72,256]{2,1,0:T(8,128)(2,1)} %get-tuple-element.54), calls=%async_computation.3 | async-start | bytes 2359296 | tf_op jit(solution)/shard_map/all_to_all | solution.py:314
  184.0 15.2 %all-to-all-start.4 = ((bf16[32,8,128]{2,1,0:T(8,128)(2,1)}), bf16[32,8,128]{2,1,0:T(8,128)(2,1)S(1)}, u32[]{:S(2)}, u32[]{:S(2)}) async-start(bf16[32,8,128]{2,1,0:T(8,128)(2,1)} %shard_map.218), calls=%async_computation.4 | async-start | bytes 131072 | tf_op jit(solution)/shard_map/all_to_all | solution.py:321

commit v4 on v3

--- a/solution.py
+++ b/solution.py
@@ -32,6 +32,28 @@
 
 def mm_nt(a, b):
     return lax.dot_general(a, b, (((1,), (1,)), ((), ())), preferred_element_type=F32)
+
+
+def mm_nt_exact(a, b):
+    return lax.dot_general(a, b, (((1,), (1,)), ((), ())), precision=lax.Precision.HIGHEST, preferred_element_type=F32)
+
+
+def mm_exact(a, b):
+    return mm(a, b, lax.Precision.HIGHEST)
+
+
+def two_parts(value):
+    high = value.astype(BF)
+    return high, (value - high.astype(F32)).astype(BF)
+
+
+def chunk_ids(slot):
+    y, core = slot >> 1, slot & 1
+    turn = 2 * core - 1
+    near, far, beyond, home = (y + turn) & 3, (y - turn) & 3, (y + 2) & 3, y & 3
+    mine, theirs = core, 1 - core
+    return (2 * home + mine, 2 * home + theirs, 2 * near + mine, 2 * near + theirs, 2 * beyond + mine,
+            2 * far + theirs, 2 * far + mine, 2 * beyond + theirs)
 
 
 def columns(row):
@@ -82,7 +104,7 @@
 
 def prepare(quarter, routes, gates, mixed, cotangent):
     whole = lambda i, q: (0, 0)
-    part = lambda i, q: (0, q[0])
+    part = lambda i, q: (0, lax.rem(q[0], 8))
     return pl.pallas_call(
         prepare_kernel,
         out_shape=(
@@ -119,12 +141,12 @@
 
 def expert_kernel(where, *refs):
     chunks = refs[:8]
-    own, other, out, g_gate, g_up, g_hid = refs[8:]
-    core = where[8]
+    own, other, near, mid, far, last, home, g_gate, g_up, g_hid = refs[8:]
+    ids = chunk_ids(where[0])
     pre = jnp.zeros((ROWS, 4 * FF), F32)
     grad_hidden = jnp.zeros((ROWS, 2 * FF), F32)
     for k in range(8):
-        at = pl.ds(pl.multiple_of(where[k] * WIDE, WIDE), WIDE)
+        at = pl.ds(pl.multiple_of(ids[k] * WIDE, WIDE), WIDE)
         toks, cots = row_blocks(chunks[k])
         pre = pre + mm_nt(toks, gate_rows(own, other, at))
         grad_hidden = grad_hidden + mm_nt(cots, jnp.concatenate([own[2, :, at], other[2, :, at]], axis=0))
@@ -139,9 +161,14 @@
     g_up[...] = up
     g_hid[...] = (active * pre_up).astype(BF)
     grads = jnp.concatenate([gate, up], axis=1)
-    for k in range(8):
-        at = pl.ds(pl.multiple_of((2 * k + core) * TOK, TOK), TOK)
-        out[k] = mm(grads, gate_rows(own, other, at)).astype(BF)
+    y, core = where[0] >> 1, where[0] & 1
+    step = 1 - 2 * core
+    for k, out in ((4, last), (3, far), (2, mid), (1, near), (0, home)):
+        chip = (y + step * k + 8) & 7
+        start = chip * WIDE if k in (1, 2, 3) else chip * WIDE + core * TOK
+        size = out.shape[1]
+        at = pl.ds(pl.multiple_of(start, TOK), size)
+        out[...] = mm(grads, gate_rows(own, other, at)).astype(BF)
 
 
 def weights_kernel(where, *refs):
@@ -149,8 +176,9 @@
     g_gate, g_up, g_hid, d_gate, d_up, d_down = refs[8:]
     gates = jnp.concatenate([g_gate[...].T[:FF], g_up[...].T[:FF]], axis=0)
     hidden = g_hid[...].T[:FF]
+    ids = chunk_ids(where[0])
     for k in range(8):
-        at = pl.ds(pl.multiple_of(where[k] * WIDE, WIDE), WIDE)
+        at = pl.ds(pl.multiple_of(ids[k] * WIDE, WIDE), WIDE)
         toks, cots = row_blocks(chunks[k])
         both = mm(gates, toks).astype(BF)
         d_gate[:, at] = both[:FF]
@@ -158,32 +186,39 @@
         d_down[:, at] = mm(hidden, cots).astype(BF)
 
 
-def combine_kernel(where, target, rows, cot, out):
+def fold_kernel(where, near, mid, far, last, home, keep, give):
+    total = near[...].astype(F32) + mid[...].astype(F32) + far[...].astype(F32)
+    first = total[:, :TOK]
+    second = total[:, TOK:]
+    top = where[0] & 1 == 0
+    keep[...] = jnp.where(top, first, second) + last[...].astype(F32) + home[...].astype(F32)
+    give[...] = jnp.where(top, second, first).astype(BF)
+
+
+def combine_kernel(where, target, rows, cotangent, out, cot, arrived):
+    at = pl.ds(pl.multiple_of(where[0] * TOK, TOK), TOK)
+    copy = pltpu.make_async_copy(cotangent.at[:, at], cot, arrived)
+    copy.start()
     lane = iota((TOK, ROWS), 1)
     places = target[...].T
     pick = jnp.where((lane == places[:, 0:1]) | (lane == places[:, 1:2]), 1.0, 0.0).astype(BF)
-    out[...] = (cot[...].astype(F32) + mm(pick, rows[...].reshape(ROWS, TOK))).astype(BF)
+    total = mm(pick, rows[...].reshape(ROWS, TOK))
+    copy.wait()
+    out[...] = (cot[...].astype(F32) + total).astype(BF)
 
 
 def combine(slot, target, rows, cotangent):
     return pl.pallas_call(
         combine_kernel,
         out_shape=jax.ShapeDtypeStruct((TOK, TOK), BF),
-        grid_spec=pltpu.PrefetchScalarGridSpec(
-            num_scalar_prefetch=1,
-            grid=(1,),
-            in_specs=[
-                pl.BlockSpec((8, TOK), lambda i, q: (0, 0)),
-                pl.BlockSpec((EXP, CAP, TOK), lambda i, q: (0, 0, 0)),
-                pl.BlockSpec((TOK, TOK), lambda i, q: (0, q[0])),
-            ],
-            out_specs=pl.BlockSpec((TOK, TOK), lambda i, q: (0, 0)),
-        ),
+        in_specs=[smem(), vmem(), vmem(), pl.BlockSpec(memory_space=pltpu.HBM)],
+        out_specs=vmem(),
+        scratch_shapes=[pltpu.VMEM((TOK, TOK), BF), pltpu.SemaphoreType.DMA],
         name="combine",
     )(slot, target, rows, cotangent)
 
 
-def project_kernel(whole, weight, gate_pre, mixer, logs, read, d_gate, grad_y, run, buf):
+def project_kernel(whole, weight, gate_pre, mixer, logs, read, d_gate, grad_y, run, buf, rest):
     back = mm_nt(whole[...], weight[...])
     pre = gate_pre[...].astype(F32)
     saved = mixer[...].astype(F32)
@@ -193,9 +228,11 @@
     gated = (saved * active).astype(BF)
     for k in range(8):
         turned = whole[:, k * WIDE : (k + 1) * WIDE].T
-        buf[4 * k : 4 * k + 4, 0:FF, :] = mm(turned, gated).astype(BF).reshape(4, FF, WIDE)
+        part = mm(turned, gated).astype(BF).reshape(4, FF, WIDE)
+        buf[4 * k : 4 * k + 4, 0:EXP, :] = part[:, 0:EXP]
+        rest[4 * k : 4 * k + 4] = part[:, EXP:]
     grad = back * active
-    grad_y[...] = grad.astype(BF)
+    grad_y[...] = grad
     upto = jnp.where(iota((TOK, TOK), 0) <= iota((TOK, TOK), 1), 1.0, 0.0)
     rates = jnp.concatenate([logs[...], jnp.zeros((4, TOK), F32)], axis=0)
     running = mm(rates, upto, lax.Precision.HIGHEST)
@@ -203,7 +240,8 @@
     start = jnp.exp(running)
     turned = grad.T
     scale = jnp.concatenate([jnp.broadcast_to(start[j : j + 1], (HD, TOK)) for j in range(HEADS)], axis=0)
-    state = mm((turned * scale).astype(BF), read[...])
+    high, low = two_parts(turned * scale)
+    state = mm(high, read[...]) + mm(low, read[...])
     total = running[0:HEADS, TOK - 1 : TOK]
     first = total.astype(BF).astype(F32)
     second = (total - first).astype(BF).astype(F32)
@@ -214,16 +252,19 @@
         note = jnp.where(line == 0, first[j : j + 1], jnp.where(line == 1, second[j : j + 1], third[j : j + 1]))
         note = jnp.where(line < 3, note, 0.0)
         notes.append(jnp.broadcast_to(note[None], (EXP // HEADS, 8, STATE)))
-    buf[:, FF:, 0:STATE] = state.reshape(EXP, 8, STATE).astype(BF)
-    buf[:, FF:, STATE:] = jnp.concatenate(notes, axis=0).astype(BF)
-
-
-def scan_kernel(received, out):
+    buf[:, EXP:, 0:STATE] = state.reshape(EXP, 8, STATE).astype(BF)
+    buf[:, EXP:, STATE:] = jnp.concatenate(notes, axis=0).astype(BF)
+
+
+def scan_kernel(received, rest, out):
+    out[:, 0:EXP, :] = rest[...]
     state = jnp.zeros((8, STATE), F32)
     for k in reversed(range(EXP)):
-        out[k] = state.astype(BF)
+        high, low = two_parts(state)
+        out[k, EXP:, 0:STATE] = high
+        out[k, EXP:, STATE:] = low
         if k > 0:
-            piece = received[k, FF:, :].astype(F32)
+            piece = received[k, EXP:, :].astype(F32)
             note = piece[:, STATE:]
             log = note[0:1] + note[1:2] + note[2:3]
             state = jnp.exp(log) * state + piece[:, :STATE]
@@ -233,7 +274,7 @@
     running = run[...]
     cols = running.T
     grads = grad_y[...]
-    vals = values[...]
+    vals = values[...].astype(F32)
     cross = mm_nt(write[...], read[...])
     later = iota((TOK, TOK), 1) >= iota((TOK, TOK), 0)
     total = jnp.zeros((TOK, TOK), F32)
@@ -243,45 +284,44 @@
         spread = running[j : j + 1] - cols[:, j : j + 1]
         decay = jnp.where(later, jnp.exp(jnp.where(later, spread, 0.0)), 0.0)
         grad = grads[:, j * HD : (j + 1) * HD]
-        parts.append(mm((cross * decay).astype(BF), grad))
-        total = total + mm_nt(vals[:, j * HD : (j + 1) * HD], grad) * decay
-        starts.append((grad.astype(F32) * jnp.exp(cols[:, j : j + 1])).astype(BF))
+        parts.append(mm_exact(cross * decay, grad))
+        total = total + mm_nt_exact(vals[:, j * HD : (j + 1) * HD], grad) * decay
+        starts.append(grad * jnp.exp(cols[:, j : j + 1]))
     dx[...] = jnp.concatenate(parts, axis=1)
-    dw[...] = mm(total.astype(BF), read[...])
-    entry_rows = entry[...].reshape(HEADS * HD, STATE).astype(BF)
-    dr[...] = mm(total.T.astype(BF), write[...]) + mm(jnp.concatenate(starts, axis=1), entry_rows)
-
-
-def outer_kernel(dx, dw, values, write, run, state, d_values, d_write):
+    dw[...] = mm_exact(total, read[...].astype(F32))
+    entry_rows = entry[...].reshape(HEADS * HD, STATE)
+    dr[...] = mm_exact(total.T, write[...].astype(F32)) + mm_exact(jnp.concatenate(starts, axis=1), entry_rows)
+
+
+def outer_kernel(dx, dw, values, write, run, half, second, d_values, d_write, d_out):
     running = run[...]
     ends = jnp.exp(running[:, TOK - 1 : TOK] - running).T
     scale = jnp.concatenate([jnp.broadcast_to(ends[:, j : j + 1], (TOK, HD)) for j in range(HEADS)], axis=1)
-    later = state[...].reshape(HEADS * HD, STATE)
-    d_values[...] = (dx[...] + scale * mm_nt(write[...], later)).astype(BF)
-    d_write[...] = dw[...] + mm((values[...].astype(F32) * scale).astype(BF), later)
+    high = second[:, EXP:, 0:STATE].reshape(HEADS * HD, STATE)
+    low = second[:, EXP:, STATE:].reshape(HEADS * HD, STATE)
+    d_values[...] = (dx[...] + scale * (mm_nt(write[...], high) + mm_nt(write[...], low))).astype(BF)
+    top, rest = two_parts(values[...].astype(F32) * scale)
+    d_write[...] = dw[...] + mm(top, high) + mm(top, low) + mm(rest, high)
+    total = second[0, 0:EXP, :].astype(F32)
+    for k in range(1, EXP):
+        total = total + second[k, 0:EXP, :].astype(F32)
+    d_out[0:EXP, :] = half[...]
+    d_out[EXP:, :] = total
 
 
 def step(mixed, cotangent, routes, gates, w_gate, w_up, w_down, out_weight, gate_pre, mixer_out, values,
          write_keys, read_keys, log_decay, entry_states):
     shape = jax.ShapeDtypeStruct
-    y = lax.axis_index("y")
-    core = lax.axis_index("core")
     swap = [(0, 1), (1, 0)]
-    ring = []
-    for k in range(8):
-        ring.append((2 * k, 2 * ((k + 1) % 8)))
-        ring.append((2 * k + 1, 2 * ((k - 1) % 8) + 1))
-    turn = 2 * core - 1
-    near, far, beyond = (y + turn) % 4, (y - turn) % 4, (y + 2) % 4
-    mine, theirs = core, 1 - core
-    home = 2 * (y % 4)
-    ids = [home + mine, home + theirs, 2 * near + mine, 2 * near + theirs, 2 * beyond + mine,
-           2 * far + theirs, 2 * far + mine, 2 * beyond + theirs, core]
-    where = jnp.stack(ids).astype(jnp.int32)
-    slot = (2 * y + core).astype(jnp.int32).reshape(1)
+    rings = []
+    for k in range(1, 5):
+        up = [(2 * y, 2 * ((y + k) % 8)) for y in range(8)]
+        rings.append(up + [(2 * y + 1, 2 * ((y - k) % 8) + 1) for y in range(8)])
+    ring = rings[0]
+    slot = lax.axis_index(TP).astype(jnp.int32).reshape(1)
     own = jnp.stack([w_gate[0].T, w_up[0].T, w_down[0]])
     other = lax.ppermute(own, "core", swap)
-    buf, target = prepare(where, routes.T, gates.T, mixed, cotangent)
+    buf, target = prepare(slot, routes.T, gates.T, mixed, cotangent)
     c0 = lax.all_to_all(buf, SP, 0, 0, tiled=True)
     c2 = lax.ppermute(c0, TP, ring)
     c1 = lax.ppermute(c0, "core", swap)
@@ -293,23 +333,31 @@
     c7 = lax.ppermute(c4, "core", swap)
     chunks = (c0, c1, c2, c3, c4, c5, c6, c7)
     grad = shape((ROWS, 2 * FF), BF)
-    parts, g_gate, g_up, g_hid = call(
-        expert_kernel, (shape((8, ROWS, TOK), BF), grad, grad, grad),
-        [smem()] + [vmem()] * 10, (where, *chunks, own, other))
-    pieces = lax.all_to_all(parts, "y", 0, 0, tiled=True)
+    full, thin = shape((ROWS, WIDE), BF), shape((ROWS, TOK), BF)
+    *parts, home, g_gate, g_up, g_hid = call(
+        expert_kernel, (full, full, full, thin, thin, grad, grad, grad),
+        [smem()] + [vmem()] * 10, (slot, *chunks, own, other))
+    pieces = []
+    for k in range(4):
+        pieces.append(lax.ppermute(parts[k], TP, rings[k]))
     wide = shape((FF, D), BF)
     d_wg, d_wu, d_wd = call(
         weights_kernel, (wide, wide, wide),
-        [smem()] + [vmem()] * 11, (where, *chunks, g_gate, g_up, g_hid), flops=10**9)
+        [smem()] + [vmem()] * 11, (slot, *chunks, g_gate, g_up, g_hid), flops=10**9)
     pieces, d_wg, d_wu, d_wd = lax.optimization_barrier((pieces, d_wg, d_wu, d_wd))
-    summed = jnp.sum(pieces.astype(F32), axis=0).astype(BF).reshape(EXP, CAP, TOK)
+    keep, give = call(
+        fold_kernel, (shape((ROWS, TOK), F32), thin),
+        [smem()] + [vmem()] * 5, (slot, *pieces, home))
+    taken = lax.ppermute(give, "core", swap)
+    summed = (keep + taken.astype(F32)).astype(BF).reshape(EXP, CAP, TOK)
     back = lax.all_to_all(summed, SP, 0, 0, tiled=True)
     d_input = combine(slot, target, back, cotangent)
     whole = lax.all_gather(d_input, TP, axis=1, tiled=True)
     flat = shape((TOK, HEADS * HD), BF)
-    d_gate, grad_y, run, sent = call(
+    d_gate, grad_y, run, sent, rest = call(
         project_kernel,
-        (flat, flat, shape((8, TOK), F32), shape((EXP, FF + 8, WIDE), BF)),
+        (flat, shape((TOK, HEADS * HD), F32), shape((8, TOK), F32), shape((EXP, EXP + 8, WIDE), BF),
+         shape((EXP, EXP, WIDE), BF)),
         [vmem()] * 6, (whole, out_weight, gate_pre, mixer_out, log_decay, read_keys))
     received = lax.all_to_all(sent, SP, 0, 0, tiled=True)
     square = shape((TOK, STATE), F32)
@@ -317,13 +365,13 @@
         inner_kernel, (shape((TOK, HEADS * HD), F32), square, square),
         [vmem()] * 6, (grad_y, values, write_keys, read_keys, run, entry_states[0]), flops=10**9)
     received, dx, dw, d_read = lax.optimization_barrier((received, dx, dw, d_read))
-    states = call(scan_kernel, shape((EXP, 8, STATE), BF), [vmem()], (received,))
-    later = lax.all_to_all(states, SP, 0, 0, tiled=True)
-    d_out_weight = jnp.sum(received[:, :FF].astype(F32), axis=0)
-    later, d_out_weight = lax.optimization_barrier((later, d_out_weight))
-    d_values, d_write = call(
-        outer_kernel, (flat, square), [vmem()] * 6,
-        (dx, dw, values, write_keys, run, later))
+    states = call(scan_kernel, shape((EXP, EXP + 8, WIDE), BF), [vmem()] * 2, (received, rest))
+    second = lax.all_to_all(states, SP, 0, 0, tiled=True)
+    half = jnp.sum(received[:, :EXP].astype(F32), axis=0)
+    second, half = lax.optimization_barrier((second, half))
+    d_values, d_write, d_out_weight = call(
+        outer_kernel, (flat, square, shape((D // EXP, HEADS * HD), F32)), [vmem()] * 7,
+        (dx, dw, values, write_keys, run, half, second))
     return (d_wg.T[None], d_wu.T[None], d_wd[None], d_out_weight, d_input, d_values, d_write, d_read, d_gate)
 
 

time: 201 us -> 194 us (0.965)
  waiting for transfers between devices: 84.3 us -> 62.6 us
  blocking collectives: 48.3 us -> 64.3 us
  starting transfers between devices: 44.7 us -> 50.8 us
  local copies, waits for them, and re-layouts: 4.41 us -> 0.05 us
  other arithmetic: 3.01 us -> 0.21 us
    all_to_all x3 -> x1, waiting for transfers between devices: 43.2 us -> 19.5 us  [step(): second = lax.all_to_all(states, SP, 0, 0, tiled=True)]
    ppermute x0 -> x5, starting transfers between devices: none -> 20.7 us  [the longest x4 18.2 us: step(): pieces.append(lax.ppermute(parts[k], TP, rings[k]))]
    all_to_all x0 -> x1, blocking collectives: none -> 15.5 us  [step(): back = lax.all_to_all(summed, SP, 0, 0, tiled=True)]
    all_to_all x3 -> x1, starting transfers between devices: 19.8 us -> 5.24 us  [step(): second = lax.all_to_all(states, SP, 0, 0, tiled=True)]
    ppermute x0 -> x5, waiting for transfers between devices: none -> 14.2 us  [the longest x4 13.2 us: step(): pieces.append(lax.ppermute(parts[k], TP, rings[k]))]
    all_to_all x1, waiting for transfers between devices: 30.6 us -> 18.5 us  [step(): received = lax.all_to_all(sent, SP, 0, 0, tiled=True)]
    unnamed x36 -> x22, local copies, waits for them, and re-layouts: 3.74 us -> 0.05 us
    reduce_sum x2 -> x1, other arithmetic: 2.92 us -> 0.09 us  [step(): half = jnp.sum(received[:, :EXP].astype(F32), axis=0)]
  transfers between devices with their start and end apart: 12 -> 15, of which waited for: 8 -> 8; matrix products, arithmetic and copies ran while one was open for 0% -> 0% of each run, Pallas kernels for 2% -> 2%
where the time goes in v4:
time: 194 us; the launch traced here: 193 us
  blocking collectives  64.3 us (33%)
  waiting for transfers between devices  62.6 us (32%)
  starting transfers between devices  50.8 us (26%)
  Pallas kernels  14.5 us (7%)
    all_to_all x1, blocking collectives, step(): c0 = lax.all_to_all(buf, SP, 0, 0, tiled=True)  31.1 us
    all_to_all x1, waiting for transfers between devices, step(): second = lax.all_to_all(states, SP, 0, 0, tiled=True)  19.5 us
    all_to_all x1, waiting for transfers between devices, step(): received = lax.all_to_all(sent, SP, 0, 0, tiled=True)  18.5 us
    ppermute x4, starting transfers between devices, step(): pieces.append(lax.ppermute(parts[k], TP, rings[k]))  18.2 us
    all_gather x1, blocking collectives, step(): whole = lax.all_gather(d_input, TP, axis=1, tiled=True)  17.8 us
    all_to_all x1, blocking collectives, step(): back = lax.all_to_all(summed, SP, 0, 0, tiled=True)  15.5 us
    ppermute x4, waiting for transfers between devices, step(): pieces.append(lax.ppermute(parts[k], TP, rings[k]))  13.2 us
    pallas_call x7, Pallas kernels, call(): pl.pallas_call(kernel, out_shape=outs, in_specs=specs, out_specs=jax.tree...  9.9 us
  transfers between devices with their start and end apart: 15, of which 8 were waited for; matrix products, arithmetic and copies ran while one was open for 0% of the time, Pallas kernels for 2%

profile of v4, /device:TPU:8, one launch (start us, length us, event | category | flops | bytes accessed | tf_op | source)
XLA Modules:
  0.0 193.4 jit_solution(18101724832477234853)
XLA Ops:
  0.6 2.3 %prepare.1 = (bf16[32,32,256]{2,1,0:T(8,128)(2,1)}, s32[8,128]{1,0:T(8,128)}) custom-call(s32[1]{0:T(128)} %bitcast.where, s32[2,128]{1,0:T(2,128)} %bitcast.26, f32[2,128]{1,0:T(2,128)} %bitcast.27, bf16[128,2048]{1,0:T(8,128)(2,1)} %mix.1, bf16[128,2048]{1,0:T(8,128)(2,1)} %cotangent.1), custom_call_target="tpu_custom_call" | custom-call | tf_op jit(solution)/shard_map/prepare/pallas_call | solution.py:108
  2.9 31.1 %all_to_all.20.refs_0_ = bf16[32,32,256]{2,1,0:T(8,128)(2,1)S(1)} all-to-all(bf16[32,32,256]{2,1,0:T(8,128)(2,1)} %get-tuple-element.50), channel_id=1, replica_groups=mesh['z'=8,'x'=4,'y'=8,'core'=2] {'z','x'}, dimensions={0} | all-to-all | bytes 1048576 | tf_op jit(solution)/shard_map/all_to_all | solution.py:325
  34.0 3.5 %collective-permute-start.1 = (bf16[32,32,256]{2,1,0:T(8,128)(2,1)S(1)}, bf16[32,32,256]{2,1,0:T(8,128)(2,1)S(1)}, u32[]{:S(2)}, u32[]{:S(2)}) collective-permute-start(bf16[32,32,256]{2,1,0:T(8,128)(2,1)S(1)} %all_to_all.20.refs_0_), channel_id=1, source_target_pairs={{0,2},{2,4},{4,6},{6,8},{8,10},{10,12},{12,14},{14,0},{1,15},{3,1}... | collective-permute-start | bytes 1572872 | tf_op jit(solution)/shard_map/ppermute | solution.py:326
  37.5 1.9 collective-permute-start
  39.5 2.4 %collective-permute-start.4 = (bf16[3,64,2048]{2,1,0:T(8,128)(2,1)S(1)}, bf16[3,64,2048]{2,1,0:T(8,128)(2,1)S(1)}, u32[]{:S(2)}, u32[]{:S(2)}) collective-permute-start(bf16[3,64,2048]{2,1,0:T(8,128)(2,1)S(1)} %pad_maximum_fusion.refs_8_), channel_id=1, source_target_pairs={{0,1},{1,0},{2,3},{3,2},{4,5},{5,4},{6,7},{7,6},{8,9},{9,8},{10,11... | collective-permute-start | bytes 2359304 | tf_op jit(solution)/shard_map/ppermute | solution.py:323
  41.9 3.1 %collective-permute-done.1.refs_2_ = bf16[32,32,256]{2,1,0:T(8,128)(2,1)S(1)} collective-permute-done((bf16[32,32,256]{2,1,0:T(8,128)(2,1)S(1)}, bf16[32,32,256]{2,1,0:T(8,128)(2,1)S(1)}, u32[]{:S(2)}, u32[]{:S(2)}) %collective-permute-start.1) | collective-permute-done | bytes 524320 | tf_op jit(solution)/shard_map/ppermute | solution.py:326
  45.0 3.5 %collective-permute-start.3 = (bf16[32,32,256]{2,1,0:T(8,128)(2,1)S(1)}, bf16[32,32,256]{2,1,0:T(8,128)(2,1)S(1)}, u32[]{:S(2)}, u32[]{:S(2)}) collective-permute-start(bf16[32,32,256]{2,1,0:T(8,128)(2,1)S(1)} %collective-permute-done.1.refs_2_), channel_id=1, source_target_pairs={{0,2},{2,4},{4,6},{6,8},{8,10},{10,12},{12,14},{14,0},{1,15},{3,1}... | collective-permute-start | bytes 1572872 | tf_op jit(solution)/shard_map/ppermute | solution.py:329
  48.5 3.8 %collective-permute-start.2 = (bf16[32,32,256]{2,1,0:T(8,128)(2,1)S(1)}, bf16[32,32,256]{2,1,0:T(8,128)(2,1)S(1)}, u32[]{:S(2)}, u32[]{:S(2)}) collective-permute-start(bf16[32,32,256]{2,1,0:T(8,128)(2,1)S(1)} %collective-permute-done.refs_1_), channel_id=1, source_target_pairs={{0,2},{2,4},{4,6},{6,8},{8,10},{10,12},{12,14},{14,0},{1,15},{3,1}... | collective-permute-start | bytes 1572872 | tf_op jit(solution)/shard_map/ppermute | solution.py:328
  52.3 1.9 collective-permute-start.5
  54.3 1.8 collective-permute-done.3.refs_4_
  56.1 1.9 collective-permute-start.7
  58.0 3.7 %collective-permute-done.2.refs_3_ = bf16[32,32,256]{2,1,0:T(8,128)(2,1)S(1)} collective-permute-done((bf16[32,32,256]{2,1,0:T(8,128)(2,1)S(1)}, bf16[32,32,256]{2,1,0:T(8,128)(2,1)S(1)}, u32[]{:S(2)}, u32[]{:S(2)}) %collective-permute-start.2) | collective-permute-done | bytes 524320 | tf_op jit(solution)/shard_map/ppermute | solution.py:328
  61.7 1.9 collective-permute-start.6
  63.7 1.9 collective-permute-done.6.refs_6_
  65.5 1.8 shard_map.214
  67.4 3.5 %collective-permute-start.8 = (bf16[512,256]{1,0:T(8,128)(2,1)S(1)}, bf16[512,256]{1,0:T(8,128)(2,1)S(1)}, u32[]{:S(2)}, u32[]{:S(2)}) collective-permute-start(bf16[512,256]{1,0:T(8,128)(2,1)S(1)} %get-tuple-element.53), channel_id=1, source_target_pairs={{0,2},{2,4},{4,6},{6,8},{8,10},{10,12},{12,14},{14,0},{1,15},{3,1}... | collective-permute-start | bytes 786440 | tf_op jit(solution)/shard_map/ppermute | solution.py:342
  70.8 8.1 %collective-permute-start.9 = (bf16[512,256]{1,0:T(8,128)(2,1)S(1)}, bf16[512,256]{1,0:T(8,128)(2,1)S(1)}, u32[]{:S(2)}, u32[]{:S(2)}) collective-permute-start(bf16[512,256]{1,0:T(8,128)(2,1)S(1)} %get-tuple-element.54), channel_id=1, source_target_pairs={{0,4},{2,6},{4,8},{6,10},{8,12},{10,14},{12,0},{14,2},{1,13},{3,15... | collective-permute-start | bytes 786440 | tf_op jit(solution)/shard_map/ppermute | solution.py:342
  79.0 1.9 collective-permute-start.10
  80.9 4.7 %collective-permute-start.11 = (bf16[512,128]{1,0:T(8,128)(2,1)S(1)}, bf16[512,128]{1,0:T(8,128)(2,1)S(1)}, u32[]{:S(2)}, u32[]{:S(2)}) collective-permute-start(bf16[512,128]{1,0:T(8,128)(2,1)S(1)} %get-tuple-element.56), channel_id=1, source_target_pairs={{0,8},{2,10},{4,12},{6,14},{8,0},{10,2},{12,4},{14,6},{1,9},{3,11}... | collective-permute-start | bytes 393224 | tf_op jit(solution)/shard_map/ppermute | solution.py:342
  85.6 1.7 shard_map.215
  87.3 13.2 %collective-permute-done.11.last = bf16[512,128]{1,0:T(8,128)(2,1)S(1)} collective-permute-done((bf16[512,128]{1,0:T(8,128)(2,1)S(1)}, bf16[512,128]{1,0:T(8,128)(2,1)S(1)}, u32[]{:S(2)}, u32[]{:S(2)}) %collective-permute-start.11) | collective-permute-done | bytes 131104 | tf_op jit(solution)/shard_map/ppermute | solution.py:342
  100.7 2.4 %collective-permute-start.12 = (bf16[512,128]{1,0:T(8,128)(2,1)S(1)}, bf16[512,128]{1,0:T(8,128)(2,1)S(1)}, u32[]{:S(2)}, u32[]{:S(2)}) collective-permute-start(bf16[512,128]{1,0:T(8,128)(2,1)S(1)} %get-tuple-element.73), channel_id=1, source_target_pairs={{0,1},{1,0},{2,3},{3,2},{4,5},{5,4},{6,7},{7,6},{8,9},{9,8},{10,11... | collective-permute-start | bytes 393224 | tf_op jit(solution)/shard_map/ppermute | solution.py:351
  104.1 15.5 %all_to_all.21.rows = bf16[32,16,128]{2,1,0:T(8,128)(2,1)} all-to-all(bf16[32,16,128]{2,1,0:T(8,128)(2,1)S(1)} %bitcast.23), channel_id=1, replica_groups=mesh['z'=8,'x'=4,'y'=8,'core'=2] {'z','x'}, dimensions={0} | all-to-all | bytes 262144 | tf_op jit(solution)/shard_map/all_to_all | solution.py:353
  119.6 2.3 %combine.1 = bf16[128,128]{1,0:T(8,128)(2,1)} custom-call(s32[1]{0:T(128)} %bitcast.where, s32[8,128]{1,0:T(8,128)} %get-tuple-element.66.target, bf16[32,16,128]{2,1,0:T(8,128)(2,1)} %all_to_all.21.rows, bf16[128,2048]{1,0:T(8,128)(2,1)} %cotangent.1), custom_call_target="tpu_custom_call" | custom-call | tf_op jit(solution)/shard_map/combine/pallas_call | solution.py:211
  122.0 17.8 %all_gather.3.whole = bf16[128,2048]{1,0:T(8,128)(2,1)S(1)} all-gather(bf16[128,128]{1,0:T(8,128)(2,1)} %combine.1), channel_id=1, replica_groups=mesh['z'=8,'x'=4,'y'=8,'core'=2] {'y','core'}, dimensions={1}, use_global_device_ids=true | all-gather | bytes 557056 | tf_op jit(solution)/shard_map/all_gather | solution.py:355
  139.8 1.9 shard_map.217
  141.7 4.0 %all-to-all-start.2 = ((bf16[32,40,256]{2,1,0:T(8,128)(2,1)}), bf16[32,40,256]{2,1,0:T(8,128)(2,1)S(1)}, u32[]{:S(2)}, u32[]{:S(2)}) async-start(bf16[32,40,256]{2,1,0:T(8,128)(2,1)} %get-tuple-element.74), calls=%async_computation.2 | async-start | bytes 1310720 | tf_op jit(solution)/shard_map/all_to_all | solution.py:362
  145.8 2.2 %shard_map.218 = (f32[128,256]{1,0:T(8,128)S(1)}, f32[128,128]{1,0:T(8,128)S(1)}, f32[128,128]{1,0:T(8,128)}) custom-call(f32[128,256]{1,0:T(8,128)S(1)} %get-tuple-element.75.grad_y, bf16[128,256]{1,0:T(8,128)(2,1)S(1)} %copy-done.3, bf16[128,128]{1,0:T(8,128)(2,1)S(1)} %copy-done.5, bf16[128,128]{1,0:T(8,128)(2,1)S(1)} %copy-done.4, ...), custom_call_target="tpu_custom_call" | custom-call | flops 1000000000 | tf_op jit(solution)/shard_map/pallas_call | solution.py:72
  148.0 18.5 %all-to-all-done.2.received = bf16[32,40,256]{2,1,0:T(8,128)(2,1)S(1)} async-done(((bf16[32,40,256]{2,1,0:T(8,128)(2,1)}), bf16[32,40,256]{2,1,0:T(8,128)(2,1)S(1)}, u32[]{:S(2)}, u32[]{:S(2)}) %all-to-all-start.2) | async-done | bytes 655392 | tf_op jit(solution)/shard_map/all_to_all | solution.py:362
  167.4 5.2 %all-to-all-start.3 = ((bf16[32,40,256]{2,1,0:T(8,128)(2,1)}), bf16[32,40,256]{2,1,0:T(8,128)(2,1)S(1)}, u32[]{:S(2)}, u32[]{:S(2)}) async-start(bf16[32,40,256]{2,1,0:T(8,128)(2,1)} %shard_map.219), calls=%async_computation.3 | async-start | bytes 1310720 | tf_op jit(solution)/shard_map/all_to_all | solution.py:369
  172.8 19.5 %all-to-all-done.3.second = bf16[32,40,256]{2,1,0:T(8,128)(2,1)S(1)} async-done(((bf16[32,40,256]{2,1,0:T(8,128)(2,1)}), bf16[32,40,256]{2,1,0:T(8,128)(2,1)S(1)}, u32[]{:S(2)}, u32[]{:S(2)}) %all-to-all-start.3) | async-done | bytes 655392 | tf_op jit(solution)/shard_map/all_to_all | solution.py:369
  192.3 1.2 shard_map.220
  (35 shorter events, 2.4 us)
Async XLA Ops:
  2.9 36.5 %copy-start.8 = (bf16[1,64,2048]{2,1,0:T(8,128)(2,1)S(1)}, bf16[1,64,2048]{2,1,0:T(8,128)(2,1)}, u32[]{:S(2)}) copy-start(bf16[1,64,2048]{2,1,0:T(8,128)(2,1)} %param.21) | copy-start | bytes 786436
  2.9 36.5 %copy-start.9 = (bf16[1,2048,64]{1,2,0:T(8,128)(2,1)S(1)}, bf16[1,2048,64]{1,2,0:T(8,128)(2,1)}, u32[]{:S(2)}) copy-start(bf16[1,2048,64]{1,2,0:T(8,128)(2,1)} %param.20) | copy-start | bytes 786436
  2.9 36.5 %copy-start.10 = (bf16[1,2048,64]{1,2,0:T(8,128)(2,1)S(1)}, bf16[1,2048,64]{1,2,0:T(8,128)(2,1)}, u32[]{:S(2)}) copy-start(bf16[1,2048,64]{1,2,0:T(8,128)(2,1)} %param.19) | copy-start | bytes 786436
  34.0 11.1 %collective-permute-start.1 = (bf16[32,32,256]{2,1,0:T(8,128)(2,1)S(1)}, bf16[32,32,256]{2,1,0:T(8,128)(2,1)S(1)}, u32[]{:S(2)}, u32[]{:S(2)}) collective-permute-start(bf16[32,32,256]{2,1,0:T(8,128)(2,1)S(1)} %all_to_all.20.refs_0_), channel_id=1, source_target_pairs={{0,2},{2,4},{4,6},{6,8},{8,10},{10,12},{12,14},{14,0},{1,15},{3,1}... | collective-permute-start | bytes 1572872 | tf_op jit(solution)/shard_map/ppermute | solution.py:326
  37.5 11.1 %collective-permute-start = (bf16[32,32,256]{2,1,0:T(8,128)(2,1)S(1)}, bf16[32,32,256]{2,1,0:T(8,128)(2,1)S(1)}, u32[]{:S(2)}, u32[]{:S(2)}) collective-permute-start(bf16[32,32,256]{2,1,0:T(8,128)(2,1)S(1)} %all_to_all.20.refs_0_), channel_id=1, source_target_pairs={{0,1},{1,0},{2,3},{3,2},{4,5},{5,4},{6,7},{7,6},{8,9},{9,8},{10,11... | collective-permute-start | bytes 1572872 | tf_op jit(solution)/shard_map/ppermute | solution.py:327
  39.5 12.8 %collective-permute-start.4 = (bf16[3,64,2048]{2,1,0:T(8,128)(2,1)S(1)}, bf16[3,64,2048]{2,1,0:T(8,128)(2,1)S(1)}, u32[]{:S(2)}, u32[]{:S(2)}) collective-permute-start(bf16[3,64,2048]{2,1,0:T(8,128)(2,1)S(1)} %pad_maximum_fusion.refs_8_), channel_id=1, source_target_pairs={{0,1},{1,0},{2,3},{3,2},{4,5},{5,4},{6,7},{7,6},{8,9},{9,8},{10,11... | collective-permute-start | bytes 2359304 | tf_op jit(solution)/shard_map/ppermute | solution.py:323
  45.0 11.1 %collective-permute-start.3 = (bf16[32,32,256]{2,1,0:T(8,128)(2,1)S(1)}, bf16[32,32,256]{2,1,0:T(8,128)(2,1)S(1)}, u32[]{:S(2)}, u32[]{:S(2)}) collective-permute-start(bf16[32,32,256]{2,1,0:T(8,128)(2,1)S(1)} %collective-permute-done.1.refs_2_), channel_id=1, source_target_pairs={{0,2},{2,4},{4,6},{6,8},{8,10},{10,12},{12,14},{14,0},{1,15},{3,1}... | collective-permute-start | bytes 1572872 | tf_op jit(solution)/shard_map/ppermute | solution.py:329
  48.5 13.2 %collective-permute-start.2 = (bf16[32,32,256]{2,1,0:T(8,128)(2,1)S(1)}, bf16[32,32,256]{2,1,0:T(8,128)(2,1)S(1)}, u32[]{:S(2)}, u32[]{:S(2)}) collective-permute-start(bf16[32,32,256]{2,1,0:T(8,128)(2,1)S(1)} %collective-permute-done.refs_1_), channel_id=1, source_target_pairs={{0,2},{2,4},{4,6},{6,8},{8,10},{10,12},{12,14},{14,0},{1,15},{3,1}... | collective-permute-start | bytes 1572872 | tf_op jit(solution)/shard_map/ppermute | solution.py:328
  52.3 11.3 %collective-permute-start.5 = (bf16[32,32,256]{2,1,0:T(8,128)(2,1)S(1)}, bf16[32,32,256]{2,1,0:T(8,128)(2,1)S(1)}, u32[]{:S(2)}, u32[]{:S(2)}) collective-permute-start(bf16[32,32,256]{2,1,0:T(8,128)(2,1)S(1)} %collective-permute-done.1.refs_2_), channel_id=1, source_target_pairs={{0,1},{1,0},{2,3},{3,2},{4,5},{5,4},{6,7},{7,6},{8,9},{9,8},{10,11... | collective-permute-start | bytes 1572872 | tf_op jit(solution)/shard_map/ppermute | solution.py:331
  56.1 7.5 %collective-permute-start.7 = (bf16[32,32,256]{2,1,0:T(8,128)(2,1)S(1)}, bf16[32,32,256]{2,1,0:T(8,128)(2,1)S(1)}, u32[]{:S(2)}, u32[]{:S(2)}) collective-permute-start(bf16[32,32,256]{2,1,0:T(8,128)(2,1)S(1)} %collective-permute-done.3.refs_4_), channel_id=1, source_target_pairs={{0,1},{1,0},{2,3},{3,2},{4,5},{5,4},{6,7},{7,6},{8,9},{9,8},{10,11... | collective-permute-start | bytes 1572872 | tf_op jit(solution)/shard_map/ppermute | solution.py:333
  61.7 3.8 %collective-permute-start.6 = (bf16[32,32,256]{2,1,0:T(8,128)(2,1)S(1)}, bf16[32,32,256]{2,1,0:T(8,128)(2,1)S(1)}, u32[]{:S(2)}, u32[]{:S(2)}) collective-permute-start(bf16[32,32,256]{2,1,0:T(8,128)(2,1)S(1)} %collective-permute-done.2.refs_3_), channel_id=1, source_target_pairs={{0,1},{1,0},{2,3},{3,2},{4,5},{5,4},{6,7},{7,6},{8,9},{9,8},{10,11... | collective-permute-start | bytes 1572872 | tf_op jit(solution)/shard_map/ppermute | solution.py:332
  67.4 33.1 %collective-permute-start.8 = (bf16[512,256]{1,0:T(8,128)(2,1)S(1)}, bf16[512,256]{1,0:T(8,128)(2,1)S(1)}, u32[]{:S(2)}, u32[]{:S(2)}) collective-permute-start(bf16[512,256]{1,0:T(8,128)(2,1)S(1)} %get-tuple-element.53), channel_id=1, source_target_pairs={{0,2},{2,4},{4,6},{6,8},{8,10},{10,12},{12,14},{14,0},{1,15},{3,1}... | collective-permute-start | bytes 786440 | tf_op jit(solution)/shard_map/ppermute | solution.py:342
  70.8 29.7 %collective-permute-start.9 = (bf16[512,256]{1,0:T(8,128)(2,1)S(1)}, bf16[512,256]{1,0:T(8,128)(2,1)S(1)}, u32[]{:S(2)}, u32[]{:S(2)}) collective-permute-start(bf16[512,256]{1,0:T(8,128)(2,1)S(1)} %get-tuple-element.54), channel_id=1, source_target_pairs={{0,4},{2,6},{4,8},{6,10},{8,12},{10,14},{12,0},{14,2},{1,13},{3,15... | collective-permute-start | bytes 786440 | tf_op jit(solution)/shard_map/ppermute | solution.py:342
  79.0 21.5 %collective-permute-start.10 = (bf16[512,256]{1,0:T(8,128)(2,1)S(1)}, bf16[512,256]{1,0:T(8,128)(2,1)S(1)}, u32[]{:S(2)}, u32[]{:S(2)}) collective-permute-start(bf16[512,256]{1,0:T(8,128)(2,1)S(1)} %get-tuple-element.55), channel_id=1, source_target_pairs={{0,6},{2,8},{4,10},{6,12},{8,14},{10,0},{12,2},{14,4},{1,11},{3,13... | collective-permute-start | bytes 786440 | tf_op jit(solution)/shard_map/ppermute | solution.py:342
  80.9 19.6 %collective-permute-start.11 = (bf16[512,128]{1,0:T(8,128)(2,1)S(1)}, bf16[512,128]{1,0:T(8,128)(2,1)S(1)}, u32[]{:S(2)}, u32[]{:S(2)}) collective-permute-start(bf16[512,128]{1,0:T(8,128)(2,1)S(1)} %get-tuple-element.56), channel_id=1, source_target_pairs={{0,8},{2,10},{4,12},{6,14},{8,0},{10,2},{12,4},{14,6},{1,9},{3,11}... | collective-permute-start | bytes 393224 | tf_op jit(solution)/shard_map/ppermute | solution.py:342
  100.7 39.1 %copy-start = (bf16[256,2048]{1,0:T(8,128)(2,1)S(1)}, bf16[256,2048]{1,0:T(8,128)(2,1)}, u32[]{:S(2)}) copy-start(bf16[256,2048]{1,0:T(8,128)(2,1)} %weight.1) | copy-start | bytes 3145732
  100.7 3.4 %collective-permute-start.12 = (bf16[512,128]{1,0:T(8,128)(2,1)S(1)}, bf16[512,128]{1,0:T(8,128)(2,1)S(1)}, u32[]{:S(2)}, u32[]{:S(2)}) collective-permute-start(bf16[512,128]{1,0:T(8,128)(2,1)S(1)} %get-tuple-element.73), channel_id=1, source_target_pairs={{0,1},{1,0},{2,3},{3,2},{4,5},{5,4},{6,7},{7,6},{8,9},{9,8},{10,11... | collective-permute-start | bytes 393224 | tf_op jit(solution)/shard_map/ppermute | solution.py:351
  121.9 17.8 %copy-start.1 = (bf16[128,256]{1,0:T(8,128)(2,1)S(1)}, bf16[128,256]{1,0:T(8,128)(2,1)}, u32[]{:S(2)}) copy-start(bf16[128,256]{1,0:T(8,128)(2,1)} %gate_pre.1) | copy-start | bytes 196612
  122.0 17.8 %copy-start.2 = (bf16[128,256]{1,0:T(8,128)(2,1)S(1)}, bf16[128,256]{1,0:T(8,128)(2,1)}, u32[]{:S(2)}) copy-start(bf16[128,256]{1,0:T(8,128)(2,1)} %mixer.1) | copy-start | bytes 196612
  122.0 17.8 %copy-start.4 = (bf16[128,128]{1,0:T(8,128)(2,1)S(1)}, bf16[128,128]{1,0:T(8,128)(2,1)}, u32[]{:S(2)}) copy-start(bf16[128,128]{1,0:T(8,128)(2,1)} %read.3) | copy-start | bytes 98308
  122.0 17.8 %copy-start.6 = (f32[4,128]{1,0:T(4,128)S(1)}, f32[4,128]{1,0:T(4,128)}, u32[]{:S(2)}) copy-start(f32[4,128]{1,0:T(4,128)} %logs.1) | copy-start | bytes 6148
  141.7 4.0 %copy-start.3 = (bf16[128,256]{1,0:T(8,128)(2,1)S(1)}, bf16[128,256]{1,0:T(8,128)(2,1)}, u32[]{:S(2)}) copy-start(bf16[128,256]{1,0:T(8,128)(2,1)} %values.3) | copy-start | bytes 196612
  141.7 4.1 %copy-start.5 = (bf16[128,128]{1,0:T(8,128)(2,1)S(1)}, bf16[128,128]{1,0:T(8,128)(2,1)}, u32[]{:S(2)}) copy-start(bf16[128,128]{1,0:T(8,128)(2,1)} %write.3) | copy-start | bytes 98308
  141.7 4.1 %copy-start.7 = (f32[1,4,64,128]{3,2,1,0:T(8,128)S(1)}, f32[1,4,64,128]{3,2,1,0:T(8,128)}, u32[]{:S(2)}) copy-start(f32[1,4,64,128]{3,2,1,0:T(8,128)} %param.29) | copy-start | bytes 393220
  141.7 24.8 %all-to-all-start.2 = ((bf16[32,40,256]{2,1,0:T(8,128)(2,1)}), bf16[32,40,256]{2,1,0:T(8,128)(2,1)S(1)}, u32[]{:S(2)}, u32[]{:S(2)}) async-start(bf16[32,40,256]{2,1,0:T(8,128)(2,1)} %get-tuple-element.74), calls=%async_computation.2 | async-start | bytes 1310720 | tf_op jit(solution)/shard_map/all_to_all | solution.py:362
  167.4 24.8 %all-to-all-start.3 = ((bf16[32,40,256]{2,1,0:T(8,128)(2,1)}), bf16[32,40,256]{2,1,0:T(8,128)(2,1)S(1)}, u32[]{:S(2)}, u32[]{:S(2)}) async-start(bf16[32,40,256]{2,1,0:T(8,128)(2,1)} %shard_map.219), calls=%async_computation.3 | async-start | bytes 1310720 | tf_op jit(solution)/shard_map/all_to_all | solution.py:369

commit v5 on v4

--- a/solution.py
+++ b/solution.py
@@ -18,6 +18,7 @@
 STATE = 128
 SP = ("z", "x")
 TP = ("y", "core")
+GRANT = 16 * 1024 * 1024
 BF = jnp.bfloat16
 F32 = jnp.float32
 
@@ -34,12 +35,14 @@
     return lax.dot_general(a, b, (((1,), (1,)), ((), ())), preferred_element_type=F32)
 
 
-def mm_nt_exact(a, b):
-    return lax.dot_general(a, b, (((1,), (1,)), ((), ())), precision=lax.Precision.HIGHEST, preferred_element_type=F32)
-
-
-def mm_exact(a, b):
-    return mm(a, b, lax.Precision.HIGHEST)
+def mm_parts(left, right, product):
+    total = None
+    for i, a in enumerate(left):
+        for j, b in enumerate(right):
+            if i + j < 2:
+                part = product(a, b)
+                total = part if total is None else total + part
+    return total
 
 
 def two_parts(value):
@@ -74,12 +77,19 @@
         out_shape=outs,
         in_specs=specs,
         out_specs=jax.tree.map(lambda _: vmem(), outs),
-        compiler_params=pltpu.CompilerParams(vmem_limit_bytes=20 * 1024 * 1024),
+        compiler_params=pltpu.CompilerParams(vmem_limit_bytes=GRANT),
         cost_estimate=pl.CostEstimate(flops=flops, bytes_accessed=0, transcendentals=0),
     )(*args)
 
 
-def prepare_kernel(where, routes, gates, mix, cot, buf, target):
+def prepare_kernel(where, routes, gates, mixed, cotangent, buf, target, mix, cot, arrived):
+    at = pl.ds(pl.multiple_of(lax.rem(where[0], 8) * WIDE, WIDE), WIDE)
+    copies = [
+        pltpu.make_async_copy(mixed.at[:, at], mix, arrived.at[0]),
+        pltpu.make_async_copy(cotangent.at[:, at], cot, arrived.at[1]),
+    ]
+    for copy in copies:
+        copy.start()
     picks = routes[...]
     expert = iota((EXP, TOK), 0)
     hits = [expert == picks[k : k + 1] for k in range(2)]
@@ -87,46 +97,41 @@
     before = jnp.where(iota((TOK, TOK), 0) < iota((TOK, TOK), 1), 1.0, 0.0).astype(BF)
     count = mm(both, before)
     row = iota((ROWS, TOK), 0)
-    cots = cot[...].astype(F32)
-    places, scaled, rows = [], [], []
+    places, rows = [], []
     for k in range(2):
         slot = jnp.sum(jnp.where(hits[k], count, 0.0), axis=0, keepdims=True)
         place = picks[k : k + 1] * CAP + slot.astype(jnp.int32)
         rows.append(place)
         places.append(jnp.where(row == place, 1.0, 0.0).astype(BF))
-        scaled.append((columns(gates[k : k + 1, :]) * cots).astype(BF))
     target[...] = jnp.concatenate(rows + [jnp.zeros((6, TOK), jnp.int32)], axis=0)
+    for copy in copies:
+        copy.wait()
+    cots = cot[...].astype(F32)
+    scaled = [(columns(gates[k : k + 1, :]) * cots).astype(BF) for k in range(2)]
     toks = mm(places[0] + places[1], mix[...]).astype(BF)
     buf[:, 0:CAP, :] = toks.reshape(EXP, CAP, WIDE)
     spread = mm(jnp.concatenate(places, axis=1), jnp.concatenate(scaled, axis=0)).astype(BF)
     buf[:, CAP : 2 * CAP, :] = spread.reshape(EXP, CAP, WIDE)
 
 
-def prepare(quarter, routes, gates, mixed, cotangent):
-    whole = lambda i, q: (0, 0)
-    part = lambda i, q: (0, lax.rem(q[0], 8))
+def prepare(slot, routes, gates, mixed, cotangent):
+    hbm = pl.BlockSpec(memory_space=pltpu.HBM)
     return pl.pallas_call(
         prepare_kernel,
         out_shape=(
             jax.ShapeDtypeStruct((EXP, 2 * CAP, WIDE), BF),
             jax.ShapeDtypeStruct((8, TOK), jnp.int32),
         ),
-        grid_spec=pltpu.PrefetchScalarGridSpec(
-            num_scalar_prefetch=1,
-            grid=(1,),
-            in_specs=[
-                pl.BlockSpec((2, TOK), whole),
-                pl.BlockSpec((2, TOK), whole),
-                pl.BlockSpec((TOK, WIDE), part),
-                pl.BlockSpec((TOK, WIDE), part),
-            ],
-            out_specs=(
-                pl.BlockSpec((EXP, 2 * CAP, WIDE), lambda i, q: (0, 0, 0)),
-                pl.BlockSpec((8, TOK), whole),
-            ),
-        ),
+        in_specs=[smem(), vmem(), vmem(), hbm, hbm],
+        out_specs=(vmem(), vmem()),
+        scratch_shapes=[
+            pltpu.VMEM((TOK, WIDE), BF),
+            pltpu.VMEM((TOK, WIDE), BF),
+            pltpu.SemaphoreType.DMA((2,)),
+        ],
+        compiler_params=pltpu.CompilerParams(vmem_limit_bytes=GRANT),
         name="prepare",
-    )(quarter, routes, gates, mixed, cotangent)
+    )(slot, routes, gates, mixed, cotangent)
 
 
 def row_blocks(chunk):
@@ -214,6 +219,7 @@
         in_specs=[smem(), vmem(), vmem(), pl.BlockSpec(memory_space=pltpu.HBM)],
         out_specs=vmem(),
         scratch_shapes=[pltpu.VMEM((TOK, TOK), BF), pltpu.SemaphoreType.DMA],
+        compiler_params=pltpu.CompilerParams(vmem_limit_bytes=GRANT),
         name="combine",
     )(slot, target, rows, cotangent)
 
@@ -274,7 +280,7 @@
     running = run[...]
     cols = running.T
     grads = grad_y[...]
-    vals = values[...].astype(F32)
+    vals = values[...]
     cross = mm_nt(write[...], read[...])
     later = iota((TOK, TOK), 1) >= iota((TOK, TOK), 0)
     total = jnp.zeros((TOK, TOK), F32)
@@ -284,16 +290,18 @@
         spread = running[j : j + 1] - cols[:, j : j + 1]
         decay = jnp.where(later, jnp.exp(jnp.where(later, spread, 0.0)), 0.0)
         grad = grads[:, j * HD : (j + 1) * HD]
-        parts.append(mm_exact(cross * decay, grad))
-        total = total + mm_nt_exact(vals[:, j * HD : (j + 1) * HD], grad) * decay
+        halves = two_parts(grad)
+        parts.append(mm_parts(two_parts(cross * decay), halves, mm))
+        total = total + mm_parts((vals[:, j * HD : (j + 1) * HD],), halves, mm_nt) * decay
         starts.append(grad * jnp.exp(cols[:, j : j + 1]))
     dx[...] = jnp.concatenate(parts, axis=1)
-    dw[...] = mm_exact(total, read[...].astype(F32))
-    entry_rows = entry[...].reshape(HEADS * HD, STATE)
-    dr[...] = mm_exact(total.T, write[...].astype(F32)) + mm_exact(jnp.concatenate(starts, axis=1), entry_rows)
-
-
-def outer_kernel(dx, dw, values, write, run, half, second, d_values, d_write, d_out):
+    dw[...] = mm_parts(two_parts(total), (read[...],), mm)
+    entry_rows = two_parts(entry[...].reshape(HEADS * HD, STATE))
+    first = mm_parts(two_parts(total.T), (write[...],), mm)
+    dr[...] = first + mm_parts(two_parts(jnp.concatenate(starts, axis=1)), entry_rows, mm)
+
+
+def outer_kernel(dx, dw, values, write, run, received, second, d_values, d_write, d_out):
     running = run[...]
     ends = jnp.exp(running[:, TOK - 1 : TOK] - running).T
     scale = jnp.concatenate([jnp.broadcast_to(ends[:, j : j + 1], (TOK, HD)) for j in range(HEADS)], axis=1)
@@ -302,11 +310,11 @@
     d_values[...] = (dx[...] + scale * (mm_nt(write[...], high) + mm_nt(write[...], low))).astype(BF)
     top, rest = two_parts(values[...].astype(F32) * scale)
     d_write[...] = dw[...] + mm(top, high) + mm(top, low) + mm(rest, high)
-    total = second[0, 0:EXP, :].astype(F32)
-    for k in range(1, EXP):
-        total = total + second[k, 0:EXP, :].astype(F32)
-    d_out[0:EXP, :] = half[...]
-    d_out[EXP:, :] = total
+    for at, block in ((0, received), (EXP, second)):
+        total = block[0, 0:EXP, :].astype(F32)
+        for k in range(1, EXP):
+            total = total + block[k, 0:EXP, :].astype(F32)
+        d_out[at : at + EXP, :] = total
 
 
 def step(mixed, cotangent, routes, gates, w_gate, w_up, w_down, out_weight, gate_pre, mixer_out, values,
@@ -359,19 +367,17 @@
         (flat, shape((TOK, HEADS * HD), F32), shape((8, TOK), F32), shape((EXP, EXP + 8, WIDE), BF),
          shape((EXP, EXP, WIDE), BF)),
         [vmem()] * 6, (whole, out_weight, gate_pre, mixer_out, log_decay, read_keys))
-    received = lax.all_to_all(sent, SP, 0, 0, tiled=True)
     square = shape((TOK, STATE), F32)
     dx, dw, d_read = call(
         inner_kernel, (shape((TOK, HEADS * HD), F32), square, square),
         [vmem()] * 6, (grad_y, values, write_keys, read_keys, run, entry_states[0]), flops=10**9)
-    received, dx, dw, d_read = lax.optimization_barrier((received, dx, dw, d_read))
+    sent, dx, dw, d_read = lax.optimization_barrier((sent, dx, dw, d_read))
+    received = lax.all_to_all(sent, SP, 0, 0, tiled=True)
     states = call(scan_kernel, shape((EXP, EXP + 8, WIDE), BF), [vmem()] * 2, (received, rest))
     second = lax.all_to_all(states, SP, 0, 0, tiled=True)
-    half = jnp.sum(received[:, :EXP].astype(F32), axis=0)
-    second, half = lax.optimization_barrier((second, half))
     d_values, d_write, d_out_weight = call(
         outer_kernel, (flat, square, shape((D // EXP, HEADS * HD), F32)), [vmem()] * 7,
-        (dx, dw, values, write_keys, run, half, second))
+        (dx, dw, values, write_keys, run, received, second))
     return (d_wg.T[None], d_wu.T[None], d_wd[None], d_out_weight, d_input, d_values, d_write, d_read, d_gate)
 
 

time: 194 us -> 193 us (level)
  blocking collectives: 64.3 us -> 112 us
  waiting for transfers between devices: 62.6 us -> 24.7 us
  starting transfers between devices: 50.8 us -> 41.5 us
  Pallas kernels: 14.5 us -> 9.82 us
  local copies, waits for them, and re-layouts: 0.05 us -> 2.84 us
    all_to_all x0 -> x2, blocking collectives: none -> 48.3 us  [the longest x1 24.2 us: step(): received = lax.all_to_all(sent, SP, 0, 0, tiled=True)]
    all_to_all x2 -> x0, waiting for transfers between devices: 38 us -> none  [the longest x1 19.5 us: step(): second = lax.all_to_all(states, SP, 0, 0, tiled=True)]
    all_to_all x2 -> x0, starting transfers between devices: 9.27 us -> none  [the longest x1 5.24 us: step(): second = lax.all_to_all(states, SP, 0, 0, tiled=True)]
    unnamed x22 -> x32, local copies, waits for them, and re-layouts: 0.05 us -> 2.84 us
  transfers between devices with their start and end apart: 15 -> 13, of which waited for: 8 -> 6; matrix products, arithmetic and copies ran while one was open for 0% -> 0% of each run, Pallas kernels for 2% -> 1%
where the time goes in v5:
time: 193 us; the launch traced here: 192 us
  blocking collectives  112 us (58%)
  starting transfers between devices  41.5 us (22%)
  waiting for transfers between devices  24.7 us (13%)
  Pallas kernels  9.82 us (5%)
  local copies, waits for them, and re-layouts  2.84 us (1%)
    all_to_all x1, blocking collectives, step(): c0 = lax.all_to_all(buf, SP, 0, 0, tiled=True)  30.9 us
    all_to_all x1, blocking collectives, step(): received = lax.all_to_all(sent, SP, 0, 0, tiled=True)  24.2 us
    all_to_all x1, blocking collectives, step(): second = lax.all_to_all(states, SP, 0, 0, tiled=True)  24.1 us
    ppermute x4, starting transfers between devices, step(): pieces.append(lax.ppermute(parts[k], TP, rings[k]))  18.2 us
    all_gather x1, blocking collectives, step(): whole = lax.all_gather(d_input, TP, axis=1, tiled=True)  17.8 us
    all_to_all x1, blocking collectives, step(): back = lax.all_to_all(summed, SP, 0, 0, tiled=True)  15.4 us
    ppermute x4, waiting for transfers between devices, step(): pieces.append(lax.ppermute(parts[k], TP, rings[k]))  13.2 us
    pallas_call x7, Pallas kernels, call(): pl.pallas_call(kernel, out_shape=outs, in_specs=specs, out_specs=jax.tree...  8.06 us
  transfers between devices with their start and end apart: 13, of which 6 were waited for; matrix products, arithmetic and copies ran while one was open for 0% of the time, Pallas kernels for 1%

profile of v5, /device:TPU:8, one launch (start us, length us, event | category | flops | bytes accessed | tf_op | source)
XLA Modules:
  0.0 192.2 jit_solution(17713535525928399804)
XLA Ops:
  1.3 1.0 copy-done
  2.4 1.0 copy-done.3
  4.3 30.9 %all_to_all.20.refs_0_ = bf16[32,32,256]{2,1,0:T(8,128)(2,1)S(1)} all-to-all(bf16[32,32,256]{2,1,0:T(8,128)(2,1)S(1)} %get-tuple-element.48), channel_id=1, replica_groups=mesh['z'=8,'x'=4,'y'=8,'core'=2] {'z','x'}, dimensions={0} | all-to-all | bytes 1048576 | tf_op jit(solution)/shard_map/all_to_all | solution.py:333
  35.1 3.5 %collective-permute-start.1 = (bf16[32,32,256]{2,1,0:T(8,128)(2,1)S(1)}, bf16[32,32,256]{2,1,0:T(8,128)(2,1)S(1)}, u32[]{:S(2)}, u32[]{:S(2)}) collective-permute-start(bf16[32,32,256]{2,1,0:T(8,128)(2,1)S(1)} %all_to_all.20.refs_0_), channel_id=1, source_target_pairs={{0,2},{2,4},{4,6},{6,8},{8,10},{10,12},{12,14},{14,0},{1,15},{3,1}... | collective-permute-start | bytes 1572872 | tf_op jit(solution)/shard_map/ppermute | solution.py:334
  38.6 1.9 collective-permute-start
  40.6 2.4 %collective-permute-start.4 = (bf16[3,64,2048]{2,1,0:T(8,128)(2,1)S(1)}, bf16[3,64,2048]{2,1,0:T(8,128)(2,1)S(1)}, u32[]{:S(2)}, u32[]{:S(2)}) collective-permute-start(bf16[3,64,2048]{2,1,0:T(8,128)(2,1)S(1)} %pad_maximum_fusion.refs_8_), channel_id=1, source_target_pairs={{0,1},{1,0},{2,3},{3,2},{4,5},{5,4},{6,7},{7,6},{8,9},{9,8},{10,11... | collective-permute-start | bytes 2359304 | tf_op jit(solution)/shard_map/ppermute | solution.py:331
  43.1 3.1 %collective-permute-done.1.refs_2_ = bf16[32,32,256]{2,1,0:T(8,128)(2,1)S(1)} collective-permute-done((bf16[32,32,256]{2,1,0:T(8,128)(2,1)S(1)}, bf16[32,32,256]{2,1,0:T(8,128)(2,1)S(1)}, u32[]{:S(2)}, u32[]{:S(2)}) %collective-permute-start.1) | collective-permute-done | bytes 524320 | tf_op jit(solution)/shard_map/ppermute | solution.py:334
  46.2 3.5 %collective-permute-start.3 = (bf16[32,32,256]{2,1,0:T(8,128)(2,1)S(1)}, bf16[32,32,256]{2,1,0:T(8,128)(2,1)S(1)}, u32[]{:S(2)}, u32[]{:S(2)}) collective-permute-start(bf16[32,32,256]{2,1,0:T(8,128)(2,1)S(1)} %collective-permute-done.1.refs_2_), channel_id=1, source_target_pairs={{0,2},{2,4},{4,6},{6,8},{8,10},{10,12},{12,14},{14,0},{1,15},{3,1}... | collective-permute-start | bytes 1572872 | tf_op jit(solution)/shard_map/ppermute | solution.py:337
  49.7 3.8 %collective-permute-start.2 = (bf16[32,32,256]{2,1,0:T(8,128)(2,1)S(1)}, bf16[32,32,256]{2,1,0:T(8,128)(2,1)S(1)}, u32[]{:S(2)}, u32[]{:S(2)}) collective-permute-start(bf16[32,32,256]{2,1,0:T(8,128)(2,1)S(1)} %collective-permute-done.refs_1_), channel_id=1, source_target_pairs={{0,2},{2,4},{4,6},{6,8},{8,10},{10,12},{12,14},{14,0},{1,15},{3,1}... | collective-permute-start | bytes 1572872 | tf_op jit(solution)/shard_map/ppermute | solution.py:336
  53.5 1.9 collective-permute-start.5
  55.4 1.8 collective-permute-done.3.refs_4_
  57.2 1.9 collective-permute-start.7
  59.1 3.7 %collective-permute-done.2.refs_3_ = bf16[32,32,256]{2,1,0:T(8,128)(2,1)S(1)} collective-permute-done((bf16[32,32,256]{2,1,0:T(8,128)(2,1)S(1)}, bf16[32,32,256]{2,1,0:T(8,128)(2,1)S(1)}, u32[]{:S(2)}, u32[]{:S(2)}) %collective-permute-start.2) | collective-permute-done | bytes 524320 | tf_op jit(solution)/shard_map/ppermute | solution.py:336
  62.9 1.9 collective-permute-start.6
  64.8 1.9 collective-permute-done.6.refs_6_
  66.6 1.8 shard_map.214
  68.5 3.5 %collective-permute-start.8 = (bf16[512,256]{1,0:T(8,128)(2,1)S(1)}, bf16[512,256]{1,0:T(8,128)(2,1)S(1)}, u32[]{:S(2)}, u32[]{:S(2)}) collective-permute-start(bf16[512,256]{1,0:T(8,128)(2,1)S(1)} %get-tuple-element.51), channel_id=1, source_target_pairs={{0,2},{2,4},{4,6},{6,8},{8,10},{10,12},{12,14},{14,0},{1,15},{3,1}... | collective-permute-start | bytes 786440 | tf_op jit(solution)/shard_map/ppermute | solution.py:350
  72.0 8.1 %collective-permute-start.9 = (bf16[512,256]{1,0:T(8,128)(2,1)S(1)}, bf16[512,256]{1,0:T(8,128)(2,1)S(1)}, u32[]{:S(2)}, u32[]{:S(2)}) collective-permute-start(bf16[512,256]{1,0:T(8,128)(2,1)S(1)} %get-tuple-element.52), channel_id=1, source_target_pairs={{0,4},{2,6},{4,8},{6,10},{8,12},{10,14},{12,0},{14,2},{1,13},{3,15... | collective-permute-start | bytes 786440 | tf_op jit(solution)/shard_map/ppermute | solution.py:350
  80.1 1.9 collective-permute-start.10
  82.0 4.7 %collective-permute-start.11 = (bf16[512,128]{1,0:T(8,128)(2,1)S(1)}, bf16[512,128]{1,0:T(8,128)(2,1)S(1)}, u32[]{:S(2)}, u32[]{:S(2)}) collective-permute-start(bf16[512,128]{1,0:T(8,128)(2,1)S(1)} %get-tuple-element.54), channel_id=1, source_target_pairs={{0,8},{2,10},{4,12},{6,14},{8,0},{10,2},{12,4},{14,6},{1,9},{3,11}... | collective-permute-start | bytes 393224 | tf_op jit(solution)/shard_map/ppermute | solution.py:350
  86.8 1.7 shard_map.215
  88.4 13.2 %collective-permute-done.11.last = bf16[512,128]{1,0:T(8,128)(2,1)S(1)} collective-permute-done((bf16[512,128]{1,0:T(8,128)(2,1)S(1)}, bf16[512,128]{1,0:T(8,128)(2,1)S(1)}, u32[]{:S(2)}, u32[]{:S(2)}) %collective-permute-start.11) | collective-permute-done | bytes 131104 | tf_op jit(solution)/shard_map/ppermute | solution.py:350
  101.8 2.4 %collective-permute-start.12 = (bf16[512,128]{1,0:T(8,128)(2,1)S(1)}, bf16[512,128]{1,0:T(8,128)(2,1)S(1)}, u32[]{:S(2)}, u32[]{:S(2)}) collective-permute-start(bf16[512,128]{1,0:T(8,128)(2,1)S(1)} %get-tuple-element.71), channel_id=1, source_target_pairs={{0,1},{1,0},{2,3},{3,2},{4,5},{5,4},{6,7},{7,6},{8,9},{9,8},{10,11... | collective-permute-start | bytes 393224 | tf_op jit(solution)/shard_map/ppermute | solution.py:359
  104.3 1.0 collective-permute-done.12
  105.2 15.4 %all_to_all.21.rows = bf16[32,16,128]{2,1,0:T(8,128)(2,1)S(1)} all-to-all(bf16[32,16,128]{2,1,0:T(8,128)(2,1)S(1)} %bitcast.25), channel_id=1, replica_groups=mesh['z'=8,'x'=4,'y'=8,'core'=2] {'z','x'}, dimensions={0} | all-to-all | bytes 262144 | tf_op jit(solution)/shard_map/all_to_all | solution.py:361
  120.7 1.0 combine.1
  121.7 17.8 %all_gather.3.whole = bf16[128,2048]{1,0:T(8,128)(2,1)S(1)} all-gather(bf16[128,128]{1,0:T(8,128)(2,1)} %combine.1), channel_id=1, replica_groups=mesh['z'=8,'x'=4,'y'=8,'core'=2] {'y','core'}, dimensions={1}, use_global_device_ids=true | all-gather | bytes 557056 | tf_op jit(solution)/shard_map/all_gather | solution.py:363
  139.5 1.6 shard_map.217
  141.2 1.5 shard_map.218
  142.6 24.2 %all_to_all.22.received = bf16[32,40,256]{2,1,0:T(8,128)(2,1)S(1)} all-to-all(bf16[32,40,256]{2,1,0:T(8,128)(2,1)S(1)} %get-tuple-element.80), channel_id=1, replica_groups=mesh['z'=8,'x'=4,'y'=8,'core'=2] {'z','x'}, dimensions={0} | all-to-all | bytes 1310720 | tf_op jit(solution)/shard_map/all_to_all | solution.py:375
  166.9 24.1 %all_to_all.23.second = bf16[32,40,256]{2,1,0:T(8,128)(2,1)S(1)} all-to-all(bf16[32,40,256]{2,1,0:T(8,128)(2,1)S(1)} %shard_map.219), channel_id=1, replica_groups=mesh['z'=8,'x'=4,'y'=8,'core'=2] {'z','x'}, dimensions={0} | all-to-all | bytes 1310720 | tf_op jit(solution)/shard_map/all_to_all | solution.py:377
  191.0 1.2 shard_map.220
  (42 shorter events, 1.9 us)
Async XLA Ops:
  0.6 0.7 copy-start.11
  0.7 0.7 copy-start.10
  1.3 1.0 copy-start
  2.4 1.0 copy-start.3
  4.2 36.3 %copy-start.13 = (bf16[1,64,2048]{2,1,0:T(8,128)(2,1)S(1)}, bf16[1,64,2048]{2,1,0:T(8,128)(2,1)}, u32[]{:S(2)}) copy-start(bf16[1,64,2048]{2,1,0:T(8,128)(2,1)} %param.21) | copy-start | bytes 786436
  4.2 36.3 %copy-start.14 = (bf16[1,2048,64]{1,2,0:T(8,128)(2,1)S(1)}, bf16[1,2048,64]{1,2,0:T(8,128)(2,1)}, u32[]{:S(2)}) copy-start(bf16[1,2048,64]{1,2,0:T(8,128)(2,1)} %param.20) | copy-start | bytes 786436
  4.2 36.3 %copy-start.15 = (bf16[1,2048,64]{1,2,0:T(8,128)(2,1)S(1)}, bf16[1,2048,64]{1,2,0:T(8,128)(2,1)}, u32[]{:S(2)}) copy-start(bf16[1,2048,64]{1,2,0:T(8,128)(2,1)} %param.19) | copy-start | bytes 786436
  35.1 11.1 %collective-permute-start.1 = (bf16[32,32,256]{2,1,0:T(8,128)(2,1)S(1)}, bf16[32,32,256]{2,1,0:T(8,128)(2,1)S(1)}, u32[]{:S(2)}, u32[]{:S(2)}) collective-permute-start(bf16[32,32,256]{2,1,0:T(8,128)(2,1)S(1)} %all_to_all.20.refs_0_), channel_id=1, source_target_pairs={{0,2},{2,4},{4,6},{6,8},{8,10},{10,12},{12,14},{14,0},{1,15},{3,1}... | collective-permute-start | bytes 1572872 | tf_op jit(solution)/shard_map/ppermute | solution.py:334
  38.6 11.1 %collective-permute-start = (bf16[32,32,256]{2,1,0:T(8,128)(2,1)S(1)}, bf16[32,32,256]{2,1,0:T(8,128)(2,1)S(1)}, u32[]{:S(2)}, u32[]{:S(2)}) collective-permute-start(bf16[32,32,256]{2,1,0:T(8,128)(2,1)S(1)} %all_to_all.20.refs_0_), channel_id=1, source_target_pairs={{0,1},{1,0},{2,3},{3,2},{4,5},{5,4},{6,7},{7,6},{8,9},{9,8},{10,11... | collective-permute-start | bytes 1572872 | tf_op jit(solution)/shard_map/ppermute | solution.py:335
  40.6 12.8 %collective-permute-start.4 = (bf16[3,64,2048]{2,1,0:T(8,128)(2,1)S(1)}, bf16[3,64,2048]{2,1,0:T(8,128)(2,1)S(1)}, u32[]{:S(2)}, u32[]{:S(2)}) collective-permute-start(bf16[3,64,2048]{2,1,0:T(8,128)(2,1)S(1)} %pad_maximum_fusion.refs_8_), channel_id=1, source_target_pairs={{0,1},{1,0},{2,3},{3,2},{4,5},{5,4},{6,7},{7,6},{8,9},{9,8},{10,11... | collective-permute-start | bytes 2359304 | tf_op jit(solution)/shard_map/ppermute | solution.py:331
  46.2 11.1 %collective-permute-start.3 = (bf16[32,32,256]{2,1,0:T(8,128)(2,1)S(1)}, bf16[32,32,256]{2,1,0:T(8,128)(2,1)S(1)}, u32[]{:S(2)}, u32[]{:S(2)}) collective-permute-start(bf16[32,32,256]{2,1,0:T(8,128)(2,1)S(1)} %collective-permute-done.1.refs_2_), channel_id=1, source_target_pairs={{0,2},{2,4},{4,6},{6,8},{8,10},{10,12},{12,14},{14,0},{1,15},{3,1}... | collective-permute-start | bytes 1572872 | tf_op jit(solution)/shard_map/ppermute | solution.py:337
  49.7 13.2 %collective-permute-start.2 = (bf16[32,32,256]{2,1,0:T(8,128)(2,1)S(1)}, bf16[32,32,256]{2,1,0:T(8,128)(2,1)S(1)}, u32[]{:S(2)}, u32[]{:S(2)}) collective-permute-start(bf16[32,32,256]{2,1,0:T(8,128)(2,1)S(1)} %collective-permute-done.refs_1_), channel_id=1, source_target_pairs={{0,2},{2,4},{4,6},{6,8},{8,10},{10,12},{12,14},{14,0},{1,15},{3,1}... | collective-permute-start | bytes 1572872 | tf_op jit(solution)/shard_map/ppermute | solution.py:336
  53.5 11.3 %collective-permute-start.5 = (bf16[32,32,256]{2,1,0:T(8,128)(2,1)S(1)}, bf16[32,32,256]{2,1,0:T(8,128)(2,1)S(1)}, u32[]{:S(2)}, u32[]{:S(2)}) collective-permute-start(bf16[32,32,256]{2,1,0:T(8,128)(2,1)S(1)} %collective-permute-done.1.refs_2_), channel_id=1, source_target_pairs={{0,1},{1,0},{2,3},{3,2},{4,5},{5,4},{6,7},{7,6},{8,9},{9,8},{10,11... | collective-permute-start | bytes 1572872 | tf_op jit(solution)/shard_map/ppermute | solution.py:339
  57.2 7.5 %collective-permute-start.7 = (bf16[32,32,256]{2,1,0:T(8,128)(2,1)S(1)}, bf16[32,32,256]{2,1,0:T(8,128)(2,1)S(1)}, u32[]{:S(2)}, u32[]{:S(2)}) collective-permute-start(bf16[32,32,256]{2,1,0:T(8,128)(2,1)S(1)} %collective-permute-done.3.refs_4_), channel_id=1, source_target_pairs={{0,1},{1,0},{2,3},{3,2},{4,5},{5,4},{6,7},{7,6},{8,9},{9,8},{10,11... | collective-permute-start | bytes 1572872 | tf_op jit(solution)/shard_map/ppermute | solution.py:341
  62.9 3.8 %collective-permute-start.6 = (bf16[32,32,256]{2,1,0:T(8,128)(2,1)S(1)}, bf16[32,32,256]{2,1,0:T(8,128)(2,1)S(1)}, u32[]{:S(2)}, u32[]{:S(2)}) collective-permute-start(bf16[32,32,256]{2,1,0:T(8,128)(2,1)S(1)} %collective-permute-done.2.refs_3_), channel_id=1, source_target_pairs={{0,1},{1,0},{2,3},{3,2},{4,5},{5,4},{6,7},{7,6},{8,9},{9,8},{10,11... | collective-permute-start | bytes 1572872 | tf_op jit(solution)/shard_map/ppermute | solution.py:340
  68.5 33.2 %collective-permute-start.8 = (bf16[512,256]{1,0:T(8,128)(2,1)S(1)}, bf16[512,256]{1,0:T(8,128)(2,1)S(1)}, u32[]{:S(2)}, u32[]{:S(2)}) collective-permute-start(bf16[512,256]{1,0:T(8,128)(2,1)S(1)} %get-tuple-element.51), channel_id=1, source_target_pairs={{0,2},{2,4},{4,6},{6,8},{8,10},{10,12},{12,14},{14,0},{1,15},{3,1}... | collective-permute-start | bytes 786440 | tf_op jit(solution)/shard_map/ppermute | solution.py:350
  72.0 29.7 %collective-permute-start.9 = (bf16[512,256]{1,0:T(8,128)(2,1)S(1)}, bf16[512,256]{1,0:T(8,128)(2,1)S(1)}, u32[]{:S(2)}, u32[]{:S(2)}) collective-permute-start(bf16[512,256]{1,0:T(8,128)(2,1)S(1)} %get-tuple-element.52), channel_id=1, source_target_pairs={{0,4},{2,6},{4,8},{6,10},{8,12},{10,14},{12,0},{14,2},{1,13},{3,15... | collective-permute-start | bytes 786440 | tf_op jit(solution)/shard_map/ppermute | solution.py:350
  80.1 21.5 %collective-permute-start.10 = (bf16[512,256]{1,0:T(8,128)(2,1)S(1)}, bf16[512,256]{1,0:T(8,128)(2,1)S(1)}, u32[]{:S(2)}, u32[]{:S(2)}) collective-permute-start(bf16[512,256]{1,0:T(8,128)(2,1)S(1)} %get-tuple-element.53), channel_id=1, source_target_pairs={{0,6},{2,8},{4,10},{6,12},{8,14},{10,0},{12,2},{14,4},{1,11},{3,13... | collective-permute-start | bytes 786440 | tf_op jit(solution)/shard_map/ppermute | solution.py:350
  82.0 19.6 %collective-permute-start.11 = (bf16[512,128]{1,0:T(8,128)(2,1)S(1)}, bf16[512,128]{1,0:T(8,128)(2,1)S(1)}, u32[]{:S(2)}, u32[]{:S(2)}) collective-permute-start(bf16[512,128]{1,0:T(8,128)(2,1)S(1)} %get-tuple-element.54), channel_id=1, source_target_pairs={{0,8},{2,10},{4,12},{6,14},{8,0},{10,2},{12,4},{14,6},{1,9},{3,11}... | collective-permute-start | bytes 393224 | tf_op jit(solution)/shard_map/ppermute | solution.py:350
  101.8 18.9 %copy-start.1 = (bf16[128,2048]{1,0:T(8,128)(2,1)S(1)}, bf16[128,2048]{1,0:T(8,128)(2,1)}, u32[]{:S(2)}) copy-start(bf16[128,2048]{1,0:T(8,128)(2,1)} %cotangent.3) | copy-start | bytes 1572868
  101.8 37.7 %copy-start.2 = (bf16[256,2048]{1,0:T(8,128)(2,1)S(1)}, bf16[256,2048]{1,0:T(8,128)(2,1)}, u32[]{:S(2)}) copy-start(bf16[256,2048]{1,0:T(8,128)(2,1)} %weight.1) | copy-start | bytes 3145732
  101.8 3.4 %collective-permute-start.12 = (bf16[512,128]{1,0:T(8,128)(2,1)S(1)}, bf16[512,128]{1,0:T(8,128)(2,1)S(1)}, u32[]{:S(2)}, u32[]{:S(2)}) collective-permute-start(bf16[512,128]{1,0:T(8,128)(2,1)S(1)} %get-tuple-element.71), channel_id=1, source_target_pairs={{0,1},{1,0},{2,3},{3,2},{4,5},{5,4},{6,7},{7,6},{8,9},{9,8},{10,11... | collective-permute-start | bytes 393224 | tf_op jit(solution)/shard_map/ppermute | solution.py:359
  121.6 17.8 %copy-start.5 = (bf16[128,256]{1,0:T(8,128)(2,1)S(1)}, bf16[128,256]{1,0:T(8,128)(2,1)}, u32[]{:S(2)}) copy-start(bf16[128,256]{1,0:T(8,128)(2,1)} %gate_pre.1) | copy-start | bytes 196612
  121.7 17.8 %copy-start.6 = (bf16[128,256]{1,0:T(8,128)(2,1)S(1)}, bf16[128,256]{1,0:T(8,128)(2,1)}, u32[]{:S(2)}) copy-start(bf16[128,256]{1,0:T(8,128)(2,1)} %mixer.1) | copy-start | bytes 196612
  121.7 17.8 %copy-start.7 = (bf16[128,128]{1,0:T(8,128)(2,1)S(1)}, bf16[128,128]{1,0:T(8,128)(2,1)}, u32[]{:S(2)}) copy-start(bf16[128,128]{1,0:T(8,128)(2,1)} %read.3) | copy-start | bytes 98308
  121.7 17.8 %copy-start.9 = (f32[4,128]{1,0:T(4,128)S(1)}, f32[4,128]{1,0:T(4,128)}, u32[]{:S(2)}) copy-start(f32[4,128]{1,0:T(4,128)} %logs.1) | copy-start | bytes 6148
  139.5 1.7 copy-start.4
  139.5 1.6 copy-start.8
  139.5 1.6 copy-start.12

commit v6 on v2

v6 whole, which is shorter than its diff:
```python
import jax
import jax.numpy as jnp
from jax import lax
from jax.experimental import pallas as pl
from jax.experimental.pallas import tpu as pltpu
from jax.sharding import Mesh
from jax.sharding import PartitionSpec as P

D = 2048
TOK = 128
EXP = 32
CAP = 16
ROWS = EXP * CAP
WIDE = 512
FF = 64
HEADS = 4
HD = 64
STATE = 128
SP = ("z", "x")
TP = ("y", "core")
GRANT = 16 * 1024 * 1024
BF = jnp.bfloat16
F32 = jnp.float32


def iota(shape, dim):
    return lax.broadcasted_iota(jnp.int32, shape, dim)


def mm(a, b, precision=None):
    return lax.dot_general(a, b, (((1,), (0,)), ((), ())), precision=precision, preferred_element_type=F32)


def mm_nt(a, b):
    return lax.dot_general(a, b, (((1,), (1,)), ((), ())), preferred_element_type=F32)


def mm_parts(left, right, product):
    total = None
    for i, a in enumerate(left):
        for j, b in enumerate(right):
            if i + j < 2:
                part = product(a, b)
                total = part if total is None else total + part
    return total


def two_parts(value):
    high = value.astype(BF)
    return high, (value - high.astype(F32)).astype(BF)


def quarter_of(slot):
    return slot & 3


def columns(row):
    return jnp.broadcast_to(row, (8, row.shape[1])).T[:, 0:1]


def vmem():
    return pl.BlockSpec(memory_space=pltpu.VMEM)


def smem():
    return pl.BlockSpec(memory_space=pltpu.SMEM)


def call(kernel, outs, specs, args, flops=0):
    return pl.pallas_call(
        kernel,
        out_shape=outs,
        in_specs=specs,
        out_specs=jax.tree.map(lambda _: vmem(), outs),
        compiler_params=pltpu.CompilerParams(vmem_limit_bytes=GRANT),
        cost_estimate=pl.CostEstimate(flops=flops, bytes_accessed=0, transcendentals=0),
    )(*args)


def prepare_kernel(where, routes, gates, mix, cot, buf, target):
    picks = routes[...]
    expert = iota((EXP, TOK), 0)
    hits = [expert == picks[k : k + 1] for k in range(2)]
    both = jnp.where(hits[0] | hits[1], 1.0, 0.0).astype(BF)
    before = jnp.where(iota((TOK, TOK), 0) < iota((TOK, TOK), 1), 1.0, 0.0).astype(BF)
    count = mm(both, before)
    row = iota((ROWS, TOK), 0)
    places, rows = [], []
    for k in range(2):
        slot = jnp.sum(jnp.where(hits[k], count, 0.0), axis=0, keepdims=True)
        place = picks[k : k + 1] * CAP + slot.astype(jnp.int32)
        rows.append(place)
        places.append(jnp.where(row == place, 1.0, 0.0).astype(BF))
    target[...] = jnp.concatenate(rows + [jnp.zeros((6, TOK), jnp.int32)], axis=0)
    cots = cot[...].astype(F32)
    scaled = [(columns(gates[k : k + 1, :]) * cots).astype(BF) for k in range(2)]
    toks = mm(places[0] + places[1], mix[...]).astype(BF)
    spread = mm(jnp.concatenate(places, axis=1), jnp.concatenate(scaled, axis=0)).astype(BF)
    for k in range(4):
        at = slice(k * TOK, (k + 1) * TOK)
        buf[:, 32 * k : 32 * k + CAP, :] = toks[:, at].reshape(EXP, CAP, TOK)
        buf[:, 32 * k + CAP : 32 * k + 32, :] = spread[:, at].reshape(EXP, CAP, TOK)


def prepare(slot, routes, gates, mixed, cotangent):
    whole = lambda i, q: (0, 0)
    part = lambda i, q: (0, quarter_of(q[0]))
    return pl.pallas_call(
        prepare_kernel,
        out_shape=(
            jax.ShapeDtypeStruct((EXP, 4 * EXP, TOK), BF),
            jax.ShapeDtypeStruct((8, TOK), jnp.int32),
        ),
        grid_spec=pltpu.PrefetchScalarGridSpec(
            num_scalar_prefetch=1,
            grid=(1,),
            in_specs=[
                pl.BlockSpec((2, TOK), whole),
                pl.BlockSpec((2, TOK), whole),
                pl.BlockSpec((TOK, WIDE), part),
                pl.BlockSpec((TOK, WIDE), part),
            ],
            out_specs=(
                pl.BlockSpec((EXP, 4 * EXP, TOK), lambda i, q: (0, 0, 0)),
                pl.BlockSpec((8, TOK), whole),
            ),
        ),
        compiler_params=pltpu.CompilerParams(vmem_limit_bytes=GRANT),
        name="prepare",
    )(slot, routes, gates, mixed, cotangent)


def row_blocks(chunk):
    toks, cots = [], []
    for k in range(4):
        toks.append(chunk[:, 32 * k : 32 * k + CAP, :].reshape(ROWS, TOK))
        cots.append(chunk[:, 32 * k + CAP : 32 * k + 32, :].reshape(ROWS, TOK))
    return jnp.concatenate(toks, axis=1), jnp.concatenate(cots, axis=1)


def gate_rows(own, other, at):
    return jnp.concatenate([own[0, :, at], other[0, :, at], own[1, :, at], other[1, :, at]], axis=0)


def expert_kernel(where, c0, c1, c2, c3, own, other, out, g_gate, g_up, g_hid):
    quarter, core = quarter_of(where[0]), where[0] & 1
    pre = jnp.zeros((ROWS, 4 * FF), F32)
    grad_hidden = jnp.zeros((ROWS, 2 * FF), F32)
    for k, chunk in enumerate((c0, c1, c2, c3)):
        at = pl.ds(pl.multiple_of((quarter ^ k) * WIDE, WIDE), WIDE)
        toks, cots = row_blocks(chunk)
        pre = pre + mm_nt(toks, gate_rows(own, other, at))
        grad_hidden = grad_hidden + mm_nt(cots, jnp.concatenate([own[2, :, at], other[2, :, at]], axis=0))
    pre_gate = pre[:, : 2 * FF]
    pre_up = pre[:, 2 * FF :]
    logistic = 1.0 / (1.0 + jnp.exp(-pre_gate))
    active = pre_gate * logistic
    slope = logistic * (1.0 + pre_gate * (1.0 - logistic))
    gate = (grad_hidden * pre_up * slope).astype(BF)
    up = (grad_hidden * active).astype(BF)
    g_gate[...] = gate
    g_up[...] = up
    g_hid[...] = (active * pre_up).astype(BF)
    grads = jnp.concatenate([gate, up], axis=1)
    for k in range(8):
        at = pl.ds(pl.multiple_of((2 * k + core) * TOK, TOK), TOK)
        part = mm(grads, gate_rows(own, other, at)).astype(BF)
        out[:, k * CAP : (k + 1) * CAP, :] = part.reshape(EXP, CAP, TOK)


def weights_kernel(where, c0, c1, c2, c3, g_gate, g_up, g_hid, d_gate, d_up, d_down):
    gates = jnp.concatenate([g_gate[...].T[:FF], g_up[...].T[:FF]], axis=0)
    hidden = g_hid[...].T[:FF]
    for k, chunk in enumerate((c0, c1, c2, c3)):
        at = pl.ds(pl.multiple_of((quarter_of(where[0]) ^ k) * WIDE, WIDE), WIDE)
        toks, cots = row_blocks(chunk)
        both = mm(gates, toks).astype(BF)
        d_gate[:, at] = both[:FF]
        d_up[:, at] = both[FF:]
        d_down[:, at] = mm(hidden, cots).astype(BF)


def combine_kernel(target, rows, out):
    lane = iota((TOK, ROWS), 1)
    places = target[...].T
    pick = jnp.where((lane == places[:, 0:1]) | (lane == places[:, 1:2]), 1.0, 0.0).astype(BF)
    for k in range(8):
        block = rows[:, k * CAP : (k + 1) * CAP, :].reshape(ROWS, TOK)
        out[k] = mm(pick, block).astype(BF)


def merge_kernel(where, pieces, cotangent, out, cot, arrived):
    at = pl.ds(pl.multiple_of(where[0] * TOK, TOK), TOK)
    copy = pltpu.make_async_copy(cotangent.at[:, at], cot, arrived)
    copy.start()
    total = pieces[0].astype(F32)
    for k in range(1, 8):
        total = total + pieces[k].astype(F32)
    copy.wait()
    out[...] = (cot[...].astype(F32) + total).astype(BF)


def merge(slot, pieces, cotangent):
    return pl.pallas_call(
        merge_kernel,
        out_shape=jax.ShapeDtypeStruct((TOK, TOK), BF),
        in_specs=[smem(), vmem(), pl.BlockSpec(memory_space=pltpu.HBM)],
        out_specs=vmem(),
        scratch_shapes=[pltpu.VMEM((TOK, TOK), BF), pltpu.SemaphoreType.DMA],
        compiler_params=pltpu.CompilerParams(vmem_limit_bytes=GRANT),
        name="merge",
    )(slot, pieces, cotangent)


def project_kernel(gathered, weight, gate_pre, mixer, logs, read, d_gate, grad_y, run, buf):
    whole = jnp.concatenate([gathered[k * TOK : (k + 1) * TOK, :] for k in range(16)], axis=1)
    back = mm_nt(whole, weight[...])
    pre = gate_pre[...].astype(F32)
    saved = mixer[...].astype(F32)
    logistic = 1.0 / (1.0 + jnp.exp(-pre))
    active = pre * logistic
    d_gate[...] = (back * saved * (logistic * (1.0 + pre * (1.0 - logistic)))).astype(BF)
    gated = (saved * active).astype(BF)
    for k in range(8):
        turned = whole[:, k * 256 : (k + 1) * 256].T
        part = mm(turned, gated).astype(BF)
        buf[4 * k : 4 * k + 4, 0:FF, :] = part[:, :TOK].reshape(4, FF, TOK)
        buf[4 * k : 4 * k + 4, FF : 2 * FF, :] = part[:, TOK:].reshape(4, FF, TOK)
    grad = back * active
    grad_y[...] = grad
    upto = jnp.where(iota((TOK, TOK), 0) <= iota((TOK, TOK), 1), 1.0, 0.0)
    rates = jnp.concatenate([logs[...], jnp.zeros((4, TOK), F32)], axis=0)
    running = mm(rates, upto, lax.Precision.HIGHEST)
    run[...] = running
    start = jnp.exp(running)
    turned = grad.T
    scale = jnp.concatenate([jnp.broadcast_to(start[j : j + 1], (HD, TOK)) for j in range(HEADS)], axis=0)
    high, low = two_parts(turned * scale)
    state = mm(high, read[...]) + mm(low, read[...])
    total = running[0:HEADS, TOK - 1 : TOK]
    first = total.astype(BF).astype(F32)
    second = (total - first).astype(BF).astype(F32)
    third = total - first - second
    line = iota((8, STATE), 0)
    notes = []
    for j in range(HEADS):
        note = jnp.where(line == 0, first[j : j + 1], jnp.where(line == 1, second[j : j + 1], third[j : j + 1]))
        note = jnp.where(line < 3, note, 0.0)
        notes.append(jnp.broadcast_to(note[None], (EXP // HEADS, 8, STATE)))
    sent = jnp.concatenate([state.reshape(EXP, 8, STATE), jnp.concatenate(notes, axis=0)], axis=1)
    buf[:, 2 * FF :, :] = sent.astype(BF)


def scan_kernel(received, out):
    state = jnp.zeros((8, STATE), F32)
    for k in reversed(range(EXP)):
        high, low = two_parts(state)
        out[k] = jnp.concatenate([high.astype(F32), low.astype(F32)], axis=0).astype(BF)
        if k > 0:
            piece = received[k, 2 * FF :, :].astype(F32)
            log = piece[8:9] + piece[9:10] + piece[10:11]
            state = jnp.exp(log) * state + piece[0:8]


def share_kernel(received, d_out):
    total = received[0, 0 : 2 * FF, :].astype(F32)
    for k in range(1, EXP):
        total = total + received[k, 0 : 2 * FF, :].astype(F32)
    d_out[:, :TOK] = total[:FF]
    d_out[:, TOK:] = total[FF:]


def inner_kernel(grad_y, values, write, read, run, entry, dx, dw, dr):
    running = run[...]
    cols = running.T
    grads = grad_y[...]
    vals = values[...]
    cross = mm_nt(write[...], read[...])
    later = iota((TOK, TOK), 1) >= iota((TOK, TOK), 0)
    total = jnp.zeros((TOK, TOK), F32)
    parts = []
    starts = []
    for j in range(HEADS):
        spread = running[j : j + 1] - cols[:, j : j + 1]
        decay = jnp.where(later, jnp.exp(jnp.where(later, spread, 0.0)), 0.0)
        grad = grads[:, j * HD : (j + 1) * HD]
        halves = two_parts(grad)
        parts.append(mm_parts(two_parts(cross * decay), halves, mm))
        total = total + mm_parts((vals[:, j * HD : (j + 1) * HD],), halves, mm_nt) * decay
        starts.append(grad * jnp.exp(cols[:, j : j + 1]))
    dx[...] = jnp.concatenate(parts, axis=1)
    dw[...] = mm_parts(two_parts(total), (read[...],), mm)
    entry_rows = two_parts(entry[...].reshape(HEADS * HD, STATE))
    first = mm_parts(two_parts(total.T), (write[...],), mm)
    dr[...] = first + mm_parts(two_parts(jnp.concatenate(starts, axis=1)), entry_rows, mm)


def outer_kernel(dx, dw, values, write, run, second, d_values, d_write):
    running = run[...]
    ends = jnp.exp(running[:, TOK - 1 : TOK] - running).T
    scale = jnp.concatenate([jnp.broadcast_to(ends[:, j : j + 1], (TOK, HD)) for j in range(HEADS)], axis=1)
    later = second[...].astype(F32)
    high = later[:, 0:8].reshape(HEADS * HD, STATE).astype(BF)
    low = later[:, 8:16].reshape(HEADS * HD, STATE).astype(BF)
    d_values[...] = (dx[...] + scale * (mm_nt(write[...], high) + mm_nt(write[...], low))).astype(BF)
    top, rest = two_parts(values[...].astype(F32) * scale)
    d_write[...] = dw[...] + mm(top, high) + mm(top, low) + mm(rest, high)


def step(mixed, cotangent, routes, gates, w_gate, w_up, w_down, out_weight, gate_pre, mixer_out, values,
         write_keys, read_keys, log_decay, entry_states):
    shape = jax.ShapeDtypeStruct
    swap = [(0, 1), (1, 0)]
    ring = []
    for k in range(8):
        ring.append((2 * k, 2 * ((k + 1) % 8)))
        ring.append((2 * k + 1, 2 * ((k - 1) % 8) + 1))
    slot = lax.axis_index(TP).astype(jnp.int32).reshape(1)
    own = jnp.stack([w_gate[0].T, w_up[0].T, w_down[0]])
    other = lax.ppermute(own, "core", swap)
    buf, target = prepare(slot, routes.T, gates.T, mixed, cotangent)
    c0 = lax.all_to_all(buf, SP, 0, 0, tiled=True)
    c2 = lax.ppermute(c0, TP, ring)
    c1 = lax.ppermute(c0, "core", swap)
    moved, other = lax.optimization_barrier((c2, other))
    c3 = lax.ppermute(moved, "core", swap)
    chunks = (c0, c1, c2, c3)
    grad = shape((ROWS, 2 * FF), BF)
    parts, g_gate, g_up, g_hid = call(
        expert_kernel, (shape((EXP, TOK, TOK), BF), grad, grad, grad),
        [smem()] + [vmem()] * 6, (slot, *chunks, own, other))
    back = lax.all_to_all(parts, SP, 0, 0, tiled=True)
    wide = shape((FF, D), BF)
    d_wg, d_wu, d_wd = call(
        weights_kernel, (wide, wide, wide),
        [smem()] + [vmem()] * 7, (slot, *chunks, g_gate, g_up, g_hid), flops=10**9)
    back, d_wg, d_wu, d_wd = lax.optimization_barrier((back, d_wg, d_wu, d_wd))
    summed = call(combine_kernel, shape((8, TOK, TOK), BF), [vmem()] * 2, (target, back))
    pieces = lax.all_to_all(summed, "y", 0, 0, tiled=True)
    d_input = merge(slot, pieces, cotangent)
    whole = lax.all_gather(d_input, TP, axis=0, tiled=True)
    flat = shape((TOK, HEADS * HD), BF)
    d_gate, grad_y, run, sent = call(
        project_kernel,
        (flat, shape((TOK, HEADS * HD), F32), shape((8, TOK), F32), shape((EXP, 2 * FF + 16, STATE), BF)),
        [vmem()] * 6, (whole, out_weight, gate_pre, mixer_out, log_decay, read_keys))
    square = shape((TOK, STATE), F32)
    dx, dw, d_read = call(
        inner_kernel, (shape((TOK, HEADS * HD), F32), square, square),
        [vmem()] * 6, (grad_y, values, write_keys, read_keys, run, entry_states[0]), flops=10**9)
    received = lax.all_to_all(sent, SP, 0, 0, tiled=True)
    received, dx, dw, d_read = lax.optimization_barrier((received, dx, dw, d_read))
    states = call(scan_kernel, shape((EXP, 16, STATE), BF), [vmem()], (received,))
    second = lax.all_to_all(states, SP, 0, 0, tiled=True)
    d_out_weight = call(share_kernel, shape((D // EXP, HEADS * HD), F32), [vmem()], (received,), flops=10**9)
    second, d_out_weight = lax.optimization_barrier((second, d_out_weight))
    d_values, d_write = call(
        outer_kernel, (flat, square), [vmem()] * 6,
        (dx, dw, values, write_keys, run, second))
    return (d_wg.T[None], d_wu.T[None], d_wd[None], d_out_weight, d_input, d_values, d_write, d_read, d_gate)


def solution(mesh):
    finer = Mesh(mesh.devices.reshape(8, 4, 8, 2), ("z", "x", "y", "core"))
    return jax.shard_map(
        step,
        mesh=finer,
        in_specs=(
            P(SP, None),
            P(SP, None),
            P(SP, None),
            P(SP, None),
            P(SP, None, TP),
            P(SP, None, TP),
            P(SP, TP, None),
            P(TP, None),
            P(SP, TP),
            P(SP, TP),
            P(SP, TP),
            P(SP, TP),
            P(SP, TP),
            P(TP, SP),
            P(SP, TP, None, None),
        ),
        out_specs=(
            P(SP, None, TP),
            P(SP, None, TP),
            P(SP, TP, None),
            P(SP, TP),
            P(SP, TP),
            P(SP, TP),
            P(SP, TP),
            P(SP, TP),
            P(SP, TP),
        ),
        check_vma=False,
    )
```

time: 212 us -> 199 us (0.939)
  blocking collectives: 109 us -> 76.1 us
  waiting for transfers between devices: 50.6 us -> 75.2 us
  other arithmetic: 3.5 us -> 0.09 us
  Pallas kernels: 14 us -> 11.6 us
  local copies, waits for them, and re-layouts: 4.73 us -> 6.93 us
    all_to_all x3 -> x2, blocking collectives: 91.9 us -> 58.9 us  [the longest x1 41.2 us: step(): c0 = lax.all_to_all(buf, SP, 0, 0, tiled=True)]
    all_to_all x3, waiting for transfers between devices: 37.4 us -> 63.9 us  [the longest x1 29.8 us: step(): received = lax.all_to_all(sent, SP, 0, 0, tiled=True)]
    unnamed x36 -> x42, local copies, waits for them, and re-layouts: 4.73 us -> 6.93 us
    pallas_call x7 -> x8, Pallas kernels: 10.7 us -> 10.3 us  [call(): pl.pallas_call(kernel, out_shape=outs, in_specs=specs, out_specs=jax.tree...]
  transfers between devices with their start and end apart: 7 -> 7, of which waited for: 5 -> 5; matrix products, arithmetic and copies ran while one was open for 1% -> 0% of each run, Pallas kernels for 2% -> 2%
where the time goes in v6:
time: 199 us; the launch traced here: 198 us
  blocking collectives  76.1 us (38%)
  waiting for transfers between devices  75.2 us (38%)
  starting transfers between devices  27.1 us (14%)
  Pallas kernels  11.6 us (6%)
  local copies, waits for them, and re-layouts  6.93 us (3%)
    all_to_all x1, blocking collectives, step(): c0 = lax.all_to_all(buf, SP, 0, 0, tiled=True)  41.2 us
    all_to_all x1, waiting for transfers between devices, step(): received = lax.all_to_all(sent, SP, 0, 0, tiled=True)  29.8 us
    all_to_all x1, waiting for transfers between devices, step(): back = lax.all_to_all(parts, SP, 0, 0, tiled=True)  24.2 us
    all_to_all x1, blocking collectives, step(): pieces = lax.all_to_all(summed, 'y', 0, 0, tiled=True)  17.7 us
    all_gather x1, blocking collectives, step(): whole = lax.all_gather(d_input, TP, axis=0, tiled=True)  17.2 us
    pallas_call x8, Pallas kernels, call(): pl.pallas_call(kernel, out_shape=outs, in_specs=specs, out_specs=jax.tree...  10.3 us
    all_to_all x1, waiting for transfers between devices, step(): second = lax.all_to_all(states, SP, 0, 0, tiled=True)  9.85 us
    ppermute x1, waiting for transfers between devices, step(): c2 = lax.ppermute(c0, TP, ring)  8.71 us
  transfers between devices with their start and end apart: 7, of which 5 were waited for; matrix products, arithmetic and copies ran while one was open for 0% of the time, Pallas kernels for 2%

profile of v6, /device:TPU:8, one launch (start us, length us, event | category | flops | bytes accessed | tf_op | source)
XLA Modules:
  0.0 198.0 jit_solution(2018922047468283220)
XLA Ops:
  0.7 1.0 copy-done.4
  1.7 1.0 copy-done.8
  2.7 0.7 copy-done.15
  3.4 0.7 copy-done.16
  4.1 0.6 prepare.1
  4.8 41.2 %all_to_all.25.c0 = bf16[32,128,128]{2,1,0:T(8,128)(2,1)S(1)} all-to-all(bf16[32,128,128]{2,1,0:T(8,128)(2,1)S(1)} %get-tuple-element.39), channel_id=1, replica_groups=mesh['z'=8,'x'=4,'y'=8,'core'=2] {'z','x'}, dimensions={0} | all-to-all | bytes 2097152 | tf_op jit(solution)/shard_map/all_to_all | solution.py:322
  45.9 3.5 %collective-permute-start.1 = (bf16[32,128,128]{2,1,0:T(8,128)(2,1)S(1)}, bf16[32,128,128]{2,1,0:T(8,128)(2,1)S(1)}, u32[]{:S(2)}, u32[]{:S(2)}) collective-permute-start(bf16[32,128,128]{2,1,0:T(8,128)(2,1)S(1)} %all_to_all.25.c0), channel_id=1, source_target_pairs={{0,2},{1,15},{2,4},{3,1},{4,6},{5,3},{6,8},{7,5},{8,10},{9,7},{10,... | collective-permute-start | bytes 3145736 | tf_op jit(solution)/shard_map/ppermute | solution.py:323
  49.6 1.9 collective-permute-start.2
  51.5 2.4 %collective-permute-start = (bf16[32,128,128]{2,1,0:T(8,128)(2,1)S(1)}, bf16[32,128,128]{2,1,0:T(8,128)(2,1)S(1)}, u32[]{:S(2)}, u32[]{:S(2)}) collective-permute-start(bf16[32,128,128]{2,1,0:T(8,128)(2,1)S(1)} %all_to_all.25.c0), channel_id=1, source_target_pairs={{0,1},{1,0},{2,3},{3,2},{4,5},{5,4},{6,7},{7,6},{8,9},{9,8},{10,11... | collective-permute-start | bytes 3145736 | tf_op jit(solution)/shard_map/ppermute | solution.py:324
  53.9 8.7 %collective-permute-done.1.c2 = bf16[32,128,128]{2,1,0:T(8,128)(2,1)S(1)} collective-permute-done((bf16[32,128,128]{2,1,0:T(8,128)(2,1)S(1)}, bf16[32,128,128]{2,1,0:T(8,128)(2,1)S(1)}, u32[]{:S(2)}, u32[]{:S(2)}) %collective-permute-start.1) | collective-permute-done | bytes 1048608 | tf_op jit(solution)/shard_map/ppermute | solution.py:323
  62.6 1.9 collective-permute-start.3
  64.6 2.6 %collective-permute-done.3.c3 = bf16[32,128,128]{2,1,0:T(8,128)(2,1)S(1)} collective-permute-done((bf16[32,128,128]{2,1,0:T(8,128)(2,1)S(1)}, bf16[32,128,128]{2,1,0:T(8,128)(2,1)S(1)}, u32[]{:S(2)}, u32[]{:S(2)}) %collective-permute-start.3) | collective-permute-done | bytes 1048608 | tf_op jit(solution)/shard_map/ppermute | solution.py:326
  67.2 1.9 shard_map.214
  69.0 1.0 copy-done.7
  70.0 5.6 %all-to-all-start.1 = ((bf16[32,128,128]{2,1,0:T(8,128)(2,1)}), bf16[32,128,128]{2,1,0:T(8,128)(2,1)S(1)}, u32[]{:S(2)}, u32[]{:S(2)}) async-start(bf16[32,128,128]{2,1,0:T(8,128)(2,1)} %copy-done.7), calls=%async_computation.1 | async-start | bytes 2097152 | tf_op jit(solution)/shard_map/all_to_all | solution.py:332
  75.6 1.2 copy-done.1
  76.8 1.2 copy-done.3
  78.1 1.7 shard_map.215
  79.7 24.2 %all-to-all-done.1.rows = bf16[32,128,128]{2,1,0:T(8,128)(2,1)S(1)} async-done(((bf16[32,128,128]{2,1,0:T(8,128)(2,1)}), bf16[32,128,128]{2,1,0:T(8,128)(2,1)S(1)}, u32[]{:S(2)}, u32[]{:S(2)}) %all-to-all-start.1) | async-done | bytes 1048608 | tf_op jit(solution)/shard_map/all_to_all | solution.py:332
  104.0 0.6 shard_map.216
  104.6 17.7 %all_to_all.26.pieces = bf16[8,128,128]{2,1,0:T(8,128)(2,1)S(1)} all-to-all(bf16[8,128,128]{2,1,0:T(8,128)(2,1)S(1)} %shard_map.216), channel_id=1, replica_groups=mesh['z'=8,'x'=4,'y'=8,'core'=2] {'y'}, dimensions={0} | all-to-all | bytes 524288 | tf_op jit(solution)/shard_map/all_to_all | solution.py:339
  122.3 0.7 merge.1
  123.0 17.2 %all_gather.3.gathered = bf16[2048,128]{1,0:T(8,128)(2,1)S(1)} all-gather(bf16[128,128]{1,0:T(8,128)(2,1)} %merge.1), channel_id=1, replica_groups=mesh['z'=8,'x'=4,'y'=8,'core'=2] {'y','core'}, dimensions={0}, use_global_device_ids=true | all-gather | bytes 557056 | tf_op jit(solution)/shard_map/all_gather | solution.py:341
  140.2 2.1 %shard_map.217 = (bf16[128,256]{1,0:T(8,128)(2,1)}, f32[128,256]{1,0:T(8,128)S(1)}, f32[8,128]{1,0:T(8,128)S(1)}, bf16[32,144,128]{2,1,0:T(8,128)(2,1)}) custom-call(bf16[2048,128]{1,0:T(8,128)(2,1)S(1)} %all_gather.3.gathered, bf16[256,2048]{1,0:T(8,128)(2,1)S(1)} %copy-done.6, bf16[128,256]{1,0:T(8,128)(2,1)S(1)} %copy-done.10, ...), custom_call_target="tpu_custom_call" | custom-call | tf_op jit(solution)/shard_map/pallas_call | solution.py:70
  142.3 6.1 %all-to-all-start.3 = ((bf16[32,144,128]{2,1,0:T(8,128)(2,1)}), bf16[32,144,128]{2,1,0:T(8,128)(2,1)S(1)}, u32[]{:S(2)}, u32[]{:S(2)}) async-start(bf16[32,144,128]{2,1,0:T(8,128)(2,1)} %get-tuple-element.54), calls=%async_computation.3 | async-start | bytes 2359296 | tf_op jit(solution)/shard_map/all_to_all | solution.py:351
  148.5 1.5 shard_map.218
  150.0 29.8 %all-to-all-done.3.received = bf16[32,144,128]{2,1,0:T(8,128)(2,1)S(1)} async-done(((bf16[32,144,128]{2,1,0:T(8,128)(2,1)}), bf16[32,144,128]{2,1,0:T(8,128)(2,1)S(1)}, u32[]{:S(2)}, u32[]{:S(2)}) %all-to-all-start.3) | async-done | bytes 1179680 | tf_op jit(solution)/shard_map/all_to_all | solution.py:351
  179.8 0.7 shard_map.219
  180.5 5.6 %all-to-all-start.4 = ((bf16[32,16,128]{2,1,0:T(8,128)(2,1)}), bf16[32,16,128]{2,1,0:T(8,128)(2,1)S(1)}, u32[]{:S(2)}, u32[]{:S(2)}) async-start(bf16[32,16,128]{2,1,0:T(8,128)(2,1)} %shard_map.219), calls=%async_computation.4 | async-start | bytes 262144 | tf_op jit(solution)/shard_map/all_to_all | solution.py:354
  186.2 0.8 shard_map.220
  187.0 9.8 %all-to-all-done.4.second = bf16[32,16,128]{2,1,0:T(8,128)(2,1)S(1)} async-done(((bf16[32,16,128]{2,1,0:T(8,128)(2,1)}), bf16[32,16,128]{2,1,0:T(8,128)(2,1)S(1)}, u32[]{:S(2)}, u32[]{:S(2)}) %all-to-all-start.4) | async-done | bytes 131104 | tf_op jit(solution)/shard_map/all_to_all | solution.py:354
  196.8 1.2 shard_map.221
  (38 shorter events, 0.2 us)
Async XLA Ops:
  0.6 1.0 copy-start.4
  1.7 1.0 copy-start.8
  2.7 0.7 copy-start.15
  3.4 0.7 copy-start.16
  4.7 44.7 %copy-start.18 = (bf16[1,64,2048]{2,1,0:T(8,128)(2,1)S(1)}, bf16[1,64,2048]{2,1,0:T(8,128)(2,1)}, u32[]{:S(2)}) copy-start(bf16[1,64,2048]{2,1,0:T(8,128)(2,1)} %param.21) | copy-start | bytes 786436
  4.7 44.7 %copy-start.19 = (bf16[1,2048,64]{1,2,0:T(8,128)(2,1)S(1)}, bf16[1,2048,64]{1,2,0:T(8,128)(2,1)}, u32[]{:S(2)}) copy-start(bf16[1,2048,64]{1,2,0:T(8,128)(2,1)} %param.20) | copy-start | bytes 786436
  4.8 44.7 %copy-start.20 = (bf16[1,2048,64]{1,2,0:T(8,128)(2,1)S(1)}, bf16[1,2048,64]{1,2,0:T(8,128)(2,1)}, u32[]{:S(2)}) copy-start(bf16[1,2048,64]{1,2,0:T(8,128)(2,1)} %param.19) | copy-start | bytes 786436
  45.9 16.7 %collective-permute-start.1 = (bf16[32,128,128]{2,1,0:T(8,128)(2,1)S(1)}, bf16[32,128,128]{2,1,0:T(8,128)(2,1)S(1)}, u32[]{:S(2)}, u32[]{:S(2)}) collective-permute-start(bf16[32,128,128]{2,1,0:T(8,128)(2,1)S(1)} %all_to_all.25.c0), channel_id=1, source_target_pairs={{0,2},{1,15},{2,4},{3,1},{4,6},{5,3},{6,8},{7,5},{8,10},{9,7},{10,... | collective-permute-start | bytes 3145736 | tf_op jit(solution)/shard_map/ppermute | solution.py:323
  49.6 4.3 %collective-permute-start.2 = (bf16[3,64,2048]{2,1,0:T(8,128)(2,1)S(1)}, bf16[3,64,2048]{2,1,0:T(8,128)(2,1)S(1)}, u32[]{:S(2)}, u32[]{:S(2)}) collective-permute-start(bf16[3,64,2048]{2,1,0:T(8,128)(2,1)S(1)} %pad_maximum_fusion.own), channel_id=1, source_target_pairs={{0,1},{1,0},{2,3},{3,2},{4,5},{5,4},{6,7},{7,6},{8,9},{9,8},{10,11... | collective-permute-start | bytes 2359304 | tf_op jit(solution)/shard_map/ppermute | solution.py:320
  51.5 13.1 %collective-permute-start = (bf16[32,128,128]{2,1,0:T(8,128)(2,1)S(1)}, bf16[32,128,128]{2,1,0:T(8,128)(2,1)S(1)}, u32[]{:S(2)}, u32[]{:S(2)}) collective-permute-start(bf16[32,128,128]{2,1,0:T(8,128)(2,1)S(1)} %all_to_all.25.c0), channel_id=1, source_target_pairs={{0,1},{1,0},{2,3},{3,2},{4,5},{5,4},{6,7},{7,6},{8,9},{9,8},{10,11... | collective-permute-start | bytes 3145736 | tf_op jit(solution)/shard_map/ppermute | solution.py:324
  62.6 4.5 %collective-permute-start.3 = (bf16[32,128,128]{2,1,0:T(8,128)(2,1)S(1)}, bf16[32,128,128]{2,1,0:T(8,128)(2,1)S(1)}, u32[]{:S(2)}, u32[]{:S(2)}) collective-permute-start(bf16[32,128,128]{2,1,0:T(8,128)(2,1)S(1)} %collective-permute-done.1.c2), channel_id=1, source_target_pairs={{0,1},{1,0},{2,3},{3,2},{4,5},{5,4},{6,7},{7,6},{8,9},{9,8},{10,11... | collective-permute-start | bytes 3145736 | tf_op jit(solution)/shard_map/ppermute | solution.py:326
  64.5 4.5 %copy-start = (bf16[32,128,128]{2,1,0:T(8,128)(2,1)}, bf16[32,128,128]{2,1,0:T(8,128)(2,1)S(1)}, u32[]{:S(2)}) copy-start(bf16[32,128,128]{2,1,0:T(8,128)(2,1)S(1)} %collective-permute-done.c1) | copy-start | bytes 3145732
  67.2 1.9 copy-start.2
  69.0 1.0 copy-start.7
  70.0 33.9 %all-to-all-start.1 = ((bf16[32,128,128]{2,1,0:T(8,128)(2,1)}), bf16[32,128,128]{2,1,0:T(8,128)(2,1)S(1)}, u32[]{:S(2)}, u32[]{:S(2)}) async-start(bf16[32,128,128]{2,1,0:T(8,128)(2,1)} %copy-done.7), calls=%async_computation.1 | async-start | bytes 2097152 | tf_op jit(solution)/shard_map/all_to_all | solution.py:332
  75.6 1.2 copy-start.1
  76.8 1.2 copy-start.3
  79.7 42.6 %copy-start.5 = (bf16[128,2048]{1,0:T(8,128)(2,1)S(1)}, bf16[128,2048]{1,0:T(8,128)(2,1)}, u32[]{:S(2)}) copy-start(bf16[128,2048]{1,0:T(8,128)(2,1)} %cotangent.1) | copy-start | bytes 1572868
  104.5 35.7 %copy-start.6 = (bf16[256,2048]{1,0:T(8,128)(2,1)S(1)}, bf16[256,2048]{1,0:T(8,128)(2,1)}, u32[]{:S(2)}) copy-start(bf16[256,2048]{1,0:T(8,128)(2,1)} %weight.1) | copy-start | bytes 3145732
  104.6 35.7 %copy-start.10 = (bf16[128,256]{1,0:T(8,128)(2,1)S(1)}, bf16[128,256]{1,0:T(8,128)(2,1)}, u32[]{:S(2)}) copy-start(bf16[128,256]{1,0:T(8,128)(2,1)} %gate_pre.1) | copy-start | bytes 196612
  104.6 35.7 %copy-start.11 = (bf16[128,256]{1,0:T(8,128)(2,1)S(1)}, bf16[128,256]{1,0:T(8,128)(2,1)}, u32[]{:S(2)}) copy-start(bf16[128,256]{1,0:T(8,128)(2,1)} %mixer.1) | copy-start | bytes 196612
  104.6 35.6 %copy-start.12 = (bf16[128,128]{1,0:T(8,128)(2,1)S(1)}, bf16[128,128]{1,0:T(8,128)(2,1)}, u32[]{:S(2)}) copy-start(bf16[128,128]{1,0:T(8,128)(2,1)} %read.3) | copy-start | bytes 98308
  104.6 35.6 %copy-start.14 = (f32[4,128]{1,0:T(4,128)S(1)}, f32[4,128]{1,0:T(4,128)}, u32[]{:S(2)}) copy-start(f32[4,128]{1,0:T(4,128)} %logs.1) | copy-start | bytes 6148
  142.3 6.2 %copy-start.9 = (bf16[128,256]{1,0:T(8,128)(2,1)S(1)}, bf16[128,256]{1,0:T(8,128)(2,1)}, u32[]{:S(2)}) copy-start(bf16[128,256]{1,0:T(8,128)(2,1)} %values.3) | copy-start | bytes 196612
  142.3 6.2 %copy-start.13 = (bf16[128,128]{1,0:T(8,128)(2,1)S(1)}, bf16[128,128]{1,0:T(8,128)(2,1)}, u32[]{:S(2)}) copy-start(bf16[128,128]{1,0:T(8,128)(2,1)} %write.3) | copy-start | bytes 98308
  142.3 6.2 %copy-start.17 = (f32[1,4,64,128]{3,2,1,0:T(8,128)S(1)}, f32[1,4,64,128]{3,2,1,0:T(8,128)}, u32[]{:S(2)}) copy-start(f32[1,4,64,128]{3,2,1,0:T(8,128)} %param.29) | copy-start | bytes 393220
  142.3 37.5 %all-to-all-start.3 = ((bf16[32,144,128]{2,1,0:T(8,128)(2,1)}), bf16[32,144,128]{2,1,0:T(8,128)(2,1)S(1)}, u32[]{:S(2)}, u32[]{:S(2)}) async-start(bf16[32,144,128]{2,1,0:T(8,128)(2,1)} %get-tuple-element.54), calls=%async_computation.3 | async-start | bytes 2359296 | tf_op jit(solution)/shard_map/all_to_all | solution.py:351
  180.5 16.3 %all-to-all-start.4 = ((bf16[32,16,128]{2,1,0:T(8,128)(2,1)}), bf16[32,16,128]{2,1,0:T(8,128)(2,1)S(1)}, u32[]{:S(2)}, u32[]{:S(2)}) async-start(bf16[32,16,128]{2,1,0:T(8,128)(2,1)} %shard_map.219), calls=%async_computation.4 | async-start | bytes 262144 | tf_op jit(solution)/shard_map/all_to_all | solution.py:354

commit v7 on v5

--- a/solution.py
+++ b/solution.py
@@ -16,6 +16,7 @@
 HEADS = 4
 HD = 64
 STATE = 128
+PLAN = ((1, True), (1, False), (3, True), (3, False), (4, True), (2, True), (2, False), (0, True))
 SP = ("z", "x")
 TP = ("y", "core")
 GRANT = 16 * 1024 * 1024
@@ -82,14 +83,7 @@
     )(*args)
 
 
-def prepare_kernel(where, routes, gates, mixed, cotangent, buf, target, mix, cot, arrived):
-    at = pl.ds(pl.multiple_of(lax.rem(where[0], 8) * WIDE, WIDE), WIDE)
-    copies = [
-        pltpu.make_async_copy(mixed.at[:, at], mix, arrived.at[0]),
-        pltpu.make_async_copy(cotangent.at[:, at], cot, arrived.at[1]),
-    ]
-    for copy in copies:
-        copy.start()
+def prepare_kernel(where, routes, gates, mix, cot, buf, target):
     picks = routes[...]
     expert = iota((EXP, TOK), 0)
     hits = [expert == picks[k : k + 1] for k in range(2)]
@@ -97,41 +91,46 @@
     before = jnp.where(iota((TOK, TOK), 0) < iota((TOK, TOK), 1), 1.0, 0.0).astype(BF)
     count = mm(both, before)
     row = iota((ROWS, TOK), 0)
-    places, rows = [], []
+    cots = cot[...].astype(F32)
+    places, scaled, rows = [], [], []
     for k in range(2):
         slot = jnp.sum(jnp.where(hits[k], count, 0.0), axis=0, keepdims=True)
         place = picks[k : k + 1] * CAP + slot.astype(jnp.int32)
         rows.append(place)
         places.append(jnp.where(row == place, 1.0, 0.0).astype(BF))
+        scaled.append((columns(gates[k : k + 1, :]) * cots).astype(BF))
     target[...] = jnp.concatenate(rows + [jnp.zeros((6, TOK), jnp.int32)], axis=0)
-    for copy in copies:
-        copy.wait()
-    cots = cot[...].astype(F32)
-    scaled = [(columns(gates[k : k + 1, :]) * cots).astype(BF) for k in range(2)]
     toks = mm(places[0] + places[1], mix[...]).astype(BF)
     buf[:, 0:CAP, :] = toks.reshape(EXP, CAP, WIDE)
     spread = mm(jnp.concatenate(places, axis=1), jnp.concatenate(scaled, axis=0)).astype(BF)
     buf[:, CAP : 2 * CAP, :] = spread.reshape(EXP, CAP, WIDE)
 
 
-def prepare(slot, routes, gates, mixed, cotangent):
-    hbm = pl.BlockSpec(memory_space=pltpu.HBM)
+def prepare(quarter, routes, gates, mixed, cotangent):
+    whole = lambda i, q: (0, 0)
+    part = lambda i, q: (0, lax.rem(q[0], 8))
     return pl.pallas_call(
         prepare_kernel,
         out_shape=(
             jax.ShapeDtypeStruct((EXP, 2 * CAP, WIDE), BF),
             jax.ShapeDtypeStruct((8, TOK), jnp.int32),
         ),
-        in_specs=[smem(), vmem(), vmem(), hbm, hbm],
-        out_specs=(vmem(), vmem()),
-        scratch_shapes=[
-            pltpu.VMEM((TOK, WIDE), BF),
-            pltpu.VMEM((TOK, WIDE), BF),
-            pltpu.SemaphoreType.DMA((2,)),
-        ],
-        compiler_params=pltpu.CompilerParams(vmem_limit_bytes=GRANT),
+        grid_spec=pltpu.PrefetchScalarGridSpec(
+            num_scalar_prefetch=1,
+            grid=(1,),
+            in_specs=[
+                pl.BlockSpec((2, TOK), whole),
+                pl.BlockSpec((2, TOK), whole),
+                pl.BlockSpec((TOK, WIDE), part),
+                pl.BlockSpec((TOK, WIDE), part),
+            ],
+            out_specs=(
+                pl.BlockSpec((EXP, 2 * CAP, WIDE), lambda i, q: (0, 0, 0)),
+                pl.BlockSpec((8, TOK), whole),
+            ),
+        ),
         name="prepare",
-    )(slot, routes, gates, mixed, cotangent)
+    )(quarter, routes, gates, mixed, cotangent)
 
 
 def row_blocks(chunk):
@@ -146,7 +145,9 @@
 
 def expert_kernel(where, *refs):
     chunks = refs[:8]
-    own, other, near, mid, far, last, home, g_gate, g_up, g_hid = refs[8:]
+    own, other = refs[8:10]
+    outs = refs[10:18]
+    g_gate, g_up, g_hid = refs[18:]
     ids = chunk_ids(where[0])
     pre = jnp.zeros((ROWS, 4 * FF), F32)
     grad_hidden = jnp.zeros((ROWS, 2 * FF), F32)
@@ -168,11 +169,10 @@
     grads = jnp.concatenate([gate, up], axis=1)
     y, core = where[0] >> 1, where[0] & 1
     step = 1 - 2 * core
-    for k, out in ((4, last), (3, far), (2, mid), (1, near), (0, home)):
+    for out, (k, same) in zip(outs, PLAN):
         chip = (y + step * k + 8) & 7
-        start = chip * WIDE if k in (1, 2, 3) else chip * WIDE + core * TOK
-        size = out.shape[1]
-        at = pl.ds(pl.multiple_of(start, TOK), size)
+        side = core if same else 1 - core
+        at = pl.ds(pl.multiple_of((2 * chip + side) * TOK, TOK), TOK)
         out[...] = mm(grads, gate_rows(own, other, at)).astype(BF)
 
 
@@ -191,13 +191,11 @@
         d_down[:, at] = mm(hidden, cots).astype(BF)
 
 
-def fold_kernel(where, near, mid, far, last, home, keep, give):
-    total = near[...].astype(F32) + mid[...].astype(F32) + far[...].astype(F32)
-    first = total[:, :TOK]
-    second = total[:, TOK:]
-    top = where[0] & 1 == 0
-    keep[...] = jnp.where(top, first, second) + last[...].astype(F32) + home[...].astype(F32)
-    give[...] = jnp.where(top, second, first).astype(BF)
+def fold_kernel(*refs):
+    total = refs[0][...].astype(F32)
+    for part in refs[1:8]:
+        total = total + part[...].astype(F32)
+    refs[8][...] = total.astype(BF).reshape(EXP, CAP, TOK)
 
 
 def combine_kernel(where, target, rows, cotangent, out, cot, arrived):
@@ -224,8 +222,9 @@
     )(slot, target, rows, cotangent)
 
 
-def project_kernel(whole, weight, gate_pre, mixer, logs, read, d_gate, grad_y, run, buf, rest):
-    back = mm_nt(whole[...], weight[...])
+def project_kernel(gathered, weight, gate_pre, mixer, logs, read, d_gate, grad_y, run, buf, rest):
+    whole = jnp.concatenate([gathered[k * TOK : (k + 1) * TOK, :] for k in range(16)], axis=1)
+    back = mm_nt(whole, weight[...])
     pre = gate_pre[...].astype(F32)
     saved = mixer[...].astype(F32)
     logistic = 1.0 / (1.0 + jnp.exp(-pre))
@@ -321,11 +320,14 @@
          write_keys, read_keys, log_decay, entry_states):
     shape = jax.ShapeDtypeStruct
     swap = [(0, 1), (1, 0)]
-    rings = []
-    for k in range(1, 5):
-        up = [(2 * y, 2 * ((y + k) % 8)) for y in range(8)]
-        rings.append(up + [(2 * y + 1, 2 * ((y - k) % 8) + 1) for y in range(8)])
-    ring = rings[0]
+    def route(k, same):
+        pairs = []
+        for y in range(8):
+            pairs.append((2 * y, 2 * ((y + k) % 8) + (0 if same else 1)))
+            pairs.append((2 * y + 1, 2 * ((y - k) % 8) + (1 if same else 0)))
+        return pairs
+
+    ring = route(1, True)
     slot = lax.axis_index(TP).astype(jnp.int32).reshape(1)
     own = jnp.stack([w_gate[0].T, w_up[0].T, w_down[0]])
     other = lax.ppermute(own, "core", swap)
@@ -341,26 +343,22 @@
     c7 = lax.ppermute(c4, "core", swap)
     chunks = (c0, c1, c2, c3, c4, c5, c6, c7)
     grad = shape((ROWS, 2 * FF), BF)
-    full, thin = shape((ROWS, WIDE), BF), shape((ROWS, TOK), BF)
-    *parts, home, g_gate, g_up, g_hid = call(
-        expert_kernel, (full, full, full, thin, thin, grad, grad, grad),
+    thin = shape((ROWS, TOK), BF)
+    *parts, g_gate, g_up, g_hid = call(
+        expert_kernel, (thin,) * 8 + (grad, grad, grad),
         [smem()] + [vmem()] * 10, (slot, *chunks, own, other))
     pieces = []
-    for k in range(4):
-        pieces.append(lax.ppermute(parts[k], TP, rings[k]))
+    for k, (far, same) in enumerate(PLAN[:7]):
+        pieces.append(lax.ppermute(parts[k], TP, route(far, same)))
     wide = shape((FF, D), BF)
     d_wg, d_wu, d_wd = call(
         weights_kernel, (wide, wide, wide),
         [smem()] + [vmem()] * 11, (slot, *chunks, g_gate, g_up, g_hid), flops=10**9)
     pieces, d_wg, d_wu, d_wd = lax.optimization_barrier((pieces, d_wg, d_wu, d_wd))
-    keep, give = call(
-        fold_kernel, (shape((ROWS, TOK), F32), thin),
-        [smem()] + [vmem()] * 5, (slot, *pieces, home))
-    taken = lax.ppermute(give, "core", swap)
-    summed = (keep + taken.astype(F32)).astype(BF).reshape(EXP, CAP, TOK)
+    summed = call(fold_kernel, shape((EXP, CAP, TOK), BF), [vmem()] * 8, (*pieces, parts[7]))
     back = lax.all_to_all(summed, SP, 0, 0, tiled=True)
     d_input = combine(slot, target, back, cotangent)
-    whole = lax.all_gather(d_input, TP, axis=1, tiled=True)
+    whole = lax.all_gather(d_input, TP, axis=0, tiled=True)
     flat = shape((TOK, HEADS * HD), BF)
     d_gate, grad_y, run, sent, rest = call(
         project_kernel,
@@ -371,8 +369,8 @@
     dx, dw, d_read = call(
         inner_kernel, (shape((TOK, HEADS * HD), F32), square, square),
         [vmem()] * 6, (grad_y, values, write_keys, read_keys, run, entry_states[0]), flops=10**9)
-    sent, dx, dw, d_read = lax.optimization_barrier((sent, dx, dw, d_read))
     received = lax.all_to_all(sent, SP, 0, 0, tiled=True)
+    received, dx, dw, d_read = lax.optimization_barrier((received, dx, dw, d_read))
     states = call(scan_kernel, shape((EXP, EXP + 8, WIDE), BF), [vmem()] * 2, (received, rest))
     second = lax.all_to_all(states, SP, 0, 0, tiled=True)
     d_values, d_write, d_out_weight = call(

time: 193 us -> 192 us (level)
  the two profiles are of different devices: /device:TPU:8 before, /device:TPU:2 now
where the time goes in v7:
time: 192 us; the launch traced here: 191 us
  blocking collectives  86.5 us (45%)
  starting transfers between devices  52.4 us (27%)
  waiting for transfers between devices  39.3 us (20%)
  Pallas kernels  11.6 us (6%)
    all_to_all x1, blocking collectives, step(): c0 = lax.all_to_all(buf, SP, 0, 0, tiled=True)  30.4 us
    ppermute x7, starting transfers between devices, step(): pieces.append(lax.ppermute(parts[k], TP, route(far, same)))  27.5 us
    all_to_all x1, blocking collectives, step(): second = lax.all_to_all(states, SP, 0, 0, tiled=True)  24.4 us
    all_to_all x1, waiting for transfers between devices, step(): received = lax.all_to_all(sent, SP, 0, 0, tiled=True)  19 us
    all_gather x1, blocking collectives, step(): whole = lax.all_gather(d_input, TP, axis=0, tiled=True)  17.4 us
    all_to_all x1, blocking collectives, step(): back = lax.all_to_all(summed, SP, 0, 0, tiled=True)  14.3 us
    pallas_call x7, Pallas kernels, call(): pl.pallas_call(kernel, out_shape=outs, in_specs=specs, out_specs=jax.tree...  8.35 us
    all_to_all x1, starting transfers between devices, step(): received = lax.all_to_all(sent, SP, 0, 0, tiled=True)  5.79 us
  transfers between devices with their start and end apart: 16, of which 7 were waited for; matrix products, arithmetic and copies ran while one was open for 0% of the time, Pallas kernels for 2%

profile of v7, /device:TPU:2, one launch (start us, length us, event | category | flops | bytes accessed | tf_op | source)
XLA Modules:
  0.0 190.9 jit_solution(1548299882056994528)
XLA Ops:
  0.6 2.2 %prepare.1 = (bf16[32,32,256]{2,1,0:T(8,128)(2,1)}, s32[8,128]{1,0:T(8,128)}) custom-call(s32[1]{0:T(128)} %bitcast.where, s32[2,128]{1,0:T(2,128)} %bitcast.24, f32[2,128]{1,0:T(2,128)} %bitcast.25, bf16[128,2048]{1,0:T(8,128)(2,1)} %mix.1, bf16[128,2048]{1,0:T(8,128)(2,1)} %cotangent.1), custom_call_target="tpu_custom_call" | custom-call | tf_op jit(solution)/shard_map/prepare/pallas_call | solution.py:112
  2.9 30.4 %all_to_all.20.refs_0_ = bf16[32,32,256]{2,1,0:T(8,128)(2,1)S(1)} all-to-all(bf16[32,32,256]{2,1,0:T(8,128)(2,1)} %get-tuple-element.52), channel_id=1, replica_groups=mesh['z'=8,'x'=4,'y'=8,'core'=2] {'z','x'}, dimensions={0} | all-to-all | bytes 1048576 | tf_op jit(solution)/shard_map/all_to_all | solution.py:335
  33.3 3.5 %collective-permute-start.1 = (bf16[32,32,256]{2,1,0:T(8,128)(2,1)S(1)}, bf16[32,32,256]{2,1,0:T(8,128)(2,1)S(1)}, u32[]{:S(2)}, u32[]{:S(2)}) collective-permute-start(bf16[32,32,256]{2,1,0:T(8,128)(2,1)S(1)} %all_to_all.20.refs_0_), channel_id=1, source_target_pairs={{0,2},{1,15},{2,4},{3,1},{4,6},{5,3},{6,8},{7,5},{8,10},{9,7},{10,... | collective-permute-start | bytes 1572872 | tf_op jit(solution)/shard_map/ppermute | solution.py:336
  36.8 2.1 %collective-permute-start = (bf16[32,32,256]{2,1,0:T(8,128)(2,1)S(1)}, bf16[32,32,256]{2,1,0:T(8,128)(2,1)S(1)}, u32[]{:S(2)}, u32[]{:S(2)}) collective-permute-start(bf16[32,32,256]{2,1,0:T(8,128)(2,1)S(1)} %all_to_all.20.refs_0_), channel_id=1, source_target_pairs={{0,1},{1,0},{2,3},{3,2},{4,5},{5,4},{6,7},{7,6},{8,9},{9,8},{10,11... | collective-permute-start | bytes 1572872 | tf_op jit(solution)/shard_map/ppermute | solution.py:337
  39.0 2.3 %collective-permute-start.4 = (bf16[3,64,2048]{2,1,0:T(8,128)(2,1)S(1)}, bf16[3,64,2048]{2,1,0:T(8,128)(2,1)S(1)}, u32[]{:S(2)}, u32[]{:S(2)}) collective-permute-start(bf16[3,64,2048]{2,1,0:T(8,128)(2,1)S(1)} %pad_maximum_fusion.refs_8_), channel_id=1, source_target_pairs={{0,1},{1,0},{2,3},{3,2},{4,5},{5,4},{6,7},{7,6},{8,9},{9,8},{10,11... | collective-permute-start | bytes 2359304 | tf_op jit(solution)/shard_map/ppermute | solution.py:333
  41.3 4.6 %collective-permute-done.1.refs_2_ = bf16[32,32,256]{2,1,0:T(8,128)(2,1)S(1)} collective-permute-done((bf16[32,32,256]{2,1,0:T(8,128)(2,1)S(1)}, bf16[32,32,256]{2,1,0:T(8,128)(2,1)S(1)}, u32[]{:S(2)}, u32[]{:S(2)}) %collective-permute-start.1) | collective-permute-done | bytes 524320 | tf_op jit(solution)/shard_map/ppermute | solution.py:336
  45.8 2.0 %collective-permute-start.3 = (bf16[32,32,256]{2,1,0:T(8,128)(2,1)S(1)}, bf16[32,32,256]{2,1,0:T(8,128)(2,1)S(1)}, u32[]{:S(2)}, u32[]{:S(2)}) collective-permute-start(bf16[32,32,256]{2,1,0:T(8,128)(2,1)S(1)} %collective-permute-done.1.refs_2_), channel_id=1, source_target_pairs={{0,2},{1,15},{2,4},{3,1},{4,6},{5,3},{6,8},{7,5},{8,10},{9,7},{10,... | collective-permute-start | bytes 1572872 | tf_op jit(solution)/shard_map/ppermute | solution.py:339
  47.9 3.5 %collective-permute-start.2 = (bf16[32,32,256]{2,1,0:T(8,128)(2,1)S(1)}, bf16[32,32,256]{2,1,0:T(8,128)(2,1)S(1)}, u32[]{:S(2)}, u32[]{:S(2)}) collective-permute-start(bf16[32,32,256]{2,1,0:T(8,128)(2,1)S(1)} %collective-permute-done.refs_1_), channel_id=1, source_target_pairs={{0,2},{1,15},{2,4},{3,1},{4,6},{5,3},{6,8},{7,5},{8,10},{9,7},{10,... | collective-permute-start | bytes 1572872 | tf_op jit(solution)/shard_map/ppermute | solution.py:338
  51.4 1.9 %collective-permute-start.5 = (bf16[32,32,256]{2,1,0:T(8,128)(2,1)S(1)}, bf16[32,32,256]{2,1,0:T(8,128)(2,1)S(1)}, u32[]{:S(2)}, u32[]{:S(2)}) collective-permute-start(bf16[32,32,256]{2,1,0:T(8,128)(2,1)S(1)} %collective-permute-done.1.refs_2_), channel_id=1, source_target_pairs={{0,1},{1,0},{2,3},{3,2},{4,5},{5,4},{6,7},{7,6},{8,9},{9,8},{10,11... | collective-permute-start | bytes 1572872 | tf_op jit(solution)/shard_map/ppermute | solution.py:341
  53.3 4.8 %collective-permute-done.3.refs_4_ = bf16[32,32,256]{2,1,0:T(8,128)(2,1)S(1)} collective-permute-done((bf16[32,32,256]{2,1,0:T(8,128)(2,1)S(1)}, bf16[32,32,256]{2,1,0:T(8,128)(2,1)S(1)}, u32[]{:S(2)}, u32[]{:S(2)}) %collective-permute-start.3) | collective-permute-done | bytes 524320 | tf_op jit(solution)/shard_map/ppermute | solution.py:339
  58.1 1.9 collective-permute-start.7
  60.0 3.7 %collective-permute-done.2.refs_3_ = bf16[32,32,256]{2,1,0:T(8,128)(2,1)S(1)} collective-permute-done((bf16[32,32,256]{2,1,0:T(8,128)(2,1)S(1)}, bf16[32,32,256]{2,1,0:T(8,128)(2,1)S(1)}, u32[]{:S(2)}, u32[]{:S(2)}) %collective-permute-start.2) | collective-permute-done | bytes 524320 | tf_op jit(solution)/shard_map/ppermute | solution.py:338
  63.7 1.9 collective-permute-start.6
  65.7 1.9 collective-permute-done.6.refs_6_
  67.5 1.9 shard_map.214
  69.4 1.9 %collective-permute-start.8 = (bf16[512,128]{1,0:T(8,128)(2,1)S(1)}, bf16[512,128]{1,0:T(8,128)(2,1)S(1)}, u32[]{:S(2)}, u32[]{:S(2)}) collective-permute-start(bf16[512,128]{1,0:T(8,128)(2,1)S(1)} %get-tuple-element.55), channel_id=1, source_target_pairs={{0,2},{1,15},{2,4},{3,1},{4,6},{5,3},{6,8},{7,5},{8,10},{9,7},{10,... | collective-permute-start | bytes 393224 | tf_op jit(solution)/shard_map/ppermute | solution.py:352
  71.3 3.4 %collective-permute-start.9 = (bf16[512,128]{1,0:T(8,128)(2,1)S(1)}, bf16[512,128]{1,0:T(8,128)(2,1)S(1)}, u32[]{:S(2)}, u32[]{:S(2)}) collective-permute-start(bf16[512,128]{1,0:T(8,128)(2,1)S(1)} %get-tuple-element.56), channel_id=1, source_target_pairs={{0,3},{1,14},{2,5},{3,0},{4,7},{5,2},{6,9},{7,4},{8,11},{9,6},{10,... | collective-permute-start | bytes 393224 | tf_op jit(solution)/shard_map/ppermute | solution.py:352
  74.7 6.6 %collective-permute-start.10 = (bf16[512,128]{1,0:T(8,128)(2,1)S(1)}, bf16[512,128]{1,0:T(8,128)(2,1)S(1)}, u32[]{:S(2)}, u32[]{:S(2)}) collective-permute-start(bf16[512,128]{1,0:T(8,128)(2,1)S(1)} %get-tuple-element.57), channel_id=1, source_target_pairs={{0,6},{1,11},{2,8},{3,13},{4,10},{5,15},{6,12},{7,1},{8,14},{9,3},... | collective-permute-start | bytes 393224 | tf_op jit(solution)/shard_map/ppermute | solution.py:352
  81.3 2.3 %collective-permute-start.11 = (bf16[512,128]{1,0:T(8,128)(2,1)S(1)}, bf16[512,128]{1,0:T(8,128)(2,1)S(1)}, u32[]{:S(2)}, u32[]{:S(2)}) collective-permute-start(bf16[512,128]{1,0:T(8,128)(2,1)S(1)} %get-tuple-element.58), channel_id=1, source_target_pairs={{0,7},{1,10},{2,9},{3,12},{4,11},{5,14},{6,13},{7,0},{8,15},{9,2},... | collective-permute-start | bytes 393224 | tf_op jit(solution)/shard_map/ppermute | solution.py:352
  83.6 7.5 %collective-permute-start.12 = (bf16[512,128]{1,0:T(8,128)(2,1)S(1)}, bf16[512,128]{1,0:T(8,128)(2,1)S(1)}, u32[]{:S(2)}, u32[]{:S(2)}) collective-permute-start(bf16[512,128]{1,0:T(8,128)(2,1)S(1)} %get-tuple-element.59), channel_id=1, source_target_pairs={{0,8},{1,9},{2,10},{3,11},{4,12},{5,13},{6,14},{7,15},{8,0},{9,1},... | collective-permute-start | bytes 393224 | tf_op jit(solution)/shard_map/ppermute | solution.py:352
  91.1 1.9 %collective-permute-start.13 = (bf16[512,128]{1,0:T(8,128)(2,1)S(1)}, bf16[512,128]{1,0:T(8,128)(2,1)S(1)}, u32[]{:S(2)}, u32[]{:S(2)}) collective-permute-start(bf16[512,128]{1,0:T(8,128)(2,1)S(1)} %get-tuple-element.60), channel_id=1, source_target_pairs={{0,4},{1,13},{2,6},{3,15},{4,8},{5,1},{6,10},{7,3},{8,12},{9,5},{1... | collective-permute-start | bytes 393224 | tf_op jit(solution)/shard_map/ppermute | solution.py:352
  93.0 4.0 %collective-permute-start.14 = (bf16[512,128]{1,0:T(8,128)(2,1)S(1)}, bf16[512,128]{1,0:T(8,128)(2,1)S(1)}, u32[]{:S(2)}, u32[]{:S(2)}) collective-permute-start(bf16[512,128]{1,0:T(8,128)(2,1)S(1)} %get-tuple-element.61), channel_id=1, source_target_pairs={{0,5},{1,12},{2,7},{3,14},{4,9},{5,0},{6,11},{7,2},{8,13},{9,4},{1... | collective-permute-start | bytes 393224 | tf_op jit(solution)/shard_map/ppermute | solution.py:352
  97.0 1.7 shard_map.215
  98.7 1.8 collective-permute-done.13.refs_5_
  100.5 3.7 %collective-permute-done.14.refs_6_ = bf16[512,128]{1,0:T(8,128)(2,1)S(1)} collective-permute-done((bf16[512,128]{1,0:T(8,128)(2,1)S(1)}, bf16[512,128]{1,0:T(8,128)(2,1)S(1)}, u32[]{:S(2)}, u32[]{:S(2)}) %collective-permute-start.14) | collective-permute-done | bytes 131104 | tf_op jit(solution)/shard_map/ppermute | solution.py:352
  104.3 14.3 %all_to_all.21.rows = bf16[32,16,128]{2,1,0:T(8,128)(2,1)S(1)} all-to-all(bf16[32,16,128]{2,1,0:T(8,128)(2,1)S(1)} %shard_map.216), channel_id=1, replica_groups=mesh['z'=8,'x'=4,'y'=8,'core'=2] {'z','x'}, dimensions={0} | all-to-all | bytes 262144 | tf_op jit(solution)/shard_map/all_to_all | solution.py:359
  119.6 17.4 %all_gather.3.gathered = bf16[2048,128]{1,0:T(8,128)(2,1)S(1)} all-gather(bf16[128,128]{1,0:T(8,128)(2,1)} %combine.1), channel_id=1, replica_groups=mesh['z'=8,'x'=4,'y'=8,'core'=2] {'y','core'}, dimensions={0}, use_global_device_ids=true | all-gather | bytes 557056 | tf_op jit(solution)/shard_map/all_gather | solution.py:361
  137.1 1.9 shard_map.217
  139.0 5.8 %all-to-all-start.2 = ((bf16[32,40,256]{2,1,0:T(8,128)(2,1)}), bf16[32,40,256]{2,1,0:T(8,128)(2,1)S(1)}, u32[]{:S(2)}, u32[]{:S(2)}) async-start(bf16[32,40,256]{2,1,0:T(8,128)(2,1)} %get-tuple-element.80), calls=%async_computation.2 | async-start | bytes 1310720 | tf_op jit(solution)/shard_map/all_to_all | solution.py:372
  144.8 1.5 shard_map.218
  146.3 19.0 %all-to-all-done.2.received = bf16[32,40,256]{2,1,0:T(8,128)(2,1)S(1)} async-done(((bf16[32,40,256]{2,1,0:T(8,128)(2,1)}), bf16[32,40,256]{2,1,0:T(8,128)(2,1)S(1)}, u32[]{:S(2)}, u32[]{:S(2)}) %all-to-all-start.2) | async-done | bytes 655392 | tf_op jit(solution)/shard_map/all_to_all | solution.py:372
  165.3 24.4 %all_to_all.22.second = bf16[32,40,256]{2,1,0:T(8,128)(2,1)S(1)} all-to-all(bf16[32,40,256]{2,1,0:T(8,128)(2,1)S(1)} %shard_map.219), channel_id=1, replica_groups=mesh['z'=8,'x'=4,'y'=8,'core'=2] {'z','x'}, dimensions={0} | all-to-all | bytes 1310720 | tf_op jit(solution)/shard_map/all_to_all | solution.py:375
  (40 shorter events, 2.6 us)
Async XLA Ops:
  2.9 36.0 %copy-start.10 = (bf16[1,64,2048]{2,1,0:T(8,128)(2,1)S(1)}, bf16[1,64,2048]{2,1,0:T(8,128)(2,1)}, u32[]{:S(2)}) copy-start(bf16[1,64,2048]{2,1,0:T(8,128)(2,1)} %param.21) | copy-start | bytes 786436
  2.9 36.0 %copy-start.11 = (bf16[1,2048,64]{1,2,0:T(8,128)(2,1)S(1)}, bf16[1,2048,64]{1,2,0:T(8,128)(2,1)}, u32[]{:S(2)}) copy-start(bf16[1,2048,64]{1,2,0:T(8,128)(2,1)} %param.20) | copy-start | bytes 786436
  2.9 36.0 %copy-start.12 = (bf16[1,2048,64]{1,2,0:T(8,128)(2,1)S(1)}, bf16[1,2048,64]{1,2,0:T(8,128)(2,1)}, u32[]{:S(2)}) copy-start(bf16[1,2048,64]{1,2,0:T(8,128)(2,1)} %param.19) | copy-start | bytes 786436
  33.3 12.5 %collective-permute-start.1 = (bf16[32,32,256]{2,1,0:T(8,128)(2,1)S(1)}, bf16[32,32,256]{2,1,0:T(8,128)(2,1)S(1)}, u32[]{:S(2)}, u32[]{:S(2)}) collective-permute-start(bf16[32,32,256]{2,1,0:T(8,128)(2,1)S(1)} %all_to_all.20.refs_0_), channel_id=1, source_target_pairs={{0,2},{1,15},{2,4},{3,1},{4,6},{5,3},{6,8},{7,5},{8,10},{9,7},{10,... | collective-permute-start | bytes 1572872 | tf_op jit(solution)/shard_map/ppermute | solution.py:336
  36.8 11.1 %collective-permute-start = (bf16[32,32,256]{2,1,0:T(8,128)(2,1)S(1)}, bf16[32,32,256]{2,1,0:T(8,128)(2,1)S(1)}, u32[]{:S(2)}, u32[]{:S(2)}) collective-permute-start(bf16[32,32,256]{2,1,0:T(8,128)(2,1)S(1)} %all_to_all.20.refs_0_), channel_id=1, source_target_pairs={{0,1},{1,0},{2,3},{3,2},{4,5},{5,4},{6,7},{7,6},{8,9},{9,8},{10,11... | collective-permute-start | bytes 1572872 | tf_op jit(solution)/shard_map/ppermute | solution.py:337
  39.0 12.4 %collective-permute-start.4 = (bf16[3,64,2048]{2,1,0:T(8,128)(2,1)S(1)}, bf16[3,64,2048]{2,1,0:T(8,128)(2,1)S(1)}, u32[]{:S(2)}, u32[]{:S(2)}) collective-permute-start(bf16[3,64,2048]{2,1,0:T(8,128)(2,1)S(1)} %pad_maximum_fusion.refs_8_), channel_id=1, source_target_pairs={{0,1},{1,0},{2,3},{3,2},{4,5},{5,4},{6,7},{7,6},{8,9},{9,8},{10,11... | collective-permute-start | bytes 2359304 | tf_op jit(solution)/shard_map/ppermute | solution.py:333
  45.8 12.3 %collective-permute-start.3 = (bf16[32,32,256]{2,1,0:T(8,128)(2,1)S(1)}, bf16[32,32,256]{2,1,0:T(8,128)(2,1)S(1)}, u32[]{:S(2)}, u32[]{:S(2)}) collective-permute-start(bf16[32,32,256]{2,1,0:T(8,128)(2,1)S(1)} %collective-permute-done.1.refs_2_), channel_id=1, source_target_pairs={{0,2},{1,15},{2,4},{3,1},{4,6},{5,3},{6,8},{7,5},{8,10},{9,7},{10,... | collective-permute-start | bytes 1572872 | tf_op jit(solution)/shard_map/ppermute | solution.py:339
  47.9 15.9 %collective-permute-start.2 = (bf16[32,32,256]{2,1,0:T(8,128)(2,1)S(1)}, bf16[32,32,256]{2,1,0:T(8,128)(2,1)S(1)}, u32[]{:S(2)}, u32[]{:S(2)}) collective-permute-start(bf16[32,32,256]{2,1,0:T(8,128)(2,1)S(1)} %collective-permute-done.refs_1_), channel_id=1, source_target_pairs={{0,2},{1,15},{2,4},{3,1},{4,6},{5,3},{6,8},{7,5},{8,10},{9,7},{10,... | collective-permute-start | bytes 1572872 | tf_op jit(solution)/shard_map/ppermute | solution.py:338
  51.4 14.3 %collective-permute-start.5 = (bf16[32,32,256]{2,1,0:T(8,128)(2,1)S(1)}, bf16[32,32,256]{2,1,0:T(8,128)(2,1)S(1)}, u32[]{:S(2)}, u32[]{:S(2)}) collective-permute-start(bf16[32,32,256]{2,1,0:T(8,128)(2,1)S(1)} %collective-permute-done.1.refs_2_), channel_id=1, source_target_pairs={{0,1},{1,0},{2,3},{3,2},{4,5},{5,4},{6,7},{7,6},{8,9},{9,8},{10,11... | collective-permute-start | bytes 1572872 | tf_op jit(solution)/shard_map/ppermute | solution.py:341
  58.1 7.5 %collective-permute-start.7 = (bf16[32,32,256]{2,1,0:T(8,128)(2,1)S(1)}, bf16[32,32,256]{2,1,0:T(8,128)(2,1)S(1)}, u32[]{:S(2)}, u32[]{:S(2)}) collective-permute-start(bf16[32,32,256]{2,1,0:T(8,128)(2,1)S(1)} %collective-permute-done.3.refs_4_), channel_id=1, source_target_pairs={{0,1},{1,0},{2,3},{3,2},{4,5},{5,4},{6,7},{7,6},{8,9},{9,8},{10,11... | collective-permute-start | bytes 1572872 | tf_op jit(solution)/shard_map/ppermute | solution.py:343
  63.7 3.8 %collective-permute-start.6 = (bf16[32,32,256]{2,1,0:T(8,128)(2,1)S(1)}, bf16[32,32,256]{2,1,0:T(8,128)(2,1)S(1)}, u32[]{:S(2)}, u32[]{:S(2)}) collective-permute-start(bf16[32,32,256]{2,1,0:T(8,128)(2,1)S(1)} %collective-permute-done.2.refs_3_), channel_id=1, source_target_pairs={{0,1},{1,0},{2,3},{3,2},{4,5},{5,4},{6,7},{7,6},{8,9},{9,8},{10,11... | collective-permute-start | bytes 1572872 | tf_op jit(solution)/shard_map/ppermute | solution.py:342
  69.4 21.7 %collective-permute-start.8 = (bf16[512,128]{1,0:T(8,128)(2,1)S(1)}, bf16[512,128]{1,0:T(8,128)(2,1)S(1)}, u32[]{:S(2)}, u32[]{:S(2)}) collective-permute-start(bf16[512,128]{1,0:T(8,128)(2,1)S(1)} %get-tuple-element.55), channel_id=1, source_target_pairs={{0,2},{1,15},{2,4},{3,1},{4,6},{5,3},{6,8},{7,5},{8,10},{9,7},{10,... | collective-permute-start | bytes 393224 | tf_op jit(solution)/shard_map/ppermute | solution.py:352
  71.3 21.7 %collective-permute-start.9 = (bf16[512,128]{1,0:T(8,128)(2,1)S(1)}, bf16[512,128]{1,0:T(8,128)(2,1)S(1)}, u32[]{:S(2)}, u32[]{:S(2)}) collective-permute-start(bf16[512,128]{1,0:T(8,128)(2,1)S(1)} %get-tuple-element.56), channel_id=1, source_target_pairs={{0,3},{1,14},{2,5},{3,0},{4,7},{5,2},{6,9},{7,4},{8,11},{9,6},{10,... | collective-permute-start | bytes 393224 | tf_op jit(solution)/shard_map/ppermute | solution.py:352
  74.7 24.0 %collective-permute-start.10 = (bf16[512,128]{1,0:T(8,128)(2,1)S(1)}, bf16[512,128]{1,0:T(8,128)(2,1)S(1)}, u32[]{:S(2)}, u32[]{:S(2)}) collective-permute-start(bf16[512,128]{1,0:T(8,128)(2,1)S(1)} %get-tuple-element.57), channel_id=1, source_target_pairs={{0,6},{1,11},{2,8},{3,13},{4,10},{5,15},{6,12},{7,1},{8,14},{9,3},... | collective-permute-start | bytes 393224 | tf_op jit(solution)/shard_map/ppermute | solution.py:352
  81.3 17.4 %collective-permute-start.11 = (bf16[512,128]{1,0:T(8,128)(2,1)S(1)}, bf16[512,128]{1,0:T(8,128)(2,1)S(1)}, u32[]{:S(2)}, u32[]{:S(2)}) collective-permute-start(bf16[512,128]{1,0:T(8,128)(2,1)S(1)} %get-tuple-element.58), channel_id=1, source_target_pairs={{0,7},{1,10},{2,9},{3,12},{4,11},{5,14},{6,13},{7,0},{8,15},{9,2},... | collective-permute-start | bytes 393224 | tf_op jit(solution)/shard_map/ppermute | solution.py:352
  83.6 15.1 %collective-permute-start.12 = (bf16[512,128]{1,0:T(8,128)(2,1)S(1)}, bf16[512,128]{1,0:T(8,128)(2,1)S(1)}, u32[]{:S(2)}, u32[]{:S(2)}) collective-permute-start(bf16[512,128]{1,0:T(8,128)(2,1)S(1)} %get-tuple-element.59), channel_id=1, source_target_pairs={{0,8},{1,9},{2,10},{3,11},{4,12},{5,13},{6,14},{7,15},{8,0},{9,1},... | collective-permute-start | bytes 393224 | tf_op jit(solution)/shard_map/ppermute | solution.py:352
  91.1 9.4 %collective-permute-start.13 = (bf16[512,128]{1,0:T(8,128)(2,1)S(1)}, bf16[512,128]{1,0:T(8,128)(2,1)S(1)}, u32[]{:S(2)}, u32[]{:S(2)}) collective-permute-start(bf16[512,128]{1,0:T(8,128)(2,1)S(1)} %get-tuple-element.60), channel_id=1, source_target_pairs={{0,4},{1,13},{2,6},{3,15},{4,8},{5,1},{6,10},{7,3},{8,12},{9,5},{1... | collective-permute-start | bytes 393224 | tf_op jit(solution)/shard_map/ppermute | solution.py:352
  93.0 11.1 %collective-permute-start.14 = (bf16[512,128]{1,0:T(8,128)(2,1)S(1)}, bf16[512,128]{1,0:T(8,128)(2,1)S(1)}, u32[]{:S(2)}, u32[]{:S(2)}) collective-permute-start(bf16[512,128]{1,0:T(8,128)(2,1)S(1)} %get-tuple-element.61), channel_id=1, source_target_pairs={{0,5},{1,12},{2,7},{3,14},{4,9},{5,0},{6,11},{7,2},{8,13},{9,4},{1... | collective-permute-start | bytes 393224 | tf_op jit(solution)/shard_map/ppermute | solution.py:352
  104.1 14.5 %copy-start = (bf16[128,2048]{1,0:T(8,128)(2,1)S(1)}, bf16[128,2048]{1,0:T(8,128)(2,1)}, u32[]{:S(2)}) copy-start(bf16[128,2048]{1,0:T(8,128)(2,1)} %cotangent.1) | copy-start | bytes 1572868
  104.1 14.5 %copy-start.7 = (s32[8,128]{1,0:T(8,128)S(1)}, s32[8,128]{1,0:T(8,128)}, u32[]{:S(2)}) copy-start(s32[8,128]{1,0:T(8,128)} %get-tuple-element.71.target) | copy-start | bytes 12292
  104.3 32.8 %copy-start.1 = (bf16[256,2048]{1,0:T(8,128)(2,1)S(1)}, bf16[256,2048]{1,0:T(8,128)(2,1)}, u32[]{:S(2)}) copy-start(bf16[256,2048]{1,0:T(8,128)(2,1)} %weight.1) | copy-start | bytes 3145732
  119.6 17.5 %copy-start.3 = (bf16[128,256]{1,0:T(8,128)(2,1)S(1)}, bf16[128,256]{1,0:T(8,128)(2,1)}, u32[]{:S(2)}) copy-start(bf16[128,256]{1,0:T(8,128)(2,1)} %gate_pre.1) | copy-start | bytes 196612
  119.6 17.5 %copy-start.4 = (bf16[128,256]{1,0:T(8,128)(2,1)S(1)}, bf16[128,256]{1,0:T(8,128)(2,1)}, u32[]{:S(2)}) copy-start(bf16[128,256]{1,0:T(8,128)(2,1)} %mixer.1) | copy-start | bytes 196612
  119.6 17.4 %copy-start.5 = (bf16[128,128]{1,0:T(8,128)(2,1)S(1)}, bf16[128,128]{1,0:T(8,128)(2,1)}, u32[]{:S(2)}) copy-start(bf16[128,128]{1,0:T(8,128)(2,1)} %read.3) | copy-start | bytes 98308
  119.6 17.4 %copy-start.8 = (f32[4,128]{1,0:T(4,128)S(1)}, f32[4,128]{1,0:T(4,128)}, u32[]{:S(2)}) copy-start(f32[4,128]{1,0:T(4,128)} %logs.1) | copy-start | bytes 6148
  139.0 5.8 %copy-start.2 = (bf16[128,256]{1,0:T(8,128)(2,1)S(1)}, bf16[128,256]{1,0:T(8,128)(2,1)}, u32[]{:S(2)}) copy-start(bf16[128,256]{1,0:T(8,128)(2,1)} %values.3) | copy-start | bytes 196612
  139.0 5.8 %copy-start.6 = (bf16[128,128]{1,0:T(8,128)(2,1)S(1)}, bf16[128,128]{1,0:T(8,128)(2,1)}, u32[]{:S(2)}) copy-start(bf16[128,128]{1,0:T(8,128)(2,1)} %write.3) | copy-start | bytes 98308
  139.0 5.8 %copy-start.9 = (f32[1,4,64,128]{3,2,1,0:T(8,128)S(1)}, f32[1,4,64,128]{3,2,1,0:T(8,128)}, u32[]{:S(2)}) copy-start(f32[1,4,64,128]{3,2,1,0:T(8,128)} %param.29) | copy-start | bytes 393220
  139.0 26.3 %all-to-all-start.2 = ((bf16[32,40,256]{2,1,0:T(8,128)(2,1)}), bf16[32,40,256]{2,1,0:T(8,128)(2,1)S(1)}, u32[]{:S(2)}, u32[]{:S(2)}) async-start(bf16[32,40,256]{2,1,0:T(8,128)(2,1)} %get-tuple-element.80), calls=%async_computation.2 | async-start | bytes 1310720 | tf_op jit(solution)/shard_map/all_to_all | solution.py:372

commit v8 on v4

--- a/solution.py
+++ b/solution.py
@@ -18,6 +18,7 @@
 STATE = 128
 SP = ("z", "x")
 TP = ("y", "core")
+GRANT = 16 * 1024 * 1024
 BF = jnp.bfloat16
 F32 = jnp.float32
 
@@ -34,12 +35,14 @@
     return lax.dot_general(a, b, (((1,), (1,)), ((), ())), preferred_element_type=F32)
 
 
-def mm_nt_exact(a, b):
-    return lax.dot_general(a, b, (((1,), (1,)), ((), ())), precision=lax.Precision.HIGHEST, preferred_element_type=F32)
-
-
-def mm_exact(a, b):
-    return mm(a, b, lax.Precision.HIGHEST)
+def mm_parts(left, right, product):
+    total = None
+    for i, a in enumerate(left):
+        for j, b in enumerate(right):
+            if i + j < 2:
+                part = product(a, b)
+                total = part if total is None else total + part
+    return total
 
 
 def two_parts(value):
@@ -68,13 +71,14 @@
     return pl.BlockSpec(memory_space=pltpu.SMEM)
 
 
-def call(kernel, outs, specs, args, flops=0):
+def call(kernel, outs, specs, args, flops=0, scratch=()):
     return pl.pallas_call(
         kernel,
         out_shape=outs,
         in_specs=specs,
         out_specs=jax.tree.map(lambda _: vmem(), outs),
-        compiler_params=pltpu.CompilerParams(vmem_limit_bytes=20 * 1024 * 1024),
+        scratch_shapes=scratch,
+        compiler_params=pltpu.CompilerParams(vmem_limit_bytes=GRANT),
         cost_estimate=pl.CostEstimate(flops=flops, bytes_accessed=0, transcendentals=0),
     )(*args)
 
@@ -214,12 +218,15 @@
         in_specs=[smem(), vmem(), vmem(), pl.BlockSpec(memory_space=pltpu.HBM)],
         out_specs=vmem(),
         scratch_shapes=[pltpu.VMEM((TOK, TOK), BF), pltpu.SemaphoreType.DMA],
+        compiler_params=pltpu.CompilerParams(vmem_limit_bytes=GRANT),
         name="combine",
     )(slot, target, rows, cotangent)
 
 
-def project_kernel(whole, weight, gate_pre, mixer, logs, read, d_gate, grad_y, run, buf, rest):
-    back = mm_nt(whole[...], weight[...])
+def project_kernel(spot, gathered, weight, gate_pre, mixer, logs, read, d_gate, grad_y, run, buf, *outs):
+    quarters = outs[4]
+    whole = jnp.concatenate([gathered[k * TOK : (k + 1) * TOK, :] for k in range(16)], axis=1)
+    back = mm_nt(whole, weight[...])
     pre = gate_pre[...].astype(F32)
     saved = mixer[...].astype(F32)
     logistic = 1.0 / (1.0 + jnp.exp(-pre))
@@ -228,9 +235,12 @@
     gated = (saved * active).astype(BF)
     for k in range(8):
         turned = whole[:, k * WIDE : (k + 1) * WIDE].T
-        part = mm(turned, gated).astype(BF).reshape(4, FF, WIDE)
-        buf[4 * k : 4 * k + 4, 0:EXP, :] = part[:, 0:EXP]
-        rest[4 * k : 4 * k + 4] = part[:, EXP:]
+        part = mm(turned, gated).astype(BF)
+        for r in range(4):
+            half = part[:, (r & 1) * TOK : (r & 1) * TOK + TOK].reshape(4, FF, TOK)
+            quarters[r, 4 * k : 4 * k + 4] = half[:, (r >> 1) * EXP : (r >> 1) * EXP + EXP]
+    for k in range(4):
+        outs[k][...] = quarters[(spot[0] + k) & 3]
     grad = back * active
     grad_y[...] = grad
     upto = jnp.where(iota((TOK, TOK), 0) <= iota((TOK, TOK), 1), 1.0, 0.0)
@@ -252,29 +262,28 @@
         note = jnp.where(line == 0, first[j : j + 1], jnp.where(line == 1, second[j : j + 1], third[j : j + 1]))
         note = jnp.where(line < 3, note, 0.0)
         notes.append(jnp.broadcast_to(note[None], (EXP // HEADS, 8, STATE)))
-    buf[:, EXP:, 0:STATE] = state.reshape(EXP, 8, STATE).astype(BF)
-    buf[:, EXP:, STATE:] = jnp.concatenate(notes, axis=0).astype(BF)
-
-
-def scan_kernel(received, rest, out):
-    out[:, 0:EXP, :] = rest[...]
+    sent = jnp.concatenate([state.reshape(EXP, 8, STATE), jnp.concatenate(notes, axis=0)], axis=1)
+    buf[...] = sent.astype(BF)
+
+
+def scan_kernel(received, p0, p1, p2, p3, out):
+    total = p0[...].astype(F32) + p1[...].astype(F32) + p2[...].astype(F32) + p3[...].astype(F32)
+    out[:, 0:EXP, :] = total.astype(BF)
     state = jnp.zeros((8, STATE), F32)
     for k in reversed(range(EXP)):
         high, low = two_parts(state)
-        out[k, EXP:, 0:STATE] = high
-        out[k, EXP:, STATE:] = low
+        out[k, EXP:, :] = jnp.concatenate([high.astype(F32), low.astype(F32)], axis=0).astype(BF)
         if k > 0:
-            piece = received[k, EXP:, :].astype(F32)
-            note = piece[:, STATE:]
-            log = note[0:1] + note[1:2] + note[2:3]
-            state = jnp.exp(log) * state + piece[:, :STATE]
+            piece = received[k].astype(F32)
+            log = piece[8:9] + piece[9:10] + piece[10:11]
+            state = jnp.exp(log) * state + piece[0:8]
 
 
 def inner_kernel(grad_y, values, write, read, run, entry, dx, dw, dr):
     running = run[...]
     cols = running.T
     grads = grad_y[...]
-    vals = values[...].astype(F32)
+    vals = values[...]
     cross = mm_nt(write[...], read[...])
     later = iota((TOK, TOK), 1) >= iota((TOK, TOK), 0)
     total = jnp.zeros((TOK, TOK), F32)
@@ -284,29 +293,32 @@
         spread = running[j : j + 1] - cols[:, j : j + 1]
         decay = jnp.where(later, jnp.exp(jnp.where(later, spread, 0.0)), 0.0)
         grad = grads[:, j * HD : (j + 1) * HD]
-        parts.append(mm_exact(cross * decay, grad))
-        total = total + mm_nt_exact(vals[:, j * HD : (j + 1) * HD], grad) * decay
+        halves = two_parts(grad)
+        parts.append(mm_parts(two_parts(cross * decay), halves, mm))
+        total = total + mm_parts((vals[:, j * HD : (j + 1) * HD],), halves, mm_nt) * decay
         starts.append(grad * jnp.exp(cols[:, j : j + 1]))
     dx[...] = jnp.concatenate(parts, axis=1)
-    dw[...] = mm_exact(total, read[...].astype(F32))
-    entry_rows = entry[...].reshape(HEADS * HD, STATE)
-    dr[...] = mm_exact(total.T, write[...].astype(F32)) + mm_exact(jnp.concatenate(starts, axis=1), entry_rows)
-
-
-def outer_kernel(dx, dw, values, write, run, half, second, d_values, d_write, d_out):
+    dw[...] = mm_parts(two_parts(total), (read[...],), mm)
+    entry_rows = two_parts(entry[...].reshape(HEADS * HD, STATE))
+    first = mm_parts(two_parts(total.T), (write[...],), mm)
+    dr[...] = first + mm_parts(two_parts(jnp.concatenate(starts, axis=1)), entry_rows, mm)
+
+
+def outer_kernel(dx, dw, values, write, run, second, d_values, d_write, d_out):
     running = run[...]
     ends = jnp.exp(running[:, TOK - 1 : TOK] - running).T
     scale = jnp.concatenate([jnp.broadcast_to(ends[:, j : j + 1], (TOK, HD)) for j in range(HEADS)], axis=1)
-    high = second[:, EXP:, 0:STATE].reshape(HEADS * HD, STATE)
-    low = second[:, EXP:, STATE:].reshape(HEADS * HD, STATE)
+    later = second[:, EXP:, :].astype(F32)
+    high = later[:, 0:8].reshape(HEADS * HD, STATE).astype(BF)
+    low = later[:, 8:16].reshape(HEADS * HD, STATE).astype(BF)
     d_values[...] = (dx[...] + scale * (mm_nt(write[...], high) + mm_nt(write[...], low))).astype(BF)
     top, rest = two_parts(values[...].astype(F32) * scale)
     d_write[...] = dw[...] + mm(top, high) + mm(top, low) + mm(rest, high)
-    total = second[0, 0:EXP, :].astype(F32)
-    for k in range(1, EXP):
-        total = total + second[k, 0:EXP, :].astype(F32)
-    d_out[0:EXP, :] = half[...]
-    d_out[EXP:, :] = total
+    for r in range(4):
+        total = second[r, 0:EXP, :].astype(F32)
+        for k in range(1, 8):
+            total = total + second[4 * k + r, 0:EXP, :].astype(F32)
+        d_out[(r >> 1) * EXP : (r >> 1) * EXP + EXP, (r & 1) * TOK : (r & 1) * TOK + TOK] = total
 
 
 def step(mixed, cotangent, routes, gates, w_gate, w_up, w_down, out_weight, gate_pre, mixer_out, values,
@@ -352,26 +364,29 @@
     summed = (keep + taken.astype(F32)).astype(BF).reshape(EXP, CAP, TOK)
     back = lax.all_to_all(summed, SP, 0, 0, tiled=True)
     d_input = combine(slot, target, back, cotangent)
-    whole = lax.all_gather(d_input, TP, axis=1, tiled=True)
+    whole = lax.all_gather(d_input, TP, axis=0, tiled=True)
     flat = shape((TOK, HEADS * HD), BF)
-    d_gate, grad_y, run, sent, rest = call(
+    quarter = shape((EXP, EXP, TOK), BF)
+    spot = lax.axis_index("x").astype(jnp.int32).reshape(1)
+    d_gate, grad_y, run, sent, *shares = call(
         project_kernel,
-        (flat, shape((TOK, HEADS * HD), F32), shape((8, TOK), F32), shape((EXP, EXP + 8, WIDE), BF),
-         shape((EXP, EXP, WIDE), BF)),
-        [vmem()] * 6, (whole, out_weight, gate_pre, mixer_out, log_decay, read_keys))
+        (flat, shape((TOK, HEADS * HD), F32), shape((8, TOK), F32), shape((EXP, 16, STATE), BF),
+         quarter, quarter, quarter, quarter),
+        [smem()] + [vmem()] * 6, (spot, whole, out_weight, gate_pre, mixer_out, log_decay, read_keys),
+        scratch=[pltpu.VMEM((4, EXP, EXP, TOK), BF)])
     received = lax.all_to_all(sent, SP, 0, 0, tiled=True)
+    for k in range(1, 4):
+        shares[k] = lax.ppermute(shares[k], "x", [(i, (i + k) % 4) for i in range(4)])
     square = shape((TOK, STATE), F32)
     dx, dw, d_read = call(
         inner_kernel, (shape((TOK, HEADS * HD), F32), square, square),
         [vmem()] * 6, (grad_y, values, write_keys, read_keys, run, entry_states[0]), flops=10**9)
     received, dx, dw, d_read = lax.optimization_barrier((received, dx, dw, d_read))
-    states = call(scan_kernel, shape((EXP, EXP + 8, WIDE), BF), [vmem()] * 2, (received, rest))
+    states = call(scan_kernel, shape((EXP, 48, STATE), BF), [vmem()] * 5, (received, *shares))
     second = lax.all_to_all(states, SP, 0, 0, tiled=True)
-    half = jnp.sum(received[:, :EXP].astype(F32), axis=0)
-    second, half = lax.optimization_barrier((second, half))
     d_values, d_write, d_out_weight = call(
-        outer_kernel, (flat, square, shape((D // EXP, HEADS * HD), F32)), [vmem()] * 7,
-        (dx, dw, values, write_keys, run, half, second))
+        outer_kernel, (flat, square, shape((D // EXP, HEADS * HD), F32)), [vmem()] * 6,
+        (dx, dw, values, write_keys, run, second))
     return (d_wg.T[None], d_wu.T[None], d_wd[None], d_out_weight, d_input, d_values, d_write, d_read, d_gate)
 
 

time: 194 us -> 185 us (0.954)
  waiting for transfers between devices: 62.6 us -> 44.7 us
  starting transfers between devices: 50.8 us -> 60.4 us
  Pallas kernels: 14.5 us -> 11.5 us
    ppermute x0 -> x3, starting transfers between devices: none -> 9.61 us  [step(): lax.ppermute(shares[k], 'x', [(i, (i + k) % 4) for i in range(4)])]
    all_to_all x1, waiting for transfers between devices: 18.5 us -> 9.04 us  [step(): received = lax.all_to_all(sent, SP, 0, 0, tiled=True)]
    all_to_all x1, waiting for transfers between devices: 19.5 us -> 11 us  [step(): back = lax.all_to_all(summed, SP, 0, 0, tiled=True)]
  transfers between devices with their start and end apart: 15 -> 18, of which waited for: 8 -> 8; matrix products, arithmetic and copies ran while one was open for 0% -> 0% of each run, Pallas kernels for 2% -> 2%
where the time goes in v8:
time: 185 us; the launch traced here: 184 us
  blocking collectives  66 us (36%)
  starting transfers between devices  60.4 us (33%)
  waiting for transfers between devices  44.7 us (24%)
  Pallas kernels  11.5 us (6%)
    all_to_all x1, blocking collectives, step(): c0 = lax.all_to_all(buf, SP, 0, 0, tiled=True)  31.1 us
    ppermute x4, starting transfers between devices, step(): pieces.append(lax.ppermute(parts[k], TP, rings[k]))  18.2 us
    all_gather x1, blocking collectives, step(): whole = lax.all_gather(d_input, TP, axis=0, tiled=True)  17.8 us
    all_to_all x1, blocking collectives, step(): second = lax.all_to_all(states, SP, 0, 0, tiled=True)  17.1 us
    ppermute x4, waiting for transfers between devices, step(): pieces.append(lax.ppermute(parts[k], TP, rings[k]))  13.2 us
    all_to_all x1, waiting for transfers between devices, step(): back = lax.all_to_all(summed, SP, 0, 0, tiled=True)  11 us
    ppermute x3, starting transfers between devices, step(): lax.ppermute(shares[k], 'x', [(i, (i + k) % 4) for i in range(4)])  9.61 us
    all_to_all x1, waiting for transfers between devices, step(): received = lax.all_to_all(sent, SP, 0, 0, tiled=True)  9.04 us
  transfers between devices with their start and end apart: 18, of which 8 were waited for; matrix products, arithmetic and copies ran while one was open for 0% of the time, Pallas kernels for 2%

profile of v8, /device:TPU:8, one launch (start us, length us, event | category | flops | bytes accessed | tf_op | source)
XLA Modules:
  0.0 184.4 jit_solution(14503086495231076682)
XLA Ops:
  0.6 2.2 %prepare.1 = (bf16[32,32,256]{2,1,0:T(8,128)(2,1)}, s32[8,128]{1,0:T(8,128)}) custom-call(s32[1]{0:T(128)} %bitcast.where, s32[2,128]{1,0:T(2,128)} %bitcast.26, f32[2,128]{1,0:T(2,128)} %bitcast.27, bf16[128,2048]{1,0:T(8,128)(2,1)} %mix.1, bf16[128,2048]{1,0:T(8,128)(2,1)} %cotangent.1), custom_call_target="tpu_custom_call" | custom-call | tf_op jit(solution)/shard_map/prepare/pallas_call | solution.py:112
  2.9 31.1 %all_to_all.20.refs_0_ = bf16[32,32,256]{2,1,0:T(8,128)(2,1)S(1)} all-to-all(bf16[32,32,256]{2,1,0:T(8,128)(2,1)} %get-tuple-element.51), channel_id=1, replica_groups=mesh['z'=8,'x'=4,'y'=8,'core'=2] {'z','x'}, dimensions={0} | all-to-all | bytes 1048576 | tf_op jit(solution)/shard_map/all_to_all | solution.py:337
  34.0 3.5 %collective-permute-start.1 = (bf16[32,32,256]{2,1,0:T(8,128)(2,1)S(1)}, bf16[32,32,256]{2,1,0:T(8,128)(2,1)S(1)}, u32[]{:S(2)}, u32[]{:S(2)}) collective-permute-start(bf16[32,32,256]{2,1,0:T(8,128)(2,1)S(1)} %all_to_all.20.refs_0_), channel_id=1, source_target_pairs={{0,2},{2,4},{4,6},{6,8},{8,10},{10,12},{12,14},{14,0},{1,15},{3,1}... | collective-permute-start | bytes 1572872 | tf_op jit(solution)/shard_map/ppermute | solution.py:338
  37.4 1.9 %collective-permute-start = (bf16[32,32,256]{2,1,0:T(8,128)(2,1)S(1)}, bf16[32,32,256]{2,1,0:T(8,128)(2,1)S(1)}, u32[]{:S(2)}, u32[]{:S(2)}) collective-permute-start(bf16[32,32,256]{2,1,0:T(8,128)(2,1)S(1)} %all_to_all.20.refs_0_), channel_id=1, source_target_pairs={{0,1},{1,0},{2,3},{3,2},{4,5},{5,4},{6,7},{7,6},{8,9},{9,8},{10,11... | collective-permute-start | bytes 1572872 | tf_op jit(solution)/shard_map/ppermute | solution.py:339
  39.5 2.4 %collective-permute-start.4 = (bf16[3,64,2048]{2,1,0:T(8,128)(2,1)S(1)}, bf16[3,64,2048]{2,1,0:T(8,128)(2,1)S(1)}, u32[]{:S(2)}, u32[]{:S(2)}) collective-permute-start(bf16[3,64,2048]{2,1,0:T(8,128)(2,1)S(1)} %pad_maximum_fusion.refs_8_), channel_id=1, source_target_pairs={{0,1},{1,0},{2,3},{3,2},{4,5},{5,4},{6,7},{7,6},{8,9},{9,8},{10,11... | collective-permute-start | bytes 2359304 | tf_op jit(solution)/shard_map/ppermute | solution.py:335
  41.9 3.1 %collective-permute-done.1.refs_2_ = bf16[32,32,256]{2,1,0:T(8,128)(2,1)S(1)} collective-permute-done((bf16[32,32,256]{2,1,0:T(8,128)(2,1)S(1)}, bf16[32,32,256]{2,1,0:T(8,128)(2,1)S(1)}, u32[]{:S(2)}, u32[]{:S(2)}) %collective-permute-start.1) | collective-permute-done | bytes 524320 | tf_op jit(solution)/shard_map/ppermute | solution.py:338
  45.0 3.5 %collective-permute-start.3 = (bf16[32,32,256]{2,1,0:T(8,128)(2,1)S(1)}, bf16[32,32,256]{2,1,0:T(8,128)(2,1)S(1)}, u32[]{:S(2)}, u32[]{:S(2)}) collective-permute-start(bf16[32,32,256]{2,1,0:T(8,128)(2,1)S(1)} %collective-permute-done.1.refs_2_), channel_id=1, source_target_pairs={{0,2},{2,4},{4,6},{6,8},{8,10},{10,12},{12,14},{14,0},{1,15},{3,1}... | collective-permute-start | bytes 1572872 | tf_op jit(solution)/shard_map/ppermute | solution.py:341
  48.5 3.8 %collective-permute-start.2 = (bf16[32,32,256]{2,1,0:T(8,128)(2,1)S(1)}, bf16[32,32,256]{2,1,0:T(8,128)(2,1)S(1)}, u32[]{:S(2)}, u32[]{:S(2)}) collective-permute-start(bf16[32,32,256]{2,1,0:T(8,128)(2,1)S(1)} %collective-permute-done.refs_1_), channel_id=1, source_target_pairs={{0,2},{2,4},{4,6},{6,8},{8,10},{10,12},{12,14},{14,0},{1,15},{3,1}... | collective-permute-start | bytes 1572872 | tf_op jit(solution)/shard_map/ppermute | solution.py:340
  52.3 1.9 %collective-permute-start.5 = (bf16[32,32,256]{2,1,0:T(8,128)(2,1)S(1)}, bf16[32,32,256]{2,1,0:T(8,128)(2,1)S(1)}, u32[]{:S(2)}, u32[]{:S(2)}) collective-permute-start(bf16[32,32,256]{2,1,0:T(8,128)(2,1)S(1)} %collective-permute-done.1.refs_2_), channel_id=1, source_target_pairs={{0,1},{1,0},{2,3},{3,2},{4,5},{5,4},{6,7},{7,6},{8,9},{9,8},{10,11... | collective-permute-start | bytes 1572872 | tf_op jit(solution)/shard_map/ppermute | solution.py:343
  54.2 1.8 collective-permute-done.3.refs_4_
  56.1 1.9 %collective-permute-start.7 = (bf16[32,32,256]{2,1,0:T(8,128)(2,1)S(1)}, bf16[32,32,256]{2,1,0:T(8,128)(2,1)S(1)}, u32[]{:S(2)}, u32[]{:S(2)}) collective-permute-start(bf16[32,32,256]{2,1,0:T(8,128)(2,1)S(1)} %collective-permute-done.3.refs_4_), channel_id=1, source_target_pairs={{0,1},{1,0},{2,3},{3,2},{4,5},{5,4},{6,7},{7,6},{8,9},{9,8},{10,11... | collective-permute-start | bytes 1572872 | tf_op jit(solution)/shard_map/ppermute | solution.py:345
  58.0 3.7 %collective-permute-done.2.refs_3_ = bf16[32,32,256]{2,1,0:T(8,128)(2,1)S(1)} collective-permute-done((bf16[32,32,256]{2,1,0:T(8,128)(2,1)S(1)}, bf16[32,32,256]{2,1,0:T(8,128)(2,1)S(1)}, u32[]{:S(2)}, u32[]{:S(2)}) %collective-permute-start.2) | collective-permute-done | bytes 524320 | tf_op jit(solution)/shard_map/ppermute | solution.py:340
  61.7 1.9 %collective-permute-start.6 = (bf16[32,32,256]{2,1,0:T(8,128)(2,1)S(1)}, bf16[32,32,256]{2,1,0:T(8,128)(2,1)S(1)}, u32[]{:S(2)}, u32[]{:S(2)}) collective-permute-start(bf16[32,32,256]{2,1,0:T(8,128)(2,1)S(1)} %collective-permute-done.2.refs_3_), channel_id=1, source_target_pairs={{0,1},{1,0},{2,3},{3,2},{4,5},{5,4},{6,7},{7,6},{8,9},{9,8},{10,11... | collective-permute-start | bytes 1572872 | tf_op jit(solution)/shard_map/ppermute | solution.py:344
  63.6 1.9 %collective-permute-done.6.refs_6_ = bf16[32,32,256]{2,1,0:T(8,128)(2,1)S(1)} collective-permute-done((bf16[32,32,256]{2,1,0:T(8,128)(2,1)S(1)}, bf16[32,32,256]{2,1,0:T(8,128)(2,1)S(1)}, u32[]{:S(2)}, u32[]{:S(2)}) %collective-permute-start.6) | collective-permute-done | bytes 524320 | tf_op jit(solution)/shard_map/ppermute | solution.py:344
  65.5 1.8 shard_map.214
  67.3 3.5 %collective-permute-start.8 = (bf16[512,256]{1,0:T(8,128)(2,1)S(1)}, bf16[512,256]{1,0:T(8,128)(2,1)S(1)}, u32[]{:S(2)}, u32[]{:S(2)}) collective-permute-start(bf16[512,256]{1,0:T(8,128)(2,1)S(1)} %get-tuple-element.54), channel_id=1, source_target_pairs={{0,2},{2,4},{4,6},{6,8},{8,10},{10,12},{12,14},{14,0},{1,15},{3,1}... | collective-permute-start | bytes 786440 | tf_op jit(solution)/shard_map/ppermute | solution.py:354
  70.8 8.1 %collective-permute-start.9 = (bf16[512,256]{1,0:T(8,128)(2,1)S(1)}, bf16[512,256]{1,0:T(8,128)(2,1)S(1)}, u32[]{:S(2)}, u32[]{:S(2)}) collective-permute-start(bf16[512,256]{1,0:T(8,128)(2,1)S(1)} %get-tuple-element.55), channel_id=1, source_target_pairs={{0,4},{2,6},{4,8},{6,10},{8,12},{10,14},{12,0},{14,2},{1,13},{3,15... | collective-permute-start | bytes 786440 | tf_op jit(solution)/shard_map/ppermute | solution.py:354
  79.0 1.9 %collective-permute-start.10 = (bf16[512,256]{1,0:T(8,128)(2,1)S(1)}, bf16[512,256]{1,0:T(8,128)(2,1)S(1)}, u32[]{:S(2)}, u32[]{:S(2)}) collective-permute-start(bf16[512,256]{1,0:T(8,128)(2,1)S(1)} %get-tuple-element.56), channel_id=1, source_target_pairs={{0,6},{2,8},{4,10},{6,12},{8,14},{10,0},{12,2},{14,4},{1,11},{3,13... | collective-permute-start | bytes 786440 | tf_op jit(solution)/shard_map/ppermute | solution.py:354
  80.9 4.7 %collective-permute-start.11 = (bf16[512,128]{1,0:T(8,128)(2,1)S(1)}, bf16[512,128]{1,0:T(8,128)(2,1)S(1)}, u32[]{:S(2)}, u32[]{:S(2)}) collective-permute-start(bf16[512,128]{1,0:T(8,128)(2,1)S(1)} %get-tuple-element.57), channel_id=1, source_target_pairs={{0,8},{2,10},{4,12},{6,14},{8,0},{10,2},{12,4},{14,6},{1,9},{3,11}... | collective-permute-start | bytes 393224 | tf_op jit(solution)/shard_map/ppermute | solution.py:354
  85.6 1.7 shard_map.215
  87.3 13.2 %collective-permute-done.11.last = bf16[512,128]{1,0:T(8,128)(2,1)S(1)} collective-permute-done((bf16[512,128]{1,0:T(8,128)(2,1)S(1)}, bf16[512,128]{1,0:T(8,128)(2,1)S(1)}, u32[]{:S(2)}, u32[]{:S(2)}) %collective-permute-start.11) | collective-permute-done | bytes 131104 | tf_op jit(solution)/shard_map/ppermute | solution.py:354
  100.7 2.4 %collective-permute-start.12 = (bf16[512,128]{1,0:T(8,128)(2,1)S(1)}, bf16[512,128]{1,0:T(8,128)(2,1)S(1)}, u32[]{:S(2)}, u32[]{:S(2)}) collective-permute-start(bf16[512,128]{1,0:T(8,128)(2,1)S(1)} %get-tuple-element.74), channel_id=1, source_target_pairs={{0,1},{1,0},{2,3},{3,2},{4,5},{5,4},{6,7},{7,6},{8,9},{9,8},{10,11... | collective-permute-start | bytes 393224 | tf_op jit(solution)/shard_map/ppermute | solution.py:363
  104.7 4.6 %all-to-all-start.1 = ((bf16[32,16,128]{2,1,0:T(8,128)(2,1)}), bf16[32,16,128]{2,1,0:T(8,128)(2,1)S(1)}, u32[]{:S(2)}, u32[]{:S(2)}) async-start(bf16[32,16,128]{2,1,0:T(8,128)(2,1)} %bitcast.15), calls=%async_computation.1 | async-start | bytes 262144 | tf_op jit(solution)/shard_map/all_to_all | solution.py:365
  109.4 11.0 %all-to-all-done.1.rows = bf16[32,16,128]{2,1,0:T(8,128)(2,1)S(1)} async-done(((bf16[32,16,128]{2,1,0:T(8,128)(2,1)}), bf16[32,16,128]{2,1,0:T(8,128)(2,1)S(1)}, u32[]{:S(2)}, u32[]{:S(2)}) %all-to-all-start.1) | async-done | bytes 131104 | tf_op jit(solution)/shard_map/all_to_all | solution.py:365
  121.4 17.8 %all_gather.3.gathered = bf16[2048,128]{1,0:T(8,128)(2,1)S(1)} all-gather(bf16[128,128]{1,0:T(8,128)(2,1)} %combine.1), channel_id=1, replica_groups=mesh['z'=8,'x'=4,'y'=8,'core'=2] {'y','core'}, dimensions={0}, use_global_device_ids=true | all-gather | bytes 557056 | tf_op jit(solution)/shard_map/all_gather | solution.py:367
  139.2 1.8 shard_map.217
  141.0 2.0 %collective-permute-start.13 = (bf16[32,32,128]{2,1,0:T(8,128)(2,1)S(1)}, bf16[32,32,128]{2,1,0:T(8,128)(2,1)S(1)}, u32[]{:S(2)}, u32[]{:S(2)}) collective-permute-start(bf16[32,32,128]{2,1,0:T(8,128)(2,1)S(1)} %get-tuple-element.85), channel_id=1, source_target_pairs={{0,16},{16,32},{32,48},{48,0},{1,17},{17,33},{33,49},{49,1},{2,18}... | collective-permute-start | bytes 786440 | tf_op jit(solution)/shard_map/ppermute | solution.py:379
  143.0 4.6 %collective-permute-start.14 = (bf16[32,32,128]{2,1,0:T(8,128)(2,1)S(1)}, bf16[32,32,128]{2,1,0:T(8,128)(2,1)S(1)}, u32[]{:S(2)}, u32[]{:S(2)}) collective-permute-start(bf16[32,32,128]{2,1,0:T(8,128)(2,1)S(1)} %get-tuple-element.86), channel_id=1, source_target_pairs={{0,32},{16,48},{32,0},{48,16},{1,33},{17,49},{33,1},{49,17},{2,34}... | collective-permute-start | bytes 786440 | tf_op jit(solution)/shard_map/ppermute | solution.py:379
  147.6 3.0 %collective-permute-start.15 = (bf16[32,32,128]{2,1,0:T(8,128)(2,1)S(1)}, bf16[32,32,128]{2,1,0:T(8,128)(2,1)S(1)}, u32[]{:S(2)}, u32[]{:S(2)}) collective-permute-start(bf16[32,32,128]{2,1,0:T(8,128)(2,1)S(1)} %get-tuple-element.87), channel_id=1, source_target_pairs={{0,48},{16,0},{32,16},{48,32},{1,49},{17,1},{33,17},{49,33},{2,50}... | collective-permute-start | bytes 786440 | tf_op jit(solution)/shard_map/ppermute | solution.py:379
  150.7 4.6 %all-to-all-start.2 = ((bf16[32,16,128]{2,1,0:T(8,128)(2,1)}), bf16[32,16,128]{2,1,0:T(8,128)(2,1)S(1)}, u32[]{:S(2)}, u32[]{:S(2)}) async-start(bf16[32,16,128]{2,1,0:T(8,128)(2,1)} %get-tuple-element.75), calls=%async_computation.2 | async-start | bytes 262144 | tf_op jit(solution)/shard_map/all_to_all | solution.py:377
  156.8 9.0 %all-to-all-done.2.received = bf16[32,16,128]{2,1,0:T(8,128)(2,1)S(1)} async-done(((bf16[32,16,128]{2,1,0:T(8,128)(2,1)}), bf16[32,16,128]{2,1,0:T(8,128)(2,1)S(1)}, u32[]{:S(2)}, u32[]{:S(2)}) %all-to-all-start.2) | async-done | bytes 131104 | tf_op jit(solution)/shard_map/all_to_all | solution.py:377
  166.1 17.1 %all_to_all.21.second = bf16[32,48,128]{2,1,0:T(8,128)(2,1)S(1)} all-to-all(bf16[32,48,128]{2,1,0:T(8,128)(2,1)S(1)} %shard_map.219), channel_id=1, replica_groups=mesh['z'=8,'x'=4,'y'=8,'core'=2] {'z','x'}, dimensions={0} | all-to-all | bytes 786432 | tf_op jit(solution)/shard_map/all_to_all | solution.py:386
  (44 shorter events, 5.8 us)
Async XLA Ops:
  2.9 36.5 %copy-start.10 = (bf16[1,64,2048]{2,1,0:T(8,128)(2,1)S(1)}, bf16[1,64,2048]{2,1,0:T(8,128)(2,1)}, u32[]{:S(2)}) copy-start(bf16[1,64,2048]{2,1,0:T(8,128)(2,1)} %param.21) | copy-start | bytes 786436
  2.9 36.5 %copy-start.11 = (bf16[1,2048,64]{1,2,0:T(8,128)(2,1)S(1)}, bf16[1,2048,64]{1,2,0:T(8,128)(2,1)}, u32[]{:S(2)}) copy-start(bf16[1,2048,64]{1,2,0:T(8,128)(2,1)} %param.20) | copy-start | bytes 786436
  2.9 36.5 %copy-start.12 = (bf16[1,2048,64]{1,2,0:T(8,128)(2,1)S(1)}, bf16[1,2048,64]{1,2,0:T(8,128)(2,1)}, u32[]{:S(2)}) copy-start(bf16[1,2048,64]{1,2,0:T(8,128)(2,1)} %param.19) | copy-start | bytes 786436
  34.0 11.1 %collective-permute-start.1 = (bf16[32,32,256]{2,1,0:T(8,128)(2,1)S(1)}, bf16[32,32,256]{2,1,0:T(8,128)(2,1)S(1)}, u32[]{:S(2)}, u32[]{:S(2)}) collective-permute-start(bf16[32,32,256]{2,1,0:T(8,128)(2,1)S(1)} %all_to_all.20.refs_0_), channel_id=1, source_target_pairs={{0,2},{2,4},{4,6},{6,8},{8,10},{10,12},{12,14},{14,0},{1,15},{3,1}... | collective-permute-start | bytes 1572872 | tf_op jit(solution)/shard_map/ppermute | solution.py:338
  37.4 11.1 %collective-permute-start = (bf16[32,32,256]{2,1,0:T(8,128)(2,1)S(1)}, bf16[32,32,256]{2,1,0:T(8,128)(2,1)S(1)}, u32[]{:S(2)}, u32[]{:S(2)}) collective-permute-start(bf16[32,32,256]{2,1,0:T(8,128)(2,1)S(1)} %all_to_all.20.refs_0_), channel_id=1, source_target_pairs={{0,1},{1,0},{2,3},{3,2},{4,5},{5,4},{6,7},{7,6},{8,9},{9,8},{10,11... | collective-permute-start | bytes 1572872 | tf_op jit(solution)/shard_map/ppermute | solution.py:339
  39.5 12.8 %collective-permute-start.4 = (bf16[3,64,2048]{2,1,0:T(8,128)(2,1)S(1)}, bf16[3,64,2048]{2,1,0:T(8,128)(2,1)S(1)}, u32[]{:S(2)}, u32[]{:S(2)}) collective-permute-start(bf16[3,64,2048]{2,1,0:T(8,128)(2,1)S(1)} %pad_maximum_fusion.refs_8_), channel_id=1, source_target_pairs={{0,1},{1,0},{2,3},{3,2},{4,5},{5,4},{6,7},{7,6},{8,9},{9,8},{10,11... | collective-permute-start | bytes 2359304 | tf_op jit(solution)/shard_map/ppermute | solution.py:335
  45.0 11.1 %collective-permute-start.3 = (bf16[32,32,256]{2,1,0:T(8,128)(2,1)S(1)}, bf16[32,32,256]{2,1,0:T(8,128)(2,1)S(1)}, u32[]{:S(2)}, u32[]{:S(2)}) collective-permute-start(bf16[32,32,256]{2,1,0:T(8,128)(2,1)S(1)} %collective-permute-done.1.refs_2_), channel_id=1, source_target_pairs={{0,2},{2,4},{4,6},{6,8},{8,10},{10,12},{12,14},{14,0},{1,15},{3,1}... | collective-permute-start | bytes 1572872 | tf_op jit(solution)/shard_map/ppermute | solution.py:341
  48.5 13.2 %collective-permute-start.2 = (bf16[32,32,256]{2,1,0:T(8,128)(2,1)S(1)}, bf16[32,32,256]{2,1,0:T(8,128)(2,1)S(1)}, u32[]{:S(2)}, u32[]{:S(2)}) collective-permute-start(bf16[32,32,256]{2,1,0:T(8,128)(2,1)S(1)} %collective-permute-done.refs_1_), channel_id=1, source_target_pairs={{0,2},{2,4},{4,6},{6,8},{8,10},{10,12},{12,14},{14,0},{1,15},{3,1}... | collective-permute-start | bytes 1572872 | tf_op jit(solution)/shard_map/ppermute | solution.py:340
  52.3 11.3 %collective-permute-start.5 = (bf16[32,32,256]{2,1,0:T(8,128)(2,1)S(1)}, bf16[32,32,256]{2,1,0:T(8,128)(2,1)S(1)}, u32[]{:S(2)}, u32[]{:S(2)}) collective-permute-start(bf16[32,32,256]{2,1,0:T(8,128)(2,1)S(1)} %collective-permute-done.1.refs_2_), channel_id=1, source_target_pairs={{0,1},{1,0},{2,3},{3,2},{4,5},{5,4},{6,7},{7,6},{8,9},{9,8},{10,11... | collective-permute-start | bytes 1572872 | tf_op jit(solution)/shard_map/ppermute | solution.py:343
  56.1 7.5 %collective-permute-start.7 = (bf16[32,32,256]{2,1,0:T(8,128)(2,1)S(1)}, bf16[32,32,256]{2,1,0:T(8,128)(2,1)S(1)}, u32[]{:S(2)}, u32[]{:S(2)}) collective-permute-start(bf16[32,32,256]{2,1,0:T(8,128)(2,1)S(1)} %collective-permute-done.3.refs_4_), channel_id=1, source_target_pairs={{0,1},{1,0},{2,3},{3,2},{4,5},{5,4},{6,7},{7,6},{8,9},{9,8},{10,11... | collective-permute-start | bytes 1572872 | tf_op jit(solution)/shard_map/ppermute | solution.py:345
  61.7 3.8 %collective-permute-start.6 = (bf16[32,32,256]{2,1,0:T(8,128)(2,1)S(1)}, bf16[32,32,256]{2,1,0:T(8,128)(2,1)S(1)}, u32[]{:S(2)}, u32[]{:S(2)}) collective-permute-start(bf16[32,32,256]{2,1,0:T(8,128)(2,1)S(1)} %collective-permute-done.2.refs_3_), channel_id=1, source_target_pairs={{0,1},{1,0},{2,3},{3,2},{4,5},{5,4},{6,7},{7,6},{8,9},{9,8},{10,11... | collective-permute-start | bytes 1572872 | tf_op jit(solution)/shard_map/ppermute | solution.py:344
  67.3 33.1 %collective-permute-start.8 = (bf16[512,256]{1,0:T(8,128)(2,1)S(1)}, bf16[512,256]{1,0:T(8,128)(2,1)S(1)}, u32[]{:S(2)}, u32[]{:S(2)}) collective-permute-start(bf16[512,256]{1,0:T(8,128)(2,1)S(1)} %get-tuple-element.54), channel_id=1, source_target_pairs={{0,2},{2,4},{4,6},{6,8},{8,10},{10,12},{12,14},{14,0},{1,15},{3,1}... | collective-permute-start | bytes 786440 | tf_op jit(solution)/shard_map/ppermute | solution.py:354
  70.8 29.6 %collective-permute-start.9 = (bf16[512,256]{1,0:T(8,128)(2,1)S(1)}, bf16[512,256]{1,0:T(8,128)(2,1)S(1)}, u32[]{:S(2)}, u32[]{:S(2)}) collective-permute-start(bf16[512,256]{1,0:T(8,128)(2,1)S(1)} %get-tuple-element.55), channel_id=1, source_target_pairs={{0,4},{2,6},{4,8},{6,10},{8,12},{10,14},{12,0},{14,2},{1,13},{3,15... | collective-permute-start | bytes 786440 | tf_op jit(solution)/shard_map/ppermute | solution.py:354
  79.0 21.5 %collective-permute-start.10 = (bf16[512,256]{1,0:T(8,128)(2,1)S(1)}, bf16[512,256]{1,0:T(8,128)(2,1)S(1)}, u32[]{:S(2)}, u32[]{:S(2)}) collective-permute-start(bf16[512,256]{1,0:T(8,128)(2,1)S(1)} %get-tuple-element.56), channel_id=1, source_target_pairs={{0,6},{2,8},{4,10},{6,12},{8,14},{10,0},{12,2},{14,4},{1,11},{3,13... | collective-permute-start | bytes 786440 | tf_op jit(solution)/shard_map/ppermute | solution.py:354
  80.9 19.6 %collective-permute-start.11 = (bf16[512,128]{1,0:T(8,128)(2,1)S(1)}, bf16[512,128]{1,0:T(8,128)(2,1)S(1)}, u32[]{:S(2)}, u32[]{:S(2)}) collective-permute-start(bf16[512,128]{1,0:T(8,128)(2,1)S(1)} %get-tuple-element.57), channel_id=1, source_target_pairs={{0,8},{2,10},{4,12},{6,14},{8,0},{10,2},{12,4},{14,6},{1,9},{3,11}... | collective-permute-start | bytes 393224 | tf_op jit(solution)/shard_map/ppermute | solution.py:354
  100.5 19.9 %copy-start.7 = (s32[8,128]{1,0:T(8,128)S(1)}, s32[8,128]{1,0:T(8,128)}, u32[]{:S(2)}) copy-start(s32[8,128]{1,0:T(8,128)} %get-tuple-element.67.target) | copy-start | bytes 12292
  100.6 19.7 %copy-start = (bf16[128,2048]{1,0:T(8,128)(2,1)S(1)}, bf16[128,2048]{1,0:T(8,128)(2,1)}, u32[]{:S(2)}) copy-start(bf16[128,2048]{1,0:T(8,128)(2,1)} %cotangent.1) | copy-start | bytes 1572868
  100.6 38.5 %copy-start.1 = (bf16[256,2048]{1,0:T(8,128)(2,1)S(1)}, bf16[256,2048]{1,0:T(8,128)(2,1)}, u32[]{:S(2)}) copy-start(bf16[256,2048]{1,0:T(8,128)(2,1)} %weight.1) | copy-start | bytes 3145732
  100.7 3.4 %collective-permute-start.12 = (bf16[512,128]{1,0:T(8,128)(2,1)S(1)}, bf16[512,128]{1,0:T(8,128)(2,1)S(1)}, u32[]{:S(2)}, u32[]{:S(2)}) collective-permute-start(bf16[512,128]{1,0:T(8,128)(2,1)S(1)} %get-tuple-element.74), channel_id=1, source_target_pairs={{0,1},{1,0},{2,3},{3,2},{4,5},{5,4},{6,7},{7,6},{8,9},{9,8},{10,11... | collective-permute-start | bytes 393224 | tf_op jit(solution)/shard_map/ppermute | solution.py:363
  104.7 15.6 %all-to-all-start.1 = ((bf16[32,16,128]{2,1,0:T(8,128)(2,1)}), bf16[32,16,128]{2,1,0:T(8,128)(2,1)S(1)}, u32[]{:S(2)}, u32[]{:S(2)}) async-start(bf16[32,16,128]{2,1,0:T(8,128)(2,1)} %bitcast.15), calls=%async_computation.1 | async-start | bytes 262144 | tf_op jit(solution)/shard_map/all_to_all | solution.py:365
  121.4 17.8 %copy-start.2 = (bf16[128,256]{1,0:T(8,128)(2,1)S(1)}, bf16[128,256]{1,0:T(8,128)(2,1)}, u32[]{:S(2)}) copy-start(bf16[128,256]{1,0:T(8,128)(2,1)} %gate_pre.1) | copy-start | bytes 196612
  121.4 17.8 %copy-start.3 = (bf16[128,256]{1,0:T(8,128)(2,1)S(1)}, bf16[128,256]{1,0:T(8,128)(2,1)}, u32[]{:S(2)}) copy-start(bf16[128,256]{1,0:T(8,128)(2,1)} %mixer.1) | copy-start | bytes 196612
  121.4 17.8 %copy-start.5 = (bf16[128,128]{1,0:T(8,128)(2,1)S(1)}, bf16[128,128]{1,0:T(8,128)(2,1)}, u32[]{:S(2)}) copy-start(bf16[128,128]{1,0:T(8,128)(2,1)} %read.3) | copy-start | bytes 98308
  121.4 17.8 %copy-start.8 = (f32[4,128]{1,0:T(4,128)S(1)}, f32[4,128]{1,0:T(4,128)}, u32[]{:S(2)}) copy-start(f32[4,128]{1,0:T(4,128)} %logs.1) | copy-start | bytes 6148
  141.0 24.9 %collective-permute-start.13 = (bf16[32,32,128]{2,1,0:T(8,128)(2,1)S(1)}, bf16[32,32,128]{2,1,0:T(8,128)(2,1)S(1)}, u32[]{:S(2)}, u32[]{:S(2)}) collective-permute-start(bf16[32,32,128]{2,1,0:T(8,128)(2,1)S(1)} %get-tuple-element.85), channel_id=1, source_target_pairs={{0,16},{16,32},{32,48},{48,0},{1,17},{17,33},{33,49},{49,1},{2,18}... | collective-permute-start | bytes 786440 | tf_op jit(solution)/shard_map/ppermute | solution.py:379
  143.0 22.9 %collective-permute-start.14 = (bf16[32,32,128]{2,1,0:T(8,128)(2,1)S(1)}, bf16[32,32,128]{2,1,0:T(8,128)(2,1)S(1)}, u32[]{:S(2)}, u32[]{:S(2)}) collective-permute-start(bf16[32,32,128]{2,1,0:T(8,128)(2,1)S(1)} %get-tuple-element.86), channel_id=1, source_target_pairs={{0,32},{16,48},{32,0},{48,16},{1,33},{17,49},{33,1},{49,17},{2,34}... | collective-permute-start | bytes 786440 | tf_op jit(solution)/shard_map/ppermute | solution.py:379
  147.6 18.3 %collective-permute-start.15 = (bf16[32,32,128]{2,1,0:T(8,128)(2,1)S(1)}, bf16[32,32,128]{2,1,0:T(8,128)(2,1)S(1)}, u32[]{:S(2)}, u32[]{:S(2)}) collective-permute-start(bf16[32,32,128]{2,1,0:T(8,128)(2,1)S(1)} %get-tuple-element.87), channel_id=1, source_target_pairs={{0,48},{16,0},{32,16},{48,32},{1,49},{17,1},{33,17},{49,33},{2,50}... | collective-permute-start | bytes 786440 | tf_op jit(solution)/shard_map/ppermute | solution.py:379
  150.7 4.7 %copy-start.4 = (bf16[128,256]{1,0:T(8,128)(2,1)S(1)}, bf16[128,256]{1,0:T(8,128)(2,1)}, u32[]{:S(2)}) copy-start(bf16[128,256]{1,0:T(8,128)(2,1)} %values.3) | copy-start | bytes 196612
  150.7 4.7 %copy-start.6 = (bf16[128,128]{1,0:T(8,128)(2,1)S(1)}, bf16[128,128]{1,0:T(8,128)(2,1)}, u32[]{:S(2)}) copy-start(bf16[128,128]{1,0:T(8,128)(2,1)} %write.3) | copy-start | bytes 98308
  150.7 4.7 %copy-start.9 = (f32[1,4,64,128]{3,2,1,0:T(8,128)S(1)}, f32[1,4,64,128]{3,2,1,0:T(8,128)}, u32[]{:S(2)}) copy-start(f32[1,4,64,128]{3,2,1,0:T(8,128)} %param.29) | copy-start | bytes 393220
  150.7 15.2 %all-to-all-start.2 = ((bf16[32,16,128]{2,1,0:T(8,128)(2,1)}), bf16[32,16,128]{2,1,0:T(8,128)(2,1)S(1)}, u32[]{:S(2)}, u32[]{:S(2)}) async-start(bf16[32,16,128]{2,1,0:T(8,128)(2,1)} %get-tuple-element.75), calls=%async_computation.2 | async-start | bytes 262144 | tf_op jit(solution)/shard_map/all_to_all | solution.py:377

commit v9 on v8

--- a/solution.py
+++ b/solution.py
@@ -143,17 +143,30 @@
     return jnp.concatenate([own[0, :, at], other[0, :, at], own[1, :, at], other[1, :, at]], axis=0)
 
 
-def expert_kernel(where, *refs):
-    chunks = refs[:8]
-    own, other, near, mid, far, last, home, g_gate, g_up, g_hid = refs[8:]
+def chunk_products(chunk, position, own, other):
+    at = pl.ds(pl.multiple_of(position * WIDE, WIDE), WIDE)
+    toks, cots = row_blocks(chunk)
+    down = jnp.concatenate([own[2, :, at], other[2, :, at]], axis=0)
+    return mm_nt(toks, gate_rows(own, other, at)), mm_nt(cots, down)
+
+
+def early_kernel(where, *refs):
+    chunks = refs[:7]
+    own, other, pre, grad_hidden = refs[7:]
     ids = chunk_ids(where[0])
-    pre = jnp.zeros((ROWS, 4 * FF), F32)
-    grad_hidden = jnp.zeros((ROWS, 2 * FF), F32)
-    for k in range(8):
-        at = pl.ds(pl.multiple_of(ids[k] * WIDE, WIDE), WIDE)
-        toks, cots = row_blocks(chunks[k])
-        pre = pre + mm_nt(toks, gate_rows(own, other, at))
-        grad_hidden = grad_hidden + mm_nt(cots, jnp.concatenate([own[2, :, at], other[2, :, at]], axis=0))
+    first, second = chunk_products(chunks[0], ids[0], own, other)
+    for k in range(1, 7):
+        more = chunk_products(chunks[k], ids[k], own, other)
+        first, second = first + more[0], second + more[1]
+    pre[...] = first
+    grad_hidden[...] = second
+
+
+def expert_kernel(where, chunk, early_pre, early_hidden, own, other, *outs):
+    near, mid, far, last, home, g_gate, g_up, g_hid = outs
+    more = chunk_products(chunk, chunk_ids(where[0])[7], own, other)
+    pre = early_pre[...] + more[0]
+    grad_hidden = early_hidden[...] + more[1]
     pre_gate = pre[:, : 2 * FF]
     pre_up = pre[:, 2 * FF :]
     logistic = 1.0 / (1.0 + jnp.exp(-pre_gate))
@@ -197,6 +210,10 @@
     top = where[0] & 1 == 0
     keep[...] = jnp.where(top, first, second) + last[...].astype(F32) + home[...].astype(F32)
     give[...] = jnp.where(top, second, first).astype(BF)
+
+
+def join_kernel(keep, taken, out):
+    out[...] = (keep[...] + taken[...].astype(F32)).astype(BF).reshape(EXP, CAP, TOK)
 
 
 def combine_kernel(where, target, rows, cotangent, out, cot, arrived):
@@ -346,9 +363,12 @@
     chunks = (c0, c1, c2, c3, c4, c5, c6, c7)
     grad = shape((ROWS, 2 * FF), BF)
     full, thin = shape((ROWS, WIDE), BF), shape((ROWS, TOK), BF)
+    early = call(
+        early_kernel, (shape((ROWS, 4 * FF), F32), shape((ROWS, 2 * FF), F32)),
+        [smem()] + [vmem()] * 9, (slot, *chunks[:7], own, other), flops=10**8)
     *parts, home, g_gate, g_up, g_hid = call(
         expert_kernel, (full, full, full, thin, thin, grad, grad, grad),
-        [smem()] + [vmem()] * 10, (slot, *chunks, own, other))
+        [smem()] + [vmem()] * 5, (slot, c7, *early, own, other))
     pieces = []
     for k in range(4):
         pieces.append(lax.ppermute(parts[k], TP, rings[k]))
@@ -361,7 +381,7 @@
         fold_kernel, (shape((ROWS, TOK), F32), thin),
         [smem()] + [vmem()] * 5, (slot, *pieces, home))
     taken = lax.ppermute(give, "core", swap)
-    summed = (keep + taken.astype(F32)).astype(BF).reshape(EXP, CAP, TOK)
+    summed = call(join_kernel, shape((EXP, CAP, TOK), BF), [vmem()] * 2, (keep, taken))
     back = lax.all_to_all(summed, SP, 0, 0, tiled=True)
     d_input = combine(slot, target, back, cotangent)
     whole = lax.all_gather(d_input, TP, axis=0, tiled=True)

time: 185 us -> 181 us (0.978)
  waiting for transfers between devices: 44.7 us -> 40.5 us
    ppermute x1, waiting for transfers between devices: 3.7 us -> 0.67 us  [step(): c3 = lax.ppermute(c1, TP, ring)]
    ppermute x1, waiting for transfers between devices: 1.84 us -> 3.7 us  [step(): c4 = lax.ppermute(c2, TP, ring)]
    ppermute x1, waiting for transfers between devices: 1.85 us -> 0.01 us  [step(): c6 = lax.ppermute(c3, 'core', swap)]
    pallas_call x7 -> x9, Pallas kernels: 8.34 us -> 9.26 us  [call(): pl.pallas_call(kernel, out_shape=outs, in_specs=specs, out_specs=jax.tree...]
  transfers between devices with their start and end apart: 18 -> 18, of which waited for: 8 -> 9; matrix products, arithmetic and copies ran while one was open for 0% -> 0% of each run, Pallas kernels for 2% -> 2%
where the time goes in v9:
time: 181 us; the launch traced here: 180 us
  blocking collectives  66.9 us (37%)
  starting transfers between devices  58.8 us (32%)
  waiting for transfers between devices  40.5 us (22%)
  Pallas kernels  12.5 us (7%)
    all_to_all x1, blocking collectives, step(): c0 = lax.all_to_all(buf, SP, 0, 0, tiled=True)  31.1 us
    all_gather x1, blocking collectives, step(): whole = lax.all_gather(d_input, TP, axis=0, tiled=True)  18.8 us
    ppermute x4, starting transfers between devices, step(): pieces.append(lax.ppermute(parts[k], TP, rings[k]))  17.6 us
    all_to_all x1, blocking collectives, step(): second = lax.all_to_all(states, SP, 0, 0, tiled=True)  17.1 us
    ppermute x4, waiting for transfers between devices, step(): pieces.append(lax.ppermute(parts[k], TP, rings[k]))  12.4 us
    all_to_all x1, waiting for transfers between devices, step(): back = lax.all_to_all(summed, SP, 0, 0, tiled=True)  10.9 us
    ppermute x3, starting transfers between devices, step(): lax.ppermute(shares[k], 'x', [(i, (i + k) % 4) for i in range(4)])  9.61 us
    pallas_call x9, Pallas kernels, call(): pl.pallas_call(kernel, out_shape=outs, in_specs=specs, out_specs=jax.tree...  9.26 us
  transfers between devices with their start and end apart: 18, of which 9 were waited for; matrix products, arithmetic and copies ran while one was open for 0% of the time, Pallas kernels for 2%

profile of v9, /device:TPU:8, one launch (start us, length us, event | category | flops | bytes accessed | tf_op | source)
XLA Modules:
  0.0 179.9 jit_solution(14282179721879273203)
XLA Ops:
  0.6 2.2 %prepare.1 = (bf16[32,32,256]{2,1,0:T(8,128)(2,1)}, s32[8,128]{1,0:T(8,128)}) custom-call(s32[1]{0:T(128)} %bitcast.where, s32[2,128]{1,0:T(2,128)} %bitcast.25, f32[2,128]{1,0:T(2,128)} %bitcast.26, bf16[128,2048]{1,0:T(8,128)(2,1)} %mix.1, bf16[128,2048]{1,0:T(8,128)(2,1)} %cotangent.1), custom_call_target="tpu_custom_call" | custom-call | tf_op jit(solution)/shard_map/prepare/pallas_call | solution.py:112
  2.9 31.1 %all_to_all.20.refs_0_ = bf16[32,32,256]{2,1,0:T(8,128)(2,1)S(1)} all-to-all(bf16[32,32,256]{2,1,0:T(8,128)(2,1)} %get-tuple-element.53), channel_id=1, replica_groups=mesh['z'=8,'x'=4,'y'=8,'core'=2] {'z','x'}, dimensions={0} | all-to-all | bytes 1048576 | tf_op jit(solution)/shard_map/all_to_all | solution.py:354
  34.0 1.9 %collective-permute-start.3 = (bf16[32,32,256]{2,1,0:T(8,128)(2,1)S(1)}, bf16[32,32,256]{2,1,0:T(8,128)(2,1)S(1)}, u32[]{:S(2)}, u32[]{:S(2)}) collective-permute-start(bf16[32,32,256]{2,1,0:T(8,128)(2,1)S(1)} %all_to_all.20.refs_0_), channel_id=1, source_target_pairs={{0,1},{1,0},{2,3},{3,2},{4,5},{5,4},{6,7},{7,6},{8,9},{9,8},{10,11... | collective-permute-start | bytes 1572872 | tf_op jit(solution)/shard_map/ppermute | solution.py:356
  35.9 3.5 %collective-permute-start = (bf16[32,32,256]{2,1,0:T(8,128)(2,1)S(1)}, bf16[32,32,256]{2,1,0:T(8,128)(2,1)S(1)}, u32[]{:S(2)}, u32[]{:S(2)}) collective-permute-start(bf16[32,32,256]{2,1,0:T(8,128)(2,1)S(1)} %all_to_all.20.refs_0_), channel_id=1, source_target_pairs={{0,2},{2,4},{4,6},{6,8},{8,10},{10,12},{12,14},{14,0},{1,15},{3,1}... | collective-permute-start | bytes 1572872 | tf_op jit(solution)/shard_map/ppermute | solution.py:355
  39.5 1.9 %collective-permute-start.5 = (bf16[3,64,2048]{2,1,0:T(8,128)(2,1)S(1)}, bf16[3,64,2048]{2,1,0:T(8,128)(2,1)S(1)}, u32[]{:S(2)}, u32[]{:S(2)}) collective-permute-start(bf16[3,64,2048]{2,1,0:T(8,128)(2,1)S(1)} %pad_maximum_fusion.refs_7_.own), channel_id=1, source_target_pairs={{0,1},{1,0},{2,3},{3,2},{4,5},{5,4},{6,7},{7,6},{8,9},{9,8},{10,11... | collective-permute-start | bytes 2359304 | tf_op jit(solution)/shard_map/ppermute | solution.py:352
  41.4 3.5 %collective-permute-start.4 = (bf16[32,32,256]{2,1,0:T(8,128)(2,1)S(1)}, bf16[32,32,256]{2,1,0:T(8,128)(2,1)S(1)}, u32[]{:S(2)}, u32[]{:S(2)}) collective-permute-start(bf16[32,32,256]{2,1,0:T(8,128)(2,1)S(1)} %collective-permute-done.3.refs_1_), channel_id=1, source_target_pairs={{0,2},{2,4},{4,6},{6,8},{8,10},{10,12},{12,14},{14,0},{1,15},{3,1}... | collective-permute-start | bytes 1572872 | tf_op jit(solution)/shard_map/ppermute | solution.py:357
  44.9 2.0 %collective-permute-done.refs_2_ = bf16[32,32,256]{2,1,0:T(8,128)(2,1)S(1)} collective-permute-done((bf16[32,32,256]{2,1,0:T(8,128)(2,1)S(1)}, bf16[32,32,256]{2,1,0:T(8,128)(2,1)S(1)}, u32[]{:S(2)}, u32[]{:S(2)}) %collective-permute-start) | collective-permute-done | bytes 524320 | tf_op jit(solution)/shard_map/ppermute | solution.py:355
  47.0 3.5 %collective-permute-start.1 = (bf16[32,32,256]{2,1,0:T(8,128)(2,1)S(1)}, bf16[32,32,256]{2,1,0:T(8,128)(2,1)S(1)}, u32[]{:S(2)}, u32[]{:S(2)}) collective-permute-start(bf16[32,32,256]{2,1,0:T(8,128)(2,1)S(1)} %collective-permute-done.refs_2_), channel_id=1, source_target_pairs={{0,2},{2,4},{4,6},{6,8},{8,10},{10,12},{12,14},{14,0},{1,15},{3,1}... | collective-permute-start | bytes 1572872 | tf_op jit(solution)/shard_map/ppermute | solution.py:358
  50.5 1.9 %collective-permute-start.6 = (bf16[32,32,256]{2,1,0:T(8,128)(2,1)S(1)}, bf16[32,32,256]{2,1,0:T(8,128)(2,1)S(1)}, u32[]{:S(2)}, u32[]{:S(2)}) collective-permute-start(bf16[32,32,256]{2,1,0:T(8,128)(2,1)S(1)} %collective-permute-done.refs_2_), channel_id=1, source_target_pairs={{0,1},{1,0},{2,3},{3,2},{4,5},{5,4},{6,7},{7,6},{8,9},{9,8},{10,11... | collective-permute-start | bytes 1572872 | tf_op jit(solution)/shard_map/ppermute | solution.py:360
  53.1 1.9 %collective-permute-start.7 = (bf16[32,32,256]{2,1,0:T(8,128)(2,1)S(1)}, bf16[32,32,256]{2,1,0:T(8,128)(2,1)S(1)}, u32[]{:S(2)}, u32[]{:S(2)}) collective-permute-start(bf16[32,32,256]{2,1,0:T(8,128)(2,1)S(1)} %collective-permute-done.4.refs_3_), channel_id=1, source_target_pairs={{0,1},{1,0},{2,3},{3,2},{4,5},{5,4},{6,7},{7,6},{8,9},{9,8},{10,11... | collective-permute-start | bytes 1572872 | tf_op jit(solution)/shard_map/ppermute | solution.py:361
  55.0 3.7 %collective-permute-done.1.refs_4_ = bf16[32,32,256]{2,1,0:T(8,128)(2,1)S(1)} collective-permute-done((bf16[32,32,256]{2,1,0:T(8,128)(2,1)S(1)}, bf16[32,32,256]{2,1,0:T(8,128)(2,1)S(1)}, u32[]{:S(2)}, u32[]{:S(2)}) %collective-permute-start.1) | collective-permute-done | bytes 524320 | tf_op jit(solution)/shard_map/ppermute | solution.py:358
  58.7 1.9 %collective-permute-start.2 = (bf16[32,32,256]{2,1,0:T(8,128)(2,1)S(1)}, bf16[32,32,256]{2,1,0:T(8,128)(2,1)S(1)}, u32[]{:S(2)}, u32[]{:S(2)}) collective-permute-start(bf16[32,32,256]{2,1,0:T(8,128)(2,1)S(1)} %collective-permute-done.1.refs_4_), channel_id=1, source_target_pairs={{0,1},{1,0},{2,3},{3,2},{4,5},{5,4},{6,7},{7,6},{8,9},{9,8},{10,11... | collective-permute-start | bytes 1572872 | tf_op jit(solution)/shard_map/ppermute | solution.py:362
  63.4 3.2 %collective-permute-start.8 = (bf16[512,256]{1,0:T(8,128)(2,1)S(1)}, bf16[512,256]{1,0:T(8,128)(2,1)S(1)}, u32[]{:S(2)}, u32[]{:S(2)}) collective-permute-start(bf16[512,256]{1,0:T(8,128)(2,1)S(1)} %get-tuple-element.58), channel_id=1, source_target_pairs={{0,2},{2,4},{4,6},{6,8},{8,10},{10,12},{12,14},{14,0},{1,15},{3,1}... | collective-permute-start | bytes 786440 | tf_op jit(solution)/shard_map/ppermute | solution.py:374
  66.6 7.7 %collective-permute-start.9 = (bf16[512,256]{1,0:T(8,128)(2,1)S(1)}, bf16[512,256]{1,0:T(8,128)(2,1)S(1)}, u32[]{:S(2)}, u32[]{:S(2)}) collective-permute-start(bf16[512,256]{1,0:T(8,128)(2,1)S(1)} %get-tuple-element.59), channel_id=1, source_target_pairs={{0,4},{2,6},{4,8},{6,10},{8,12},{10,14},{12,0},{14,2},{1,13},{3,15... | collective-permute-start | bytes 786440 | tf_op jit(solution)/shard_map/ppermute | solution.py:374
  74.4 1.9 %collective-permute-start.10 = (bf16[512,256]{1,0:T(8,128)(2,1)S(1)}, bf16[512,256]{1,0:T(8,128)(2,1)S(1)}, u32[]{:S(2)}, u32[]{:S(2)}) collective-permute-start(bf16[512,256]{1,0:T(8,128)(2,1)S(1)} %get-tuple-element.60), channel_id=1, source_target_pairs={{0,6},{2,8},{4,10},{6,12},{8,14},{10,0},{12,2},{14,4},{1,11},{3,13... | collective-permute-start | bytes 786440 | tf_op jit(solution)/shard_map/ppermute | solution.py:374
  76.3 4.7 %collective-permute-start.11 = (bf16[512,128]{1,0:T(8,128)(2,1)S(1)}, bf16[512,128]{1,0:T(8,128)(2,1)S(1)}, u32[]{:S(2)}, u32[]{:S(2)}) collective-permute-start(bf16[512,128]{1,0:T(8,128)(2,1)S(1)} %get-tuple-element.61), channel_id=1, source_target_pairs={{0,8},{2,10},{4,12},{6,14},{8,0},{10,2},{12,4},{14,6},{1,9},{3,11}... | collective-permute-start | bytes 393224 | tf_op jit(solution)/shard_map/ppermute | solution.py:374
  81.0 1.7 shard_map.216
  82.7 8.1 %collective-permute-done.11.last = bf16[512,128]{1,0:T(8,128)(2,1)S(1)} collective-permute-done((bf16[512,128]{1,0:T(8,128)(2,1)S(1)}, bf16[512,128]{1,0:T(8,128)(2,1)S(1)}, u32[]{:S(2)}, u32[]{:S(2)}) %collective-permute-start.11) | collective-permute-done | bytes 131104 | tf_op jit(solution)/shard_map/ppermute | solution.py:374
  90.8 4.3 %collective-permute-done.10.far = bf16[512,256]{1,0:T(8,128)(2,1)S(1)} collective-permute-done((bf16[512,256]{1,0:T(8,128)(2,1)S(1)}, bf16[512,256]{1,0:T(8,128)(2,1)S(1)}, u32[]{:S(2)}, u32[]{:S(2)}) %collective-permute-start.10) | collective-permute-done | bytes 262176 | tf_op jit(solution)/shard_map/ppermute | solution.py:374
  95.2 2.3 %collective-permute-start.12 = (bf16[512,128]{1,0:T(8,128)(2,1)S(1)}, bf16[512,128]{1,0:T(8,128)(2,1)S(1)}, u32[]{:S(2)}, u32[]{:S(2)}) collective-permute-start(bf16[512,128]{1,0:T(8,128)(2,1)S(1)} %get-tuple-element.78), channel_id=1, source_target_pairs={{0,1},{1,0},{2,3},{3,2},{4,5},{5,4},{6,7},{7,6},{8,9},{9,8},{10,11... | collective-permute-start | bytes 393224 | tf_op jit(solution)/shard_map/ppermute | solution.py:383
  99.3 4.6 %all-to-all-start.1 = ((bf16[32,16,128]{2,1,0:T(8,128)(2,1)}), bf16[32,16,128]{2,1,0:T(8,128)(2,1)S(1)}, u32[]{:S(2)}, u32[]{:S(2)}) async-start(bf16[32,16,128]{2,1,0:T(8,128)(2,1)} %shard_map.218), calls=%async_computation.1 | async-start | bytes 262144 | tf_op jit(solution)/shard_map/all_to_all | solution.py:385
  104.0 10.9 %all-to-all-done.1.rows = bf16[32,16,128]{2,1,0:T(8,128)(2,1)S(1)} async-done(((bf16[32,16,128]{2,1,0:T(8,128)(2,1)}), bf16[32,16,128]{2,1,0:T(8,128)(2,1)S(1)}, u32[]{:S(2)}, u32[]{:S(2)}) %all-to-all-start.1) | async-done | bytes 131104 | tf_op jit(solution)/shard_map/all_to_all | solution.py:385
  115.9 18.8 %all_gather.3.gathered = bf16[2048,128]{1,0:T(8,128)(2,1)S(1)} all-gather(bf16[128,128]{1,0:T(8,128)(2,1)} %combine.1), channel_id=1, replica_groups=mesh['z'=8,'x'=4,'y'=8,'core'=2] {'y','core'}, dimensions={0}, use_global_device_ids=true | all-gather | bytes 557056 | tf_op jit(solution)/shard_map/all_gather | solution.py:387
  134.7 1.8 %shard_map.219 = (bf16[128,256]{1,0:T(8,128)(2,1)}, f32[128,256]{1,0:T(8,128)S(1)}, f32[8,128]{1,0:T(8,128)S(1)}, bf16[32,16,128]{2,1,0:T(8,128)(2,1)}, bf16[32,...) custom-call(s32[1]{0:T(128)} %bitcast.14.spot, ...), custom_call_target="tpu_custom_call" | custom-call | tf_op jit(solution)/shard_map/pallas_call | solution.py:75
  136.5 2.0 %collective-permute-start.13 = (bf16[32,32,128]{2,1,0:T(8,128)(2,1)S(1)}, bf16[32,32,128]{2,1,0:T(8,128)(2,1)S(1)}, u32[]{:S(2)}, u32[]{:S(2)}) collective-permute-start(bf16[32,32,128]{2,1,0:T(8,128)(2,1)S(1)} %get-tuple-element.89), channel_id=1, source_target_pairs={{0,16},{16,32},{32,48},{48,0},{1,17},{17,33},{33,49},{49,1},{2,18}... | collective-permute-start | bytes 786440 | tf_op jit(solution)/shard_map/ppermute | solution.py:399
  138.5 4.6 %collective-permute-start.14 = (bf16[32,32,128]{2,1,0:T(8,128)(2,1)S(1)}, bf16[32,32,128]{2,1,0:T(8,128)(2,1)S(1)}, u32[]{:S(2)}, u32[]{:S(2)}) collective-permute-start(bf16[32,32,128]{2,1,0:T(8,128)(2,1)S(1)} %get-tuple-element.90), channel_id=1, source_target_pairs={{0,32},{16,48},{32,0},{48,16},{1,33},{17,49},{33,1},{49,17},{2,34}... | collective-permute-start | bytes 786440 | tf_op jit(solution)/shard_map/ppermute | solution.py:399
  143.1 3.0 %collective-permute-start.15 = (bf16[32,32,128]{2,1,0:T(8,128)(2,1)S(1)}, bf16[32,32,128]{2,1,0:T(8,128)(2,1)S(1)}, u32[]{:S(2)}, u32[]{:S(2)}) collective-permute-start(bf16[32,32,128]{2,1,0:T(8,128)(2,1)S(1)} %get-tuple-element.91), channel_id=1, source_target_pairs={{0,48},{16,0},{32,16},{48,32},{1,49},{17,1},{33,17},{49,33},{2,50}... | collective-permute-start | bytes 786440 | tf_op jit(solution)/shard_map/ppermute | solution.py:399
  146.2 4.6 %all-to-all-start.2 = ((bf16[32,16,128]{2,1,0:T(8,128)(2,1)}), bf16[32,16,128]{2,1,0:T(8,128)(2,1)S(1)}, u32[]{:S(2)}, u32[]{:S(2)}) async-start(bf16[32,16,128]{2,1,0:T(8,128)(2,1)} %get-tuple-element.79), calls=%async_computation.2 | async-start | bytes 262144 | tf_op jit(solution)/shard_map/all_to_all | solution.py:397
  150.8 1.5 shard_map.220
  152.3 9.0 %all-to-all-done.2.received = bf16[32,16,128]{2,1,0:T(8,128)(2,1)S(1)} async-done(((bf16[32,16,128]{2,1,0:T(8,128)(2,1)}), bf16[32,16,128]{2,1,0:T(8,128)(2,1)S(1)}, u32[]{:S(2)}, u32[]{:S(2)}) %all-to-all-start.2) | async-done | bytes 131104 | tf_op jit(solution)/shard_map/all_to_all | solution.py:397
  161.6 17.1 %all_to_all.21.second = bf16[32,48,128]{2,1,0:T(8,128)(2,1)S(1)} all-to-all(bf16[32,48,128]{2,1,0:T(8,128)(2,1)S(1)} %shard_map.221), channel_id=1, replica_groups=mesh['z'=8,'x'=4,'y'=8,'core'=2] {'z','x'}, dimensions={0} | all-to-all | bytes 786432 | tf_op jit(solution)/shard_map/all_to_all | solution.py:406
  178.7 1.2 shard_map.222
  (45 shorter events, 6.7 us)
Async XLA Ops:
  2.9 36.5 %copy-start.10 = (bf16[1,64,2048]{2,1,0:T(8,128)(2,1)S(1)}, bf16[1,64,2048]{2,1,0:T(8,128)(2,1)}, u32[]{:S(2)}) copy-start(bf16[1,64,2048]{2,1,0:T(8,128)(2,1)} %param.21) | copy-start | bytes 786436
  2.9 36.5 %copy-start.11 = (bf16[1,2048,64]{1,2,0:T(8,128)(2,1)S(1)}, bf16[1,2048,64]{1,2,0:T(8,128)(2,1)}, u32[]{:S(2)}) copy-start(bf16[1,2048,64]{1,2,0:T(8,128)(2,1)} %param.20) | copy-start | bytes 786436
  2.9 36.5 %copy-start.12 = (bf16[1,2048,64]{1,2,0:T(8,128)(2,1)S(1)}, bf16[1,2048,64]{1,2,0:T(8,128)(2,1)}, u32[]{:S(2)}) copy-start(bf16[1,2048,64]{1,2,0:T(8,128)(2,1)} %param.19) | copy-start | bytes 786436
  34.0 7.5 %collective-permute-start.3 = (bf16[32,32,256]{2,1,0:T(8,128)(2,1)S(1)}, bf16[32,32,256]{2,1,0:T(8,128)(2,1)S(1)}, u32[]{:S(2)}, u32[]{:S(2)}) collective-permute-start(bf16[32,32,256]{2,1,0:T(8,128)(2,1)S(1)} %all_to_all.20.refs_0_), channel_id=1, source_target_pairs={{0,1},{1,0},{2,3},{3,2},{4,5},{5,4},{6,7},{7,6},{8,9},{9,8},{10,11... | collective-permute-start | bytes 1572872 | tf_op jit(solution)/shard_map/ppermute | solution.py:356
  35.9 11.1 %collective-permute-start = (bf16[32,32,256]{2,1,0:T(8,128)(2,1)S(1)}, bf16[32,32,256]{2,1,0:T(8,128)(2,1)S(1)}, u32[]{:S(2)}, u32[]{:S(2)}) collective-permute-start(bf16[32,32,256]{2,1,0:T(8,128)(2,1)S(1)} %all_to_all.20.refs_0_), channel_id=1, source_target_pairs={{0,2},{2,4},{4,6},{6,8},{8,10},{10,12},{12,14},{14,0},{1,15},{3,1}... | collective-permute-start | bytes 1572872 | tf_op jit(solution)/shard_map/ppermute | solution.py:355
  39.5 10.9 %collective-permute-start.5 = (bf16[3,64,2048]{2,1,0:T(8,128)(2,1)S(1)}, bf16[3,64,2048]{2,1,0:T(8,128)(2,1)S(1)}, u32[]{:S(2)}, u32[]{:S(2)}) collective-permute-start(bf16[3,64,2048]{2,1,0:T(8,128)(2,1)S(1)} %pad_maximum_fusion.refs_7_.own), channel_id=1, source_target_pairs={{0,1},{1,0},{2,3},{3,2},{4,5},{5,4},{6,7},{7,6},{8,9},{9,8},{10,11... | collective-permute-start | bytes 2359304 | tf_op jit(solution)/shard_map/ppermute | solution.py:352
  41.4 11.6 %collective-permute-start.4 = (bf16[32,32,256]{2,1,0:T(8,128)(2,1)S(1)}, bf16[32,32,256]{2,1,0:T(8,128)(2,1)S(1)}, u32[]{:S(2)}, u32[]{:S(2)}) collective-permute-start(bf16[32,32,256]{2,1,0:T(8,128)(2,1)S(1)} %collective-permute-done.3.refs_1_), channel_id=1, source_target_pairs={{0,2},{2,4},{4,6},{6,8},{8,10},{10,12},{12,14},{14,0},{1,15},{3,1}... | collective-permute-start | bytes 1572872 | tf_op jit(solution)/shard_map/ppermute | solution.py:357
  47.0 11.7 %collective-permute-start.1 = (bf16[32,32,256]{2,1,0:T(8,128)(2,1)S(1)}, bf16[32,32,256]{2,1,0:T(8,128)(2,1)S(1)}, u32[]{:S(2)}, u32[]{:S(2)}) collective-permute-start(bf16[32,32,256]{2,1,0:T(8,128)(2,1)S(1)} %collective-permute-done.refs_2_), channel_id=1, source_target_pairs={{0,2},{2,4},{4,6},{6,8},{8,10},{10,12},{12,14},{14,0},{1,15},{3,1}... | collective-permute-start | bytes 1572872 | tf_op jit(solution)/shard_map/ppermute | solution.py:358
  50.5 10.1 %collective-permute-start.6 = (bf16[32,32,256]{2,1,0:T(8,128)(2,1)S(1)}, bf16[32,32,256]{2,1,0:T(8,128)(2,1)S(1)}, u32[]{:S(2)}, u32[]{:S(2)}) collective-permute-start(bf16[32,32,256]{2,1,0:T(8,128)(2,1)S(1)} %collective-permute-done.refs_2_), channel_id=1, source_target_pairs={{0,1},{1,0},{2,3},{3,2},{4,5},{5,4},{6,7},{7,6},{8,9},{9,8},{10,11... | collective-permute-start | bytes 1572872 | tf_op jit(solution)/shard_map/ppermute | solution.py:360
  53.1 7.5 %collective-permute-start.7 = (bf16[32,32,256]{2,1,0:T(8,128)(2,1)S(1)}, bf16[32,32,256]{2,1,0:T(8,128)(2,1)S(1)}, u32[]{:S(2)}, u32[]{:S(2)}) collective-permute-start(bf16[32,32,256]{2,1,0:T(8,128)(2,1)S(1)} %collective-permute-done.4.refs_3_), channel_id=1, source_target_pairs={{0,1},{1,0},{2,3},{3,2},{4,5},{5,4},{6,7},{7,6},{8,9},{9,8},{10,11... | collective-permute-start | bytes 1572872 | tf_op jit(solution)/shard_map/ppermute | solution.py:361
  58.7 3.8 %collective-permute-start.2 = (bf16[32,32,256]{2,1,0:T(8,128)(2,1)S(1)}, bf16[32,32,256]{2,1,0:T(8,128)(2,1)S(1)}, u32[]{:S(2)}, u32[]{:S(2)}) collective-permute-start(bf16[32,32,256]{2,1,0:T(8,128)(2,1)S(1)} %collective-permute-done.1.refs_4_), channel_id=1, source_target_pairs={{0,1},{1,0},{2,3},{3,2},{4,5},{5,4},{6,7},{7,6},{8,9},{9,8},{10,11... | collective-permute-start | bytes 1572872 | tf_op jit(solution)/shard_map/ppermute | solution.py:362
  63.4 27.4 %collective-permute-start.8 = (bf16[512,256]{1,0:T(8,128)(2,1)S(1)}, bf16[512,256]{1,0:T(8,128)(2,1)S(1)}, u32[]{:S(2)}, u32[]{:S(2)}) collective-permute-start(bf16[512,256]{1,0:T(8,128)(2,1)S(1)} %get-tuple-element.58), channel_id=1, source_target_pairs={{0,2},{2,4},{4,6},{6,8},{8,10},{10,12},{12,14},{14,0},{1,15},{3,1}... | collective-permute-start | bytes 786440 | tf_op jit(solution)/shard_map/ppermute | solution.py:374
  66.6 24.2 %collective-permute-start.9 = (bf16[512,256]{1,0:T(8,128)(2,1)S(1)}, bf16[512,256]{1,0:T(8,128)(2,1)S(1)}, u32[]{:S(2)}, u32[]{:S(2)}) collective-permute-start(bf16[512,256]{1,0:T(8,128)(2,1)S(1)} %get-tuple-element.59), channel_id=1, source_target_pairs={{0,4},{2,6},{4,8},{6,10},{8,12},{10,14},{12,0},{14,2},{1,13},{3,15... | collective-permute-start | bytes 786440 | tf_op jit(solution)/shard_map/ppermute | solution.py:374
  74.4 20.7 %collective-permute-start.10 = (bf16[512,256]{1,0:T(8,128)(2,1)S(1)}, bf16[512,256]{1,0:T(8,128)(2,1)S(1)}, u32[]{:S(2)}, u32[]{:S(2)}) collective-permute-start(bf16[512,256]{1,0:T(8,128)(2,1)S(1)} %get-tuple-element.60), channel_id=1, source_target_pairs={{0,6},{2,8},{4,10},{6,12},{8,14},{10,0},{12,2},{14,4},{1,11},{3,13... | collective-permute-start | bytes 786440 | tf_op jit(solution)/shard_map/ppermute | solution.py:374
  76.3 14.5 %collective-permute-start.11 = (bf16[512,128]{1,0:T(8,128)(2,1)S(1)}, bf16[512,128]{1,0:T(8,128)(2,1)S(1)}, u32[]{:S(2)}, u32[]{:S(2)}) collective-permute-start(bf16[512,128]{1,0:T(8,128)(2,1)S(1)} %get-tuple-element.61), channel_id=1, source_target_pairs={{0,8},{2,10},{4,12},{6,14},{8,0},{10,2},{12,4},{14,6},{1,9},{3,11}... | collective-permute-start | bytes 393224 | tf_op jit(solution)/shard_map/ppermute | solution.py:374
  95.1 19.8 %copy-start.7 = (s32[8,128]{1,0:T(8,128)S(1)}, s32[8,128]{1,0:T(8,128)}, u32[]{:S(2)}) copy-start(s32[8,128]{1,0:T(8,128)} %get-tuple-element.71.target) | copy-start | bytes 12292
  95.2 19.6 %copy-start = (bf16[128,2048]{1,0:T(8,128)(2,1)S(1)}, bf16[128,2048]{1,0:T(8,128)(2,1)}, u32[]{:S(2)}) copy-start(bf16[128,2048]{1,0:T(8,128)(2,1)} %cotangent.1) | copy-start | bytes 1572868
  95.2 39.4 %copy-start.1 = (bf16[256,2048]{1,0:T(8,128)(2,1)S(1)}, bf16[256,2048]{1,0:T(8,128)(2,1)}, u32[]{:S(2)}) copy-start(bf16[256,2048]{1,0:T(8,128)(2,1)} %weight.1) | copy-start | bytes 3145732
  95.2 3.4 %collective-permute-start.12 = (bf16[512,128]{1,0:T(8,128)(2,1)S(1)}, bf16[512,128]{1,0:T(8,128)(2,1)S(1)}, u32[]{:S(2)}, u32[]{:S(2)}) collective-permute-start(bf16[512,128]{1,0:T(8,128)(2,1)S(1)} %get-tuple-element.78), channel_id=1, source_target_pairs={{0,1},{1,0},{2,3},{3,2},{4,5},{5,4},{6,7},{7,6},{8,9},{9,8},{10,11... | collective-permute-start | bytes 393224 | tf_op jit(solution)/shard_map/ppermute | solution.py:383
  99.3 15.5 %all-to-all-start.1 = ((bf16[32,16,128]{2,1,0:T(8,128)(2,1)}), bf16[32,16,128]{2,1,0:T(8,128)(2,1)S(1)}, u32[]{:S(2)}, u32[]{:S(2)}) async-start(bf16[32,16,128]{2,1,0:T(8,128)(2,1)} %shard_map.218), calls=%async_computation.1 | async-start | bytes 262144 | tf_op jit(solution)/shard_map/all_to_all | solution.py:385
  115.8 18.8 %copy-start.2 = (bf16[128,256]{1,0:T(8,128)(2,1)S(1)}, bf16[128,256]{1,0:T(8,128)(2,1)}, u32[]{:S(2)}) copy-start(bf16[128,256]{1,0:T(8,128)(2,1)} %gate_pre.1) | copy-start | bytes 196612
  115.8 18.8 %copy-start.3 = (bf16[128,256]{1,0:T(8,128)(2,1)S(1)}, bf16[128,256]{1,0:T(8,128)(2,1)}, u32[]{:S(2)}) copy-start(bf16[128,256]{1,0:T(8,128)(2,1)} %mixer.1) | copy-start | bytes 196612
  115.8 18.8 %copy-start.5 = (bf16[128,128]{1,0:T(8,128)(2,1)S(1)}, bf16[128,128]{1,0:T(8,128)(2,1)}, u32[]{:S(2)}) copy-start(bf16[128,128]{1,0:T(8,128)(2,1)} %read.3) | copy-start | bytes 98308
  115.9 18.8 %copy-start.8 = (f32[4,128]{1,0:T(4,128)S(1)}, f32[4,128]{1,0:T(4,128)}, u32[]{:S(2)}) copy-start(f32[4,128]{1,0:T(4,128)} %logs.1) | copy-start | bytes 6148
  136.5 24.9 %collective-permute-start.13 = (bf16[32,32,128]{2,1,0:T(8,128)(2,1)S(1)}, bf16[32,32,128]{2,1,0:T(8,128)(2,1)S(1)}, u32[]{:S(2)}, u32[]{:S(2)}) collective-permute-start(bf16[32,32,128]{2,1,0:T(8,128)(2,1)S(1)} %get-tuple-element.89), channel_id=1, source_target_pairs={{0,16},{16,32},{32,48},{48,0},{1,17},{17,33},{33,49},{49,1},{2,18}... | collective-permute-start | bytes 786440 | tf_op jit(solution)/shard_map/ppermute | solution.py:399
  138.5 22.9 %collective-permute-start.14 = (bf16[32,32,128]{2,1,0:T(8,128)(2,1)S(1)}, bf16[32,32,128]{2,1,0:T(8,128)(2,1)S(1)}, u32[]{:S(2)}, u32[]{:S(2)}) collective-permute-start(bf16[32,32,128]{2,1,0:T(8,128)(2,1)S(1)} %get-tuple-element.90), channel_id=1, source_target_pairs={{0,32},{16,48},{32,0},{48,16},{1,33},{17,49},{33,1},{49,17},{2,34}... | collective-permute-start | bytes 786440 | tf_op jit(solution)/shard_map/ppermute | solution.py:399
  143.1 18.3 %collective-permute-start.15 = (bf16[32,32,128]{2,1,0:T(8,128)(2,1)S(1)}, bf16[32,32,128]{2,1,0:T(8,128)(2,1)S(1)}, u32[]{:S(2)}, u32[]{:S(2)}) collective-permute-start(bf16[32,32,128]{2,1,0:T(8,128)(2,1)S(1)} %get-tuple-element.91), channel_id=1, source_target_pairs={{0,48},{16,0},{32,16},{48,32},{1,49},{17,1},{33,17},{49,33},{2,50}... | collective-permute-start | bytes 786440 | tf_op jit(solution)/shard_map/ppermute | solution.py:399
  146.1 4.7 %copy-start.4 = (bf16[128,256]{1,0:T(8,128)(2,1)S(1)}, bf16[128,256]{1,0:T(8,128)(2,1)}, u32[]{:S(2)}) copy-start(bf16[128,256]{1,0:T(8,128)(2,1)} %values.3) | copy-start | bytes 196612
  146.1 4.7 %copy-start.6 = (bf16[128,128]{1,0:T(8,128)(2,1)S(1)}, bf16[128,128]{1,0:T(8,128)(2,1)}, u32[]{:S(2)}) copy-start(bf16[128,128]{1,0:T(8,128)(2,1)} %write.3) | copy-start | bytes 98308
  146.1 4.7 %copy-start.9 = (f32[1,4,64,128]{3,2,1,0:T(8,128)S(1)}, f32[1,4,64,128]{3,2,1,0:T(8,128)}, u32[]{:S(2)}) copy-start(f32[1,4,64,128]{3,2,1,0:T(8,128)} %param.29) | copy-start | bytes 393220
  146.2 15.2 %all-to-all-start.2 = ((bf16[32,16,128]{2,1,0:T(8,128)(2,1)}), bf16[32,16,128]{2,1,0:T(8,128)(2,1)S(1)}, u32[]{:S(2)}, u32[]{:S(2)}) async-start(bf16[32,16,128]{2,1,0:T(8,128)(2,1)} %get-tuple-element.79), calls=%async_computation.2 | async-start | bytes 262144 | tf_op jit(solution)/shard_map/all_to_all | solution.py:397

commit v10 on v9

--- a/solution.py
+++ b/solution.py
@@ -16,6 +16,7 @@
 HEADS = 4
 HD = 64
 STATE = 128
+PLAN = ((3, True), (3, False), (2, True), (2, False), (1, True), (1, False), (4, True), (0, True))
 SP = ("z", "x")
 TP = ("y", "core")
 GRANT = 16 * 1024 * 1024
@@ -163,7 +164,7 @@
 
 
 def expert_kernel(where, chunk, early_pre, early_hidden, own, other, *outs):
-    near, mid, far, last, home, g_gate, g_up, g_hid = outs
+    g_gate, g_up, g_hid = outs[8:]
     more = chunk_products(chunk, chunk_ids(where[0])[7], own, other)
     pre = early_pre[...] + more[0]
     grad_hidden = early_hidden[...] + more[1]
@@ -180,11 +181,10 @@
     grads = jnp.concatenate([gate, up], axis=1)
     y, core = where[0] >> 1, where[0] & 1
     step = 1 - 2 * core
-    for k, out in ((4, last), (3, far), (2, mid), (1, near), (0, home)):
+    for out, (k, same) in zip(outs[:8], PLAN):
         chip = (y + step * k + 8) & 7
-        start = chip * WIDE if k in (1, 2, 3) else chip * WIDE + core * TOK
-        size = out.shape[1]
-        at = pl.ds(pl.multiple_of(start, TOK), size)
+        side = core if same else 1 - core
+        at = pl.ds(pl.multiple_of((2 * chip + side) * TOK, TOK), TOK)
         out[...] = mm(grads, gate_rows(own, other, at)).astype(BF)
 
 
@@ -203,17 +203,11 @@
         d_down[:, at] = mm(hidden, cots).astype(BF)
 
 
-def fold_kernel(where, near, mid, far, last, home, keep, give):
-    total = near[...].astype(F32) + mid[...].astype(F32) + far[...].astype(F32)
-    first = total[:, :TOK]
-    second = total[:, TOK:]
-    top = where[0] & 1 == 0
-    keep[...] = jnp.where(top, first, second) + last[...].astype(F32) + home[...].astype(F32)
-    give[...] = jnp.where(top, second, first).astype(BF)
-
-
-def join_kernel(keep, taken, out):
-    out[...] = (keep[...] + taken[...].astype(F32)).astype(BF).reshape(EXP, CAP, TOK)
+def fold_kernel(*refs):
+    total = refs[0][...].astype(F32)
+    for part in refs[1:8]:
+        total = total + part[...].astype(F32)
+    refs[8][...] = total.astype(BF).reshape(EXP, CAP, TOK)
 
 
 def combine_kernel(where, target, rows, cotangent, out, cot, arrived):
@@ -342,11 +336,14 @@
          write_keys, read_keys, log_decay, entry_states):
     shape = jax.ShapeDtypeStruct
     swap = [(0, 1), (1, 0)]
-    rings = []
-    for k in range(1, 5):
-        up = [(2 * y, 2 * ((y + k) % 8)) for y in range(8)]
-        rings.append(up + [(2 * y + 1, 2 * ((y - k) % 8) + 1) for y in range(8)])
-    ring = rings[0]
+    def route(k, same):
+        pairs = []
+        for y in range(8):
+            pairs.append((2 * y, 2 * ((y + k) % 8) + (0 if same else 1)))
+            pairs.append((2 * y + 1, 2 * ((y - k) % 8) + (1 if same else 0)))
+        return pairs
+
+    ring = route(1, True)
     slot = lax.axis_index(TP).astype(jnp.int32).reshape(1)
     own = jnp.stack([w_gate[0].T, w_up[0].T, w_down[0]])
     other = lax.ppermute(own, "core", swap)
@@ -362,26 +359,22 @@
     c7 = lax.ppermute(c4, "core", swap)
     chunks = (c0, c1, c2, c3, c4, c5, c6, c7)
     grad = shape((ROWS, 2 * FF), BF)
-    full, thin = shape((ROWS, WIDE), BF), shape((ROWS, TOK), BF)
+    thin = shape((ROWS, TOK), BF)
     early = call(
         early_kernel, (shape((ROWS, 4 * FF), F32), shape((ROWS, 2 * FF), F32)),
         [smem()] + [vmem()] * 9, (slot, *chunks[:7], own, other), flops=10**8)
-    *parts, home, g_gate, g_up, g_hid = call(
-        expert_kernel, (full, full, full, thin, thin, grad, grad, grad),
+    *parts, g_gate, g_up, g_hid = call(
+        expert_kernel, (thin,) * 8 + (grad, grad, grad),
         [smem()] + [vmem()] * 5, (slot, c7, *early, own, other))
     pieces = []
-    for k in range(4):
-        pieces.append(lax.ppermute(parts[k], TP, rings[k]))
+    for k, (far, same) in enumerate(PLAN[:7]):
+        pieces.append(lax.ppermute(parts[k], TP, route(far, same)))
     wide = shape((FF, D), BF)
     d_wg, d_wu, d_wd = call(
         weights_kernel, (wide, wide, wide),
         [smem()] + [vmem()] * 11, (slot, *chunks, g_gate, g_up, g_hid), flops=10**9)
     pieces, d_wg, d_wu, d_wd = lax.optimization_barrier((pieces, d_wg, d_wu, d_wd))
-    keep, give = call(
-        fold_kernel, (shape((ROWS, TOK), F32), thin),
-        [smem()] + [vmem()] * 5, (slot, *pieces, home))
-    taken = lax.ppermute(give, "core", swap)
-    summed = call(join_kernel, shape((EXP, CAP, TOK), BF), [vmem()] * 2, (keep, taken))
+    summed = call(fold_kernel, shape((EXP, CAP, TOK), BF), [vmem()] * 8, (*pieces, parts[7]))
     back = lax.all_to_all(summed, SP, 0, 0, tiled=True)
     d_input = combine(slot, target, back, cotangent)
     whole = lax.all_gather(d_input, TP, axis=0, tiled=True)

time: 181 us -> 182 us (level)
  starting transfers between devices: 58.8 us -> 67.3 us
  waiting for transfers between devices: 40.5 us -> 33.2 us
    ppermute x5 -> x7, starting transfers between devices: 19.9 us -> 28.3 us  [step(): pieces.append(lax.ppermute(parts[k], TP, route(far, same)))]
    ppermute x5 -> x7, waiting for transfers between devices: 13.4 us -> 6.54 us  [step(): pieces.append(lax.ppermute(parts[k], TP, route(far, same)))]
    pallas_call x9 -> x8, Pallas kernels: 9.26 us -> 9.22 us  [call(): pl.pallas_call(kernel, out_shape=outs, in_specs=specs, out_specs=jax.tree...]
  transfers between devices with their start and end apart: 18 -> 20, of which waited for: 9 -> 7; matrix products, arithmetic and copies ran while one was open for 0% -> 0% of each run, Pallas kernels for 2% -> 2%
where the time goes in v10:
time: 182 us; the launch traced here: 181 us
  starting transfers between devices  67.3 us (37%)
  blocking collectives  66.4 us (36%)
  waiting for transfers between devices  33.2 us (18%)
  Pallas kernels  12.4 us (7%)
    all_to_all x1, blocking collectives, step(): c0 = lax.all_to_all(buf, SP, 0, 0, tiled=True)  31.1 us
    ppermute x7, starting transfers between devices, step(): pieces.append(lax.ppermute(parts[k], TP, route(far, same)))  28.3 us
    all_gather x1, blocking collectives, step(): whole = lax.all_gather(d_input, TP, axis=0, tiled=True)  18.2 us
    all_to_all x1, blocking collectives, step(): second = lax.all_to_all(states, SP, 0, 0, tiled=True)  17.1 us
    all_to_all x1, waiting for transfers between devices, step(): back = lax.all_to_all(summed, SP, 0, 0, tiled=True)  10.5 us
    ppermute x3, starting transfers between devices, step(): lax.ppermute(shares[k], 'x', [(i, (i + k) % 4) for i in range(4)])  9.66 us
    pallas_call x8, Pallas kernels, call(): pl.pallas_call(kernel, out_shape=outs, in_specs=specs, out_specs=jax.tree...  9.22 us
    all_to_all x1, waiting for transfers between devices, step(): received = lax.all_to_all(sent, SP, 0, 0, tiled=True)  9.04 us
  transfers between devices with their start and end apart: 20, of which 7 were waited for; matrix products, arithmetic and copies ran while one was open for 0% of the time, Pallas kernels for 2%

profile of v10, /device:TPU:8, one launch (start us, length us, event | category | flops | bytes accessed | tf_op | source)
XLA Modules:
  0.0 180.6 jit_solution(17742803884650679023)
XLA Ops:
  0.6 2.2 %prepare.1 = (bf16[32,32,256]{2,1,0:T(8,128)(2,1)}, s32[8,128]{1,0:T(8,128)}) custom-call(s32[1]{0:T(128)} %bitcast.where, s32[2,128]{1,0:T(2,128)} %bitcast.25, f32[2,128]{1,0:T(2,128)} %bitcast.26, bf16[128,2048]{1,0:T(8,128)(2,1)} %mix.1, bf16[128,2048]{1,0:T(8,128)(2,1)} %cotangent.1), custom_call_target="tpu_custom_call" | custom-call | tf_op jit(solution)/shard_map/prepare/pallas_call | solution.py:113
  2.9 31.1 %all_to_all.20.refs_0_ = bf16[32,32,256]{2,1,0:T(8,128)(2,1)S(1)} all-to-all(bf16[32,32,256]{2,1,0:T(8,128)(2,1)} %get-tuple-element.57), channel_id=1, replica_groups=mesh['z'=8,'x'=4,'y'=8,'core'=2] {'z','x'}, dimensions={0} | all-to-all | bytes 1048576 | tf_op jit(solution)/shard_map/all_to_all | solution.py:351
  34.0 1.9 %collective-permute-start.3 = (bf16[32,32,256]{2,1,0:T(8,128)(2,1)S(1)}, bf16[32,32,256]{2,1,0:T(8,128)(2,1)S(1)}, u32[]{:S(2)}, u32[]{:S(2)}) collective-permute-start(bf16[32,32,256]{2,1,0:T(8,128)(2,1)S(1)} %all_to_all.20.refs_0_), channel_id=1, source_target_pairs={{0,1},{1,0},{2,3},{3,2},{4,5},{5,4},{6,7},{7,6},{8,9},{9,8},{10,11... | collective-permute-start | bytes 1572872 | tf_op jit(solution)/shard_map/ppermute | solution.py:353
  35.9 3.5 %collective-permute-start = (bf16[32,32,256]{2,1,0:T(8,128)(2,1)S(1)}, bf16[32,32,256]{2,1,0:T(8,128)(2,1)S(1)}, u32[]{:S(2)}, u32[]{:S(2)}) collective-permute-start(bf16[32,32,256]{2,1,0:T(8,128)(2,1)S(1)} %all_to_all.20.refs_0_), channel_id=1, source_target_pairs={{0,2},{1,15},{2,4},{3,1},{4,6},{5,3},{6,8},{7,5},{8,10},{9,7},{10,... | collective-permute-start | bytes 1572872 | tf_op jit(solution)/shard_map/ppermute | solution.py:352
  39.5 1.9 %collective-permute-start.5 = (bf16[3,64,2048]{2,1,0:T(8,128)(2,1)S(1)}, bf16[3,64,2048]{2,1,0:T(8,128)(2,1)S(1)}, u32[]{:S(2)}, u32[]{:S(2)}) collective-permute-start(bf16[3,64,2048]{2,1,0:T(8,128)(2,1)S(1)} %pad_maximum_fusion.refs_7_.own), channel_id=1, source_target_pairs={{0,1},{1,0},{2,3},{3,2},{4,5},{5,4},{6,7},{7,6},{8,9},{9,8},{10,11... | collective-permute-start | bytes 2359304 | tf_op jit(solution)/shard_map/ppermute | solution.py:349
  41.4 3.5 %collective-permute-start.4 = (bf16[32,32,256]{2,1,0:T(8,128)(2,1)S(1)}, bf16[32,32,256]{2,1,0:T(8,128)(2,1)S(1)}, u32[]{:S(2)}, u32[]{:S(2)}) collective-permute-start(bf16[32,32,256]{2,1,0:T(8,128)(2,1)S(1)} %collective-permute-done.3.refs_1_), channel_id=1, source_target_pairs={{0,2},{1,15},{2,4},{3,1},{4,6},{5,3},{6,8},{7,5},{8,10},{9,7},{10,... | collective-permute-start | bytes 1572872 | tf_op jit(solution)/shard_map/ppermute | solution.py:354
  44.9 2.0 %collective-permute-done.refs_2_ = bf16[32,32,256]{2,1,0:T(8,128)(2,1)S(1)} collective-permute-done((bf16[32,32,256]{2,1,0:T(8,128)(2,1)S(1)}, bf16[32,32,256]{2,1,0:T(8,128)(2,1)S(1)}, u32[]{:S(2)}, u32[]{:S(2)}) %collective-permute-start) | collective-permute-done | bytes 524320 | tf_op jit(solution)/shard_map/ppermute | solution.py:352
  46.9 3.5 %collective-permute-start.1 = (bf16[32,32,256]{2,1,0:T(8,128)(2,1)S(1)}, bf16[32,32,256]{2,1,0:T(8,128)(2,1)S(1)}, u32[]{:S(2)}, u32[]{:S(2)}) collective-permute-start(bf16[32,32,256]{2,1,0:T(8,128)(2,1)S(1)} %collective-permute-done.refs_2_), channel_id=1, source_target_pairs={{0,2},{1,15},{2,4},{3,1},{4,6},{5,3},{6,8},{7,5},{8,10},{9,7},{10,... | collective-permute-start | bytes 1572872 | tf_op jit(solution)/shard_map/ppermute | solution.py:355
  50.4 1.9 %collective-permute-start.6 = (bf16[32,32,256]{2,1,0:T(8,128)(2,1)S(1)}, bf16[32,32,256]{2,1,0:T(8,128)(2,1)S(1)}, u32[]{:S(2)}, u32[]{:S(2)}) collective-permute-start(bf16[32,32,256]{2,1,0:T(8,128)(2,1)S(1)} %collective-permute-done.refs_2_), channel_id=1, source_target_pairs={{0,1},{1,0},{2,3},{3,2},{4,5},{5,4},{6,7},{7,6},{8,9},{9,8},{10,11... | collective-permute-start | bytes 1572872 | tf_op jit(solution)/shard_map/ppermute | solution.py:357
  53.0 1.9 %collective-permute-start.7 = (bf16[32,32,256]{2,1,0:T(8,128)(2,1)S(1)}, bf16[32,32,256]{2,1,0:T(8,128)(2,1)S(1)}, u32[]{:S(2)}, u32[]{:S(2)}) collective-permute-start(bf16[32,32,256]{2,1,0:T(8,128)(2,1)S(1)} %collective-permute-done.4.refs_3_), channel_id=1, source_target_pairs={{0,1},{1,0},{2,3},{3,2},{4,5},{5,4},{6,7},{7,6},{8,9},{9,8},{10,11... | collective-permute-start | bytes 1572872 | tf_op jit(solution)/shard_map/ppermute | solution.py:358
  54.9 3.7 %collective-permute-done.1.refs_4_ = bf16[32,32,256]{2,1,0:T(8,128)(2,1)S(1)} collective-permute-done((bf16[32,32,256]{2,1,0:T(8,128)(2,1)S(1)}, bf16[32,32,256]{2,1,0:T(8,128)(2,1)S(1)}, u32[]{:S(2)}, u32[]{:S(2)}) %collective-permute-start.1) | collective-permute-done | bytes 524320 | tf_op jit(solution)/shard_map/ppermute | solution.py:355
  58.7 1.9 %collective-permute-start.2 = (bf16[32,32,256]{2,1,0:T(8,128)(2,1)S(1)}, bf16[32,32,256]{2,1,0:T(8,128)(2,1)S(1)}, u32[]{:S(2)}, u32[]{:S(2)}) collective-permute-start(bf16[32,32,256]{2,1,0:T(8,128)(2,1)S(1)} %collective-permute-done.1.refs_4_), channel_id=1, source_target_pairs={{0,1},{1,0},{2,3},{3,2},{4,5},{5,4},{6,7},{7,6},{8,9},{9,8},{10,11... | collective-permute-start | bytes 1572872 | tf_op jit(solution)/shard_map/ppermute | solution.py:359
  63.4 8.5 %collective-permute-start.8 = (bf16[512,128]{1,0:T(8,128)(2,1)S(1)}, bf16[512,128]{1,0:T(8,128)(2,1)S(1)}, u32[]{:S(2)}, u32[]{:S(2)}) collective-permute-start(bf16[512,128]{1,0:T(8,128)(2,1)S(1)} %get-tuple-element.62), channel_id=1, source_target_pairs={{0,6},{1,11},{2,8},{3,13},{4,10},{5,15},{6,12},{7,1},{8,14},{9,3},... | collective-permute-start | bytes 393224 | tf_op jit(solution)/shard_map/ppermute | solution.py:371
  71.9 1.9 %collective-permute-start.9 = (bf16[512,128]{1,0:T(8,128)(2,1)S(1)}, bf16[512,128]{1,0:T(8,128)(2,1)S(1)}, u32[]{:S(2)}, u32[]{:S(2)}) collective-permute-start(bf16[512,128]{1,0:T(8,128)(2,1)S(1)} %get-tuple-element.63), channel_id=1, source_target_pairs={{0,7},{1,10},{2,9},{3,12},{4,11},{5,14},{6,13},{7,0},{8,15},{9,2},... | collective-permute-start | bytes 393224 | tf_op jit(solution)/shard_map/ppermute | solution.py:371
  73.8 3.5 %collective-permute-start.10 = (bf16[512,128]{1,0:T(8,128)(2,1)S(1)}, bf16[512,128]{1,0:T(8,128)(2,1)S(1)}, u32[]{:S(2)}, u32[]{:S(2)}) collective-permute-start(bf16[512,128]{1,0:T(8,128)(2,1)S(1)} %get-tuple-element.64), channel_id=1, source_target_pairs={{0,4},{1,13},{2,6},{3,15},{4,8},{5,1},{6,10},{7,3},{8,12},{9,5},{1... | collective-permute-start | bytes 393224 | tf_op jit(solution)/shard_map/ppermute | solution.py:371
  77.3 1.9 %collective-permute-start.11 = (bf16[512,128]{1,0:T(8,128)(2,1)S(1)}, bf16[512,128]{1,0:T(8,128)(2,1)S(1)}, u32[]{:S(2)}, u32[]{:S(2)}) collective-permute-start(bf16[512,128]{1,0:T(8,128)(2,1)S(1)} %get-tuple-element.65), channel_id=1, source_target_pairs={{0,5},{1,12},{2,7},{3,14},{4,9},{5,0},{6,11},{7,2},{8,13},{9,4},{1... | collective-permute-start | bytes 393224 | tf_op jit(solution)/shard_map/ppermute | solution.py:371
  79.2 5.6 %collective-permute-start.12 = (bf16[512,128]{1,0:T(8,128)(2,1)S(1)}, bf16[512,128]{1,0:T(8,128)(2,1)S(1)}, u32[]{:S(2)}, u32[]{:S(2)}) collective-permute-start(bf16[512,128]{1,0:T(8,128)(2,1)S(1)} %get-tuple-element.66), channel_id=1, source_target_pairs={{0,2},{1,15},{2,4},{3,1},{4,6},{5,3},{6,8},{7,5},{8,10},{9,7},{10,... | collective-permute-start | bytes 393224 | tf_op jit(solution)/shard_map/ppermute | solution.py:371
  84.9 2.2 %collective-permute-start.13 = (bf16[512,128]{1,0:T(8,128)(2,1)S(1)}, bf16[512,128]{1,0:T(8,128)(2,1)S(1)}, u32[]{:S(2)}, u32[]{:S(2)}) collective-permute-start(bf16[512,128]{1,0:T(8,128)(2,1)S(1)} %get-tuple-element.67), channel_id=1, source_target_pairs={{0,3},{1,14},{2,5},{3,0},{4,7},{5,2},{6,9},{7,4},{8,11},{9,6},{10,... | collective-permute-start | bytes 393224 | tf_op jit(solution)/shard_map/ppermute | solution.py:371
  87.1 4.6 %collective-permute-start.14 = (bf16[512,128]{1,0:T(8,128)(2,1)S(1)}, bf16[512,128]{1,0:T(8,128)(2,1)S(1)}, u32[]{:S(2)}, u32[]{:S(2)}) collective-permute-start(bf16[512,128]{1,0:T(8,128)(2,1)S(1)} %get-tuple-element.68), channel_id=1, source_target_pairs={{0,8},{1,9},{2,10},{3,11},{4,12},{5,13},{6,14},{7,15},{8,0},{9,1},... | collective-permute-start | bytes 393224 | tf_op jit(solution)/shard_map/ppermute | solution.py:371
  91.7 1.7 shard_map.216
  93.4 6.5 %collective-permute-done.14.refs_6_ = bf16[512,128]{1,0:T(8,128)(2,1)S(1)} collective-permute-done((bf16[512,128]{1,0:T(8,128)(2,1)S(1)}, bf16[512,128]{1,0:T(8,128)(2,1)S(1)}, u32[]{:S(2)}, u32[]{:S(2)}) %collective-permute-start.14) | collective-permute-done | bytes 131104 | tf_op jit(solution)/shard_map/ppermute | solution.py:371
  100.8 4.8 %all-to-all-start.1 = ((bf16[32,16,128]{2,1,0:T(8,128)(2,1)}), bf16[32,16,128]{2,1,0:T(8,128)(2,1)S(1)}, u32[]{:S(2)}, u32[]{:S(2)}) async-start(bf16[32,16,128]{2,1,0:T(8,128)(2,1)} %shard_map.217), calls=%async_computation.1 | async-start | bytes 262144 | tf_op jit(solution)/shard_map/all_to_all | solution.py:378
  105.5 10.5 %all-to-all-done.1.rows = bf16[32,16,128]{2,1,0:T(8,128)(2,1)S(1)} async-done(((bf16[32,16,128]{2,1,0:T(8,128)(2,1)}), bf16[32,16,128]{2,1,0:T(8,128)(2,1)S(1)}, u32[]{:S(2)}, u32[]{:S(2)}) %all-to-all-start.1) | async-done | bytes 131104 | tf_op jit(solution)/shard_map/all_to_all | solution.py:378
  117.1 18.2 %all_gather.3.gathered = bf16[2048,128]{1,0:T(8,128)(2,1)S(1)} all-gather(bf16[128,128]{1,0:T(8,128)(2,1)} %combine.1), channel_id=1, replica_groups=mesh['z'=8,'x'=4,'y'=8,'core'=2] {'y','core'}, dimensions={0}, use_global_device_ids=true | all-gather | bytes 557056 | tf_op jit(solution)/shard_map/all_gather | solution.py:380
  135.4 1.8 %shard_map.218 = (bf16[128,256]{1,0:T(8,128)(2,1)}, f32[128,256]{1,0:T(8,128)S(1)}, f32[8,128]{1,0:T(8,128)S(1)}, bf16[32,16,128]{2,1,0:T(8,128)(2,1)}, bf16[32,...) custom-call(s32[1]{0:T(128)} %bitcast.14.spot, ...), custom_call_target="tpu_custom_call" | custom-call | tf_op jit(solution)/shard_map/pallas_call | solution.py:76
  137.2 1.9 %collective-permute-start.15 = (bf16[32,32,128]{2,1,0:T(8,128)(2,1)S(1)}, bf16[32,32,128]{2,1,0:T(8,128)(2,1)S(1)}, u32[]{:S(2)}, u32[]{:S(2)}) collective-permute-start(bf16[32,32,128]{2,1,0:T(8,128)(2,1)S(1)} %get-tuple-element.97), channel_id=1, source_target_pairs={{0,16},{16,32},{32,48},{48,0},{1,17},{17,33},{33,49},{49,1},{2,18}... | collective-permute-start | bytes 786440 | tf_op jit(solution)/shard_map/ppermute | solution.py:392
  139.1 4.8 %collective-permute-start.16 = (bf16[32,32,128]{2,1,0:T(8,128)(2,1)S(1)}, bf16[32,32,128]{2,1,0:T(8,128)(2,1)S(1)}, u32[]{:S(2)}, u32[]{:S(2)}) collective-permute-start(bf16[32,32,128]{2,1,0:T(8,128)(2,1)S(1)} %get-tuple-element.98), channel_id=1, source_target_pairs={{0,32},{16,48},{32,0},{48,16},{1,33},{17,49},{33,1},{49,17},{2,34}... | collective-permute-start | bytes 786440 | tf_op jit(solution)/shard_map/ppermute | solution.py:392
  143.9 2.9 %collective-permute-start.17 = (bf16[32,32,128]{2,1,0:T(8,128)(2,1)S(1)}, bf16[32,32,128]{2,1,0:T(8,128)(2,1)S(1)}, u32[]{:S(2)}, u32[]{:S(2)}) collective-permute-start(bf16[32,32,128]{2,1,0:T(8,128)(2,1)S(1)} %get-tuple-element.99), channel_id=1, source_target_pairs={{0,48},{16,0},{32,16},{48,32},{1,49},{17,1},{33,17},{49,33},{2,50}... | collective-permute-start | bytes 786440 | tf_op jit(solution)/shard_map/ppermute | solution.py:392
  146.9 4.6 %all-to-all-start.2 = ((bf16[32,16,128]{2,1,0:T(8,128)(2,1)}), bf16[32,16,128]{2,1,0:T(8,128)(2,1)S(1)}, u32[]{:S(2)}, u32[]{:S(2)}) async-start(bf16[32,16,128]{2,1,0:T(8,128)(2,1)} %get-tuple-element.87), calls=%async_computation.2 | async-start | bytes 262144 | tf_op jit(solution)/shard_map/all_to_all | solution.py:390
  151.5 1.5 shard_map.219
  153.0 9.0 %all-to-all-done.2.received = bf16[32,16,128]{2,1,0:T(8,128)(2,1)S(1)} async-done(((bf16[32,16,128]{2,1,0:T(8,128)(2,1)}), bf16[32,16,128]{2,1,0:T(8,128)(2,1)S(1)}, u32[]{:S(2)}, u32[]{:S(2)}) %all-to-all-start.2) | async-done | bytes 131104 | tf_op jit(solution)/shard_map/all_to_all | solution.py:390
  162.3 17.1 %all_to_all.21.second = bf16[32,48,128]{2,1,0:T(8,128)(2,1)S(1)} all-to-all(bf16[32,48,128]{2,1,0:T(8,128)(2,1)S(1)} %shard_map.220), channel_id=1, replica_groups=mesh['z'=8,'x'=4,'y'=8,'core'=2] {'z','x'}, dimensions={0} | all-to-all | bytes 786432 | tf_op jit(solution)/shard_map/all_to_all | solution.py:399
  (48 shorter events, 6.8 us)
Async XLA Ops:
  2.9 36.5 %copy-start.10 = (bf16[1,64,2048]{2,1,0:T(8,128)(2,1)S(1)}, bf16[1,64,2048]{2,1,0:T(8,128)(2,1)}, u32[]{:S(2)}) copy-start(bf16[1,64,2048]{2,1,0:T(8,128)(2,1)} %param.21) | copy-start | bytes 786436
  2.9 36.5 %copy-start.11 = (bf16[1,2048,64]{1,2,0:T(8,128)(2,1)S(1)}, bf16[1,2048,64]{1,2,0:T(8,128)(2,1)}, u32[]{:S(2)}) copy-start(bf16[1,2048,64]{1,2,0:T(8,128)(2,1)} %param.20) | copy-start | bytes 786436
  2.9 36.5 %copy-start.12 = (bf16[1,2048,64]{1,2,0:T(8,128)(2,1)S(1)}, bf16[1,2048,64]{1,2,0:T(8,128)(2,1)}, u32[]{:S(2)}) copy-start(bf16[1,2048,64]{1,2,0:T(8,128)(2,1)} %param.19) | copy-start | bytes 786436
  34.0 7.5 %collective-permute-start.3 = (bf16[32,32,256]{2,1,0:T(8,128)(2,1)S(1)}, bf16[32,32,256]{2,1,0:T(8,128)(2,1)S(1)}, u32[]{:S(2)}, u32[]{:S(2)}) collective-permute-start(bf16[32,32,256]{2,1,0:T(8,128)(2,1)S(1)} %all_to_all.20.refs_0_), channel_id=1, source_target_pairs={{0,1},{1,0},{2,3},{3,2},{4,5},{5,4},{6,7},{7,6},{8,9},{9,8},{10,11... | collective-permute-start | bytes 1572872 | tf_op jit(solution)/shard_map/ppermute | solution.py:353
  35.9 11.1 %collective-permute-start = (bf16[32,32,256]{2,1,0:T(8,128)(2,1)S(1)}, bf16[32,32,256]{2,1,0:T(8,128)(2,1)S(1)}, u32[]{:S(2)}, u32[]{:S(2)}) collective-permute-start(bf16[32,32,256]{2,1,0:T(8,128)(2,1)S(1)} %all_to_all.20.refs_0_), channel_id=1, source_target_pairs={{0,2},{1,15},{2,4},{3,1},{4,6},{5,3},{6,8},{7,5},{8,10},{9,7},{10,... | collective-permute-start | bytes 1572872 | tf_op jit(solution)/shard_map/ppermute | solution.py:352
  39.5 10.9 %collective-permute-start.5 = (bf16[3,64,2048]{2,1,0:T(8,128)(2,1)S(1)}, bf16[3,64,2048]{2,1,0:T(8,128)(2,1)S(1)}, u32[]{:S(2)}, u32[]{:S(2)}) collective-permute-start(bf16[3,64,2048]{2,1,0:T(8,128)(2,1)S(1)} %pad_maximum_fusion.refs_7_.own), channel_id=1, source_target_pairs={{0,1},{1,0},{2,3},{3,2},{4,5},{5,4},{6,7},{7,6},{8,9},{9,8},{10,11... | collective-permute-start | bytes 2359304 | tf_op jit(solution)/shard_map/ppermute | solution.py:349
  41.4 11.6 %collective-permute-start.4 = (bf16[32,32,256]{2,1,0:T(8,128)(2,1)S(1)}, bf16[32,32,256]{2,1,0:T(8,128)(2,1)S(1)}, u32[]{:S(2)}, u32[]{:S(2)}) collective-permute-start(bf16[32,32,256]{2,1,0:T(8,128)(2,1)S(1)} %collective-permute-done.3.refs_1_), channel_id=1, source_target_pairs={{0,2},{1,15},{2,4},{3,1},{4,6},{5,3},{6,8},{7,5},{8,10},{9,7},{10,... | collective-permute-start | bytes 1572872 | tf_op jit(solution)/shard_map/ppermute | solution.py:354
  46.9 11.7 %collective-permute-start.1 = (bf16[32,32,256]{2,1,0:T(8,128)(2,1)S(1)}, bf16[32,32,256]{2,1,0:T(8,128)(2,1)S(1)}, u32[]{:S(2)}, u32[]{:S(2)}) collective-permute-start(bf16[32,32,256]{2,1,0:T(8,128)(2,1)S(1)} %collective-permute-done.refs_2_), channel_id=1, source_target_pairs={{0,2},{1,15},{2,4},{3,1},{4,6},{5,3},{6,8},{7,5},{8,10},{9,7},{10,... | collective-permute-start | bytes 1572872 | tf_op jit(solution)/shard_map/ppermute | solution.py:355
  50.4 10.1 %collective-permute-start.6 = (bf16[32,32,256]{2,1,0:T(8,128)(2,1)S(1)}, bf16[32,32,256]{2,1,0:T(8,128)(2,1)S(1)}, u32[]{:S(2)}, u32[]{:S(2)}) collective-permute-start(bf16[32,32,256]{2,1,0:T(8,128)(2,1)S(1)} %collective-permute-done.refs_2_), channel_id=1, source_target_pairs={{0,1},{1,0},{2,3},{3,2},{4,5},{5,4},{6,7},{7,6},{8,9},{9,8},{10,11... | collective-permute-start | bytes 1572872 | tf_op jit(solution)/shard_map/ppermute | solution.py:357
  53.0 7.5 %collective-permute-start.7 = (bf16[32,32,256]{2,1,0:T(8,128)(2,1)S(1)}, bf16[32,32,256]{2,1,0:T(8,128)(2,1)S(1)}, u32[]{:S(2)}, u32[]{:S(2)}) collective-permute-start(bf16[32,32,256]{2,1,0:T(8,128)(2,1)S(1)} %collective-permute-done.4.refs_3_), channel_id=1, source_target_pairs={{0,1},{1,0},{2,3},{3,2},{4,5},{5,4},{6,7},{7,6},{8,9},{9,8},{10,11... | collective-permute-start | bytes 1572872 | tf_op jit(solution)/shard_map/ppermute | solution.py:358
  58.7 3.8 %collective-permute-start.2 = (bf16[32,32,256]{2,1,0:T(8,128)(2,1)S(1)}, bf16[32,32,256]{2,1,0:T(8,128)(2,1)S(1)}, u32[]{:S(2)}, u32[]{:S(2)}) collective-permute-start(bf16[32,32,256]{2,1,0:T(8,128)(2,1)S(1)} %collective-permute-done.1.refs_4_), channel_id=1, source_target_pairs={{0,1},{1,0},{2,3},{3,2},{4,5},{5,4},{6,7},{7,6},{8,9},{9,8},{10,11... | collective-permute-start | bytes 1572872 | tf_op jit(solution)/shard_map/ppermute | solution.py:359
  63.4 21.5 %collective-permute-start.8 = (bf16[512,128]{1,0:T(8,128)(2,1)S(1)}, bf16[512,128]{1,0:T(8,128)(2,1)S(1)}, u32[]{:S(2)}, u32[]{:S(2)}) collective-permute-start(bf16[512,128]{1,0:T(8,128)(2,1)S(1)} %get-tuple-element.62), channel_id=1, source_target_pairs={{0,6},{1,11},{2,8},{3,13},{4,10},{5,15},{6,12},{7,1},{8,14},{9,3},... | collective-permute-start | bytes 393224 | tf_op jit(solution)/shard_map/ppermute | solution.py:371
  71.9 15.2 %collective-permute-start.9 = (bf16[512,128]{1,0:T(8,128)(2,1)S(1)}, bf16[512,128]{1,0:T(8,128)(2,1)S(1)}, u32[]{:S(2)}, u32[]{:S(2)}) collective-permute-start(bf16[512,128]{1,0:T(8,128)(2,1)S(1)} %get-tuple-element.63), channel_id=1, source_target_pairs={{0,7},{1,10},{2,9},{3,12},{4,11},{5,14},{6,13},{7,0},{8,15},{9,2},... | collective-permute-start | bytes 393224 | tf_op jit(solution)/shard_map/ppermute | solution.py:371
  73.8 19.6 %collective-permute-start.10 = (bf16[512,128]{1,0:T(8,128)(2,1)S(1)}, bf16[512,128]{1,0:T(8,128)(2,1)S(1)}, u32[]{:S(2)}, u32[]{:S(2)}) collective-permute-start(bf16[512,128]{1,0:T(8,128)(2,1)S(1)} %get-tuple-element.64), channel_id=1, source_target_pairs={{0,4},{1,13},{2,6},{3,15},{4,8},{5,1},{6,10},{7,3},{8,12},{9,5},{1... | collective-permute-start | bytes 393224 | tf_op jit(solution)/shard_map/ppermute | solution.py:371
  77.3 16.1 %collective-permute-start.11 = (bf16[512,128]{1,0:T(8,128)(2,1)S(1)}, bf16[512,128]{1,0:T(8,128)(2,1)S(1)}, u32[]{:S(2)}, u32[]{:S(2)}) collective-permute-start(bf16[512,128]{1,0:T(8,128)(2,1)S(1)} %get-tuple-element.65), channel_id=1, source_target_pairs={{0,5},{1,12},{2,7},{3,14},{4,9},{5,0},{6,11},{7,2},{8,13},{9,4},{1... | collective-permute-start | bytes 393224 | tf_op jit(solution)/shard_map/ppermute | solution.py:371
  79.2 14.2 %collective-permute-start.12 = (bf16[512,128]{1,0:T(8,128)(2,1)S(1)}, bf16[512,128]{1,0:T(8,128)(2,1)S(1)}, u32[]{:S(2)}, u32[]{:S(2)}) collective-permute-start(bf16[512,128]{1,0:T(8,128)(2,1)S(1)} %get-tuple-element.66), channel_id=1, source_target_pairs={{0,2},{1,15},{2,4},{3,1},{4,6},{5,3},{6,8},{7,5},{8,10},{9,7},{10,... | collective-permute-start | bytes 393224 | tf_op jit(solution)/shard_map/ppermute | solution.py:371
  84.9 8.5 %collective-permute-start.13 = (bf16[512,128]{1,0:T(8,128)(2,1)S(1)}, bf16[512,128]{1,0:T(8,128)(2,1)S(1)}, u32[]{:S(2)}, u32[]{:S(2)}) collective-permute-start(bf16[512,128]{1,0:T(8,128)(2,1)S(1)} %get-tuple-element.67), channel_id=1, source_target_pairs={{0,3},{1,14},{2,5},{3,0},{4,7},{5,2},{6,9},{7,4},{8,11},{9,6},{10,... | collective-permute-start | bytes 393224 | tf_op jit(solution)/shard_map/ppermute | solution.py:371
  87.1 12.9 %collective-permute-start.14 = (bf16[512,128]{1,0:T(8,128)(2,1)S(1)}, bf16[512,128]{1,0:T(8,128)(2,1)S(1)}, u32[]{:S(2)}, u32[]{:S(2)}) collective-permute-start(bf16[512,128]{1,0:T(8,128)(2,1)S(1)} %get-tuple-element.68), channel_id=1, source_target_pairs={{0,8},{1,9},{2,10},{3,11},{4,12},{5,13},{6,14},{7,15},{8,0},{9,1},... | collective-permute-start | bytes 393224 | tf_op jit(solution)/shard_map/ppermute | solution.py:371
  100.0 16.1 %copy-start = (bf16[128,2048]{1,0:T(8,128)(2,1)S(1)}, bf16[128,2048]{1,0:T(8,128)(2,1)}, u32[]{:S(2)}) copy-start(bf16[128,2048]{1,0:T(8,128)(2,1)} %cotangent.1) | copy-start | bytes 1572868
  100.0 16.1 %copy-start.7 = (s32[8,128]{1,0:T(8,128)S(1)}, s32[8,128]{1,0:T(8,128)}, u32[]{:S(2)}) copy-start(s32[8,128]{1,0:T(8,128)} %get-tuple-element.78.target) | copy-start | bytes 12292
  100.8 34.6 %copy-start.1 = (bf16[256,2048]{1,0:T(8,128)(2,1)S(1)}, bf16[256,2048]{1,0:T(8,128)(2,1)}, u32[]{:S(2)}) copy-start(bf16[256,2048]{1,0:T(8,128)(2,1)} %weight.1) | copy-start | bytes 3145732
  100.8 15.3 %all-to-all-start.1 = ((bf16[32,16,128]{2,1,0:T(8,128)(2,1)}), bf16[32,16,128]{2,1,0:T(8,128)(2,1)S(1)}, u32[]{:S(2)}, u32[]{:S(2)}) async-start(bf16[32,16,128]{2,1,0:T(8,128)(2,1)} %shard_map.217), calls=%async_computation.1 | async-start | bytes 262144 | tf_op jit(solution)/shard_map/all_to_all | solution.py:378
  117.1 18.3 %copy-start.2 = (bf16[128,256]{1,0:T(8,128)(2,1)S(1)}, bf16[128,256]{1,0:T(8,128)(2,1)}, u32[]{:S(2)}) copy-start(bf16[128,256]{1,0:T(8,128)(2,1)} %gate_pre.1) | copy-start | bytes 196612
  117.1 18.3 %copy-start.3 = (bf16[128,256]{1,0:T(8,128)(2,1)S(1)}, bf16[128,256]{1,0:T(8,128)(2,1)}, u32[]{:S(2)}) copy-start(bf16[128,256]{1,0:T(8,128)(2,1)} %mixer.1) | copy-start | bytes 196612
  117.1 18.3 %copy-start.5 = (bf16[128,128]{1,0:T(8,128)(2,1)S(1)}, bf16[128,128]{1,0:T(8,128)(2,1)}, u32[]{:S(2)}) copy-start(bf16[128,128]{1,0:T(8,128)(2,1)} %read.3) | copy-start | bytes 98308
  117.1 18.3 %copy-start.8 = (f32[4,128]{1,0:T(4,128)S(1)}, f32[4,128]{1,0:T(4,128)}, u32[]{:S(2)}) copy-start(f32[4,128]{1,0:T(4,128)} %logs.1) | copy-start | bytes 6148
  137.2 24.9 %collective-permute-start.15 = (bf16[32,32,128]{2,1,0:T(8,128)(2,1)S(1)}, bf16[32,32,128]{2,1,0:T(8,128)(2,1)S(1)}, u32[]{:S(2)}, u32[]{:S(2)}) collective-permute-start(bf16[32,32,128]{2,1,0:T(8,128)(2,1)S(1)} %get-tuple-element.97), channel_id=1, source_target_pairs={{0,16},{16,32},{32,48},{48,0},{1,17},{17,33},{33,49},{49,1},{2,18}... | collective-permute-start | bytes 786440 | tf_op jit(solution)/shard_map/ppermute | solution.py:392
  139.1 22.9 %collective-permute-start.16 = (bf16[32,32,128]{2,1,0:T(8,128)(2,1)S(1)}, bf16[32,32,128]{2,1,0:T(8,128)(2,1)S(1)}, u32[]{:S(2)}, u32[]{:S(2)}) collective-permute-start(bf16[32,32,128]{2,1,0:T(8,128)(2,1)S(1)} %get-tuple-element.98), channel_id=1, source_target_pairs={{0,32},{16,48},{32,0},{48,16},{1,33},{17,49},{33,1},{49,17},{2,34}... | collective-permute-start | bytes 786440 | tf_op jit(solution)/shard_map/ppermute | solution.py:392
  143.9 18.1 %collective-permute-start.17 = (bf16[32,32,128]{2,1,0:T(8,128)(2,1)S(1)}, bf16[32,32,128]{2,1,0:T(8,128)(2,1)S(1)}, u32[]{:S(2)}, u32[]{:S(2)}) collective-permute-start(bf16[32,32,128]{2,1,0:T(8,128)(2,1)S(1)} %get-tuple-element.99), channel_id=1, source_target_pairs={{0,48},{16,0},{32,16},{48,32},{1,49},{17,1},{33,17},{49,33},{2,50}... | collective-permute-start | bytes 786440 | tf_op jit(solution)/shard_map/ppermute | solution.py:392
  146.9 4.7 %copy-start.4 = (bf16[128,256]{1,0:T(8,128)(2,1)S(1)}, bf16[128,256]{1,0:T(8,128)(2,1)}, u32[]{:S(2)}) copy-start(bf16[128,256]{1,0:T(8,128)(2,1)} %values.3) | copy-start | bytes 196612
  146.9 4.7 %copy-start.6 = (bf16[128,128]{1,0:T(8,128)(2,1)S(1)}, bf16[128,128]{1,0:T(8,128)(2,1)}, u32[]{:S(2)}) copy-start(bf16[128,128]{1,0:T(8,128)(2,1)} %write.3) | copy-start | bytes 98308
  146.9 15.2 %all-to-all-start.2 = ((bf16[32,16,128]{2,1,0:T(8,128)(2,1)}), bf16[32,16,128]{2,1,0:T(8,128)(2,1)S(1)}, u32[]{:S(2)}, u32[]{:S(2)}) async-start(bf16[32,16,128]{2,1,0:T(8,128)(2,1)} %get-tuple-element.87), calls=%async_computation.2 | async-start | bytes 262144 | tf_op jit(solution)/shard_map/all_to_all | solution.py:390
  (1 other events, 4.7 us)

commit v11 on v9

--- a/solution.py
+++ b/solution.py
@@ -203,17 +203,13 @@
         d_down[:, at] = mm(hidden, cots).astype(BF)
 
 
-def fold_kernel(where, near, mid, far, last, home, keep, give):
+def fold_kernel(where, near, mid, far, last, home, out):
     total = near[...].astype(F32) + mid[...].astype(F32) + far[...].astype(F32)
-    first = total[:, :TOK]
-    second = total[:, TOK:]
-    top = where[0] & 1 == 0
-    keep[...] = jnp.where(top, first, second) + last[...].astype(F32) + home[...].astype(F32)
-    give[...] = jnp.where(top, second, first).astype(BF)
-
-
-def join_kernel(keep, taken, out):
-    out[...] = (keep[...] + taken[...].astype(F32)).astype(BF).reshape(EXP, CAP, TOK)
+    extra = last[...].astype(F32) + home[...].astype(F32)
+    for side in range(2):
+        own = jnp.where((where[0] & 1) == side, extra, 0.0)
+        part = total[:, side * TOK : (side + 1) * TOK] + own
+        out[:, side * CAP : (side + 1) * CAP, :] = part.astype(BF).reshape(EXP, CAP, TOK)
 
 
 def combine_kernel(where, target, rows, cotangent, out, cot, arrived):
@@ -223,7 +219,7 @@
     lane = iota((TOK, ROWS), 1)
     places = target[...].T
     pick = jnp.where((lane == places[:, 0:1]) | (lane == places[:, 1:2]), 1.0, 0.0).astype(BF)
-    total = mm(pick, rows[...].reshape(ROWS, TOK))
+    total = mm(pick, rows[:, 0:CAP, :].reshape(ROWS, TOK)) + mm(pick, rows[:, CAP:, :].reshape(ROWS, TOK))
     copy.wait()
     out[...] = (cot[...].astype(F32) + total).astype(BF)
 
@@ -377,12 +373,11 @@
         weights_kernel, (wide, wide, wide),
         [smem()] + [vmem()] * 11, (slot, *chunks, g_gate, g_up, g_hid), flops=10**9)
     pieces, d_wg, d_wu, d_wd = lax.optimization_barrier((pieces, d_wg, d_wu, d_wd))
-    keep, give = call(
-        fold_kernel, (shape((ROWS, TOK), F32), thin),
+    summed = call(
+        fold_kernel, shape((EXP, 2 * CAP, TOK), BF),
         [smem()] + [vmem()] * 5, (slot, *pieces, home))
-    taken = lax.ppermute(give, "core", swap)
-    summed = call(join_kernel, shape((EXP, CAP, TOK), BF), [vmem()] * 2, (keep, taken))
-    back = lax.all_to_all(summed, SP, 0, 0, tiled=True)
+    back = lax.all_to_all(summed.reshape(2 * EXP, CAP, TOK), SP + ("core",), 0, 0, tiled=True)
+    back = back.reshape(EXP, 2 * CAP, TOK)
     d_input = combine(slot, target, back, cotangent)
     whole = lax.all_gather(d_input, TP, axis=0, tiled=True)
     flat = shape((TOK, HEADS * HD), BF)

time: 181 us -> 181 us (level)
    ppermute x1 -> x0, starting transfers between devices: 2.33 us -> none  [step(): taken = lax.ppermute(give, 'core', swap)]
    all_to_all x1, waiting for transfers between devices: 10.9 us -> 12.9 us  [step(): lax.all_to_all(summed.reshape(2 * EXP, CAP, TOK), SP + ('core',), 0, 0, t...]
    pallas_call x9 -> x8, Pallas kernels: 9.26 us -> 9.28 us  [call(): pl.pallas_call(kernel, out_shape=outs, in_specs=specs, out_specs=jax.tree...]
  transfers between devices with their start and end apart: 18 -> 17, of which waited for: 9 -> 8; matrix products, arithmetic and copies ran while one was open for 0% -> 0% of each run, Pallas kernels for 2% -> 2%
where the time goes in v11:
time: 181 us; the launch traced here: 180 us
  blocking collectives  67 us (37%)
  starting transfers between devices  58.2 us (32%)
  waiting for transfers between devices  41.4 us (23%)
  Pallas kernels  12.5 us (7%)
    all_to_all x1, blocking collectives, step(): c0 = lax.all_to_all(buf, SP, 0, 0, tiled=True)  31.1 us
    all_gather x1, blocking collectives, step(): whole = lax.all_gather(d_input, TP, axis=0, tiled=True)  18.8 us
    ppermute x4, starting transfers between devices, step(): pieces.append(lax.ppermute(parts[k], TP, rings[k]))  17.6 us
    all_to_all x1, blocking collectives, step(): second = lax.all_to_all(states, SP, 0, 0, tiled=True)  17.1 us
    all_to_all x1, waiting for transfers between devices, step(): lax.all_to_all(summed.reshape(2 * EXP, CAP, TOK), SP + ('core',), 0, 0, t...  12.9 us
    ppermute x4, waiting for transfers between devices, step(): pieces.append(lax.ppermute(parts[k], TP, rings[k]))  12.4 us
    ppermute x3, starting transfers between devices, step(): lax.ppermute(shares[k], 'x', [(i, (i + k) % 4) for i in range(4)])  10.5 us
    pallas_call x8, Pallas kernels, call(): pl.pallas_call(kernel, out_shape=outs, in_specs=specs, out_specs=jax.tree...  9.28 us
  transfers between devices with their start and end apart: 17, of which 8 were waited for; matrix products, arithmetic and copies ran while one was open for 0% of the time, Pallas kernels for 2%

profile of v11, /device:TPU:8, one launch (start us, length us, event | category | flops | bytes accessed | tf_op | source)
XLA Modules:
  0.0 180.3 jit_solution(10557144764623773425)
XLA Ops:
  0.6 2.2 %prepare.1 = (bf16[32,32,256]{2,1,0:T(8,128)(2,1)}, s32[8,128]{1,0:T(8,128)}) custom-call(s32[1]{0:T(128)} %bitcast.where, s32[2,128]{1,0:T(2,128)} %bitcast.28, f32[2,128]{1,0:T(2,128)} %bitcast.29, bf16[128,2048]{1,0:T(8,128)(2,1)} %mix.1, bf16[128,2048]{1,0:T(8,128)(2,1)} %cotangent.1), custom_call_target="tpu_custom_call" | custom-call | tf_op jit(solution)/shard_map/prepare/pallas_call | solution.py:112
  2.9 31.1 %all_to_all.20.refs_0_ = bf16[32,32,256]{2,1,0:T(8,128)(2,1)S(1)} all-to-all(bf16[32,32,256]{2,1,0:T(8,128)(2,1)} %get-tuple-element.51), channel_id=1, replica_groups=mesh['z'=8,'x'=4,'y'=8,'core'=2] {'z','x'}, dimensions={0} | all-to-all | bytes 1048576 | tf_op jit(solution)/shard_map/all_to_all | solution.py:350
  34.0 1.9 %collective-permute-start.3 = (bf16[32,32,256]{2,1,0:T(8,128)(2,1)S(1)}, bf16[32,32,256]{2,1,0:T(8,128)(2,1)S(1)}, u32[]{:S(2)}, u32[]{:S(2)}) collective-permute-start(bf16[32,32,256]{2,1,0:T(8,128)(2,1)S(1)} %all_to_all.20.refs_0_), channel_id=1, source_target_pairs={{0,1},{1,0},{2,3},{3,2},{4,5},{5,4},{6,7},{7,6},{8,9},{9,8},{10,11... | collective-permute-start | bytes 1572872 | tf_op jit(solution)/shard_map/ppermute | solution.py:352
  35.9 3.5 %collective-permute-start = (bf16[32,32,256]{2,1,0:T(8,128)(2,1)S(1)}, bf16[32,32,256]{2,1,0:T(8,128)(2,1)S(1)}, u32[]{:S(2)}, u32[]{:S(2)}) collective-permute-start(bf16[32,32,256]{2,1,0:T(8,128)(2,1)S(1)} %all_to_all.20.refs_0_), channel_id=1, source_target_pairs={{0,2},{2,4},{4,6},{6,8},{8,10},{10,12},{12,14},{14,0},{1,15},{3,1}... | collective-permute-start | bytes 1572872 | tf_op jit(solution)/shard_map/ppermute | solution.py:351
  39.5 1.9 %collective-permute-start.5 = (bf16[3,64,2048]{2,1,0:T(8,128)(2,1)S(1)}, bf16[3,64,2048]{2,1,0:T(8,128)(2,1)S(1)}, u32[]{:S(2)}, u32[]{:S(2)}) collective-permute-start(bf16[3,64,2048]{2,1,0:T(8,128)(2,1)S(1)} %pad_maximum_fusion.refs_7_.own), channel_id=1, source_target_pairs={{0,1},{1,0},{2,3},{3,2},{4,5},{5,4},{6,7},{7,6},{8,9},{9,8},{10,11... | collective-permute-start | bytes 2359304 | tf_op jit(solution)/shard_map/ppermute | solution.py:348
  41.4 3.5 %collective-permute-start.4 = (bf16[32,32,256]{2,1,0:T(8,128)(2,1)S(1)}, bf16[32,32,256]{2,1,0:T(8,128)(2,1)S(1)}, u32[]{:S(2)}, u32[]{:S(2)}) collective-permute-start(bf16[32,32,256]{2,1,0:T(8,128)(2,1)S(1)} %collective-permute-done.3.refs_1_), channel_id=1, source_target_pairs={{0,2},{2,4},{4,6},{6,8},{8,10},{10,12},{12,14},{14,0},{1,15},{3,1}... | collective-permute-start | bytes 1572872 | tf_op jit(solution)/shard_map/ppermute | solution.py:353
  44.9 2.0 %collective-permute-done.refs_2_ = bf16[32,32,256]{2,1,0:T(8,128)(2,1)S(1)} collective-permute-done((bf16[32,32,256]{2,1,0:T(8,128)(2,1)S(1)}, bf16[32,32,256]{2,1,0:T(8,128)(2,1)S(1)}, u32[]{:S(2)}, u32[]{:S(2)}) %collective-permute-start) | collective-permute-done | bytes 524320 | tf_op jit(solution)/shard_map/ppermute | solution.py:351
  47.0 3.5 %collective-permute-start.1 = (bf16[32,32,256]{2,1,0:T(8,128)(2,1)S(1)}, bf16[32,32,256]{2,1,0:T(8,128)(2,1)S(1)}, u32[]{:S(2)}, u32[]{:S(2)}) collective-permute-start(bf16[32,32,256]{2,1,0:T(8,128)(2,1)S(1)} %collective-permute-done.refs_2_), channel_id=1, source_target_pairs={{0,2},{2,4},{4,6},{6,8},{8,10},{10,12},{12,14},{14,0},{1,15},{3,1}... | collective-permute-start | bytes 1572872 | tf_op jit(solution)/shard_map/ppermute | solution.py:354
  50.4 1.9 %collective-permute-start.6 = (bf16[32,32,256]{2,1,0:T(8,128)(2,1)S(1)}, bf16[32,32,256]{2,1,0:T(8,128)(2,1)S(1)}, u32[]{:S(2)}, u32[]{:S(2)}) collective-permute-start(bf16[32,32,256]{2,1,0:T(8,128)(2,1)S(1)} %collective-permute-done.refs_2_), channel_id=1, source_target_pairs={{0,1},{1,0},{2,3},{3,2},{4,5},{5,4},{6,7},{7,6},{8,9},{9,8},{10,11... | collective-permute-start | bytes 1572872 | tf_op jit(solution)/shard_map/ppermute | solution.py:356
  53.0 1.9 %collective-permute-start.7 = (bf16[32,32,256]{2,1,0:T(8,128)(2,1)S(1)}, bf16[32,32,256]{2,1,0:T(8,128)(2,1)S(1)}, u32[]{:S(2)}, u32[]{:S(2)}) collective-permute-start(bf16[32,32,256]{2,1,0:T(8,128)(2,1)S(1)} %collective-permute-done.4.refs_3_), channel_id=1, source_target_pairs={{0,1},{1,0},{2,3},{3,2},{4,5},{5,4},{6,7},{7,6},{8,9},{9,8},{10,11... | collective-permute-start | bytes 1572872 | tf_op jit(solution)/shard_map/ppermute | solution.py:357
  55.0 3.7 %collective-permute-done.1.refs_4_ = bf16[32,32,256]{2,1,0:T(8,128)(2,1)S(1)} collective-permute-done((bf16[32,32,256]{2,1,0:T(8,128)(2,1)S(1)}, bf16[32,32,256]{2,1,0:T(8,128)(2,1)S(1)}, u32[]{:S(2)}, u32[]{:S(2)}) %collective-permute-start.1) | collective-permute-done | bytes 524320 | tf_op jit(solution)/shard_map/ppermute | solution.py:354
  58.7 1.9 %collective-permute-start.2 = (bf16[32,32,256]{2,1,0:T(8,128)(2,1)S(1)}, bf16[32,32,256]{2,1,0:T(8,128)(2,1)S(1)}, u32[]{:S(2)}, u32[]{:S(2)}) collective-permute-start(bf16[32,32,256]{2,1,0:T(8,128)(2,1)S(1)} %collective-permute-done.1.refs_4_), channel_id=1, source_target_pairs={{0,1},{1,0},{2,3},{3,2},{4,5},{5,4},{6,7},{7,6},{8,9},{9,8},{10,11... | collective-permute-start | bytes 1572872 | tf_op jit(solution)/shard_map/ppermute | solution.py:358
  60.6 1.1 shard_map.214
  63.4 3.2 %collective-permute-start.8 = (bf16[512,256]{1,0:T(8,128)(2,1)S(1)}, bf16[512,256]{1,0:T(8,128)(2,1)S(1)}, u32[]{:S(2)}, u32[]{:S(2)}) collective-permute-start(bf16[512,256]{1,0:T(8,128)(2,1)S(1)} %get-tuple-element.56), channel_id=1, source_target_pairs={{0,2},{2,4},{4,6},{6,8},{8,10},{10,12},{12,14},{14,0},{1,15},{3,1}... | collective-permute-start | bytes 786440 | tf_op jit(solution)/shard_map/ppermute | solution.py:370
  66.6 7.7 %collective-permute-start.9 = (bf16[512,256]{1,0:T(8,128)(2,1)S(1)}, bf16[512,256]{1,0:T(8,128)(2,1)S(1)}, u32[]{:S(2)}, u32[]{:S(2)}) collective-permute-start(bf16[512,256]{1,0:T(8,128)(2,1)S(1)} %get-tuple-element.57), channel_id=1, source_target_pairs={{0,4},{2,6},{4,8},{6,10},{8,12},{10,14},{12,0},{14,2},{1,13},{3,15... | collective-permute-start | bytes 786440 | tf_op jit(solution)/shard_map/ppermute | solution.py:370
  74.4 1.9 %collective-permute-start.10 = (bf16[512,256]{1,0:T(8,128)(2,1)S(1)}, bf16[512,256]{1,0:T(8,128)(2,1)S(1)}, u32[]{:S(2)}, u32[]{:S(2)}) collective-permute-start(bf16[512,256]{1,0:T(8,128)(2,1)S(1)} %get-tuple-element.58), channel_id=1, source_target_pairs={{0,6},{2,8},{4,10},{6,12},{8,14},{10,0},{12,2},{14,4},{1,11},{3,13... | collective-permute-start | bytes 786440 | tf_op jit(solution)/shard_map/ppermute | solution.py:370
  76.3 4.7 %collective-permute-start.11 = (bf16[512,128]{1,0:T(8,128)(2,1)S(1)}, bf16[512,128]{1,0:T(8,128)(2,1)S(1)}, u32[]{:S(2)}, u32[]{:S(2)}) collective-permute-start(bf16[512,128]{1,0:T(8,128)(2,1)S(1)} %get-tuple-element.59), channel_id=1, source_target_pairs={{0,8},{2,10},{4,12},{6,14},{8,0},{10,2},{12,4},{14,6},{1,9},{3,11}... | collective-permute-start | bytes 393224 | tf_op jit(solution)/shard_map/ppermute | solution.py:370
  81.0 1.7 shard_map.216
  82.7 8.1 %collective-permute-done.11.last = bf16[512,128]{1,0:T(8,128)(2,1)S(1)} collective-permute-done((bf16[512,128]{1,0:T(8,128)(2,1)S(1)}, bf16[512,128]{1,0:T(8,128)(2,1)S(1)}, u32[]{:S(2)}, u32[]{:S(2)}) %collective-permute-start.11) | collective-permute-done | bytes 131104 | tf_op jit(solution)/shard_map/ppermute | solution.py:370
  90.8 4.3 %collective-permute-done.10.far = bf16[512,256]{1,0:T(8,128)(2,1)S(1)} collective-permute-done((bf16[512,256]{1,0:T(8,128)(2,1)S(1)}, bf16[512,256]{1,0:T(8,128)(2,1)S(1)}, u32[]{:S(2)}, u32[]{:S(2)}) %collective-permute-start.10) | collective-permute-done | bytes 262176 | tf_op jit(solution)/shard_map/ppermute | solution.py:370
  95.9 5.4 %all-to-all-start.1 = ((bf16[64,16,128]{2,1,0:T(8,128)(2,1)}), bf16[64,16,128]{2,1,0:T(8,128)(2,1)S(1)}, u32[]{:S(2)}, u32[]{:S(2)}) async-start(bf16[64,16,128]{2,1,0:T(8,128)(2,1)} %bitcast.15), calls=%async_computation.1 | async-start | bytes 524288 | tf_op jit(solution)/shard_map/all_to_all | solution.py:379
  101.3 12.9 %all-to-all-done.1 = bf16[64,16,128]{2,1,0:T(8,128)(2,1)S(1)} async-done(((bf16[64,16,128]{2,1,0:T(8,128)(2,1)}), bf16[64,16,128]{2,1,0:T(8,128)(2,1)S(1)}, u32[]{:S(2)}, u32[]{:S(2)}) %all-to-all-start.1) | async-done | bytes 262176 | tf_op jit(solution)/shard_map/all_to_all | solution.py:379
  115.3 18.8 %all_gather.3.gathered = bf16[2048,128]{1,0:T(8,128)(2,1)S(1)} all-gather(bf16[128,128]{1,0:T(8,128)(2,1)} %combine.1), channel_id=1, replica_groups=mesh['z'=8,'x'=4,'y'=8,'core'=2] {'y','core'}, dimensions={0}, use_global_device_ids=true | all-gather | bytes 557056 | tf_op jit(solution)/shard_map/all_gather | solution.py:382
  134.2 1.8 %shard_map.218 = (bf16[128,256]{1,0:T(8,128)(2,1)}, f32[128,256]{1,0:T(8,128)S(1)}, f32[8,128]{1,0:T(8,128)S(1)}, bf16[32,16,128]{2,1,0:T(8,128)(2,1)}, bf16[32,...) custom-call(s32[1]{0:T(128)} %bitcast.14.spot, ...), custom_call_target="tpu_custom_call" | custom-call | tf_op jit(solution)/shard_map/pallas_call | solution.py:75
  136.0 2.8 %collective-permute-start.12 = (bf16[32,32,128]{2,1,0:T(8,128)(2,1)S(1)}, bf16[32,32,128]{2,1,0:T(8,128)(2,1)S(1)}, u32[]{:S(2)}, u32[]{:S(2)}) collective-permute-start(bf16[32,32,128]{2,1,0:T(8,128)(2,1)S(1)} %get-tuple-element.85), channel_id=1, source_target_pairs={{0,16},{16,32},{32,48},{48,0},{1,17},{17,33},{33,49},{49,1},{2,18}... | collective-permute-start | bytes 786440 | tf_op jit(solution)/shard_map/ppermute | solution.py:394
  138.8 4.3 %collective-permute-start.13 = (bf16[32,32,128]{2,1,0:T(8,128)(2,1)S(1)}, bf16[32,32,128]{2,1,0:T(8,128)(2,1)S(1)}, u32[]{:S(2)}, u32[]{:S(2)}) collective-permute-start(bf16[32,32,128]{2,1,0:T(8,128)(2,1)S(1)} %get-tuple-element.86), channel_id=1, source_target_pairs={{0,32},{16,48},{32,0},{48,16},{1,33},{17,49},{33,1},{49,17},{2,34}... | collective-permute-start | bytes 786440 | tf_op jit(solution)/shard_map/ppermute | solution.py:394
  143.2 3.3 %collective-permute-start.14 = (bf16[32,32,128]{2,1,0:T(8,128)(2,1)S(1)}, bf16[32,32,128]{2,1,0:T(8,128)(2,1)S(1)}, u32[]{:S(2)}, u32[]{:S(2)}) collective-permute-start(bf16[32,32,128]{2,1,0:T(8,128)(2,1)S(1)} %get-tuple-element.87), channel_id=1, source_target_pairs={{0,48},{16,0},{32,16},{48,32},{1,49},{17,1},{33,17},{49,33},{2,50}... | collective-permute-start | bytes 786440 | tf_op jit(solution)/shard_map/ppermute | solution.py:394
  146.5 4.7 %all-to-all-start.2 = ((bf16[32,16,128]{2,1,0:T(8,128)(2,1)}), bf16[32,16,128]{2,1,0:T(8,128)(2,1)S(1)}, u32[]{:S(2)}, u32[]{:S(2)}) async-start(bf16[32,16,128]{2,1,0:T(8,128)(2,1)} %get-tuple-element.75), calls=%async_computation.2 | async-start | bytes 262144 | tf_op jit(solution)/shard_map/all_to_all | solution.py:392
  151.3 1.5 shard_map.219
  152.7 9.0 %all-to-all-done.2.received = bf16[32,16,128]{2,1,0:T(8,128)(2,1)S(1)} async-done(((bf16[32,16,128]{2,1,0:T(8,128)(2,1)}), bf16[32,16,128]{2,1,0:T(8,128)(2,1)S(1)}, u32[]{:S(2)}, u32[]{:S(2)}) %all-to-all-start.2) | async-done | bytes 131104 | tf_op jit(solution)/shard_map/all_to_all | solution.py:392
  162.0 17.1 %all_to_all.21.second = bf16[32,48,128]{2,1,0:T(8,128)(2,1)S(1)} all-to-all(bf16[32,48,128]{2,1,0:T(8,128)(2,1)S(1)} %shard_map.220), channel_id=1, replica_groups=mesh['z'=8,'x'=4,'y'=8,'core'=2] {'z','x'}, dimensions={0} | all-to-all | bytes 786432 | tf_op jit(solution)/shard_map/all_to_all | solution.py:401
  179.1 1.2 shard_map.221
  (42 shorter events, 4.6 us)
Async XLA Ops:
  2.9 36.5 %copy-start.10 = (bf16[1,64,2048]{2,1,0:T(8,128)(2,1)S(1)}, bf16[1,64,2048]{2,1,0:T(8,128)(2,1)}, u32[]{:S(2)}) copy-start(bf16[1,64,2048]{2,1,0:T(8,128)(2,1)} %param.21) | copy-start | bytes 786436
  2.9 36.5 %copy-start.11 = (bf16[1,2048,64]{1,2,0:T(8,128)(2,1)S(1)}, bf16[1,2048,64]{1,2,0:T(8,128)(2,1)}, u32[]{:S(2)}) copy-start(bf16[1,2048,64]{1,2,0:T(8,128)(2,1)} %param.20) | copy-start | bytes 786436
  2.9 36.5 %copy-start.12 = (bf16[1,2048,64]{1,2,0:T(8,128)(2,1)S(1)}, bf16[1,2048,64]{1,2,0:T(8,128)(2,1)}, u32[]{:S(2)}) copy-start(bf16[1,2048,64]{1,2,0:T(8,128)(2,1)} %param.19) | copy-start | bytes 786436
  34.0 7.5 %collective-permute-start.3 = (bf16[32,32,256]{2,1,0:T(8,128)(2,1)S(1)}, bf16[32,32,256]{2,1,0:T(8,128)(2,1)S(1)}, u32[]{:S(2)}, u32[]{:S(2)}) collective-permute-start(bf16[32,32,256]{2,1,0:T(8,128)(2,1)S(1)} %all_to_all.20.refs_0_), channel_id=1, source_target_pairs={{0,1},{1,0},{2,3},{3,2},{4,5},{5,4},{6,7},{7,6},{8,9},{9,8},{10,11... | collective-permute-start | bytes 1572872 | tf_op jit(solution)/shard_map/ppermute | solution.py:352
  35.9 11.1 %collective-permute-start = (bf16[32,32,256]{2,1,0:T(8,128)(2,1)S(1)}, bf16[32,32,256]{2,1,0:T(8,128)(2,1)S(1)}, u32[]{:S(2)}, u32[]{:S(2)}) collective-permute-start(bf16[32,32,256]{2,1,0:T(8,128)(2,1)S(1)} %all_to_all.20.refs_0_), channel_id=1, source_target_pairs={{0,2},{2,4},{4,6},{6,8},{8,10},{10,12},{12,14},{14,0},{1,15},{3,1}... | collective-permute-start | bytes 1572872 | tf_op jit(solution)/shard_map/ppermute | solution.py:351
  39.5 10.9 %collective-permute-start.5 = (bf16[3,64,2048]{2,1,0:T(8,128)(2,1)S(1)}, bf16[3,64,2048]{2,1,0:T(8,128)(2,1)S(1)}, u32[]{:S(2)}, u32[]{:S(2)}) collective-permute-start(bf16[3,64,2048]{2,1,0:T(8,128)(2,1)S(1)} %pad_maximum_fusion.refs_7_.own), channel_id=1, source_target_pairs={{0,1},{1,0},{2,3},{3,2},{4,5},{5,4},{6,7},{7,6},{8,9},{9,8},{10,11... | collective-permute-start | bytes 2359304 | tf_op jit(solution)/shard_map/ppermute | solution.py:348
  41.4 11.6 %collective-permute-start.4 = (bf16[32,32,256]{2,1,0:T(8,128)(2,1)S(1)}, bf16[32,32,256]{2,1,0:T(8,128)(2,1)S(1)}, u32[]{:S(2)}, u32[]{:S(2)}) collective-permute-start(bf16[32,32,256]{2,1,0:T(8,128)(2,1)S(1)} %collective-permute-done.3.refs_1_), channel_id=1, source_target_pairs={{0,2},{2,4},{4,6},{6,8},{8,10},{10,12},{12,14},{14,0},{1,15},{3,1}... | collective-permute-start | bytes 1572872 | tf_op jit(solution)/shard_map/ppermute | solution.py:353
  47.0 11.7 %collective-permute-start.1 = (bf16[32,32,256]{2,1,0:T(8,128)(2,1)S(1)}, bf16[32,32,256]{2,1,0:T(8,128)(2,1)S(1)}, u32[]{:S(2)}, u32[]{:S(2)}) collective-permute-start(bf16[32,32,256]{2,1,0:T(8,128)(2,1)S(1)} %collective-permute-done.refs_2_), channel_id=1, source_target_pairs={{0,2},{2,4},{4,6},{6,8},{8,10},{10,12},{12,14},{14,0},{1,15},{3,1}... | collective-permute-start | bytes 1572872 | tf_op jit(solution)/shard_map/ppermute | solution.py:354
  50.4 10.1 %collective-permute-start.6 = (bf16[32,32,256]{2,1,0:T(8,128)(2,1)S(1)}, bf16[32,32,256]{2,1,0:T(8,128)(2,1)S(1)}, u32[]{:S(2)}, u32[]{:S(2)}) collective-permute-start(bf16[32,32,256]{2,1,0:T(8,128)(2,1)S(1)} %collective-permute-done.refs_2_), channel_id=1, source_target_pairs={{0,1},{1,0},{2,3},{3,2},{4,5},{5,4},{6,7},{7,6},{8,9},{9,8},{10,11... | collective-permute-start | bytes 1572872 | tf_op jit(solution)/shard_map/ppermute | solution.py:356
  53.0 7.5 %collective-permute-start.7 = (bf16[32,32,256]{2,1,0:T(8,128)(2,1)S(1)}, bf16[32,32,256]{2,1,0:T(8,128)(2,1)S(1)}, u32[]{:S(2)}, u32[]{:S(2)}) collective-permute-start(bf16[32,32,256]{2,1,0:T(8,128)(2,1)S(1)} %collective-permute-done.4.refs_3_), channel_id=1, source_target_pairs={{0,1},{1,0},{2,3},{3,2},{4,5},{5,4},{6,7},{7,6},{8,9},{9,8},{10,11... | collective-permute-start | bytes 1572872 | tf_op jit(solution)/shard_map/ppermute | solution.py:357
  58.7 3.8 %collective-permute-start.2 = (bf16[32,32,256]{2,1,0:T(8,128)(2,1)S(1)}, bf16[32,32,256]{2,1,0:T(8,128)(2,1)S(1)}, u32[]{:S(2)}, u32[]{:S(2)}) collective-permute-start(bf16[32,32,256]{2,1,0:T(8,128)(2,1)S(1)} %collective-permute-done.1.refs_4_), channel_id=1, source_target_pairs={{0,1},{1,0},{2,3},{3,2},{4,5},{5,4},{6,7},{7,6},{8,9},{9,8},{10,11... | collective-permute-start | bytes 1572872 | tf_op jit(solution)/shard_map/ppermute | solution.py:358
  63.4 27.4 %collective-permute-start.8 = (bf16[512,256]{1,0:T(8,128)(2,1)S(1)}, bf16[512,256]{1,0:T(8,128)(2,1)S(1)}, u32[]{:S(2)}, u32[]{:S(2)}) collective-permute-start(bf16[512,256]{1,0:T(8,128)(2,1)S(1)} %get-tuple-element.56), channel_id=1, source_target_pairs={{0,2},{2,4},{4,6},{6,8},{8,10},{10,12},{12,14},{14,0},{1,15},{3,1}... | collective-permute-start | bytes 786440 | tf_op jit(solution)/shard_map/ppermute | solution.py:370
  66.6 24.2 %collective-permute-start.9 = (bf16[512,256]{1,0:T(8,128)(2,1)S(1)}, bf16[512,256]{1,0:T(8,128)(2,1)S(1)}, u32[]{:S(2)}, u32[]{:S(2)}) collective-permute-start(bf16[512,256]{1,0:T(8,128)(2,1)S(1)} %get-tuple-element.57), channel_id=1, source_target_pairs={{0,4},{2,6},{4,8},{6,10},{8,12},{10,14},{12,0},{14,2},{1,13},{3,15... | collective-permute-start | bytes 786440 | tf_op jit(solution)/shard_map/ppermute | solution.py:370
  74.4 20.7 %collective-permute-start.10 = (bf16[512,256]{1,0:T(8,128)(2,1)S(1)}, bf16[512,256]{1,0:T(8,128)(2,1)S(1)}, u32[]{:S(2)}, u32[]{:S(2)}) collective-permute-start(bf16[512,256]{1,0:T(8,128)(2,1)S(1)} %get-tuple-element.58), channel_id=1, source_target_pairs={{0,6},{2,8},{4,10},{6,12},{8,14},{10,0},{12,2},{14,4},{1,11},{3,13... | collective-permute-start | bytes 786440 | tf_op jit(solution)/shard_map/ppermute | solution.py:370
  76.3 14.5 %collective-permute-start.11 = (bf16[512,128]{1,0:T(8,128)(2,1)S(1)}, bf16[512,128]{1,0:T(8,128)(2,1)S(1)}, u32[]{:S(2)}, u32[]{:S(2)}) collective-permute-start(bf16[512,128]{1,0:T(8,128)(2,1)S(1)} %get-tuple-element.59), channel_id=1, source_target_pairs={{0,8},{2,10},{4,12},{6,14},{8,0},{10,2},{12,4},{14,6},{1,9},{3,11}... | collective-permute-start | bytes 393224 | tf_op jit(solution)/shard_map/ppermute | solution.py:370
  95.1 19.2 %copy-start.7 = (s32[8,128]{1,0:T(8,128)S(1)}, s32[8,128]{1,0:T(8,128)}, u32[]{:S(2)}) copy-start(s32[8,128]{1,0:T(8,128)} %get-tuple-element.69.target) | copy-start | bytes 12292
  95.9 18.3 %copy-start = (bf16[128,2048]{1,0:T(8,128)(2,1)S(1)}, bf16[128,2048]{1,0:T(8,128)(2,1)}, u32[]{:S(2)}) copy-start(bf16[128,2048]{1,0:T(8,128)(2,1)} %cotangent.1) | copy-start | bytes 1572868
  95.9 38.2 %copy-start.1 = (bf16[256,2048]{1,0:T(8,128)(2,1)S(1)}, bf16[256,2048]{1,0:T(8,128)(2,1)}, u32[]{:S(2)}) copy-start(bf16[256,2048]{1,0:T(8,128)(2,1)} %weight.1) | copy-start | bytes 3145732
  95.9 18.3 %all-to-all-start.1 = ((bf16[64,16,128]{2,1,0:T(8,128)(2,1)}), bf16[64,16,128]{2,1,0:T(8,128)(2,1)S(1)}, u32[]{:S(2)}, u32[]{:S(2)}) async-start(bf16[64,16,128]{2,1,0:T(8,128)(2,1)} %bitcast.15), calls=%async_computation.1 | async-start | bytes 524288 | tf_op jit(solution)/shard_map/all_to_all | solution.py:379
  115.2 18.9 %copy-start.2 = (bf16[128,256]{1,0:T(8,128)(2,1)S(1)}, bf16[128,256]{1,0:T(8,128)(2,1)}, u32[]{:S(2)}) copy-start(bf16[128,256]{1,0:T(8,128)(2,1)} %gate_pre.1) | copy-start | bytes 196612
  115.3 18.9 %copy-start.3 = (bf16[128,256]{1,0:T(8,128)(2,1)S(1)}, bf16[128,256]{1,0:T(8,128)(2,1)}, u32[]{:S(2)}) copy-start(bf16[128,256]{1,0:T(8,128)(2,1)} %mixer.1) | copy-start | bytes 196612
  115.3 18.9 %copy-start.5 = (bf16[128,128]{1,0:T(8,128)(2,1)S(1)}, bf16[128,128]{1,0:T(8,128)(2,1)}, u32[]{:S(2)}) copy-start(bf16[128,128]{1,0:T(8,128)(2,1)} %read.3) | copy-start | bytes 98308
  115.3 18.9 %copy-start.8 = (f32[4,128]{1,0:T(4,128)S(1)}, f32[4,128]{1,0:T(4,128)}, u32[]{:S(2)}) copy-start(f32[4,128]{1,0:T(4,128)} %logs.1) | copy-start | bytes 6148
  136.0 25.8 %collective-permute-start.12 = (bf16[32,32,128]{2,1,0:T(8,128)(2,1)S(1)}, bf16[32,32,128]{2,1,0:T(8,128)(2,1)S(1)}, u32[]{:S(2)}, u32[]{:S(2)}) collective-permute-start(bf16[32,32,128]{2,1,0:T(8,128)(2,1)S(1)} %get-tuple-element.85), channel_id=1, source_target_pairs={{0,16},{16,32},{32,48},{48,0},{1,17},{17,33},{33,49},{49,1},{2,18}... | collective-permute-start | bytes 786440 | tf_op jit(solution)/shard_map/ppermute | solution.py:394
  138.8 23.0 %collective-permute-start.13 = (bf16[32,32,128]{2,1,0:T(8,128)(2,1)S(1)}, bf16[32,32,128]{2,1,0:T(8,128)(2,1)S(1)}, u32[]{:S(2)}, u32[]{:S(2)}) collective-permute-start(bf16[32,32,128]{2,1,0:T(8,128)(2,1)S(1)} %get-tuple-element.86), channel_id=1, source_target_pairs={{0,32},{16,48},{32,0},{48,16},{1,33},{17,49},{33,1},{49,17},{2,34}... | collective-permute-start | bytes 786440 | tf_op jit(solution)/shard_map/ppermute | solution.py:394
  143.2 18.6 %collective-permute-start.14 = (bf16[32,32,128]{2,1,0:T(8,128)(2,1)S(1)}, bf16[32,32,128]{2,1,0:T(8,128)(2,1)S(1)}, u32[]{:S(2)}, u32[]{:S(2)}) collective-permute-start(bf16[32,32,128]{2,1,0:T(8,128)(2,1)S(1)} %get-tuple-element.87), channel_id=1, source_target_pairs={{0,48},{16,0},{32,16},{48,32},{1,49},{17,1},{33,17},{49,33},{2,50}... | collective-permute-start | bytes 786440 | tf_op jit(solution)/shard_map/ppermute | solution.py:394
  146.5 4.8 %copy-start.4 = (bf16[128,256]{1,0:T(8,128)(2,1)S(1)}, bf16[128,256]{1,0:T(8,128)(2,1)}, u32[]{:S(2)}) copy-start(bf16[128,256]{1,0:T(8,128)(2,1)} %values.3) | copy-start | bytes 196612
  146.5 4.7 %copy-start.6 = (bf16[128,128]{1,0:T(8,128)(2,1)S(1)}, bf16[128,128]{1,0:T(8,128)(2,1)}, u32[]{:S(2)}) copy-start(bf16[128,128]{1,0:T(8,128)(2,1)} %write.3) | copy-start | bytes 98308
  146.5 4.7 %copy-start.9 = (f32[1,4,64,128]{3,2,1,0:T(8,128)S(1)}, f32[1,4,64,128]{3,2,1,0:T(8,128)}, u32[]{:S(2)}) copy-start(f32[1,4,64,128]{3,2,1,0:T(8,128)} %param.29) | copy-start | bytes 393220
  146.5 15.3 %all-to-all-start.2 = ((bf16[32,16,128]{2,1,0:T(8,128)(2,1)}), bf16[32,16,128]{2,1,0:T(8,128)(2,1)S(1)}, u32[]{:S(2)}, u32[]{:S(2)}) async-start(bf16[32,16,128]{2,1,0:T(8,128)(2,1)} %get-tuple-element.75), calls=%async_computation.2 | async-start | bytes 262144 | tf_op jit(solution)/shard_map/all_to_all | solution.py:392

commit v12 on v9

--- a/solution.py
+++ b/solution.py
@@ -288,8 +288,7 @@
     out[:, 0:EXP, :] = total.astype(BF)
     state = jnp.zeros((8, STATE), F32)
     for k in reversed(range(EXP)):
-        high, low = two_parts(state)
-        out[k, EXP:, :] = jnp.concatenate([high.astype(F32), low.astype(F32)], axis=0).astype(BF)
+        out[k, EXP:, :] = state.astype(BF)
         if k > 0:
             piece = received[k].astype(F32)
             log = piece[8:9] + piece[9:10] + piece[10:11]
@@ -325,12 +324,10 @@
     running = run[...]
     ends = jnp.exp(running[:, TOK - 1 : TOK] - running).T
     scale = jnp.concatenate([jnp.broadcast_to(ends[:, j : j + 1], (TOK, HD)) for j in range(HEADS)], axis=1)
-    later = second[:, EXP:, :].astype(F32)
-    high = later[:, 0:8].reshape(HEADS * HD, STATE).astype(BF)
-    low = later[:, 8:16].reshape(HEADS * HD, STATE).astype(BF)
-    d_values[...] = (dx[...] + scale * (mm_nt(write[...], high) + mm_nt(write[...], low))).astype(BF)
+    later = second[:, EXP:, :].astype(F32).reshape(HEADS * HD, STATE).astype(BF)
+    d_values[...] = (dx[...] + scale * mm_nt(write[...], later)).astype(BF)
     top, rest = two_parts(values[...].astype(F32) * scale)
-    d_write[...] = dw[...] + mm(top, high) + mm(top, low) + mm(rest, high)
+    d_write[...] = dw[...] + mm(top, later) + mm(rest, later)
     for r in range(4):
         total = second[r, 0:EXP, :].astype(F32)
         for k in range(1, 8):
@@ -402,7 +399,7 @@
         inner_kernel, (shape((TOK, HEADS * HD), F32), square, square),
         [vmem()] * 6, (grad_y, values, write_keys, read_keys, run, entry_states[0]), flops=10**9)
     received, dx, dw, d_read = lax.optimization_barrier((received, dx, dw, d_read))
-    states = call(scan_kernel, shape((EXP, 48, STATE), BF), [vmem()] * 5, (received, *shares))
+    states = call(scan_kernel, shape((EXP, 40, STATE), BF), [vmem()] * 5, (received, *shares))
     second = lax.all_to_all(states, SP, 0, 0, tiled=True)
     d_values, d_write, d_out_weight = call(
         outer_kernel, (flat, square, shape((D // EXP, HEADS * HD), F32)), [vmem()] * 6,

time: 181 us -> 180 us (level)
  no operation moved by 1% of the time
where the time goes in v12:
time: 180 us; the launch traced here: 179 us
  blocking collectives  66.1 us (37%)
  starting transfers between devices  58.8 us (33%)
  waiting for transfers between devices  40.5 us (22%)
  Pallas kernels  12.4 us (7%)
    all_to_all x1, blocking collectives, step(): c0 = lax.all_to_all(buf, SP, 0, 0, tiled=True)  31.1 us
    all_gather x1, blocking collectives, step(): whole = lax.all_gather(d_input, TP, axis=0, tiled=True)  18.8 us
    ppermute x4, starting transfers between devices, step(): pieces.append(lax.ppermute(parts[k], TP, rings[k]))  17.6 us
    all_to_all x1, blocking collectives, step(): second = lax.all_to_all(states, SP, 0, 0, tiled=True)  16.3 us
    ppermute x4, waiting for transfers between devices, step(): pieces.append(lax.ppermute(parts[k], TP, rings[k]))  12.4 us
    all_to_all x1, waiting for transfers between devices, step(): back = lax.all_to_all(summed, SP, 0, 0, tiled=True)  10.9 us
    ppermute x3, starting transfers between devices, step(): lax.ppermute(shares[k], 'x', [(i, (i + k) % 4) for i in range(4)])  9.61 us
    pallas_call x9, Pallas kernels, call(): pl.pallas_call(kernel, out_shape=outs, in_specs=specs, out_specs=jax.tree...  9.22 us
  transfers between devices with their start and end apart: 18, of which 9 were waited for; matrix products, arithmetic and copies ran while one was open for 0% of the time, Pallas kernels for 2%

profile of v12, /device:TPU:8, one launch (start us, length us, event | category | flops | bytes accessed | tf_op | source)
XLA Modules:
  0.0 179.0 jit_solution(17107258227126059407)
XLA Ops:
  0.6 2.2 %prepare.1 = (bf16[32,32,256]{2,1,0:T(8,128)(2,1)}, s32[8,128]{1,0:T(8,128)}) custom-call(s32[1]{0:T(128)} %bitcast.where, s32[2,128]{1,0:T(2,128)} %bitcast.25, f32[2,128]{1,0:T(2,128)} %bitcast.26, bf16[128,2048]{1,0:T(8,128)(2,1)} %mix.1, bf16[128,2048]{1,0:T(8,128)(2,1)} %cotangent.1), custom_call_target="tpu_custom_call" | custom-call | tf_op jit(solution)/shard_map/prepare/pallas_call | solution.py:112
  2.9 31.1 %all_to_all.20.refs_0_ = bf16[32,32,256]{2,1,0:T(8,128)(2,1)S(1)} all-to-all(bf16[32,32,256]{2,1,0:T(8,128)(2,1)} %get-tuple-element.53), channel_id=1, replica_groups=mesh['z'=8,'x'=4,'y'=8,'core'=2] {'z','x'}, dimensions={0} | all-to-all | bytes 1048576 | tf_op jit(solution)/shard_map/all_to_all | solution.py:351
  34.0 1.9 %collective-permute-start.3 = (bf16[32,32,256]{2,1,0:T(8,128)(2,1)S(1)}, bf16[32,32,256]{2,1,0:T(8,128)(2,1)S(1)}, u32[]{:S(2)}, u32[]{:S(2)}) collective-permute-start(bf16[32,32,256]{2,1,0:T(8,128)(2,1)S(1)} %all_to_all.20.refs_0_), channel_id=1, source_target_pairs={{0,1},{1,0},{2,3},{3,2},{4,5},{5,4},{6,7},{7,6},{8,9},{9,8},{10,11... | collective-permute-start | bytes 1572872 | tf_op jit(solution)/shard_map/ppermute | solution.py:353
  35.9 3.5 %collective-permute-start = (bf16[32,32,256]{2,1,0:T(8,128)(2,1)S(1)}, bf16[32,32,256]{2,1,0:T(8,128)(2,1)S(1)}, u32[]{:S(2)}, u32[]{:S(2)}) collective-permute-start(bf16[32,32,256]{2,1,0:T(8,128)(2,1)S(1)} %all_to_all.20.refs_0_), channel_id=1, source_target_pairs={{0,2},{2,4},{4,6},{6,8},{8,10},{10,12},{12,14},{14,0},{1,15},{3,1}... | collective-permute-start | bytes 1572872 | tf_op jit(solution)/shard_map/ppermute | solution.py:352
  39.5 1.9 %collective-permute-start.5 = (bf16[3,64,2048]{2,1,0:T(8,128)(2,1)S(1)}, bf16[3,64,2048]{2,1,0:T(8,128)(2,1)S(1)}, u32[]{:S(2)}, u32[]{:S(2)}) collective-permute-start(bf16[3,64,2048]{2,1,0:T(8,128)(2,1)S(1)} %pad_maximum_fusion.refs_7_.own), channel_id=1, source_target_pairs={{0,1},{1,0},{2,3},{3,2},{4,5},{5,4},{6,7},{7,6},{8,9},{9,8},{10,11... | collective-permute-start | bytes 2359304 | tf_op jit(solution)/shard_map/ppermute | solution.py:349
  41.4 3.5 %collective-permute-start.4 = (bf16[32,32,256]{2,1,0:T(8,128)(2,1)S(1)}, bf16[32,32,256]{2,1,0:T(8,128)(2,1)S(1)}, u32[]{:S(2)}, u32[]{:S(2)}) collective-permute-start(bf16[32,32,256]{2,1,0:T(8,128)(2,1)S(1)} %collective-permute-done.3.refs_1_), channel_id=1, source_target_pairs={{0,2},{2,4},{4,6},{6,8},{8,10},{10,12},{12,14},{14,0},{1,15},{3,1}... | collective-permute-start | bytes 1572872 | tf_op jit(solution)/shard_map/ppermute | solution.py:354
  44.9 2.0 %collective-permute-done.refs_2_ = bf16[32,32,256]{2,1,0:T(8,128)(2,1)S(1)} collective-permute-done((bf16[32,32,256]{2,1,0:T(8,128)(2,1)S(1)}, bf16[32,32,256]{2,1,0:T(8,128)(2,1)S(1)}, u32[]{:S(2)}, u32[]{:S(2)}) %collective-permute-start) | collective-permute-done | bytes 524320 | tf_op jit(solution)/shard_map/ppermute | solution.py:352
  47.0 3.5 %collective-permute-start.1 = (bf16[32,32,256]{2,1,0:T(8,128)(2,1)S(1)}, bf16[32,32,256]{2,1,0:T(8,128)(2,1)S(1)}, u32[]{:S(2)}, u32[]{:S(2)}) collective-permute-start(bf16[32,32,256]{2,1,0:T(8,128)(2,1)S(1)} %collective-permute-done.refs_2_), channel_id=1, source_target_pairs={{0,2},{2,4},{4,6},{6,8},{8,10},{10,12},{12,14},{14,0},{1,15},{3,1}... | collective-permute-start | bytes 1572872 | tf_op jit(solution)/shard_map/ppermute | solution.py:355
  50.5 1.9 %collective-permute-start.6 = (bf16[32,32,256]{2,1,0:T(8,128)(2,1)S(1)}, bf16[32,32,256]{2,1,0:T(8,128)(2,1)S(1)}, u32[]{:S(2)}, u32[]{:S(2)}) collective-permute-start(bf16[32,32,256]{2,1,0:T(8,128)(2,1)S(1)} %collective-permute-done.refs_2_), channel_id=1, source_target_pairs={{0,1},{1,0},{2,3},{3,2},{4,5},{5,4},{6,7},{7,6},{8,9},{9,8},{10,11... | collective-permute-start | bytes 1572872 | tf_op jit(solution)/shard_map/ppermute | solution.py:357
  53.1 1.9 %collective-permute-start.7 = (bf16[32,32,256]{2,1,0:T(8,128)(2,1)S(1)}, bf16[32,32,256]{2,1,0:T(8,128)(2,1)S(1)}, u32[]{:S(2)}, u32[]{:S(2)}) collective-permute-start(bf16[32,32,256]{2,1,0:T(8,128)(2,1)S(1)} %collective-permute-done.4.refs_3_), channel_id=1, source_target_pairs={{0,1},{1,0},{2,3},{3,2},{4,5},{5,4},{6,7},{7,6},{8,9},{9,8},{10,11... | collective-permute-start | bytes 1572872 | tf_op jit(solution)/shard_map/ppermute | solution.py:358
  55.0 3.7 %collective-permute-done.1.refs_4_ = bf16[32,32,256]{2,1,0:T(8,128)(2,1)S(1)} collective-permute-done((bf16[32,32,256]{2,1,0:T(8,128)(2,1)S(1)}, bf16[32,32,256]{2,1,0:T(8,128)(2,1)S(1)}, u32[]{:S(2)}, u32[]{:S(2)}) %collective-permute-start.1) | collective-permute-done | bytes 524320 | tf_op jit(solution)/shard_map/ppermute | solution.py:355
  58.7 1.9 %collective-permute-start.2 = (bf16[32,32,256]{2,1,0:T(8,128)(2,1)S(1)}, bf16[32,32,256]{2,1,0:T(8,128)(2,1)S(1)}, u32[]{:S(2)}, u32[]{:S(2)}) collective-permute-start(bf16[32,32,256]{2,1,0:T(8,128)(2,1)S(1)} %collective-permute-done.1.refs_4_), channel_id=1, source_target_pairs={{0,1},{1,0},{2,3},{3,2},{4,5},{5,4},{6,7},{7,6},{8,9},{9,8},{10,11... | collective-permute-start | bytes 1572872 | tf_op jit(solution)/shard_map/ppermute | solution.py:359
  63.4 3.2 %collective-permute-start.8 = (bf16[512,256]{1,0:T(8,128)(2,1)S(1)}, bf16[512,256]{1,0:T(8,128)(2,1)S(1)}, u32[]{:S(2)}, u32[]{:S(2)}) collective-permute-start(bf16[512,256]{1,0:T(8,128)(2,1)S(1)} %get-tuple-element.58), channel_id=1, source_target_pairs={{0,2},{2,4},{4,6},{6,8},{8,10},{10,12},{12,14},{14,0},{1,15},{3,1}... | collective-permute-start | bytes 786440 | tf_op jit(solution)/shard_map/ppermute | solution.py:371
  66.6 7.7 %collective-permute-start.9 = (bf16[512,256]{1,0:T(8,128)(2,1)S(1)}, bf16[512,256]{1,0:T(8,128)(2,1)S(1)}, u32[]{:S(2)}, u32[]{:S(2)}) collective-permute-start(bf16[512,256]{1,0:T(8,128)(2,1)S(1)} %get-tuple-element.59), channel_id=1, source_target_pairs={{0,4},{2,6},{4,8},{6,10},{8,12},{10,14},{12,0},{14,2},{1,13},{3,15... | collective-permute-start | bytes 786440 | tf_op jit(solution)/shard_map/ppermute | solution.py:371
  74.4 1.9 %collective-permute-start.10 = (bf16[512,256]{1,0:T(8,128)(2,1)S(1)}, bf16[512,256]{1,0:T(8,128)(2,1)S(1)}, u32[]{:S(2)}, u32[]{:S(2)}) collective-permute-start(bf16[512,256]{1,0:T(8,128)(2,1)S(1)} %get-tuple-element.60), channel_id=1, source_target_pairs={{0,6},{2,8},{4,10},{6,12},{8,14},{10,0},{12,2},{14,4},{1,11},{3,13... | collective-permute-start | bytes 786440 | tf_op jit(solution)/shard_map/ppermute | solution.py:371
  76.3 4.7 %collective-permute-start.11 = (bf16[512,128]{1,0:T(8,128)(2,1)S(1)}, bf16[512,128]{1,0:T(8,128)(2,1)S(1)}, u32[]{:S(2)}, u32[]{:S(2)}) collective-permute-start(bf16[512,128]{1,0:T(8,128)(2,1)S(1)} %get-tuple-element.61), channel_id=1, source_target_pairs={{0,8},{2,10},{4,12},{6,14},{8,0},{10,2},{12,4},{14,6},{1,9},{3,11}... | collective-permute-start | bytes 393224 | tf_op jit(solution)/shard_map/ppermute | solution.py:371
  81.0 1.7 shard_map.216
  82.7 8.1 %collective-permute-done.11.last = bf16[512,128]{1,0:T(8,128)(2,1)S(1)} collective-permute-done((bf16[512,128]{1,0:T(8,128)(2,1)S(1)}, bf16[512,128]{1,0:T(8,128)(2,1)S(1)}, u32[]{:S(2)}, u32[]{:S(2)}) %collective-permute-start.11) | collective-permute-done | bytes 131104 | tf_op jit(solution)/shard_map/ppermute | solution.py:371
  90.8 4.3 %collective-permute-done.10.far = bf16[512,256]{1,0:T(8,128)(2,1)S(1)} collective-permute-done((bf16[512,256]{1,0:T(8,128)(2,1)S(1)}, bf16[512,256]{1,0:T(8,128)(2,1)S(1)}, u32[]{:S(2)}, u32[]{:S(2)}) %collective-permute-start.10) | collective-permute-done | bytes 262176 | tf_op jit(solution)/shard_map/ppermute | solution.py:371
  95.2 2.3 %collective-permute-start.12 = (bf16[512,128]{1,0:T(8,128)(2,1)S(1)}, bf16[512,128]{1,0:T(8,128)(2,1)S(1)}, u32[]{:S(2)}, u32[]{:S(2)}) collective-permute-start(bf16[512,128]{1,0:T(8,128)(2,1)S(1)} %get-tuple-element.78), channel_id=1, source_target_pairs={{0,1},{1,0},{2,3},{3,2},{4,5},{5,4},{6,7},{7,6},{8,9},{9,8},{10,11... | collective-permute-start | bytes 393224 | tf_op jit(solution)/shard_map/ppermute | solution.py:380
  99.3 4.6 %all-to-all-start.1 = ((bf16[32,16,128]{2,1,0:T(8,128)(2,1)}), bf16[32,16,128]{2,1,0:T(8,128)(2,1)S(1)}, u32[]{:S(2)}, u32[]{:S(2)}) async-start(bf16[32,16,128]{2,1,0:T(8,128)(2,1)} %shard_map.218), calls=%async_computation.1 | async-start | bytes 262144 | tf_op jit(solution)/shard_map/all_to_all | solution.py:382
  104.0 10.9 %all-to-all-done.1.rows = bf16[32,16,128]{2,1,0:T(8,128)(2,1)S(1)} async-done(((bf16[32,16,128]{2,1,0:T(8,128)(2,1)}), bf16[32,16,128]{2,1,0:T(8,128)(2,1)S(1)}, u32[]{:S(2)}, u32[]{:S(2)}) %all-to-all-start.1) | async-done | bytes 131104 | tf_op jit(solution)/shard_map/all_to_all | solution.py:382
  115.9 18.8 %all_gather.3.gathered = bf16[2048,128]{1,0:T(8,128)(2,1)S(1)} all-gather(bf16[128,128]{1,0:T(8,128)(2,1)} %combine.1), channel_id=1, replica_groups=mesh['z'=8,'x'=4,'y'=8,'core'=2] {'y','core'}, dimensions={0}, use_global_device_ids=true | all-gather | bytes 557056 | tf_op jit(solution)/shard_map/all_gather | solution.py:384
  134.7 1.8 %shard_map.219 = (bf16[128,256]{1,0:T(8,128)(2,1)}, f32[128,256]{1,0:T(8,128)S(1)}, f32[8,128]{1,0:T(8,128)S(1)}, bf16[32,16,128]{2,1,0:T(8,128)(2,1)}, bf16[32,...) custom-call(s32[1]{0:T(128)} %bitcast.14.spot, ...), custom_call_target="tpu_custom_call" | custom-call | tf_op jit(solution)/shard_map/pallas_call | solution.py:75
  136.5 2.0 %collective-permute-start.13 = (bf16[32,32,128]{2,1,0:T(8,128)(2,1)S(1)}, bf16[32,32,128]{2,1,0:T(8,128)(2,1)S(1)}, u32[]{:S(2)}, u32[]{:S(2)}) collective-permute-start(bf16[32,32,128]{2,1,0:T(8,128)(2,1)S(1)} %get-tuple-element.89), channel_id=1, source_target_pairs={{0,16},{16,32},{32,48},{48,0},{1,17},{17,33},{33,49},{49,1},{2,18}... | collective-permute-start | bytes 786440 | tf_op jit(solution)/shard_map/ppermute | solution.py:396
  138.5 4.6 %collective-permute-start.14 = (bf16[32,32,128]{2,1,0:T(8,128)(2,1)S(1)}, bf16[32,32,128]{2,1,0:T(8,128)(2,1)S(1)}, u32[]{:S(2)}, u32[]{:S(2)}) collective-permute-start(bf16[32,32,128]{2,1,0:T(8,128)(2,1)S(1)} %get-tuple-element.90), channel_id=1, source_target_pairs={{0,32},{16,48},{32,0},{48,16},{1,33},{17,49},{33,1},{49,17},{2,34}... | collective-permute-start | bytes 786440 | tf_op jit(solution)/shard_map/ppermute | solution.py:396
  143.1 3.0 %collective-permute-start.15 = (bf16[32,32,128]{2,1,0:T(8,128)(2,1)S(1)}, bf16[32,32,128]{2,1,0:T(8,128)(2,1)S(1)}, u32[]{:S(2)}, u32[]{:S(2)}) collective-permute-start(bf16[32,32,128]{2,1,0:T(8,128)(2,1)S(1)} %get-tuple-element.91), channel_id=1, source_target_pairs={{0,48},{16,0},{32,16},{48,32},{1,49},{17,1},{33,17},{49,33},{2,50}... | collective-permute-start | bytes 786440 | tf_op jit(solution)/shard_map/ppermute | solution.py:396
  146.2 4.6 %all-to-all-start.2 = ((bf16[32,16,128]{2,1,0:T(8,128)(2,1)}), bf16[32,16,128]{2,1,0:T(8,128)(2,1)S(1)}, u32[]{:S(2)}, u32[]{:S(2)}) async-start(bf16[32,16,128]{2,1,0:T(8,128)(2,1)} %get-tuple-element.79), calls=%async_computation.2 | async-start | bytes 262144 | tf_op jit(solution)/shard_map/all_to_all | solution.py:394
  150.8 1.5 shard_map.220
  152.3 9.0 %all-to-all-done.2.received = bf16[32,16,128]{2,1,0:T(8,128)(2,1)S(1)} async-done(((bf16[32,16,128]{2,1,0:T(8,128)(2,1)}), bf16[32,16,128]{2,1,0:T(8,128)(2,1)S(1)}, u32[]{:S(2)}, u32[]{:S(2)}) %all-to-all-start.2) | async-done | bytes 131104 | tf_op jit(solution)/shard_map/all_to_all | solution.py:394
  161.6 16.3 %all_to_all.21.second = bf16[32,40,128]{2,1,0:T(8,128)(2,1)S(1)} all-to-all(bf16[32,40,128]{2,1,0:T(8,128)(2,1)S(1)} %shard_map.221), channel_id=1, replica_groups=mesh['z'=8,'x'=4,'y'=8,'core'=2] {'z','x'}, dimensions={0} | all-to-all | bytes 655360 | tf_op jit(solution)/shard_map/all_to_all | solution.py:403
  177.9 1.2 shard_map.222
  (45 shorter events, 6.7 us)
Async XLA Ops:
  2.9 36.5 %copy-start.10 = (bf16[1,64,2048]{2,1,0:T(8,128)(2,1)S(1)}, bf16[1,64,2048]{2,1,0:T(8,128)(2,1)}, u32[]{:S(2)}) copy-start(bf16[1,64,2048]{2,1,0:T(8,128)(2,1)} %param.21) | copy-start | bytes 786436
  2.9 36.5 %copy-start.11 = (bf16[1,2048,64]{1,2,0:T(8,128)(2,1)S(1)}, bf16[1,2048,64]{1,2,0:T(8,128)(2,1)}, u32[]{:S(2)}) copy-start(bf16[1,2048,64]{1,2,0:T(8,128)(2,1)} %param.20) | copy-start | bytes 786436
  2.9 36.5 %copy-start.12 = (bf16[1,2048,64]{1,2,0:T(8,128)(2,1)S(1)}, bf16[1,2048,64]{1,2,0:T(8,128)(2,1)}, u32[]{:S(2)}) copy-start(bf16[1,2048,64]{1,2,0:T(8,128)(2,1)} %param.19) | copy-start | bytes 786436
  34.0 7.5 %collective-permute-start.3 = (bf16[32,32,256]{2,1,0:T(8,128)(2,1)S(1)}, bf16[32,32,256]{2,1,0:T(8,128)(2,1)S(1)}, u32[]{:S(2)}, u32[]{:S(2)}) collective-permute-start(bf16[32,32,256]{2,1,0:T(8,128)(2,1)S(1)} %all_to_all.20.refs_0_), channel_id=1, source_target_pairs={{0,1},{1,0},{2,3},{3,2},{4,5},{5,4},{6,7},{7,6},{8,9},{9,8},{10,11... | collective-permute-start | bytes 1572872 | tf_op jit(solution)/shard_map/ppermute | solution.py:353
  35.9 11.1 %collective-permute-start = (bf16[32,32,256]{2,1,0:T(8,128)(2,1)S(1)}, bf16[32,32,256]{2,1,0:T(8,128)(2,1)S(1)}, u32[]{:S(2)}, u32[]{:S(2)}) collective-permute-start(bf16[32,32,256]{2,1,0:T(8,128)(2,1)S(1)} %all_to_all.20.refs_0_), channel_id=1, source_target_pairs={{0,2},{2,4},{4,6},{6,8},{8,10},{10,12},{12,14},{14,0},{1,15},{3,1}... | collective-permute-start | bytes 1572872 | tf_op jit(solution)/shard_map/ppermute | solution.py:352
  39.5 10.9 %collective-permute-start.5 = (bf16[3,64,2048]{2,1,0:T(8,128)(2,1)S(1)}, bf16[3,64,2048]{2,1,0:T(8,128)(2,1)S(1)}, u32[]{:S(2)}, u32[]{:S(2)}) collective-permute-start(bf16[3,64,2048]{2,1,0:T(8,128)(2,1)S(1)} %pad_maximum_fusion.refs_7_.own), channel_id=1, source_target_pairs={{0,1},{1,0},{2,3},{3,2},{4,5},{5,4},{6,7},{7,6},{8,9},{9,8},{10,11... | collective-permute-start | bytes 2359304 | tf_op jit(solution)/shard_map/ppermute | solution.py:349
  41.4 11.6 %collective-permute-start.4 = (bf16[32,32,256]{2,1,0:T(8,128)(2,1)S(1)}, bf16[32,32,256]{2,1,0:T(8,128)(2,1)S(1)}, u32[]{:S(2)}, u32[]{:S(2)}) collective-permute-start(bf16[32,32,256]{2,1,0:T(8,128)(2,1)S(1)} %collective-permute-done.3.refs_1_), channel_id=1, source_target_pairs={{0,2},{2,4},{4,6},{6,8},{8,10},{10,12},{12,14},{14,0},{1,15},{3,1}... | collective-permute-start | bytes 1572872 | tf_op jit(solution)/shard_map/ppermute | solution.py:354
  47.0 11.7 %collective-permute-start.1 = (bf16[32,32,256]{2,1,0:T(8,128)(2,1)S(1)}, bf16[32,32,256]{2,1,0:T(8,128)(2,1)S(1)}, u32[]{:S(2)}, u32[]{:S(2)}) collective-permute-start(bf16[32,32,256]{2,1,0:T(8,128)(2,1)S(1)} %collective-permute-done.refs_2_), channel_id=1, source_target_pairs={{0,2},{2,4},{4,6},{6,8},{8,10},{10,12},{12,14},{14,0},{1,15},{3,1}... | collective-permute-start | bytes 1572872 | tf_op jit(solution)/shard_map/ppermute | solution.py:355
  50.5 10.1 %collective-permute-start.6 = (bf16[32,32,256]{2,1,0:T(8,128)(2,1)S(1)}, bf16[32,32,256]{2,1,0:T(8,128)(2,1)S(1)}, u32[]{:S(2)}, u32[]{:S(2)}) collective-permute-start(bf16[32,32,256]{2,1,0:T(8,128)(2,1)S(1)} %collective-permute-done.refs_2_), channel_id=1, source_target_pairs={{0,1},{1,0},{2,3},{3,2},{4,5},{5,4},{6,7},{7,6},{8,9},{9,8},{10,11... | collective-permute-start | bytes 1572872 | tf_op jit(solution)/shard_map/ppermute | solution.py:357
  53.1 7.5 %collective-permute-start.7 = (bf16[32,32,256]{2,1,0:T(8,128)(2,1)S(1)}, bf16[32,32,256]{2,1,0:T(8,128)(2,1)S(1)}, u32[]{:S(2)}, u32[]{:S(2)}) collective-permute-start(bf16[32,32,256]{2,1,0:T(8,128)(2,1)S(1)} %collective-permute-done.4.refs_3_), channel_id=1, source_target_pairs={{0,1},{1,0},{2,3},{3,2},{4,5},{5,4},{6,7},{7,6},{8,9},{9,8},{10,11... | collective-permute-start | bytes 1572872 | tf_op jit(solution)/shard_map/ppermute | solution.py:358
  58.7 3.8 %collective-permute-start.2 = (bf16[32,32,256]{2,1,0:T(8,128)(2,1)S(1)}, bf16[32,32,256]{2,1,0:T(8,128)(2,1)S(1)}, u32[]{:S(2)}, u32[]{:S(2)}) collective-permute-start(bf16[32,32,256]{2,1,0:T(8,128)(2,1)S(1)} %collective-permute-done.1.refs_4_), channel_id=1, source_target_pairs={{0,1},{1,0},{2,3},{3,2},{4,5},{5,4},{6,7},{7,6},{8,9},{9,8},{10,11... | collective-permute-start | bytes 1572872 | tf_op jit(solution)/shard_map/ppermute | solution.py:359
  63.4 27.4 %collective-permute-start.8 = (bf16[512,256]{1,0:T(8,128)(2,1)S(1)}, bf16[512,256]{1,0:T(8,128)(2,1)S(1)}, u32[]{:S(2)}, u32[]{:S(2)}) collective-permute-start(bf16[512,256]{1,0:T(8,128)(2,1)S(1)} %get-tuple-element.58), channel_id=1, source_target_pairs={{0,2},{2,4},{4,6},{6,8},{8,10},{10,12},{12,14},{14,0},{1,15},{3,1}... | collective-permute-start | bytes 786440 | tf_op jit(solution)/shard_map/ppermute | solution.py:371
  66.6 24.2 %collective-permute-start.9 = (bf16[512,256]{1,0:T(8,128)(2,1)S(1)}, bf16[512,256]{1,0:T(8,128)(2,1)S(1)}, u32[]{:S(2)}, u32[]{:S(2)}) collective-permute-start(bf16[512,256]{1,0:T(8,128)(2,1)S(1)} %get-tuple-element.59), channel_id=1, source_target_pairs={{0,4},{2,6},{4,8},{6,10},{8,12},{10,14},{12,0},{14,2},{1,13},{3,15... | collective-permute-start | bytes 786440 | tf_op jit(solution)/shard_map/ppermute | solution.py:371
  74.4 20.7 %collective-permute-start.10 = (bf16[512,256]{1,0:T(8,128)(2,1)S(1)}, bf16[512,256]{1,0:T(8,128)(2,1)S(1)}, u32[]{:S(2)}, u32[]{:S(2)}) collective-permute-start(bf16[512,256]{1,0:T(8,128)(2,1)S(1)} %get-tuple-element.60), channel_id=1, source_target_pairs={{0,6},{2,8},{4,10},{6,12},{8,14},{10,0},{12,2},{14,4},{1,11},{3,13... | collective-permute-start | bytes 786440 | tf_op jit(solution)/shard_map/ppermute | solution.py:371
  76.3 14.5 %collective-permute-start.11 = (bf16[512,128]{1,0:T(8,128)(2,1)S(1)}, bf16[512,128]{1,0:T(8,128)(2,1)S(1)}, u32[]{:S(2)}, u32[]{:S(2)}) collective-permute-start(bf16[512,128]{1,0:T(8,128)(2,1)S(1)} %get-tuple-element.61), channel_id=1, source_target_pairs={{0,8},{2,10},{4,12},{6,14},{8,0},{10,2},{12,4},{14,6},{1,9},{3,11}... | collective-permute-start | bytes 393224 | tf_op jit(solution)/shard_map/ppermute | solution.py:371
  95.1 19.8 %copy-start.7 = (s32[8,128]{1,0:T(8,128)S(1)}, s32[8,128]{1,0:T(8,128)}, u32[]{:S(2)}) copy-start(s32[8,128]{1,0:T(8,128)} %get-tuple-element.71.target) | copy-start | bytes 12292
  95.2 19.6 %copy-start = (bf16[128,2048]{1,0:T(8,128)(2,1)S(1)}, bf16[128,2048]{1,0:T(8,128)(2,1)}, u32[]{:S(2)}) copy-start(bf16[128,2048]{1,0:T(8,128)(2,1)} %cotangent.1) | copy-start | bytes 1572868
  95.2 39.4 %copy-start.1 = (bf16[256,2048]{1,0:T(8,128)(2,1)S(1)}, bf16[256,2048]{1,0:T(8,128)(2,1)}, u32[]{:S(2)}) copy-start(bf16[256,2048]{1,0:T(8,128)(2,1)} %weight.1) | copy-start | bytes 3145732
  95.2 3.4 %collective-permute-start.12 = (bf16[512,128]{1,0:T(8,128)(2,1)S(1)}, bf16[512,128]{1,0:T(8,128)(2,1)S(1)}, u32[]{:S(2)}, u32[]{:S(2)}) collective-permute-start(bf16[512,128]{1,0:T(8,128)(2,1)S(1)} %get-tuple-element.78), channel_id=1, source_target_pairs={{0,1},{1,0},{2,3},{3,2},{4,5},{5,4},{6,7},{7,6},{8,9},{9,8},{10,11... | collective-permute-start | bytes 393224 | tf_op jit(solution)/shard_map/ppermute | solution.py:380
  99.3 15.5 %all-to-all-start.1 = ((bf16[32,16,128]{2,1,0:T(8,128)(2,1)}), bf16[32,16,128]{2,1,0:T(8,128)(2,1)S(1)}, u32[]{:S(2)}, u32[]{:S(2)}) async-start(bf16[32,16,128]{2,1,0:T(8,128)(2,1)} %shard_map.218), calls=%async_computation.1 | async-start | bytes 262144 | tf_op jit(solution)/shard_map/all_to_all | solution.py:382
  115.8 18.8 %copy-start.2 = (bf16[128,256]{1,0:T(8,128)(2,1)S(1)}, bf16[128,256]{1,0:T(8,128)(2,1)}, u32[]{:S(2)}) copy-start(bf16[128,256]{1,0:T(8,128)(2,1)} %gate_pre.1) | copy-start | bytes 196612
  115.8 18.8 %copy-start.3 = (bf16[128,256]{1,0:T(8,128)(2,1)S(1)}, bf16[128,256]{1,0:T(8,128)(2,1)}, u32[]{:S(2)}) copy-start(bf16[128,256]{1,0:T(8,128)(2,1)} %mixer.1) | copy-start | bytes 196612
  115.8 18.8 %copy-start.5 = (bf16[128,128]{1,0:T(8,128)(2,1)S(1)}, bf16[128,128]{1,0:T(8,128)(2,1)}, u32[]{:S(2)}) copy-start(bf16[128,128]{1,0:T(8,128)(2,1)} %read.3) | copy-start | bytes 98308
  115.9 18.8 %copy-start.8 = (f32[4,128]{1,0:T(4,128)S(1)}, f32[4,128]{1,0:T(4,128)}, u32[]{:S(2)}) copy-start(f32[4,128]{1,0:T(4,128)} %logs.1) | copy-start | bytes 6148
  136.5 24.9 %collective-permute-start.13 = (bf16[32,32,128]{2,1,0:T(8,128)(2,1)S(1)}, bf16[32,32,128]{2,1,0:T(8,128)(2,1)S(1)}, u32[]{:S(2)}, u32[]{:S(2)}) collective-permute-start(bf16[32,32,128]{2,1,0:T(8,128)(2,1)S(1)} %get-tuple-element.89), channel_id=1, source_target_pairs={{0,16},{16,32},{32,48},{48,0},{1,17},{17,33},{33,49},{49,1},{2,18}... | collective-permute-start | bytes 786440 | tf_op jit(solution)/shard_map/ppermute | solution.py:396
  138.5 22.9 %collective-permute-start.14 = (bf16[32,32,128]{2,1,0:T(8,128)(2,1)S(1)}, bf16[32,32,128]{2,1,0:T(8,128)(2,1)S(1)}, u32[]{:S(2)}, u32[]{:S(2)}) collective-permute-start(bf16[32,32,128]{2,1,0:T(8,128)(2,1)S(1)} %get-tuple-element.90), channel_id=1, source_target_pairs={{0,32},{16,48},{32,0},{48,16},{1,33},{17,49},{33,1},{49,17},{2,34}... | collective-permute-start | bytes 786440 | tf_op jit(solution)/shard_map/ppermute | solution.py:396
  143.1 18.3 %collective-permute-start.15 = (bf16[32,32,128]{2,1,0:T(8,128)(2,1)S(1)}, bf16[32,32,128]{2,1,0:T(8,128)(2,1)S(1)}, u32[]{:S(2)}, u32[]{:S(2)}) collective-permute-start(bf16[32,32,128]{2,1,0:T(8,128)(2,1)S(1)} %get-tuple-element.91), channel_id=1, source_target_pairs={{0,48},{16,0},{32,16},{48,32},{1,49},{17,1},{33,17},{49,33},{2,50}... | collective-permute-start | bytes 786440 | tf_op jit(solution)/shard_map/ppermute | solution.py:396
  146.1 4.7 %copy-start.4 = (bf16[128,256]{1,0:T(8,128)(2,1)S(1)}, bf16[128,256]{1,0:T(8,128)(2,1)}, u32[]{:S(2)}) copy-start(bf16[128,256]{1,0:T(8,128)(2,1)} %values.3) | copy-start | bytes 196612
  146.1 4.7 %copy-start.6 = (bf16[128,128]{1,0:T(8,128)(2,1)S(1)}, bf16[128,128]{1,0:T(8,128)(2,1)}, u32[]{:S(2)}) copy-start(bf16[128,128]{1,0:T(8,128)(2,1)} %write.3) | copy-start | bytes 98308
  146.1 4.7 %copy-start.9 = (f32[1,4,64,128]{3,2,1,0:T(8,128)S(1)}, f32[1,4,64,128]{3,2,1,0:T(8,128)}, u32[]{:S(2)}) copy-start(f32[1,4,64,128]{3,2,1,0:T(8,128)} %param.29) | copy-start | bytes 393220
  146.2 15.2 %all-to-all-start.2 = ((bf16[32,16,128]{2,1,0:T(8,128)(2,1)}), bf16[32,16,128]{2,1,0:T(8,128)(2,1)S(1)}, u32[]{:S(2)}, u32[]{:S(2)}) async-start(bf16[32,16,128]{2,1,0:T(8,128)(2,1)} %get-tuple-element.79), calls=%async_computation.2 | async-start | bytes 262144 | tf_op jit(solution)/shard_map/all_to_all | solution.py:394
